TPU v7x, 512 devices: a whole 4x4x16 slice. The times are simulated.
512 devices in a mesh: sp: 16 (over z), fs: 4 (over y), tp: 8 (over x, core).
Axes of the slice: x: 4, y: 4, z: 16, core: 2. Of those that a mesh axis runs over, the one named last changes fastest.
Arguments:
- layer_entering_vectors: bfloat16 [4, 4096, 2048], P('fs', ('sp', 'tp')), may hold values from -6 to 6
- entering_rms_coefficients: float32 [2048], replicated, may hold values from 0.1 to 1.9
- question_projection: bfloat16 [2048, 1536], P('fs', 'tp'), may hold values from -0.125 to 0.125
- compressing_projection: bfloat16 [2048, 256], P('fs'), may hold values from -0.125 to 0.125
- spinning_address_projection: bfloat16 [2048, 32], P('fs'), may hold values from -0.125 to 0.125
- compact_rms_coefficients: float32 [256], replicated, may hold values from 0.1 to 1.9
- compact_to_plain_address: bfloat16 [256, 1024], P(None, 'tp'), may hold values from -0.375 to 0.375
- compact_to_content: bfloat16 [256, 1024], P(None, 'tp'), may hold values from -0.375 to 0.375
- question_rms_coefficients: float32 [96], replicated, may hold values from 0.7 to 6
- address_rms_coefficients: float32 [96], replicated, may hold values from 0.7 to 6
- acceptance_projection: bfloat16 [2048, 1024], P('fs', 'tp'), may hold values from -0.125 to 0.125
- state_address_projection: bfloat16 [2048, 1024], P('fs', 'tp'), may hold values from -0.125 to 0.125
- state_content_projection: bfloat16 [2048, 1024], P('fs', 'tp'), may hold values from -0.125 to 0.125
- fading_first_lowrank: bfloat16 [2048, 128], replicated, may hold values from -0.125 to 0.125
- fading_second_lowrank: bfloat16 [128, 1024], P(None, 'tp'), may hold values from -0.375 to 0.375
- fading_channel_bias: float32 [1024], P('tp'), may hold values from -20 to -2
- fading_speed_multiplier: float32 [4, 16, 4096], P('fs', 'tp', 'sp'), may hold values from 0.5 to 2, as said below
- fading_extra_exponent: float32 [4, 16, 4096], P('fs', 'tp', 'sp'), may hold values from -0.7 to 0
- adaptation_first_lowrank: bfloat16 [2048, 128], replicated, may hold values from -0.125 to 0.125
- adaptation_second_lowrank: bfloat16 [128, 1024], P(None, 'tp'), may hold values from -0.5 to 0.5
- adaptation_channel_bias: float32 [1024], P('tp'), may hold values from -12 to -1
- present_token_coefficients: float32 [16, 64], P('tp'), may hold values from -1.5 to 1.5
- branch_rms_coefficients: float32 [1024], P('tp'), may hold values from 0.1 to 1.9
- softmax_merge_projection: bfloat16 [1024, 2048], P('tp', 'fs'), may hold values from -0.1875 to 0.1875
- state_merge_projection: bfloat16 [1024, 2048], P('tp', 'fs'), may hold values from -0.1875 to 0.1875
Outputs:
- mixed: bfloat16 [4, 4096, 2048], P('fs', ('sp', 'tp'))
- log_total: float32 [4, 16, 4096], P('fs', 'tp', 'sp')
Inputs may be any that keep to these rules, and one draw needn't show every extreme that they name: `fading_speed_multiplier`: constant over aligned blocks of 256 positions.
All inputs are finite; a program needn't handle non-finite values.
Results may differ from a plain program's by a relative error of at most 0.015.
Values may be sent and summed in bfloat16 or wider, within the bound.
No kernel may reach another device: no remote copies, remote signals or barrier semaphores. Data moves between devices by JAX's collectives and lax.ppermute only.
A program may use at most 64 MiB of HBM per device.

v0:
```python
import jax
import jax.numpy as jnp
from jax import lax
from jax.sharding import PartitionSpec as P

NOPE = 64
ROPE = 32
VHEAD = 64
BRANCH_CHANNELS = 64
TOK_DEV = 256


norm_epsilon = 1e-06
group_epsilon = 0.00064
highest = lax.Precision.HIGHEST


def laid_out(parts, dim):
    parts = jnp.moveaxis(parts, 0, dim)
    shape = parts.shape
    return parts.reshape(*shape[:dim], shape[dim] * shape[dim + 1], *shape[dim + 2 :])


def from_everyone(value, axis):
    devices = lax.axis_size(axis)
    return lax.all_to_all(
        jnp.broadcast_to(value[None], (devices, *value.shape)), axis, 0, 0, tiled=True
    )


def gather_directly(value, axis, dim):
    return laid_out(from_everyone(value, axis), dim)


def sent_together(arrays, axis, dim, along):
    widths = [a.shape[along] for a in arrays]
    both = jnp.concatenate(arrays, axis=along)
    result = lax.all_gather(both, axis, axis=dim, tiled=True)
    return tuple(jnp.split(result, [sum(widths[:k]) for k in range(1, len(widths))], axis=along))


def gathered_once(value, axis):
    leaves = jax.tree.leaves(value)
    sequence = sorted(range(len(leaves)), key=lambda k: -leaves[k].size)
    width = (1, *leaves[sequence[0]].shape)[-1]
    lines = [
        jnp.pad(leaves[k].reshape(-1), (0, -leaves[k].size % width)).reshape(-1, width)
        for k in sequence
    ]
    both, at, found = (from_everyone(jnp.concatenate(lines), axis), 0, {})
    for k, line in zip(sequence, lines):
        slab = both[:, at : at + len(line)].reshape(len(both), -1)
        found[k] = slab[:, : leaves[k].size].reshape(-1, *leaves[k].shape)
        at += len(line)
    numbers = iter(range(len(leaves)))
    return jax.tree.map(lambda _: found[next(numbers)], value)


def combined_pairwise(pieces, combine):
    while len(jax.tree.leaves(pieces)[0]) > 1:
        pieces = jax.vmap(combine)(
            *(jax.tree.map(lambda part: part[side::2], pieces) for side in (0, 1))
        )
    return jax.tree.map(lambda part: part[0], pieces)


def carried_in(value, axis, combine, identity):
    devices, position = (lax.axis_size(axis), lax.axis_index(axis))
    passed = jnp.arange(devices) < position

    def kept(part, zero, own):
        part = jnp.where(
            passed.reshape(-1, *(1 for _ in own.shape)),
            part.astype(own.dtype),
            jnp.asarray(zero, own.dtype),
        )
        return part

    pieces = gathered_once(
        jax.tree.map(lambda part, kind: part.astype(kind), value, (jnp.bfloat16, jnp.bfloat16)),
        axis,
    )
    return combined_pairwise(jax.tree.map(kept, pieces, identity, value), combine)


def split_up(value, dim, devices):
    before, after = (value.shape[:dim], value.shape[dim + 1 :])
    return jnp.moveaxis(value.reshape(*before, devices, -1, *after), dim, 0)


def summed_on_arrival(value, axis, dim):
    devices = lax.axis_size(axis)
    parts = lax.all_to_all(split_up(value, dim, devices), axis, 0, 0, tiled=True)
    return jnp.sum(parts.astype(jnp.float32), axis=0)


def rms_rows(values, gain):
    floats = values.astype(jnp.float32)
    return (
        floats * lax.rsqrt(jnp.mean(floats * floats, axis=-1, keepdims=True) + norm_epsilon) * gain
    )


def rotate(values, positions):
    half = values.shape[-1] // 2
    inverse = 10000.0 ** (-jnp.arange(half, dtype=jnp.float32) / half)
    angle = positions.astype(jnp.float32)[:, None] * inverse[None, :]
    cosine = jnp.cos(angle)[:, None, :]
    sine = jnp.sin(angle)[:, None, :]
    first = values[..., :half]
    second = values[..., half:]
    return jnp.concatenate(
        [first * cosine - second * sine, second * cosine + first * sine], axis=-1
    )


def finish(stacked, gain, positions):
    normed = rms_rows(stacked, gain)
    return jnp.concatenate(
        [normed[..., :NOPE], rotate(normed[..., NOPE:], positions)], axis=-1
    ).astype(jnp.bfloat16)


def matmul(left, right):
    return jnp.dot(left, right, preferred_element_type=jnp.float32)


def pair_decay(later, earlier, mask):
    differ = later[:, :, :, None, :] - earlier[:, :, None, :, :]
    return jnp.exp(jnp.where(mask[None, None, :, :, None], differ, -jnp.inf))


def shards(
    layer_entering_vectors,
    entering_rms_coefficients,
    question_projection,
    compressing_projection,
    spinning_address_projection,
    compact_rms_coefficients,
    compact_to_plain_address,
    compact_to_content,
    question_rms_coefficients,
    address_rms_coefficients,
    acceptance_projection,
    state_address_projection,
    state_content_projection,
    fading_first_lowrank,
    fading_second_lowrank,
    fading_channel_bias,
    fading_speed_multiplier,
    fading_extra_exponent,
    adaptation_first_lowrank,
    adaptation_second_lowrank,
    adaptation_channel_bias,
    present_token_coefficients,
    branch_rms_coefficients,
    softmax_merge_projection,
    state_merge_projection,
):
    gathered = (
        lax.all_gather(question_projection, "fs", axis=0, tiled=True),
        lax.all_gather(compressing_projection, "fs", axis=0, tiled=True),
        lax.all_gather(spinning_address_projection, "fs", axis=0, tiled=True),
        lax.all_gather(acceptance_projection, "fs", axis=0, tiled=True),
        lax.all_gather(state_address_projection, "fs", axis=0, tiled=True),
        lax.all_gather(state_content_projection, "fs", axis=0, tiled=True),
    )
    widths = [stream_position_entry.shape[1] for stream_position_entry in gathered] + [
        fading_first_lowrank.shape[1],
        adaptation_first_lowrank.shape[1],
    ]
    joined = jnp.concatenate(
        list(gathered) + [fading_first_lowrank, adaptation_first_lowrank], axis=1
    )
    bounds = [0]
    for width in widths:
        bounds.append(bounds[-1] + width)
    normed = rms_rows(
        gather_directly(layer_entering_vectors, "tp", 1)[0], entering_rms_coefficients
    ).astype(jnp.bfloat16)
    projected = matmul(normed, joined).astype(jnp.bfloat16)[None][0]
    columns = [projected[:, bounds[index] : bounds[index + 1]] for index in range(len(widths))]
    query, latent, rope_key, recept_in, rkey_in, rvalue_in, decay_in, rate_low = columns
    row_count = projected.shape[0]
    attn_heads = compact_to_plain_address.shape[1] // NOPE
    qk_size = NOPE + ROPE
    own_positions = lax.axis_index("sp") * row_count + jnp.arange(row_count, dtype=jnp.int32)
    last_position = lax.axis_index("sp") * row_count + row_count - 1
    latent_normed = rms_rows(latent, compact_rms_coefficients).astype(jnp.bfloat16)
    query_ready = finish(
        query.reshape(row_count, attn_heads, qk_size), question_rms_coefficients, own_positions
    )
    scale = qk_size ** (-0.5)
    start_carry = (
        jnp.full((attn_heads, row_count), -jnp.inf, jnp.float32),
        jnp.zeros((attn_heads, row_count), jnp.float32),
        jnp.zeros((attn_heads, row_count, VHEAD), jnp.float32),
    )
    pieces = sent_together((latent_normed, rope_key), "sp", 0, 1)
    positions = jnp.arange(pieces[0].shape[0], dtype=jnp.int32)
    latent_rows = pieces[0]
    length_here = latent_rows.shape[0]
    key_nope = (
        matmul(latent_rows, compact_to_plain_address)
        .astype(jnp.bfloat16)
        .reshape(length_here, attn_heads, NOPE)
    )
    values_here = (
        matmul(latent_rows, compact_to_content)
        .astype(jnp.bfloat16)
        .reshape(length_here, attn_heads, VHEAD)
    )
    key_stack = jnp.concatenate(
        [key_nope, jnp.broadcast_to(pieces[1][:, None, :], (length_here, attn_heads, ROPE))],
        axis=-1,
    )
    key_piece = finish(key_stack, address_rms_coefficients, positions)
    carry = start_carry
    length_here = key_piece.shape[0]
    block = TOK_DEV
    blocks = length_here // block
    keys_blocked = key_piece.reshape(blocks, block, attn_heads, qk_size)
    values_blocked = values_here.reshape(blocks, block, attn_heads, VHEAD)

    def visit(state, inputs):
        key_block, value_block, index = inputs
        block_start = index * block

        def compute(running):
            running_max, running_total, running_sum = running
            scores = (
                jnp.einsum(
                    "qhd,khd->hqk", query_ready, key_block, preferred_element_type=jnp.float32
                )
                * scale
            )
            key_positions = block_start + jnp.arange(block, dtype=jnp.int32)
            allowed = key_positions[None, :] <= own_positions[:, None]
            scores = jnp.where(allowed[None], scores, -jnp.inf)
            new_max = jnp.maximum(running_max, jnp.max(scores, axis=-1))
            safe_max = jnp.where(jnp.isfinite(new_max), new_max, 0.0)
            weights = jnp.exp(scores - safe_max[..., None])
            factor = jnp.exp(running_max - safe_max)
            new_total = running_total * factor + jnp.sum(weights, axis=-1)
            new_sum = running_sum * factor[..., None] + jnp.einsum(
                "hqk,khd->hqd",
                weights.astype(jnp.bfloat16),
                value_block,
                preferred_element_type=jnp.float32,
            )
            return (new_max, new_total, new_sum)

        def keep(running):
            return running

        return (lax.cond(block_start > last_position, keep, compute, state), None)

    carry, _ = lax.scan(
        visit, carry, (keys_blocked, values_blocked, jnp.arange(blocks, dtype=jnp.int32))
    )
    final_max, final_total, final_sum = carry
    attended = (final_sum / final_total[..., None]).astype(jnp.bfloat16)
    attended = jnp.transpose(attended, (1, 0, 2)).reshape(row_count, attn_heads * VHEAD)
    log_total = final_max + jnp.log(final_total)
    recurrent_heads = fading_second_lowrank.shape[1] // BRANCH_CHANNELS

    def heads(values):
        return values.astype(jnp.float32).reshape(row_count, recurrent_heads, BRANCH_CHANNELS)

    acceptance_tokens_flat = heads(recept_in)
    state_address = heads(rkey_in)
    state_content = heads(rvalue_in)
    decay_low = jnp.tanh(decay_in.astype(jnp.float32)).astype(jnp.bfloat16)
    rate_logarithm = (
        -jax.nn.softplus(-(fading_channel_bias + matmul(decay_low, fading_second_lowrank))) - 0.5
    )
    log_decay = (
        -jnp.exp(rate_logarithm).reshape(row_count, recurrent_heads, BRANCH_CHANNELS)
        * jnp.transpose(fading_speed_multiplier[0])[:, :, None]
        + jnp.transpose(fading_extra_exponent[0])[:, :, None]
    )
    learn = jax.nn.sigmoid(
        adaptation_channel_bias + matmul(rate_low, adaptation_second_lowrank)
    ).reshape(row_count, recurrent_heads, BRANCH_CHANNELS)
    unit = state_address * lax.rsqrt(
        jnp.sum(state_address * state_address, axis=-1, keepdims=True) + 1e-06
    )
    span = 16
    spans = row_count // span

    def by_span(values):
        return jnp.transpose(
            values.reshape(spans, span, recurrent_heads, BRANCH_CHANNELS), (0, 2, 1, 3)
        )

    cum_log = jnp.cumsum(by_span(log_decay), axis=2)
    prev_log = cum_log - by_span(log_decay)
    toward = -by_span(unit)
    remove = by_span(unit * learn)
    span_key = by_span(state_address)
    span_value = by_span(state_content)
    span_recept = by_span(acceptance_tokens_flat)
    rows_index = jnp.arange(span, dtype=jnp.int32)
    strict = rows_index[:, None] > rows_index[None, :]
    inclusive = rows_index[:, None] >= rows_index[None, :]
    before = pair_decay(prev_log, cum_log, strict)
    upto = pair_decay(cum_log, cum_log, inclusive)
    remove_before = jnp.einsum("nhtsk,nhsk,nhtk->nhts", before, remove, toward, precision=highest)
    key_before = jnp.einsum("nhtsk,nhsk,nhtk->nhts", before, span_key, toward, precision=highest)
    remove_upto = jnp.einsum("nhtsk,nhsk,nhtk->nhts", upto, remove, span_recept, precision=highest)
    key_upto = jnp.einsum("nhtsk,nhsk,nhtk->nhts", upto, span_key, span_recept, precision=highest)
    system = jnp.eye(span, dtype=jnp.float32) - remove_before
    start_coef = jnp.exp(prev_log) * toward
    lead_coef = lax.linalg.triangular_solve(
        system, start_coef, left_side=True, lower=True, unit_diagonal=True
    )
    lead_free = lax.linalg.triangular_solve(
        system,
        jnp.einsum("nhts,nhsv->nhtv", key_before, span_value, precision=highest),
        left_side=True,
        lower=True,
        unit_diagonal=True,
    )
    read_coef_span = jnp.exp(cum_log) * span_recept + jnp.einsum(
        "nhts,nhsk->nhtk", remove_upto, lead_coef, precision=highest
    )
    read_free_span = jnp.einsum(
        "nhts,nhsv->nhtv", remove_upto, lead_free, precision=highest
    ) + jnp.einsum("nhts,nhsv->nhtv", key_upto, span_value, precision=highest)
    tail = jnp.exp(cum_log[:, :, -1:, :] - cum_log)
    remove_tail = remove * tail
    key_tail = span_key * tail
    identity = jnp.broadcast_to(
        jnp.eye(BRANCH_CHANNELS, dtype=jnp.float32),
        (recurrent_heads, BRANCH_CHANNELS, BRANCH_CHANNELS),
    )
    span_map = jnp.exp(cum_log[:, :, -1, :])[:, :, None, :] * identity[None] + jnp.einsum(
        "nhsk,nhsj->nhkj", lead_coef, remove_tail, precision=highest
    )
    span_add = jnp.einsum(
        "nhsv,nhsj->nhvj", lead_free, remove_tail, precision=highest
    ) + jnp.einsum("nhsv,nhsj->nhvj", span_value, key_tail, precision=highest)

    def advance(carry, inputs):
        local_now, transfer_now = carry
        map_here, add_here, coef_here, free_here = inputs
        read_local = free_here + jnp.einsum("hvk,htk->htv", local_now, coef_here, precision=highest)
        read_along = jnp.einsum("hjk,htk->htj", transfer_now, coef_here, precision=highest)
        local_next = jnp.einsum("hvk,hkj->hvj", local_now, map_here, precision=highest) + add_here
        transfer_next = jnp.einsum("hik,hkj->hij", transfer_now, map_here, precision=highest)
        return ((local_next, transfer_next), (read_local, read_along))

    (local_state, transfer), (read_free, read_along) = lax.scan(
        advance,
        (jnp.zeros_like(identity), identity),
        (span_map, span_add, read_coef_span, read_free_span),
    )
    read_free = jnp.transpose(read_free, (0, 2, 1, 3)).reshape(
        row_count, recurrent_heads, BRANCH_CHANNELS
    )
    read_along = jnp.transpose(read_along, (0, 2, 1, 3)).reshape(
        row_count, recurrent_heads, BRANCH_CHANNELS
    )

    def compose(earlier, later):
        return (
            jnp.einsum("hij,hjk->hik", earlier[0], later[0], precision=highest),
            jnp.einsum("hij,hjk->hik", earlier[1], later[0], precision=highest) + later[1],
        )

    entering = carried_in(
        (transfer, local_state), "sp", compose, (identity, jnp.zeros_like(local_state))
    )[1]
    read = read_free + jnp.einsum("hvk,thk->thv", entering, read_along, precision=highest)
    center = jnp.mean(read, axis=-1, keepdims=True)
    spread = jnp.mean(jnp.square(read - center), axis=-1, keepdims=True)
    retrieved_rescaled = (
        (read - center)
        * lax.rsqrt(spread + group_epsilon)
        * branch_rms_coefficients.reshape(recurrent_heads, BRANCH_CHANNELS)
    )
    present_token_term = (
        jnp.sum(
            acceptance_tokens_flat * state_address * present_token_coefficients,
            axis=-1,
            keepdims=True,
        )
        * state_content
    )
    state_branch_result = (
        (retrieved_rescaled + present_token_term)
        .reshape(row_count, recurrent_heads * BRANCH_CHANNELS)
        .astype(jnp.bfloat16)
    )
    out_attn_full, out_rec_full = sent_together(
        (softmax_merge_projection, state_merge_projection), "fs", 1, 0
    )
    mixed = summed_on_arrival(
        (matmul(attended, out_attn_full) + matmul(state_branch_result, out_rec_full)).astype(
            jnp.bfloat16
        ),
        "tp",
        0,
    )
    return (mixed.astype(jnp.bfloat16)[None], log_total[None])


def solution(mesh):
    placed = (
        P("fs", ("sp", "tp"), None),
        P(),
        P("fs", "tp"),
        P("fs", None),
        P("fs", None),
        P(),
        P(None, "tp"),
        P(None, "tp"),
        P(),
        P(),
        P("fs", "tp"),
        P("fs", "tp"),
        P("fs", "tp"),
        P(),
        P(None, "tp"),
        P("tp"),
        P("fs", "tp", "sp"),
        P("fs", "tp", "sp"),
        P(),
        P(None, "tp"),
        P("tp"),
        P("tp", None),
        P("tp"),
        P("tp", "fs"),
        P("tp", "fs"),
    )
    return jax.shard_map(
        shards,
        mesh=mesh,
        in_specs=placed,
        out_specs=(P("fs", ("sp", "tp"), None), P("fs", "tp", "sp")),
        check_vma=False,
    )
```

profile of v0, /device:TPU:480, one launch (start us, length us, event | category | flops | bytes accessed | tf_op | source)
XLA Modules:
  0.0 343.4 jit_solution(10507651100894332351)
XLA Ops:
  7.2 2.1 broadcast_in_dim.93
  9.3 4.3 %all-to-all-start = ((bf16[8,1,32,2048]{3,2,1,0:T(8,128)(2,1)}), bf16[8,1,32,2048]{3,2,1,0:T(8,128)(2,1)S(1)}, u32[]{:S(2)}, u32[]{:S(2)}) async-start(bf16[8,1,32,2048]{3,2,1,0:T(8,128)(2,1)} %broadcast_in_dim.93), calls=%async_computation | async-start | bytes 2097152 | tf_op jit(solution)/shard_map/all_to_all | solution.py:26
  14.6 12.5 %all_gather.26 = bf16[2048,32]{0,1:T(8,128)(2,1)S(1)} all-gather(bf16[512,32]{0,1:T(8,128)(2,1)S(1)} %copy-done.21), channel_id=1, replica_groups=mesh['sp'=16,'fs'=4,'tp'=8] {'fs'}, dimensions={0}, use_global_device_ids=true | all-gather | bytes 163840 | tf_op jit(solution)/shard_map/all_gather | solution.py:163
  27.4 15.4 %all_gather.27 = bf16[2048,128]{1,0:T(8,128)(2,1)S(1)} all-gather(bf16[512,128]{1,0:T(8,128)(2,1)S(1)} %copy-done.11), channel_id=1, replica_groups=mesh['sp'=16,'fs'=4,'tp'=8] {'fs'}, dimensions={0}, use_global_device_ids=true | all-gather | bytes 655360 | tf_op jit(solution)/shard_map/all_gather | solution.py:164
  42.8 14.2 %all_gather.28 = bf16[2048,128]{1,0:T(8,128)(2,1)} all-gather(bf16[512,128]{1,0:T(8,128)(2,1)S(1)} %copy-done.12), channel_id=1, replica_groups=mesh['sp'=16,'fs'=4,'tp'=8] {'fs'}, dimensions={0}, use_global_device_ids=true | all-gather | bytes 655360 | tf_op jit(solution)/shard_map/all_gather | solution.py:165
  57.0 13.6 %all_gather.29 = bf16[2048,128]{1,0:T(8,128)(2,1)} all-gather(bf16[512,128]{1,0:T(8,128)(2,1)S(1)} %copy-done.13), channel_id=1, replica_groups=mesh['sp'=16,'fs'=4,'tp'=8] {'fs'}, dimensions={0}, use_global_device_ids=true | all-gather | bytes 655360 | tf_op jit(solution)/shard_map/all_gather | solution.py:166
  70.7 13.8 %all_gather.24 = bf16[2048,192]{1,0:T(8,128)(2,1)S(1)} all-gather(bf16[512,192]{1,0:T(8,128)(2,1)S(1)} %copy.161), channel_id=1, replica_groups=mesh['sp'=16,'fs'=4,'tp'=8] {'fs'}, dimensions={0}, use_global_device_ids=true | all-gather | bytes 983040 | tf_op jit(solution)/shard_map/all_gather | solution.py:161
  86.2 8.7 %concatenate.30 = bf16[2048,1120]{1,0:T(8,128)(2,1)} concatenate(bf16[2048,192]{1,0:T(8,128)(2,1)S(1)} %all_gather.24, bf16[2048,256]{1,0:T(8,128)(2,1)} %all-gather.4.cloned.1.call-done, bf16[2048,32]{1,0:T(8,128)(2,1)S(1)} %copy.162, bf16[2048,128]{1,0:T(8,128)(2,1)S(1)} %all_gather.27, bf16[2048,128]{1,0:T(8,128)(2,1)} %all_gather.28, bf16[2048,128]{1,0:T(8,128)(2,1)} %all_gather.29, ...), dimensions={1} | concatenate | bytes 9175040 | tf_op jit(solution)/shard_map/concatenate | solution.py:172
  95.0 4.4 %convolution_convert_fusion.2 = bf16[256,1120]{0,1:T(8,128)(2,1)S(1)} fusion(bf16[256,2048]{1,0:T(8,128)(2,1)S(1)} %copy-done.2, bf16[2048,1120]{1,0:T(8,128)(2,1)} %concatenate.30), kind=kOutput, calls=%fused_computation.73 | convolution fusion | flops 1174691840 | bytes 6209536 | tf_op jit(solution)/shard_map/dot_general | solution.py:125
  109.7 8.2 %fusion.45 = f32[16,2,16,1,16]{4,3,2,1,0:T(1,128)S(1)} fusion(f32[16,2,16,64]{3,2,1,0:T(8,128)S(1)} %copy.177, f32[16,2,16,64]{3,2,1,0:T(8,128)S(1)} %copy.175, f32[16,2,16,64]{3,2,1,0:T(8,128)S(1)} %copy.174, pred[16,16]{1,0:T(8,128)(4,1)S(1)} %iota_compare_fusion.4, f32[16,2,16,64,1]{3,0,1,2,4:T(8,128)} %negate_bitcast_fusion), kind=kOutput, calls=%fused_computation.59 | convolution fusion | flops 7864320 | bytes 557312 | tf_op jit(solution)/shard_map/nhtsk,nhsk,nhtk->nhts/dot_general | solution.py:308
  117.9 8.2 %fusion.43 = f32[16,2,16,1,16]{4,3,2,1,0:T(1,128)} fusion(f32[16,2,16,64]{3,2,1,0:T(8,128)S(1)} %bitcast.262, f32[16,2,16,64]{3,2,1,0:T(8,128)S(1)} %copy.175, f32[16,2,16,64]{3,2,1,0:T(8,128)S(1)} %copy.174, pred[16,16]{1,0:T(8,128)(4,1)S(1)} %iota_compare_fusion.4, f32[16,2,16,64,1]{3,0,1,2,4:T(8,128)S(1)} %copy-done.9), kind=kOutput, calls=%fused_computation.57 | convolution fusion | flops 7864320 | bytes 557312 | tf_op jit(solution)/shard_map/nhtsk,nhsk,nhtk->nhts/dot_general | solution.py:309
  126.0 4.1 %fusion.41 = f32[16,2,16,1,16]{4,3,2,1,0:T(1,128)S(1)} fusion(f32[16,2,16,64]{3,2,1,0:T(8,128)S(1)} %copy.175, f32[16,2,16,64]{3,2,1,0:T(8,128)S(1)} %copy.177, pred[16,16]{1,0:T(8,128)(4,1)S(1)} %iota_compare_fusion.3, bf16[16,2,16,64,1]{3,1,2,0,4:T(2,128)(2,1)S(1)} %bitcast.269), kind=kOutput, calls=%fused_computation.55 | convolution fusion | flops 7864320 | bytes 360704 | tf_op jit(solution)/shard_map/nhtsk,nhsk,nhtk->nhts/dot_general | solution.py:310
  130.2 5.2 %fusion.39 = f32[16,2,16,1,16]{4,3,2,1,0:T(1,128)S(1)} fusion(f32[16,2,16,64]{3,2,1,0:T(8,128)S(1)} %copy.175, f32[16,2,16,64]{3,2,1,0:T(8,128)S(1)} %bitcast.263, pred[16,16]{1,0:T(8,128)(4,1)} %copy-done.28, bf16[16,2,16,64,1]{3,1,2,0,4:T(2,128)(2,1)S(1)} %bitcast.270), kind=kOutput, calls=%fused_computation.53 | convolution fusion | flops 7864320 | bytes 360704 | tf_op jit(solution)/shard_map/nhtsk,nhsk,nhtk->nhts/dot_general | solution.py:311
  135.4 39.6 %custom-call.5 = f32[16,2,1,16,16]{3,4,2,1,0:T(8,128)S(1)} custom-call(f32[16,2,1,16,16]{4,3,2,1,0:T(8,128)S(1)} %add_bitcast_fusion), custom_call_target="InvertDiagBlocksLowerTriangular" | custom-call | tf_op jit(solution)/shard_map/triangular_solve/custom-call.1 | solution.py:314
  178.5 1.8 fusion.113
  180.9 1.8 convolution_add_fusion.4
  183.7 36.7 %while.33 = (s32[]{:T(128)}, f32[2,64,64]{1,2,0:T(8,128)S(1)}, f32[2,64,64]{1,2,0:T(8,128)S(1)}, f32[16,2,16,64]{3,2,1,0:T(8,128)}, f32[16,2,16,64]{3,2,1,0:T(8,...) while((s32[]{:T(128)}, f32[2,64,64]{1,2,0:T(8,128)S(1)}, ...), condition=%wide.region_13.15_spmd.clone, body=%wide.region_12.14_spmd.clone.sunk | while | flops 15755267 | bytes 870532 | solution.py:353
  221.6 10.0 %all-to-all-start.1 = ((bf16[16,256,64]{1,2,0:T(8,128)(2,1)}), bf16[16,256,64]{1,2,0:T(8,128)(2,1)S(1)}, u32[]{:S(2)}, u32[]{:S(2)}) async-start(bf16[16,256,64]{1,2,0:T(8,128)(2,1)} %broadcast_in_dim.156), calls=%async_computation.1 | async-start | bytes 1048576 | tf_op jit(solution)/shard_map/all_to_all | solution.py:26
  236.9 12.7 %all-to-all-done.1 = bf16[16,256,64]{1,2,0:T(8,128)(2,1)S(1)} async-done(((bf16[16,256,64]{1,2,0:T(8,128)(2,1)}), bf16[16,256,64]{1,2,0:T(8,128)(2,1)S(1)}, u32[]{:S(2)}, u32[]{:S(2)}) %all-to-all-start.1) | async-done | bytes 524320 | tf_op jit(solution)/shard_map/all_to_all | solution.py:26
  254.2 2.1 convolution_convert_fusion.1
  263.1 48.0 %while.32 = (s32[]{:T(128)}, f32[2,256]{1,0:T(2,128)S(1)}, f32[2,256]{1,0:T(2,128)S(1)}, f32[2,256,64]{1,2,0:T(8,128)S(1)}, s32[16]{0:T(128)S(1)}, /*index=5*/s3...) while((s32[]{:T(128)}, f32[2,256]{1,0:T(2,128)S(1)}, ...), condition=%wide.region_9.10_spmd.clone, body=%wide.region_4.9_spmd.clone.sunk | while | flops 42995204 | bytes 2269991 | solution.py:258
  312.6 2.5 fusion.53
  315.1 4.9 %all-to-all-start.2 = ((bf16[8,32,2048]{2,1,0:T(8,128)(2,1)}), bf16[8,32,2048]{2,1,0:T(8,128)(2,1)S(1)}, u32[]{:S(2)}, u32[]{:S(2)}) async-start(bf16[8,32,2048]{2,1,0:T(8,128)(2,1)} %bitcast.58), calls=%async_computation.2 | async-start | bytes 2097152 | tf_op jit(solution)/shard_map/all_to_all | solution.py:93
  320.5 15.3 %all-to-all-done.2 = bf16[8,32,2048]{2,1,0:T(8,128)(2,1)S(1)} async-done(((bf16[8,32,2048]{2,1,0:T(8,128)(2,1)}), bf16[8,32,2048]{2,1,0:T(8,128)(2,1)S(1)}, u32[]{:S(2)}, u32[]{:S(2)}) %all-to-all-start.2) | async-done | bytes 1048608 | tf_op jit(solution)/shard_map/all_to_all | solution.py:93
  (523 shorter events, 137.2 us)
Async XLA Ops:
  7.2 247.0 %copy-start = (bf16[256,128]{1,0:T(8,128)(2,1)S(1)}, bf16[256,128]{1,0:T(8,128)(2,1)}, u32[]{:S(2)}) copy-start(bf16[256,128]{1,0:T(8,128)(2,1)} %param.39) | copy-start | bytes 196612
  7.2 20.2 %copy-start.11 = (bf16[512,128]{1,0:T(8,128)(2,1)S(1)}, bf16[512,128]{1,0:T(8,128)(2,1)}, u32[]{:S(2)}) copy-start(bf16[512,128]{1,0:T(8,128)(2,1)} %param.43) | copy-start | bytes 393220
  7.2 35.6 %copy-start.12 = (bf16[512,128]{1,0:T(8,128)(2,1)S(1)}, bf16[512,128]{1,0:T(8,128)(2,1)}, u32[]{:S(2)}) copy-start(bf16[512,128]{1,0:T(8,128)(2,1)} %param.44) | copy-start | bytes 393220
  7.2 49.8 %copy-start.13 = (bf16[512,128]{1,0:T(8,128)(2,1)S(1)}, bf16[512,128]{1,0:T(8,128)(2,1)}, u32[]{:S(2)}) copy-start(bf16[512,128]{1,0:T(8,128)(2,1)} %param.45) | copy-start | bytes 393220
  9.3 75.2 %all-to-all-start = ((bf16[8,1,32,2048]{3,2,1,0:T(8,128)(2,1)}), bf16[8,1,32,2048]{3,2,1,0:T(8,128)(2,1)S(1)}, u32[]{:S(2)}, u32[]{:S(2)}) async-start(bf16[8,1,32,2048]{3,2,1,0:T(8,128)(2,1)} %broadcast_in_dim.93), calls=%async_computation | async-start | bytes 2097152 | tf_op jit(solution)/shard_map/all_to_all | solution.py:26
  13.6 71.2 %copy-start.22 = (f32[2048]{0:T(1024)S(1)}, f32[2048]{0:T(1024)}, u32[]{:S(2)}) copy-start(f32[2048]{0:T(1024)} %param.34) | copy-start | bytes 24580
  13.6 72.6 %all-gather.4.cloned.1.call-start = ((), (), s32[]{:S(2)}) async-start(), calls=%async_computation.3 | async-start | bytes 1310720 | tf_op jit(solution)/shard_map/all_gather | solution.py:162
  14.4 239.8 %all-gather.6.cloned.1.call-start = ((), (), s32[]{:S(2)}) async-start(), calls=%async_computation.4 | async-start | bytes 2506752 | tf_op jit(solution)/shard_map/all_gather | solution.py:38
  86.2 8.7 %copy-start.2 = (bf16[256,2048]{1,0:T(8,128)(2,1)S(1)}, bf16[256,2048]{1,0:T(8,128)(2,1)}, u32[]{:S(2)}) copy-start(bf16[256,2048]{1,0:T(8,128)(2,1)} %fusion.55) | copy-start | bytes 3145732
  95.0 8.5 %copy-start.38 = (f32[128]{0:T(128)S(1)}, f32[128]{0:T(128)}, u32[]{:S(2)}) copy-start(f32[128]{0:T(128)} %param.55) | copy-start | bytes 1540
  95.0 9.9 %copy-start.36 = (bf16[128,128]{1,0:T(8,128)(2,1)S(1)}, bf16[128,128]{1,0:T(8,128)(2,1)}, u32[]{:S(2)}) copy-start(bf16[128,128]{1,0:T(8,128)(2,1)} %param.47) | copy-start | bytes 98308
  95.0 9.9 %copy-start.39 = (f32[128]{0:T(128)S(1)}, f32[128]{0:T(128)}, u32[]{:S(2)}) copy-start(f32[128]{0:T(128)} %param.48) | copy-start | bytes 1540
  100.3 210.7 %all-gather.8.cloned.1.call-start = ((), (), s32[]{:S(2)}) async-start(), calls=%async_computation.5 | async-start | bytes 1310720 | tf_op jit(solution)/shard_map/all_gather | solution.py:38
  101.8 24.2 %copy-start.28 = (pred[16,16]{1,0:T(8,128)(4,1)}, pred[16,16]{1,0:T(8,128)(4,1)S(1)}, u32[]{:S(2)}) copy-start(pred[16,16]{1,0:T(8,128)(4,1)S(1)} %iota_compare_fusion.3) | copy-start | bytes 772
  135.4 45.0 %copy-start.16 = (f32[16,2,64]{2,0,1:T(8,128)S(1)}, f32[16,2,64]{2,0,1:T(8,128)}, u32[]{:S(2)}) copy-start(f32[16,2,64]{2,0,1:T(8,128)} %get-tuple-element.393) | copy-start | bytes 24580
  183.7 47.9 %copy-start.25 = (f32[16]{0:T(128)S(1)}, f32[16]{0:T(128)}, u32[]{:S(2)}) copy-start(f32[16]{0:T(128)} %copy-done.24) | copy-start | bytes 196
  183.7 50.6 %copy-start.32 = (f32[96]{0:T(128)S(1)}, f32[96]{0:T(128)}, u32[]{:S(2)}) copy-start(f32[96]{0:T(128)} %param.41) | copy-start | bytes 1156
  220.4 14.0 %copy-start.7 = (f32[16,2,16,64]{3,2,1,0:T(8,128)S(1)}, f32[16,2,16,64]{3,2,1,0:T(8,128)}, u32[]{:S(2)}) copy-start(f32[16,2,16,64]{3,2,1,0:T(8,128)} %get-tuple-element.192) | copy-start | bytes 393220
  220.4 14.8 %copy-start.8 = (f32[16,2,16,64]{3,2,1,0:T(8,128)S(1)}, f32[16,2,16,64]{3,2,1,0:T(8,128)}, u32[]{:S(2)}) copy-start(f32[16,2,16,64]{3,2,1,0:T(8,128)} %get-tuple-element.193) | copy-start | bytes 393220
  220.4 14.8 %copy-start.17 = (f32[256,16]{0,1:T(8,128)S(1)}, f32[256,16]{0,1:T(8,128)}, u32[]{:S(2)}) copy-start(f32[256,16]{0,1:T(8,128)} %get-tuple-element.399) | copy-start | bytes 49156
  220.4 14.8 %copy-start.18 = (f32[256,16]{0,1:T(8,128)S(1)}, f32[256,16]{0,1:T(8,128)}, u32[]{:S(2)}) copy-start(f32[256,16]{0,1:T(8,128)} %get-tuple-element.400) | copy-start | bytes 49156
  221.6 27.9 %all-to-all-start.1 = ((bf16[16,256,64]{1,2,0:T(8,128)(2,1)}), bf16[16,256,64]{1,2,0:T(8,128)(2,1)S(1)}, u32[]{:S(2)}, u32[]{:S(2)}) async-start(bf16[16,256,64]{1,2,0:T(8,128)(2,1)} %broadcast_in_dim.156), calls=%async_computation.1 | async-start | bytes 1048576 | tf_op jit(solution)/shard_map/all_to_all | solution.py:26
  234.5 15.9 %copy-start.34 = (pred[16]{0:T(512)(128)(4,1)S(1)}, pred[16]{0:T(512)(128)(4,1)}, u32[]{:S(2)}) copy-start(pred[16]{0:T(512)(128)(4,1)} %iota_compare_fusion.6) | copy-start | bytes 52
  315.1 20.8 %all-to-all-start.2 = ((bf16[8,32,2048]{2,1,0:T(8,128)(2,1)}), bf16[8,32,2048]{2,1,0:T(8,128)(2,1)S(1)}, u32[]{:S(2)}, u32[]{:S(2)}) async-start(bf16[8,32,2048]{2,1,0:T(8,128)(2,1)} %bitcast.58), calls=%async_computation.2 | async-start | bytes 2097152 | tf_op jit(solution)/shard_map/all_to_all | solution.py:93
  (24 other events, 118.7 us)
Sparse Core Ops, SparseCore 0:
  16.6 32.5 all-gather.3
  100.5 79.7 all-gather.5
  182.4 31.1 all-gather.7
where the time goes:
time: 349 us; the launch traced here: 343 us
  matrix products  106 us (30%)
  blocking collectives  69.6 us (20%)
  other arithmetic  57.8 us (17%)
  local copies, waits for them, and re-layouts  34.4 us (10%)
  waiting for transfers between devices  28.8 us (8%)
  starting transfers between devices  19.3 us (6%)
  between operations  15.2 us (4%)
  loops' own time  12.8 us (4%)
    another operation x5, other arithmetic, shards(): lax.linalg.triangular_solve(system, start_coef, left_side=True, lower=Tru...  40.9 us
    dot_general x16, matrix products, compute(): jnp.einsum('qhd,khd->hqk', query_ready, key_block, preferred_element_type...  19 us
    all_gather x1, blocking collectives, shards(): lax.all_gather(acceptance_projection, 'fs', axis=0, tiled=True)  15.4 us
    all_to_all x1, waiting for transfers between devices, summed_on_arrival(): lax.all_to_all(split_up(value, dim, devices), axis, 0, 0, tiled=True)  15.3 us
    all_to_all x2, starting transfers between devices, from_everyone(): lax.all_to_all(jnp.broadcast_to(value[None], (devices, *value.shape)), ax...  14.3 us
    all_gather x1, blocking collectives, shards(): lax.all_gather(state_address_projection, 'fs', axis=0, tiled=True)  14.2 us
    all_gather x1, blocking collectives, shards(): lax.all_gather(question_projection, 'fs', axis=0, tiled=True)  13.8 us
    all_gather x1, blocking collectives, shards(): lax.all_gather(state_content_projection, 'fs', axis=0, tiled=True)  13.6 us
  transfers between devices with their start and end apart: 6, of which 2 were waited for; matrix products, arithmetic and copies ran while one was open for 51% of the time, Pallas kernels for 0%

commit v1 on v0

v1 whole, which is shorter than its diff:
```python
import jax
import jax.numpy as jnp
import numpy as np
from jax import lax
from jax.experimental import pallas as pl
from jax.experimental.pallas import tpu as pltpu
from jax.sharding import PartitionSpec as P

F32 = jnp.float32
BF16 = jnp.bfloat16
HIGHEST = lax.Precision.HIGHEST

ROWS = 256
NOPE = 64
ROPE = 32
QK = NOPE + ROPE
CHUNK = 64
CHUNKS = ROWS // CHUNK
EPS = 1e-6
GROUP_EPS = 0.00064
NN = (((1,), (0,)), ((), ()))
NT = (((1,), (1,)), ((), ()))
TN = (((0,), (0,)), ((), ()))

VMEM = pl.BlockSpec(memory_space=pltpu.VMEM)
SMEM = pl.BlockSpec(memory_space=pltpu.SMEM)


def dot(a, b, dims=NN):
    return lax.dot_general(a, b, dims, preferred_element_type=F32)


def exact(a, b, dims=NN):
    return lax.dot_general(a, b, dims, precision=HIGHEST, preferred_element_type=F32)


def halves(a):
    high = a.astype(BF16)
    return high, (a - high.astype(F32)).astype(BF16)


def dot_wide(a, b):
    high, low = halves(a)
    return dot(jnp.concatenate([high, low], axis=1), jnp.concatenate([b, b], axis=0))


def iota(shape, dim):
    return lax.broadcasted_iota(jnp.int32, shape, dim)


def call(body, outs, args, flops, scratch=(), specs=None):
    return pl.pallas_call(
        body,
        out_shape=outs,
        in_specs=specs or [VMEM] * len(args),
        out_specs=jax.tree.map(lambda _: VMEM, outs),
        scratch_shapes=scratch,
        cost_estimate=pl.CostEstimate(flops=flops, bytes_accessed=4 << 20, transcendentals=0),
    )(*args)


def turned(n, table):
    half = ROPE // 2
    a, b = n[NOPE : NOPE + half], n[NOPE + half :]
    cosine, sine = table[:half], table[half:]
    return a * cosine - b * sine, b * cosine + a * sine


def project_body(place, x, w, fd, fa, table, gain, rkv, pay, q, dlow, rlow):
    y = dot(x[...], w[...]).astype(BF16)
    rkv[...] = y[:, :384]
    t = y[:, 384:640].astype(F32).T
    tp = place[1]
    group = jnp.zeros((8, ROWS), F32)
    for g in range(4):
        group += jnp.where(tp // 2 == g, t[224 + 8 * g : 232 + 8 * g], 0.0)
    group = jnp.where(iota((8, ROWS), 0) // 4 == lax.rem(tp, 2), group, 0.0)
    pay[...] = jnp.concatenate([t[192:224], group], axis=0).astype(BF16)
    turn = table[place[0]]
    for h in range(2):
        v = t[QK * h : QK * (h + 1)]
        n = v * lax.rsqrt(jnp.mean(v * v, axis=0, keepdims=True) + EPS) * gain[...]
        a, b = turned(n, turn)
        ready = jnp.concatenate([n[:NOPE], a, b, jnp.zeros((128 - QK, ROWS), F32)], axis=0)
        q[h] = ready.T.astype(BF16)
    dlow[...] = jnp.tanh(dot(x[...], fd[...]).astype(BF16).astype(F32)).astype(BF16)
    rlow[...] = dot(x[...], fa[...]).astype(BF16)


def project(place, x, w, fd, fa, table, gain):
    outs = [
        jax.ShapeDtypeStruct((ROWS, 384), BF16),
        jax.ShapeDtypeStruct((40, ROWS), BF16),
        jax.ShapeDtypeStruct((2, ROWS, 128), BF16),
        jax.ShapeDtypeStruct((ROWS, 128), BF16),
        jax.ShapeDtypeStruct((ROWS, 128), BF16),
    ]
    args = (place, x, w, fd, fa, table, gain)
    return call(project_body, outs, args, 4 << 30, specs=[SMEM] + [VMEM] * 6)


def recur_body(rkv, dlow, rlow, wd, bd, wa, ba, mult, extra, present, free, along, bonus, state):
    lane = iota((ROWS, 128), 1)
    recept, key, value = (rkv[:, 128 * i : 128 * (i + 1)].astype(F32) for i in range(3))
    speed = jax.nn.sigmoid(bd[...] + dot(dlow[...], wd[...])) * np.float32(np.exp(-0.5))
    added = jnp.where(lane < 64, extra[:, 0:1], extra[:, 1:2])
    ld = added - speed * mult[...]
    learn = jax.nn.sigmoid(ba[...] + dot(rlow[...], wa[...]))
    same = (iota((128, 128), 0) // 64 == iota((128, 128), 1) // 64).astype(F32)
    unit = key * lax.rsqrt(exact(key * key, same) + EPS)
    bonus[...] = exact(recept * key * present[...], same) * value
    r, c = iota((ROWS, ROWS), 0), iota((ROWS, ROWS), 1)
    block = r // CHUNK == c // CHUNK
    sums = jnp.concatenate(
        [
            jnp.where(block & (c <= r), 1.0, 0.0),
            jnp.where(block & (lax.rem(c, CHUNK) < CHUNK // 2), 1.0, 0.0),
            jnp.where(block, 1.0, 0.0),
        ],
        axis=0,
    )
    sums = exact(sums, ld)
    cum, mid, end = sums[:ROWS], sums[ROWS : 2 * ROWS], sums[2 * ROWS :]
    prev = cum - ld
    toward = -unit
    remove = unit * learn
    grow, shrink = jnp.exp(cum - mid), jnp.exp(mid - cum)
    left1, left2 = toward * jnp.exp(prev - mid), recept * grow
    right1, right2 = remove * shrink, key * shrink
    start1, start2 = toward * jnp.exp(prev), recept * jnp.exp(cum)
    tail = jnp.exp(end - cum)
    tail1, tail2 = remove * tail, key * tail
    whole = jnp.exp(end)
    m0 = iota((CHUNK, 128), 1) < 64

    def stacked(v, k):
        v = v[CHUNK * k : CHUNK * (k + 1)]
        return jnp.concatenate([jnp.where(m0, v, 0.0), jnp.where(m0, 0.0, v)], axis=0)

    rr, cc = iota((128, 128), 0), iota((128, 128), 1)
    head = rr // 64 == cc // 64
    eye = jnp.where(rr == cc, 1.0, 0.0)
    in16, in32 = rr // 16 == cc // 16, rr // 32 == cc // 32
    strict, upto = head & (rr > cc), head & (rr >= cc)

    def square(top, mask):
        both = jnp.concatenate([top, top], axis=1)
        return jnp.where(mask, both, 0.0)

    stage = []
    for k in range(CHUNKS):
        rows = jnp.concatenate([stacked(left1, k), stacked(left2, k)], axis=0)
        part = slice(CHUNK * k, CHUNK * (k + 1))
        cols = jnp.concatenate([right1[part], right2[part]], axis=0)
        g = exact(rows, cols, NT)
        a = square(g[:128, :64], strict)
        kb = square(g[:128, 64:], strict)
        ru = square(g[128:, :64], upto)
        ku = square(g[128:, 64:], upto)
        stage.append([a, kb, ru, ku])
    inverse = []
    for k in range(CHUNKS):
        a = stage[k][0]
        small = jnp.where(in16, a, 0.0)
        power = small
        t = eye + small
        for _ in range(3):
            power = exact(power, power)
            t = t + exact(t, power)
        t = t + exact(exact(t, jnp.where(in32 & ~in16, a, 0.0)), t)
        t = t + exact(exact(t, jnp.where(in32, 0.0, a)), t)
        inverse.append(t)
    pair = jnp.concatenate([jnp.zeros((128, 128), F32), eye], axis=0)
    for k in range(CHUNKS):
        _, kb, ru, ku = stage[k]
        v = stacked(value, k)
        xy = exact(inverse[k], jnp.concatenate([stacked(start1, k), exact(kb, v)], axis=1))
        read = exact(ru, xy)
        coef = stacked(start2, k) + read[:, :128]
        rest = read[:, 128:] + exact(ku, v)
        t1, t2 = stacked(tail1, k), stacked(tail2, k)
        moved = exact(xy, t1, TN)
        decay = whole[CHUNK * k : CHUNK * k + 1]
        step = moved[:128] + jnp.where(rr == cc, decay, 0.0)
        add = moved[128:] + exact(v, t2, TN)
        out = exact(coef, pair, NT)
        near = out[:, :128] + rest
        far = out[:, 128:]
        part = slice(CHUNK * k, CHUNK * (k + 1))
        free[part] = near[:64] + near[64:]
        along[part] = far[:64] + far[64:]
        pair = exact(pair, step) + jnp.concatenate([add, jnp.zeros((128, 128), F32)], axis=0)
    state[0] = (pair[128:192] + pair[192:]).astype(BF16)
    state[1] = (pair[:64] + pair[64:128]).astype(BF16)


def recur(*args):
    wide = jax.ShapeDtypeStruct((ROWS, 128), F32)
    outs = [wide, wide, wide, jax.ShapeDtypeStruct((2, 64, 128), BF16)]
    return call(recur_body, outs, args, 8 << 30)


def attend_body(place, q, own, peer, w, glat, gain, table, att, logs, acc, top):
    sp = place[0]
    factor = np.float32(QK**-0.5 * np.log2(np.e))
    ones = jnp.where(iota((NOPE, ROWS), 0) == 0, 1.0, 0.0).astype(BF16)

    def block(j, first):
        lat = jnp.concatenate(
            [own[:, j, 0:32, :].reshape(128, ROWS), peer[:, j, 0:32, :].reshape(128, ROWS)], axis=0
        ).astype(F32)
        rope = (own[:, j, 32:40, :].astype(F32) + peer[:, j, 32:40, :].astype(F32)).reshape(
            ROPE, ROWS
        )
        lat = lat * lax.rsqrt(jnp.mean(lat * lat, axis=0, keepdims=True) + EPS) * glat[...]
        kv = dot(w[...], lat.astype(BF16)).astype(BF16)
        rope_sum = jnp.sum(rope * rope, axis=0, keepdims=True)
        turn = table[j]
        cosine, sine = turn[:16], turn[16:]
        ra, rb = rope[:16] * gain[64:80], rope[16:] * gain[80:96]
        ra, rb = ra * cosine - rb * sine, rb * cosine + ra * sine
        for h in range(2):
            k = kv[64 * h : 64 * (h + 1)].astype(F32)
            scale = lax.rsqrt(
                (jnp.sum(k * k, axis=0, keepdims=True) + rope_sum) * np.float32(1 / QK) + EPS
            )
            ready = jnp.concatenate(
                [k * scale * gain[0:64], ra * scale, rb * scale], axis=0
            ).astype(BF16)
            s = dot(q[h, :, 0:QK], ready) * factor
            if first:
                s = jnp.where(iota((ROWS, ROWS), 1) <= iota((ROWS, ROWS), 0), s, -jnp.inf)
            peak = jnp.max(s, axis=1, keepdims=True)
            v = jnp.concatenate([kv[128 + 64 * h : 192 + 64 * h], ones], axis=0)
            if first:
                top[h] = jnp.broadcast_to(peak, (ROWS, 128))
                acc[h] = dot(jnp.exp2(s - peak).astype(BF16), v, NT)
            else:
                old = top[h]
                new = jnp.maximum(old, peak)
                top[h] = new
                p = jnp.exp2(s - new[:, 0:1]).astype(BF16)
                acc[h] = acc[h] * jnp.exp2(old - new) + dot(p, v, NT)

    block(sp, True)

    def loop(j, carry):
        block(j, False)
        return carry

    lax.fori_loop(0, sp, loop, 0)
    parts = []
    rows = []
    for h in range(2):
        total = acc[h][:, 64:65]
        parts.append(acc[h][:, 0:64] / total)
        full = top[h] * np.float32(np.log(2.0)) + jnp.log(jnp.broadcast_to(total, (ROWS, 128)))
        rows.append(full.T[0:1])
    att[...] = jnp.concatenate(parts, axis=1).astype(BF16)
    logs[...] = jnp.concatenate(rows, axis=0)


def attend(*args):
    outs = [jax.ShapeDtypeStruct((ROWS, 128), BF16), jax.ShapeDtypeStruct((2, ROWS), F32)]
    scratch = [pltpu.VMEM((2, ROWS, 128), F32), pltpu.VMEM((2, ROWS, 128), F32)]
    return call(attend_body, outs, args, 8 << 30, scratch, [SMEM] + [VMEM] * 7)


def merge_body(place, att, free, along, bonus, states, branch, wo, out):
    head = iota((128, 128), 0) // 64 == iota((128, 128), 1) // 64

    def spread(v):
        return jnp.where(head, jnp.concatenate([v, v], axis=0), jnp.zeros((), v.dtype))

    def step(r, entering):
        return dot_wide(entering, spread(states[r, 0])) + spread(states[r, 1]).astype(F32)

    entering = lax.fori_loop(0, place[0], step, jnp.zeros((128, 128), F32))
    read = free[...] + exact(along[...], entering, NT)
    mean = jnp.where(head, 1.0 / 64, 0.0).astype(BF16)
    read = read - dot_wide(read, mean)
    spread_of = dot_wide(read * read, mean)
    rec = read * lax.rsqrt(spread_of + GROUP_EPS) * branch[...] + bonus[...]
    both = jnp.concatenate([att[...], rec.astype(BF16)], axis=1)
    for f in range(4):
        out[:, 512 * f : 512 * (f + 1)] = dot(both, wo[f]).astype(BF16)


def merge(*args):
    outs = jax.ShapeDtypeStruct((ROWS, 2048), BF16)
    return call(merge_body, outs, args, 4 << 30, specs=[SMEM] + [VMEM] * 7)


def from_everyone(value, axis, groups=None):
    count = len(groups[0]) if groups else lax.axis_size(axis)
    return lax.all_to_all(
        jnp.broadcast_to(value[None], (count, *value.shape)),
        axis,
        0,
        0,
        axis_index_groups=groups,
        tiled=True,
    )


def other_core(value):
    return lax.ppermute(value, "tp", [(i, i ^ 1) for i in range(8)])


def turn_table():
    half = ROPE // 2
    inverse = np.float32(10000.0) ** (-np.arange(half, dtype=np.float32) / np.float32(half))
    angle = np.arange(4096, dtype=np.float32)[:, None] * inverse.astype(np.float32)[None, :]
    both = np.concatenate([np.cos(angle), np.sin(angle)], axis=1).astype(np.float32)
    return both.reshape(16, ROWS, ROPE).transpose(0, 2, 1)


def shards(
    entering,
    entering_gain,
    wq,
    wc,
    wr,
    compact_gain,
    wk_up,
    wv_up,
    q_gain,
    k_gain,
    w_accept,
    w_key,
    w_value,
    fade1,
    fade2,
    fade_bias,
    fade_mult,
    fade_extra,
    adapt1,
    adapt2,
    adapt_bias,
    present,
    branch,
    wo_att,
    wo_rec,
):
    tp = lax.axis_index("tp")
    sp = lax.axis_index("sp")
    core = lax.rem(tp, 2)
    place = jnp.stack([sp, tp]).astype(jnp.int32)
    own_cols = lax.dynamic_slice_in_dim(wc, tp * 32, 32, 1)
    joined = jnp.concatenate([w_accept, w_key, w_value, wq, own_cols, wr], axis=1)
    weights = from_everyone(joined, "fs").reshape(2048, 640)
    x = entering[0].astype(F32)
    x = x * lax.rsqrt(jnp.mean(x * x, axis=-1, keepdims=True) + EPS) * entering_gain
    normed = from_everyone(x.astype(BF16), "tp").reshape(ROWS, 2048)
    table = jnp.asarray(turn_table())
    rkv, pay, q, dlow, rlow = project(
        place, normed, weights, fade1, adapt1, table, q_gain.reshape(QK, 1)
    )
    lat = from_everyone(pay, "sp")
    same_core = [[0, 2, 4, 6], [1, 3, 5, 7]]
    lat_own = from_everyone(lat, "tp", same_core)
    lat_peer = other_core(lat_own)
    free, along, bonus, state = recur(
        rkv,
        dlow,
        rlow,
        fade2,
        fade_bias.reshape(1, 128),
        adapt2,
        adapt_bias.reshape(1, 128),
        jnp.repeat(fade_mult[0, :, 0], 64).reshape(1, 128),
        fade_extra[0].T,
        present.reshape(1, 128),
    )
    states = from_everyone(state, "sp")

    def reordered(v):
        v = v.reshape(4, 2, 32, *v.shape[1:])
        v = jnp.where(core == 0, v, v[:, ::-1])
        return jnp.moveaxis(v, 1, 0).reshape(256, *v.shape[3:])

    up = reordered(jnp.concatenate([wk_up, wv_up], axis=1)).T
    att, logs = attend(
        place,
        q,
        lat_own,
        lat_peer,
        up,
        reordered(compact_gain).reshape(256, 1),
        k_gain.reshape(QK, 1),
        table,
    )
    wo = from_everyone(jnp.concatenate([wo_att, wo_rec], axis=0), "fs")
    partial = merge(place, att, free, along, bonus, states, branch.reshape(1, 128), wo)
    parts = lax.all_to_all(partial.reshape(8, 32, 2048), "tp", 0, 0, tiled=True)
    mixed = jnp.sum(parts.astype(F32), axis=0).astype(BF16)
    return mixed[None], logs[None]


def solution(mesh):
    placed = (
        P("fs", ("sp", "tp"), None),
        P(),
        P("fs", "tp"),
        P("fs", None),
        P("fs", None),
        P(),
        P(None, "tp"),
        P(None, "tp"),
        P(),
        P(),
        P("fs", "tp"),
        P("fs", "tp"),
        P("fs", "tp"),
        P(),
        P(None, "tp"),
        P("tp"),
        P("fs", "tp", "sp"),
        P("fs", "tp", "sp"),
        P(),
        P(None, "tp"),
        P("tp"),
        P("tp", None),
        P("tp"),
        P("tp", "fs"),
        P("tp", "fs"),
    )
    return jax.shard_map(
        shards,
        mesh=mesh,
        in_specs=placed,
        out_specs=(P("fs", ("sp", "tp"), None), P("fs", "tp", "sp")),
        check_vma=False,
    )
```

time: 349 us -> 211 us (0.60)
  the two profiles are of different devices: /device:TPU:480 before, /device:TPU:40 now
where the time goes in v1:
time: 211 us
  waiting for transfers between devices  81.2 us (38%)
  blocking collectives  53.2 us (25%)
  starting transfers between devices  27.6 us (13%)
  Pallas kernels  27.4 us (13%)
  local copies, waits for them, and re-layouts  16.7 us (8%)
  other arithmetic  3.57 us (2%)
    all_to_all x5, waiting for transfers between devices, from_everyone(): lax.all_to_all(jnp.broadcast_to(value[None], (count, *value.shape)), axis...  81.2 us
    all_to_all x1, blocking collectives, from_everyone(): lax.all_to_all(jnp.broadcast_to(value[None], (count, *value.shape)), axis...  33.8 us
    pallas_call x4, Pallas kernels, call(): pl.pallas_call(body, out_shape=outs, in_specs=specs or [VMEM] * len(args)...  27.4 us
    all_to_all x5, starting transfers between devices, from_everyone(): lax.all_to_all(jnp.broadcast_to(value[None], (count, *value.shape)), axis...  25.5 us
    all_to_all x1, blocking collectives, shards(): parts = lax.all_to_all(partial.reshape(8, 32, 2048), 'tp', 0, 0, tiled=True)  19.4 us
    broadcast_in_dim x6, local copies, waits for them, and re-layouts, from_everyone(): jnp.broadcast_to(value[None], (count, *value.shape))  7.84 us
  transfers between devices with their start and end apart: 6, of which 4 were waited for; matrix products, arithmetic and copies ran while one was open for 4% of the time, Pallas kernels for 9%

profile of v1, /device:TPU:40, one launch (start us, length us, event | category | flops | bytes accessed | tf_op | source)
XLA Modules:
  0.0 210.6 jit_solution(12365664233674965282)
XLA Ops:
  0.6 1.1 fusion
  1.7 1.0 fusion.4
  2.8 1.1 broadcast_in_dim.21
  3.9 4.4 %all-to-all-start = ((bf16[8,32,2048]{2,1,0:T(8,128)(2,1)}), bf16[8,32,2048]{2,1,0:T(8,128)(2,1)S(1)}, u32[]{:S(2)}, u32[]{:S(2)}) async-start(bf16[8,32,2048]{2,1,0:T(8,128)(2,1)} %broadcast_in_dim.21), calls=%async_computation | async-start | bytes 2097152 | tf_op jit(solution)/shard_map/all_to_all | solution.py:296
  9.6 14.7 %all-to-all-done = bf16[8,32,2048]{2,1,0:T(8,128)(2,1)S(1)} async-done(((bf16[8,32,2048]{2,1,0:T(8,128)(2,1)}), bf16[8,32,2048]{2,1,0:T(8,128)(2,1)S(1)}, u32[]{:S(2)}, u32[]{:S(2)}) %all-to-all-start) | async-done | bytes 1048608 | tf_op jit(solution)/shard_map/all_to_all | solution.py:296
  24.3 1.8 broadcast_in_dim.22
  26.1 5.0 %all-to-all-start.1 = ((bf16[4,512,640]{2,1,0:T(8,128)(2,1)}), bf16[4,512,640]{2,1,0:T(8,128)(2,1)S(1)}, u32[]{:S(2)}, u32[]{:S(2)}) async-start(bf16[4,512,640]{2,1,0:T(8,128)(2,1)} %broadcast_in_dim.22), calls=%async_computation.1 | async-start | bytes 5242880 | tf_op jit(solution)/shard_map/all_to_all | solution.py:296
  32.4 28.9 %all-to-all-done.1 = bf16[4,512,640]{2,1,0:T(8,128)(2,1)S(1)} async-done(((bf16[4,512,640]{2,1,0:T(8,128)(2,1)}), bf16[4,512,640]{2,1,0:T(8,128)(2,1)S(1)}, u32[]{:S(2)}, u32[]{:S(2)}) %all-to-all-start.1) | async-done | bytes 2621472 | tf_op jit(solution)/shard_map/all_to_all | solution.py:296
  61.3 1.5 copy-done.1
  62.8 4.6 %shard_map.257 = (bf16[256,384]{1,0:T(8,128)(2,1)}, bf16[40,256]{1,0:T(8,128)(2,1)}, bf16[2,256,128]{2,1,0:T(8,128)(2,1)}, bf16[256,128]{1,0:T(8,128)(2,1)}, bf16[256,128]{1,0:T(8,128)(2,1)}) custom-call(s32[2]{0:T(128)} %pad_add_fusion.place, bf16[256,2048]{1,0:T(8,128)(2,1)} %bitcast.25, bf16[2048,640]{1,0:T(8,128)(2,1)} %bitcast.24, ...), custom_call_target="tpu_custom_call" | custom-call | flops 4294967296 | bytes 4194304 | tf_op jit(solution)/shard_map/pallas_call | solution.py:52
  68.2 33.8 %all_to_all.35 = bf16[16,40,256]{2,1,0:T(8,128)(2,1)S(1)} all-to-all(bf16[16,40,256]{2,1,0:T(8,128)(2,1)S(1)} %broadcast_in_dim.23), channel_id=1, replica_groups=mesh['sp'=16,'fs'=4,'tp'=8] {'sp'}, dimensions={0} | all-to-all | bytes 655360 | tf_op jit(solution)/shard_map/all_to_all | solution.py:296
  102.0 1.2 broadcast_in_dim.24
  103.1 3.7 %all-to-all-start.3 = ((bf16[4,16,40,256]{3,2,1,0:T(8,128)(2,1)}), bf16[4,16,40,256]{3,2,1,0:T(8,128)(2,1)S(1)}, u32[]{:S(2)}, u32[]{:S(2)}) async-start(bf16[4,16,40,256]{3,2,1,0:T(8,128)(2,1)} %broadcast_in_dim.24), calls=%async_computation.3 | async-start | bytes 2621440 | tf_op jit(solution)/shard_map/all_to_all | solution.py:296
  109.1 14.7 %all-to-all-done.3.own = bf16[4,16,40,256]{3,2,1,0:T(8,128)(2,1)S(1)} async-done(((bf16[4,16,40,256]{3,2,1,0:T(8,128)(2,1)}), bf16[4,16,40,256]{3,2,1,0:T(8,128)(2,1)S(1)}, u32[]{:S(2)}, u32[]{:S(2)}) %all-to-all-start.3) | async-done | bytes 1310752 | tf_op jit(solution)/shard_map/all_to_all | solution.py:296
  123.8 1.1 broadcast_in_dim.27
  124.9 4.9 %all-to-all-start.5 = ((bf16[4,256,512]{2,1,0:T(8,128)(2,1)}), bf16[4,256,512]{2,1,0:T(8,128)(2,1)S(1)}, u32[]{:S(2)}, u32[]{:S(2)}) async-start(bf16[4,256,512]{2,1,0:T(8,128)(2,1)} %broadcast_in_dim.27), calls=%async_computation.5 | async-start | bytes 2097152 | tf_op jit(solution)/shard_map/all_to_all | solution.py:296
  129.9 2.1 collective-permute-start
  132.0 14.5 %shard_map.259 = (f32[256,128]{1,0:T(8,128)}, f32[256,128]{1,0:T(8,128)}, f32[256,128]{1,0:T(8,128)}, bf16[2,64,128]{2,1,0:T(8,128)(2,1)}) custom-call(bf16[256,384]{1,0:T(8,128)(2,1)} %get-tuple-element.16.rkv, bf16[256,128]{1,0:T(8,128)(2,1)} %get-tuple-element.17.dlow, bf16[256,128]{1,0:T(8,128)(2,1)} %get-tuple-element.18.rlow, bf16[128,128]{1,0:T(8,128)(2,1)} %wd.1, ...), custom_call_target="tpu_custom_call" | custom-call | flops 8589934592 | bytes 4194304 | tf_op jit(solution)/shard_map/pallas_call | solution.py:52
  146.5 1.9 broadcast_in_dim.26
  148.3 7.4 %all-to-all-start.4 = ((bf16[16,2,64,128]{3,2,1,0:T(8,128)(2,1)}), bf16[16,2,64,128]{3,2,1,0:T(8,128)(2,1)S(1)}, u32[]{:S(2)}, u32[]{:S(2)}) async-start(bf16[16,2,64,128]{3,2,1,0:T(8,128)(2,1)} %broadcast_in_dim.26), calls=%async_computation.4 | async-start | bytes 1048576 | tf_op jit(solution)/shard_map/all_to_all | solution.py:296
  158.2 4.5 %shard_map.258 = (bf16[256,128]{1,0:T(8,128)(2,1)}, f32[2,256]{1,0:T(2,128)}) custom-call(s32[2]{0:T(128)} %pad_add_fusion.place, bf16[2,256,128]{2,1,0:T(8,128)(2,1)} %get-tuple-element.13.q, bf16[4,16,40,256]{3,2,1,0:T(8,128)(2,1)} %copy-done.2, bf16[4,16,40,256]{3,2,1,0:T(8,128)(2,1)} %collective-permute-done.peer, bf16[256,256]{1,0:T(8,128)(2,1)} %bitcast.31, ...), custom_call_target="tpu_custom_call" | custom-call | flops 8589934592 | bytes 4194304 | tf_op jit(solution)/shard_map/pallas_call | solution.py:52
  162.7 23.0 %all-to-all-done.4.states = bf16[16,2,64,128]{3,2,1,0:T(8,128)(2,1)S(1)} async-done(((bf16[16,2,64,128]{3,2,1,0:T(8,128)(2,1)}), bf16[16,2,64,128]{3,2,1,0:T(8,128)(2,1)S(1)}, u32[]{:S(2)}, u32[]{:S(2)}) %all-to-all-start.4) | async-done | bytes 524320 | tf_op jit(solution)/shard_map/all_to_all | solution.py:296
  186.5 3.9 %shard_map.260 = bf16[256,2048]{1,0:T(8,128)(2,1)} custom-call(s32[2]{0:T(128)} %pad_add_fusion.place, bf16[256,128]{1,0:T(8,128)(2,1)} %get-tuple-element.15.att, f32[256,128]{1,0:T(8,128)} %get-tuple-element.19.free, f32[256,128]{1,0:T(8,128)} %get-tuple-element.20.along, f32[256,128]{1,0:T(8,128)} %get-tuple-element.21.bonus, ...), custom_call_target="tpu_custom_call" | custom-call | flops 4294967296 | bytes 4194304 | tf_op jit(solution)/shard_map/pallas_call | solution.py:52
  190.3 19.4 %all_to_all.36 = bf16[8,32,2048]{2,1,0:T(8,128)(2,1)S(1)} all-to-all(bf16[8,32,2048]{2,1,0:T(8,128)(2,1)} %bitcast.26), channel_id=1, replica_groups=mesh['sp'=16,'fs'=4,'tp'=8] {'tp'}, dimensions={0} | all-to-all | bytes 2097152 | tf_op jit(solution)/shard_map/all_to_all | solution.py:395
  (76 shorter events, 9.6 us)
Async XLA Ops:
  0.6 7.7 %copy-start = (bf16[512,256]{1,0:T(8,128)(2,1)S(1)}, bf16[512,256]{1,0:T(8,128)(2,1)}, u32[]{:S(2)}) copy-start(bf16[512,256]{1,0:T(8,128)(2,1)} %param.29) | copy-start | bytes 786436
  3.9 4.7 %copy-start.7 = (bf16[512,128]{1,0:T(8,128)(2,1)S(1)}, bf16[512,128]{1,0:T(8,128)(2,1)}, u32[]{:S(2)}) copy-start(bf16[512,128]{1,0:T(8,128)(2,1)} %param.36) | copy-start | bytes 393220
  3.9 4.8 %copy-start.8 = (bf16[512,128]{1,0:T(8,128)(2,1)S(1)}, bf16[512,128]{1,0:T(8,128)(2,1)}, u32[]{:S(2)}) copy-start(bf16[512,128]{1,0:T(8,128)(2,1)} %param.37) | copy-start | bytes 393220
  3.9 4.9 %copy-start.9 = (bf16[512,128]{1,0:T(8,128)(2,1)S(1)}, bf16[512,128]{1,0:T(8,128)(2,1)}, u32[]{:S(2)}) copy-start(bf16[512,128]{1,0:T(8,128)(2,1)} %param.38) | copy-start | bytes 393220
  3.9 20.4 %all-to-all-start = ((bf16[8,32,2048]{2,1,0:T(8,128)(2,1)}), bf16[8,32,2048]{2,1,0:T(8,128)(2,1)S(1)}, u32[]{:S(2)}, u32[]{:S(2)}) async-start(bf16[8,32,2048]{2,1,0:T(8,128)(2,1)} %broadcast_in_dim.21), calls=%async_computation | async-start | bytes 2097152 | tf_op jit(solution)/shard_map/all_to_all | solution.py:296
  24.3 1.8 copy-start.4
  26.1 5.0 %copy-start.17 = (f32[96]{0:T(128)S(1)}, f32[96]{0:T(128)}, u32[]{:S(2)}) copy-start(f32[96]{0:T(128)} %param.34) | copy-start | bytes 1156
  26.1 35.2 %all-to-all-start.1 = ((bf16[4,512,640]{2,1,0:T(8,128)(2,1)}), bf16[4,512,640]{2,1,0:T(8,128)(2,1)S(1)}, u32[]{:S(2)}, u32[]{:S(2)}) async-start(bf16[4,512,640]{2,1,0:T(8,128)(2,1)} %broadcast_in_dim.22), calls=%async_computation.1 | async-start | bytes 5242880 | tf_op jit(solution)/shard_map/all_to_all | solution.py:296
  61.3 1.5 copy-start.1
  103.1 3.7 %copy-start.15 = (f32[1,2,256]{2,1,0:T(2,128)S(1)}, f32[1,2,256]{2,1,0:T(2,128)}, u32[]{:S(2)}) copy-start(f32[1,2,256]{2,1,0:T(2,128)} %param.43) | copy-start | bytes 6148
  103.1 4.5 %copy-start.19 = (f32[1,2,256]{2,1,0:T(2,128)S(1)}, f32[1,2,256]{2,1,0:T(2,128)}, u32[]{:S(2)}) copy-start(f32[1,2,256]{2,1,0:T(2,128)} %param.42) | copy-start | bytes 6148
  103.1 5.4 %copy-start.20 = (f32[2,64]{1,0:T(2,128)S(1)}, f32[2,64]{1,0:T(2,128)}, u32[]{:S(2)}) copy-start(f32[2,64]{1,0:T(2,128)} %param.47) | copy-start | bytes 1540
  103.1 6.0 %copy-start.10 = (bf16[128,512]{1,0:T(8,128)(2,1)S(1)}, bf16[128,512]{1,0:T(8,128)(2,1)}, u32[]{:S(2)}) copy-start(bf16[128,512]{1,0:T(8,128)(2,1)} %param.50) | copy-start | bytes 393220
  103.1 6.0 %copy-start.11 = (bf16[128,512]{1,0:T(8,128)(2,1)S(1)}, bf16[128,512]{1,0:T(8,128)(2,1)}, u32[]{:S(2)}) copy-start(bf16[128,512]{1,0:T(8,128)(2,1)} %param.49) | copy-start | bytes 393220
  103.1 20.7 %all-to-all-start.3 = ((bf16[4,16,40,256]{3,2,1,0:T(8,128)(2,1)}), bf16[4,16,40,256]{3,2,1,0:T(8,128)(2,1)S(1)}, u32[]{:S(2)}, u32[]{:S(2)}) async-start(bf16[4,16,40,256]{3,2,1,0:T(8,128)(2,1)} %broadcast_in_dim.24), calls=%async_computation.3 | async-start | bytes 2621440 | tf_op jit(solution)/shard_map/all_to_all | solution.py:296
  123.8 6.1 %copy-start.2 = (bf16[4,16,40,256]{3,2,1,0:T(8,128)(2,1)}, bf16[4,16,40,256]{3,2,1,0:T(8,128)(2,1)S(1)}, u32[]{:S(2)}) copy-start(bf16[4,16,40,256]{3,2,1,0:T(8,128)(2,1)S(1)} %all-to-all-done.3.own) | copy-start | bytes 3932164
  124.9 21.5 %all-to-all-start.5 = ((bf16[4,256,512]{2,1,0:T(8,128)(2,1)}), bf16[4,256,512]{2,1,0:T(8,128)(2,1)S(1)}, u32[]{:S(2)}, u32[]{:S(2)}) async-start(bf16[4,256,512]{2,1,0:T(8,128)(2,1)} %broadcast_in_dim.27), calls=%async_computation.5 | async-start | bytes 2097152 | tf_op jit(solution)/shard_map/all_to_all | solution.py:296
  129.9 28.3 %collective-permute-start = (bf16[4,16,40,256]{3,2,1,0:T(8,128)(2,1)S(1)}, bf16[4,16,40,256]{3,2,1,0:T(8,128)(2,1)}, u32[]{:S(2)}, u32[]{:S(2)}) collective-permute-start(bf16[4,16,40,256]{3,2,1,0:T(8,128)(2,1)S(1)} %all-to-all-done.3.own), channel_id=1, source_target_pairs={{0,1},{1,0},{2,3},{3,2},{4,5},{5,4},{6,7},{7,6},{8,9},{9,8},{10,11... | collective-permute-start | bytes 3932168 | tf_op jit(solution)/shard_map/ppermute | solution.py:307
  146.4 9.3 %copy-start.16 = (f32[256]{0:T(256)S(1)}, f32[256]{0:T(256)}, u32[]{:S(2)}) copy-start(f32[256]{0:T(256)} %param.31) | copy-start | bytes 3076
  146.4 10.2 %copy-start.12 = (bf16[256,128]{1,0:T(8,128)(2,1)S(1)}, bf16[256,128]{1,0:T(8,128)(2,1)}, u32[]{:S(2)}) copy-start(bf16[256,128]{1,0:T(8,128)(2,1)} %param.33) | copy-start | bytes 196612
  146.4 10.2 %copy-start.13 = (bf16[256,128]{1,0:T(8,128)(2,1)S(1)}, bf16[256,128]{1,0:T(8,128)(2,1)}, u32[]{:S(2)}) copy-start(bf16[256,128]{1,0:T(8,128)(2,1)} %param.32) | copy-start | bytes 196612
  146.5 11.0 %copy-start.3 = (bf16[4,256,512]{2,1,0:T(8,128)(2,1)}, bf16[4,256,512]{2,1,0:T(8,128)(2,1)S(1)}, u32[]{:S(2)}) copy-start(bf16[4,256,512]{2,1,0:T(8,128)(2,1)S(1)} %all-to-all-done.5.wo) | copy-start | bytes 3145732
  146.5 11.0 %copy-start.18 = (f32[96]{0:T(128)S(1)}, f32[96]{0:T(128)}, u32[]{:S(2)}) copy-start(f32[96]{0:T(128)} %param.35) | copy-start | bytes 1156
  148.3 37.3 %all-to-all-start.4 = ((bf16[16,2,64,128]{3,2,1,0:T(8,128)(2,1)}), bf16[16,2,64,128]{3,2,1,0:T(8,128)(2,1)S(1)}, u32[]{:S(2)}, u32[]{:S(2)}) async-start(bf16[16,2,64,128]{3,2,1,0:T(8,128)(2,1)} %broadcast_in_dim.26), calls=%async_computation.4 | async-start | bytes 1048576 | tf_op jit(solution)/shard_map/all_to_all | solution.py:296
  (3 other events, 2.7 us)

commit v2 on v1

v2 whole, which is shorter than its diff:
```python
import jax
import jax.numpy as jnp
import numpy as np
from jax import lax
from jax.experimental import pallas as pl
from jax.experimental.pallas import tpu as pltpu
from jax.sharding import PartitionSpec as P


F32 = jnp.float32
BF16 = jnp.bfloat16

ROWS = 256
NOPE = 64
ROPE = 32
QK = NOPE + ROPE
CHUNK = 64
CHUNKS = ROWS // CHUNK
EPS = 1e-6
GROUP_EPS = 0.00064
NN = (((1,), (0,)), ((), ()))
NT = (((1,), (1,)), ((), ()))
TN = (((0,), (0,)), ((), ()))

VMEM = pl.BlockSpec(memory_space=pltpu.VMEM)
SMEM = pl.BlockSpec(memory_space=pltpu.SMEM)
ANY = pl.BlockSpec(memory_space=pl.ANY)


def dot(a, b, dims=NN):
    return lax.dot_general(a, b, dims, preferred_element_type=F32)


def halves(a):
    high = a.astype(BF16)
    return high, (a - high.astype(F32)).astype(BF16)


def fine(a, b, dims=NN):
    (i,), (j,) = dims[0]
    ah, al = halves(a)
    bh, bl = halves(b)
    wide = dot(jnp.concatenate([ah, al], axis=i), jnp.concatenate([bh, bh], axis=j), dims)
    return wide + dot(ah, bl, dims)


def dot_wide(a, b):
    high, low = halves(a)
    return dot(jnp.concatenate([high, low], axis=1), jnp.concatenate([b, b], axis=0))


def iota(shape, dim):
    return lax.broadcasted_iota(jnp.int32, shape, dim)


def call(body, outs, args, flops, scratch=(), specs=None, limit=24):
    return pl.pallas_call(
        body,
        out_shape=outs,
        in_specs=specs or [VMEM] * len(args),
        out_specs=jax.tree.map(lambda _: VMEM, outs),
        scratch_shapes=scratch,
        compiler_params=pltpu.CompilerParams(vmem_limit_bytes=limit << 20),
        cost_estimate=pl.CostEstimate(flops=flops, bytes_accessed=4 << 20, transcendentals=0),
    )(*args)


def turned(n, table):
    half = ROPE // 2
    a, b = n[NOPE : NOPE + half], n[NOPE + half :]
    cosine, sine = table[:half], table[half:]
    return a * cosine - b * sine, b * cosine + a * sine


def prepare_body(place, x, gain, wa, wk, wv, wq, wc, wr, xs, small, big, turned_wc):
    v = x[...].astype(F32)
    v = v * lax.rsqrt(jnp.mean(v * v, axis=-1, keepdims=True) + EPS) * gain[...]
    v = v.astype(BF16)
    for i in range(8):
        xs[i] = v
    turned_wc[...] = wc[...].astype(F32).T
    start = pl.multiple_of(place[1] * 32, 32)
    small[0:32] = turned_wc[pl.ds(start, 32), :].astype(BF16)
    small[32:64] = wr[...]
    big[:, 0:128] = wa[...]
    big[:, 128:256] = wk[...]
    big[:, 256:384] = wv[...]
    big[0:192, 384:640] = wq[:, 0:256]
    big[192:384, 384:640] = wq[:, 256:512]
    big[384:512, 384:640] = jnp.zeros((128, 256), BF16)


def prepare(*args):
    outs = [
        jax.ShapeDtypeStruct((8, 32, 2048), BF16),
        jax.ShapeDtypeStruct((64, 512), BF16),
        jax.ShapeDtypeStruct((512, 640), BF16),
    ]
    scratch = [pltpu.VMEM((256, 512), F32)]
    return call(prepare_body, outs, args, 1 << 29, scratch, [SMEM] + [VMEM] * 8)


def columns(place, k):
    shard = lax.rem(place[2] + (0, 3, 1, 2)[k], 4)
    return pl.ds(pl.multiple_of(shard * 512, 512), 512)


def latents_body(place, x, w0, w1, w2, w3, pay):
    t = jnp.zeros((64, ROWS), F32)
    for k, w in enumerate((w0, w1, w2, w3)):
        t += dot(w[...], x[:, columns(place, k)], NT)
    tp = place[1]
    group = jnp.zeros((8, ROWS), F32)
    for g in range(4):
        group += jnp.where(tp // 2 == g, t[32 + 8 * g : 40 + 8 * g], 0.0)
    group = jnp.where(iota((8, ROWS), 0) // 4 == lax.rem(tp, 2), group, 0.0)
    both = jnp.concatenate([t[0:32], group], axis=0).astype(BF16)
    for i in range(16):
        pay[i] = both


def latents(*args):
    outs = jax.ShapeDtypeStruct((16, 40, ROWS), BF16)
    return call(latents_body, outs, args, 1 << 29, specs=[SMEM] + [VMEM] * 5)


def project_body(
    place, x, w0, w1, w2, w3, fd, fa, table, gain, up, glat, kgain, mult, extra, present,
    rkv, q, dlow, rlow,
):
    y = jnp.zeros((ROWS, 384), F32)
    t = jnp.zeros((192, ROWS), F32)
    for k, w in enumerate((w0, w1, w2, w3)):
        part = x[:, columns(place, k)]
        y += dot(part, w[:, 0:384])
        t += dot(jnp.concatenate([w[0:192, 384:640], w[192:384, 384:640]], axis=1), part, NT)
    rkv[...] = y.astype(BF16)
    t = t.astype(BF16).astype(F32)
    turn = table[place[0]]
    for h in range(2):
        v = t[QK * h : QK * (h + 1)]
        n = v * lax.rsqrt(jnp.mean(v * v, axis=0, keepdims=True) + EPS) * gain[...]
        a, b = turned(n, turn)
        ready = jnp.concatenate([n[:NOPE], a, b, jnp.zeros((128 - QK, ROWS), F32)], axis=0)
        q[h] = ready.T.astype(BF16)
    dlow[...] = jnp.tanh(dot(x[...], fd[...]).astype(BF16).astype(F32)).astype(BF16)
    rlow[...] = dot(x[...], fa[...]).astype(BF16)


def project(*args):
    outs = [
        jax.ShapeDtypeStruct((ROWS, 384), BF16),
        jax.ShapeDtypeStruct((2, ROWS, 128), BF16),
        jax.ShapeDtypeStruct((ROWS, 128), BF16),
        jax.ShapeDtypeStruct((ROWS, 128), BF16),
    ]
    return call(project_body, outs, args, 4 << 30, specs=[SMEM] + [VMEM] * 9 + [ANY] * 6)


def recur_body(rkv, dlow, rlow, wd, bd, wa, ba, mult, extra, present, free, along, bonus, state):
    lane = iota((ROWS, 128), 1)
    recept, key, value = (rkv[:, 128 * i : 128 * (i + 1)].astype(F32) for i in range(3))
    speed = jax.nn.sigmoid(bd[...] + dot(dlow[...], wd[...])) * np.float32(np.exp(-0.5))
    added = jnp.where(lane < 64, extra[:, 0:1], extra[:, 1:2])
    ld = added - speed * mult[...]
    learn = jax.nn.sigmoid(ba[...] + dot(rlow[...], wa[...]))
    same = (iota((128, 128), 0) // 64 == iota((128, 128), 1) // 64).astype(BF16)
    unit = key * lax.rsqrt(dot_wide(key * key, same) + EPS)
    bonus[...] = dot_wide(recept * key * present[...], same) * value
    r, c = iota((ROWS, ROWS), 0), iota((ROWS, ROWS), 1)
    block = r // CHUNK == c // CHUNK
    sums = jnp.concatenate(
        [
            jnp.where(block & (c <= r), 1.0, 0.0),
            jnp.where(block & (lax.rem(c, CHUNK) < CHUNK // 2), 1.0, 0.0),
            jnp.where(block, 1.0, 0.0),
        ],
        axis=0,
    )
    sums = sums.astype(BF16)
    high, low = halves(ld)
    last = (ld - high.astype(F32) - low.astype(F32)).astype(BF16)
    sums = dot(
        jnp.concatenate([sums, sums, sums], axis=1), jnp.concatenate([high, low, last], axis=0)
    )
    cum, mid, end = sums[:ROWS], sums[ROWS : 2 * ROWS], sums[2 * ROWS :]
    prev = cum - ld
    toward = -unit
    remove = unit * learn
    grow, shrink = jnp.exp(cum - mid), jnp.exp(mid - cum)
    left1, left2 = toward * jnp.exp(prev - mid), recept * grow
    right1, right2 = remove * shrink, key * shrink
    start1, start2 = toward * jnp.exp(prev), recept * jnp.exp(cum)
    tail = jnp.exp(end - cum)
    tail1, tail2 = remove * tail, key * tail
    whole = jnp.exp(end)
    m0 = iota((CHUNK, 128), 1) < 64

    def stacked(v, k):
        v = v[CHUNK * k : CHUNK * (k + 1)]
        return jnp.concatenate([jnp.where(m0, v, 0.0), jnp.where(m0, 0.0, v)], axis=0)

    rr, cc = iota((128, 128), 0), iota((128, 128), 1)
    head = rr // 64 == cc // 64
    eye = jnp.where(rr == cc, 1.0, 0.0)
    in16, in32 = rr // 16 == cc // 16, rr // 32 == cc // 32
    strict, upto = head & (rr > cc), head & (rr >= cc)

    def square(top, mask):
        both = jnp.concatenate([top, top], axis=1)
        return jnp.where(mask, both, 0.0)

    stage = []
    for k in range(CHUNKS):
        rows = jnp.concatenate([stacked(left1, k), stacked(left2, k)], axis=0)
        part = slice(CHUNK * k, CHUNK * (k + 1))
        cols = jnp.concatenate([right1[part], right2[part]], axis=0)
        g = fine(rows, cols, NT)
        a = square(g[:128, :64], strict)
        kb = square(g[:128, 64:], strict)
        ru = square(g[128:, :64], upto)
        ku = square(g[128:, 64:], upto)
        stage.append([a, kb, ru, ku])
    inverse = []
    for k in range(CHUNKS):
        a = stage[k][0]
        small = jnp.where(in16, a, 0.0)
        power = small
        t = eye + small
        for _ in range(3):
            power = fine(power, power)
            t = t + fine(t, power)
        t = t + fine(fine(t, jnp.where(in32 & ~in16, a, 0.0)), t)
        t = t + fine(fine(t, jnp.where(in32, 0.0, a)), t)
        inverse.append(t)
    pair = jnp.concatenate([jnp.zeros((128, 128), F32), eye], axis=0)
    for k in range(CHUNKS):
        _, kb, ru, ku = stage[k]
        v = stacked(value, k)
        xy = fine(inverse[k], jnp.concatenate([stacked(start1, k), fine(kb, v)], axis=1))
        read = fine(ru, xy)
        coef = stacked(start2, k) + read[:, :128]
        rest = read[:, 128:] + fine(ku, v)
        t1, t2 = stacked(tail1, k), stacked(tail2, k)
        moved = fine(xy, t1, TN)
        decay = whole[CHUNK * k : CHUNK * k + 1]
        step = moved[:128] + jnp.where(rr == cc, decay, 0.0)
        add = moved[128:] + fine(v, t2, TN)
        out = fine(coef, pair, NT)
        near = out[:, :128] + rest
        far = out[:, 128:]
        part = slice(CHUNK * k, CHUNK * (k + 1))
        free[part] = near[:64] + near[64:]
        along[part] = far[:64] + far[64:]
        pair = fine(pair, step) + jnp.concatenate([add, jnp.zeros((128, 128), F32)], axis=0)
    far = (pair[128:192] + pair[192:]).astype(BF16)
    near = (pair[:64] + pair[64:128]).astype(BF16)
    for i in range(16):
        state[i, 0] = far
        state[i, 1] = near


def recur(*args):
    wide = jax.ShapeDtypeStruct((ROWS, 128), F32)
    outs = [wide, wide, wide, jax.ShapeDtypeStruct((16, 2, 64, 128), BF16)]
    return call(recur_body, outs, args, 8 << 30)


def attend_body(place, q, own, peer, w, glat, gain, table, att, logs, acc, top):
    sp = place[0]
    factor = np.float32(QK**-0.5 * np.log2(np.e))
    ones = jnp.where(iota((NOPE, ROWS), 0) == 0, 1.0, 0.0).astype(BF16)

    def keys(j):
        lat = jnp.concatenate(
            [own[:, j, 0:32, :].reshape(128, ROWS), peer[:, j, 0:32, :].reshape(128, ROWS)], axis=0
        ).astype(F32)
        rope = (own[:, j, 32:40, :].astype(F32) + peer[:, j, 32:40, :].astype(F32)).reshape(
            ROPE, ROWS
        )
        lat = lat * lax.rsqrt(jnp.mean(lat * lat, axis=0, keepdims=True) + EPS) * glat[...]
        kv = dot(w[...], lat.astype(BF16)).astype(BF16)
        rope_sum = jnp.sum(rope * rope, axis=0, keepdims=True)
        turn = table[j]
        cosine, sine = turn[:16], turn[16:]
        ra, rb = rope[:16] * gain[64:80], rope[16:] * gain[80:96]
        ra, rb = ra * cosine - rb * sine, rb * cosine + ra * sine
        ready, values = [], []
        for h in range(2):
            k = kv[64 * h : 64 * (h + 1)].astype(F32)
            scale = lax.rsqrt(
                (jnp.sum(k * k, axis=0, keepdims=True) + rope_sum) * np.float32(1 / QK) + EPS
            )
            ready.append(
                jnp.concatenate([k * scale * gain[0:64], ra * scale, rb * scale], axis=0).astype(
                    BF16
                )
            )
            values.append(jnp.concatenate([kv[128 + 64 * h : 192 + 64 * h], ones], axis=0))
        return ready, values

    def block(places, first):
        made = [keys(j) for j in places]
        for h in range(2):
            ready = jnp.concatenate([m[0][h] for m in made], axis=1)
            v = jnp.concatenate([m[1][h] for m in made], axis=1)
            s = dot(q[h, :, 0:QK], ready) * factor
            if first:
                s = jnp.where(iota((ROWS, ROWS), 1) <= iota((ROWS, ROWS), 0), s, -jnp.inf)
            peak = jnp.max(s, axis=1, keepdims=True)
            if first:
                top[h] = jnp.broadcast_to(peak, (ROWS, 128))
                acc[h] = dot(jnp.exp2(s - peak).astype(BF16), v, NT)
            else:
                old = top[h]
                new = jnp.maximum(old, peak)
                top[h] = new
                p = jnp.exp2(s - new[:, 0:1]).astype(BF16)
                acc[h] = acc[h] * jnp.exp2(old - new) + dot(p, v, NT)

    block([sp], True)

    def loop(i, carry):
        block([2 * i, 2 * i + 1], False)
        return carry

    lax.fori_loop(0, sp // 2, loop, 0)

    @pl.when(lax.rem(sp, 2) == 1)
    def _():
        block([sp - 1], False)

    parts = []
    rows = []
    for h in range(2):
        total = acc[h][:, 64:65]
        parts.append(acc[h][:, 0:64] / total)
        full = top[h] * np.float32(np.log(2.0)) + jnp.log(jnp.broadcast_to(total, (ROWS, 128)))
        rows.append(full.T[0:1])
    att[...] = jnp.concatenate(parts, axis=1).astype(BF16)
    logs[...] = jnp.concatenate(rows, axis=0)


def attend(*args):
    outs = [jax.ShapeDtypeStruct((ROWS, 128), BF16), jax.ShapeDtypeStruct((2, ROWS), F32)]
    scratch = [pltpu.VMEM((2, ROWS, 128), F32), pltpu.VMEM((2, ROWS, 128), F32)]
    return call(attend_body, outs, args, 8 << 30, scratch, [SMEM] + [VMEM] * 7)


def merge_body(place, att, free, along, bonus, states, branch, o0, o1, o2, o3, out):
    head = iota((128, 128), 0) // 64 == iota((128, 128), 1) // 64

    def spread(v):
        return jnp.where(head, jnp.concatenate([v, v], axis=0), jnp.zeros((), v.dtype))

    def step(r, entering):
        return dot_wide(entering, spread(states[r, 0])) + spread(states[r, 1]).astype(F32)

    entering = lax.fori_loop(0, place[0], step, jnp.zeros((128, 128), F32))
    read = free[...] + fine(along[...], entering, NT)
    mean = jnp.where(head, 1.0 / 64, 0.0).astype(BF16)
    read = read - dot_wide(read, mean)
    spread_of = dot_wide(read * read, mean)
    rec = read * lax.rsqrt(spread_of + GROUP_EPS) * branch[...] + bonus[...]
    both = jnp.concatenate([att[...], rec.astype(BF16)], axis=1)
    for k, o in enumerate((o0, o1, o2, o3)):
        out[:, columns(place, k)] = dot(both, o[...]).astype(BF16)


def merge(*args):
    outs = jax.ShapeDtypeStruct((ROWS, 2048), BF16)
    return call(merge_body, outs, args, 4 << 30, specs=[SMEM] + [VMEM] * 10)


def exchanged(copies, axis, groups=None):
    return lax.all_to_all(copies, axis, 0, 0, axis_index_groups=groups, tiled=True)


def around(value):
    moves = [[(i, (i + by) % 4) for i in range(4)] for by in (1, 3, 2)]
    return [value] + [lax.ppermute(value, "fs", move) for move in moves]


def other_core(value):
    return lax.ppermute(value, "tp", [(i, i ^ 1) for i in range(8)])


def turn_table():
    half = ROPE // 2
    inverse = np.float32(10000.0) ** (-np.arange(half, dtype=np.float32) / np.float32(half))
    angle = np.arange(4096, dtype=np.float32)[:, None] * inverse.astype(np.float32)[None, :]
    both = np.concatenate([np.cos(angle), np.sin(angle)], axis=1).astype(np.float32)
    return both.reshape(16, ROWS, ROPE).transpose(0, 2, 1)


def shards(
    entering,
    entering_gain,
    wq,
    wc,
    wr,
    compact_gain,
    wk_up,
    wv_up,
    q_gain,
    k_gain,
    w_accept,
    w_key,
    w_value,
    fade1,
    fade2,
    fade_bias,
    fade_mult,
    fade_extra,
    adapt1,
    adapt2,
    adapt_bias,
    present,
    branch,
    wo_att,
    wo_rec,
):
    tp = lax.axis_index("tp")
    sp = lax.axis_index("sp")
    core = lax.rem(tp, 2)
    place = jnp.stack([sp, tp, lax.axis_index("fs")]).astype(jnp.int32)
    xs, small, big = prepare(
        place,
        entering[0],
        entering_gain.reshape(1, 2048),
        w_accept,
        w_key,
        w_value,
        wq.T,
        wc,
        wr.T,
    )
    normed = exchanged(xs, "tp").reshape(ROWS, 2048)
    smalls = around(small)
    bigs = around(big)

    def reordered(v):
        v = v.reshape(4, 2, 32, *v.shape[1:])
        v = jnp.where(core == 0, v, v[:, ::-1])
        return jnp.moveaxis(v, 1, 0).reshape(256, *v.shape[3:])

    up = reordered(jnp.concatenate([wk_up, wv_up], axis=1)).T
    glat = reordered(compact_gain).reshape(256, 1)
    key_gain = k_gain.reshape(QK, 1)
    mult = jnp.repeat(fade_mult[0, :, 0], 64).reshape(1, 128)
    extra = fade_extra[0].T
    present = present.reshape(1, 128)
    table = jnp.asarray(turn_table())
    pay = latents(place, normed, *smalls)
    lat = exchanged(pay, "sp")
    wo = around(jnp.concatenate([wo_att, wo_rec], axis=0))
    projected = project(
        place,
        normed,
        *bigs,
        fade1,
        adapt1,
        table,
        q_gain.reshape(QK, 1),
        up,
        glat,
        key_gain,
        mult,
        extra,
        present,
    )
    lat, (rkv, q, dlow, rlow) = lax.optimization_barrier((lat, tuple(projected)))
    same_core = [[0, 2, 4, 6], [1, 3, 5, 7]]
    lat_own = exchanged(jnp.broadcast_to(lat[None], (4, *lat.shape)), "tp", same_core)
    recurrent = recur(
        rkv,
        dlow,
        rlow,
        fade2,
        fade_bias.reshape(1, 128),
        adapt2,
        adapt_bias.reshape(1, 128),
        mult,
        extra,
        present,
    )
    lat_own, (free, along, bonus, state) = lax.optimization_barrier((lat_own, tuple(recurrent)))
    states = exchanged(state, "sp")
    lat_peer = other_core(lat_own)
    att, logs = attend(place, q, lat_own, lat_peer, up, glat, key_gain, table)
    partial = merge(place, att, free, along, bonus, states, branch.reshape(1, 128), *wo)
    parts = exchanged(partial.reshape(8, 32, 2048), "tp")
    mixed = jnp.sum(parts.astype(F32), axis=0).astype(BF16)
    return mixed[None], logs[None]


def solution(mesh):
    placed = (
        P("fs", ("sp", "tp"), None),
        P(),
        P("fs", "tp"),
        P("fs", None),
        P("fs", None),
        P(),
        P(None, "tp"),
        P(None, "tp"),
        P(),
        P(),
        P("fs", "tp"),
        P("fs", "tp"),
        P("fs", "tp"),
        P(),
        P(None, "tp"),
        P("tp"),
        P("fs", "tp", "sp"),
        P("fs", "tp", "sp"),
        P(),
        P(None, "tp"),
        P("tp"),
        P("tp", None),
        P("tp"),
        P("tp", "fs"),
        P("tp", "fs"),
    )

    return jax.shard_map(
        shards,
        mesh=mesh,
        in_specs=placed,
        out_specs=(P("fs", ("sp", "tp"), None), P("fs", "tp", "sp")),
        check_vma=False,
    )
```

time: 211 us -> 178 us (0.84)
  starting transfers between devices: 27.6 us -> 66.4 us
  blocking collectives: 53.2 us -> 18.4 us
  waiting for transfers between devices: 81.2 us -> 52.4 us
  Pallas kernels: 27.4 us -> 21.1 us
  other arithmetic: 3.57 us -> 0.94 us
    all_to_all x5 -> x4, waiting for transfers between devices: 81.2 us -> 19.9 us  [exchanged(): lax.all_to_all(copies, axis, 0, 0, axis_index_groups=groups, tiled=True)]
    all_to_all x2 -> x1, blocking collectives: 53.2 us -> 18.4 us  [exchanged(): lax.all_to_all(copies, axis, 0, 0, axis_index_groups=groups, tiled=True)]
    ppermute x0 -> x9, waiting for transfers between devices: none -> 32.5 us  [around(): return [value] + [lax.ppermute(value, 'fs', move) for move in moves]]
    ppermute x0 -> x9, starting transfers between devices: none -> 29.1 us  [around(): return [value] + [lax.ppermute(value, 'fs', move) for move in moves]]
    unnamed x51 -> x64, local copies, waits for them, and re-layouts: 3.82 us -> 13.8 us
    all_to_all x5 -> x4, starting transfers between devices: 25.5 us -> 35.4 us  [exchanged(): lax.all_to_all(copies, axis, 0, 0, axis_index_groups=groups, tiled=True)]
    pallas_call x4 -> x6, Pallas kernels: 27.4 us -> 21.1 us  [call(): pl.pallas_call(body, out_shape=outs, in_specs=specs or [VMEM] * len(args)...]
    broadcast_in_dim x7 -> x2, local copies, waits for them, and re-layouts: 7.91 us -> 2.25 us  [the longest x1 2.17 us: shards(): jnp.broadcast_to(lat[None], (4, *lat.shape))]
  transfers between devices with their start and end apart: 6 -> 14, of which waited for: 4 -> 8; matrix products, arithmetic and copies ran while one was open for 4% -> 1% of each run, Pallas kernels for 9% -> 9%
where the time goes in v2:
time: 178 us; the launch traced here: 177 us
  starting transfers between devices  66.4 us (37%)
  waiting for transfers between devices  52.4 us (29%)
  Pallas kernels  21.1 us (12%)
  blocking collectives  18.4 us (10%)
  local copies, waits for them, and re-layouts  16.9 us (9%)
    all_to_all x4, starting transfers between devices, exchanged(): lax.all_to_all(copies, axis, 0, 0, axis_index_groups=groups, tiled=True)  35.4 us
    ppermute x9, waiting for transfers between devices, around(): return [value] + [lax.ppermute(value, 'fs', move) for move in moves]  32.5 us
    ppermute x9, starting transfers between devices, around(): return [value] + [lax.ppermute(value, 'fs', move) for move in moves]  29.1 us
    pallas_call x6, Pallas kernels, call(): pl.pallas_call(body, out_shape=outs, in_specs=specs or [VMEM] * len(args)...  21.1 us
    all_to_all x4, waiting for transfers between devices, exchanged(): lax.all_to_all(copies, axis, 0, 0, axis_index_groups=groups, tiled=True)  19.9 us
    all_to_all x1, blocking collectives, exchanged(): lax.all_to_all(copies, axis, 0, 0, axis_index_groups=groups, tiled=True)  18.4 us
    unnamed x64, local copies, waits for them, and re-layouts  13.8 us
  transfers between devices with their start and end apart: 14, of which 8 were waited for; matrix products, arithmetic and copies ran while one was open for 1% of the time, Pallas kernels for 9%

profile of v2, /device:TPU:40, one launch (start us, length us, event | category | flops | bytes accessed | tf_op | source)
XLA Modules:
  0.0 177.1 jit_solution(6361969534769045874)
XLA Ops:
  9.4 4.3 %all-to-all-start = ((bf16[8,32,2048]{2,1,0:T(8,128)(2,1)}), bf16[8,32,2048]{2,1,0:T(8,128)(2,1)S(1)}, u32[]{:S(2)}, u32[]{:S(2)}) async-start(bf16[8,32,2048]{2,1,0:T(8,128)(2,1)} %get-tuple-element.25), calls=%async_computation | async-start | bytes 2097152 | tf_op jit(solution)/shard_map/all_to_all | solution.py:376
  13.7 3.5 %collective-permute-start = (bf16[64,512]{1,0:T(8,128)(2,1)S(1)}, bf16[64,512]{1,0:T(8,128)(2,1)S(1)}, u32[]{:S(2)}, u32[]{:S(2)}) collective-permute-start(bf16[64,512]{1,0:T(8,128)(2,1)S(1)} %get-tuple-element.26.w0), channel_id=1, source_target_pairs={{0,8},{8,16},{16,24},{24,0},{1,9},{9,17},{17,25},{25,1},{2,10},{10... | collective-permute-start | bytes 196616 | tf_op jit(solution)/shard_map/ppermute | solution.py:381
  17.2 2.4 %collective-permute-start.1 = (bf16[64,512]{1,0:T(8,128)(2,1)S(1)}, bf16[64,512]{1,0:T(8,128)(2,1)S(1)}, u32[]{:S(2)}, u32[]{:S(2)}) collective-permute-start(bf16[64,512]{1,0:T(8,128)(2,1)S(1)} %get-tuple-element.26.w0), channel_id=1, source_target_pairs={{0,24},{8,0},{16,8},{24,16},{1,25},{9,1},{17,9},{25,17},{2,26},{10... | collective-permute-start | bytes 196616 | tf_op jit(solution)/shard_map/ppermute | solution.py:381
  19.5 4.2 %collective-permute-start.2 = (bf16[64,512]{1,0:T(8,128)(2,1)S(1)}, bf16[64,512]{1,0:T(8,128)(2,1)S(1)}, u32[]{:S(2)}, u32[]{:S(2)}) collective-permute-start(bf16[64,512]{1,0:T(8,128)(2,1)S(1)} %get-tuple-element.26.w0), channel_id=1, source_target_pairs={{0,16},{8,24},{16,0},{24,8},{1,17},{9,25},{17,1},{25,9},{2,18},{10... | collective-permute-start | bytes 196616 | tf_op jit(solution)/shard_map/ppermute | solution.py:381
  23.8 3.4 %collective-permute-done.2.w3 = bf16[64,512]{1,0:T(8,128)(2,1)S(1)} collective-permute-done((bf16[64,512]{1,0:T(8,128)(2,1)S(1)}, bf16[64,512]{1,0:T(8,128)(2,1)S(1)}, u32[]{:S(2)}, u32[]{:S(2)}) %collective-permute-start.2) | collective-permute-done | bytes 65568 | tf_op jit(solution)/shard_map/ppermute | solution.py:381
  27.2 2.4 %all-to-all-done = bf16[8,32,2048]{2,1,0:T(8,128)(2,1)S(1)} async-done(((bf16[8,32,2048]{2,1,0:T(8,128)(2,1)}), bf16[8,32,2048]{2,1,0:T(8,128)(2,1)S(1)}, u32[]{:S(2)}, u32[]{:S(2)}) %all-to-all-start) | async-done | bytes 1048608 | tf_op jit(solution)/shard_map/all_to_all | solution.py:376
  31.4 15.4 %all-to-all-start.1 = ((bf16[16,40,256]{2,1,0:T(8,128)(2,1)}), bf16[16,40,256]{2,1,0:T(8,128)(2,1)}, u32[]{:S(2)}, u32[]{:S(2)}) async-start(bf16[16,40,256]{2,1,0:T(8,128)(2,1)} %shard_map.258), calls=%async_computation.1 | async-start | bytes 655360 | tf_op jit(solution)/shard_map/all_to_all | solution.py:376
  46.8 3.5 %collective-permute-start.3 = (bf16[512,640]{1,0:T(8,128)(2,1)S(1)}, bf16[512,640]{1,0:T(8,128)(2,1)}, u32[]{:S(2)}, u32[]{:S(2)}) collective-permute-start(bf16[512,640]{1,0:T(8,128)(2,1)S(1)} %get-tuple-element.27.w0), channel_id=1, source_target_pairs={{0,8},{8,16},{16,24},{24,0},{1,9},{9,17},{17,25},{25,1},{2,10},{10... | collective-permute-start | bytes 1966088 | tf_op jit(solution)/shard_map/ppermute | solution.py:381
  50.2 2.4 %collective-permute-start.4 = (bf16[512,640]{1,0:T(8,128)(2,1)S(1)}, bf16[512,640]{1,0:T(8,128)(2,1)}, u32[]{:S(2)}, u32[]{:S(2)}) collective-permute-start(bf16[512,640]{1,0:T(8,128)(2,1)S(1)} %get-tuple-element.27.w0), channel_id=1, source_target_pairs={{0,24},{8,0},{16,8},{24,16},{1,25},{9,1},{17,9},{25,17},{2,26},{10... | collective-permute-start | bytes 1966088 | tf_op jit(solution)/shard_map/ppermute | solution.py:381
  52.6 4.2 %collective-permute-start.5 = (bf16[512,640]{1,0:T(8,128)(2,1)S(1)}, bf16[512,640]{1,0:T(8,128)(2,1)}, u32[]{:S(2)}, u32[]{:S(2)}) collective-permute-start(bf16[512,640]{1,0:T(8,128)(2,1)S(1)} %get-tuple-element.27.w0), channel_id=1, source_target_pairs={{0,16},{8,24},{16,0},{24,8},{1,17},{9,25},{17,1},{25,9},{2,18},{10... | collective-permute-start | bytes 1966088 | tf_op jit(solution)/shard_map/ppermute | solution.py:381
  58.1 8.3 %collective-permute-done.3.w1 = bf16[512,640]{1,0:T(8,128)(2,1)} collective-permute-done((bf16[512,640]{1,0:T(8,128)(2,1)S(1)}, bf16[512,640]{1,0:T(8,128)(2,1)}, u32[]{:S(2)}, u32[]{:S(2)}) %collective-permute-start.3) | collective-permute-done | bytes 655392 | tf_op jit(solution)/shard_map/ppermute | solution.py:381
  66.4 2.8 %collective-permute-done.4.w2 = bf16[512,640]{1,0:T(8,128)(2,1)} collective-permute-done((bf16[512,640]{1,0:T(8,128)(2,1)S(1)}, bf16[512,640]{1,0:T(8,128)(2,1)}, u32[]{:S(2)}, u32[]{:S(2)}) %collective-permute-start.4) | collective-permute-done | bytes 655392 | tf_op jit(solution)/shard_map/ppermute | solution.py:381
  69.1 13.2 %collective-permute-done.5.w3 = bf16[512,640]{1,0:T(8,128)(2,1)} collective-permute-done((bf16[512,640]{1,0:T(8,128)(2,1)S(1)}, bf16[512,640]{1,0:T(8,128)(2,1)}, u32[]{:S(2)}, u32[]{:S(2)}) %collective-permute-start.5) | collective-permute-done | bytes 655392 | tf_op jit(solution)/shard_map/ppermute | solution.py:381
  85.5 3.0 %shard_map.259 = (bf16[256,384]{1,0:T(8,128)(2,1)S(1)}, bf16[2,256,128]{2,1,0:T(8,128)(2,1)S(1)}, bf16[256,128]{1,0:T(8,128)(2,1)S(1)}, bf16[256,128]{1,0:T(8,128)(2,1)S(1)}) custom-call(s32[3]{0:T(128)S(1)} %pad_add_fusion.place, bf16[256,2048]{1,0:T(8,128)(2,1)S(1)} %bitcast.27, bf16[512,640]{1,0:T(8,128)(2,1)S(1)} %get-tuple-element.27.w0, ...), custom_call_target="tpu_custom_call" | custom-call | flops 4294967296 | bytes 4194304 | tf_op jit(solution)/shard_map/pallas_call | solution.py:57
  90.7 3.7 %all-to-all-start.2 = ((bf16[4,16,40,256]{3,2,1,0:T(8,128)(2,1)}), bf16[4,16,40,256]{3,2,1,0:T(8,128)(2,1)S(1)}, u32[]{:S(2)}, u32[]{:S(2)}) async-start(bf16[4,16,40,256]{3,2,1,0:T(8,128)(2,1)} %broadcast_in_dim.16), calls=%async_computation.2 | async-start | bytes 2621440 | tf_op jit(solution)/shard_map/all_to_all | solution.py:376
  94.5 9.3 %shard_map.260 = (f32[256,128]{1,0:T(8,128)S(1)}, f32[256,128]{1,0:T(8,128)S(1)}, f32[256,128]{1,0:T(8,128)S(1)}, bf16[16,2,64,128]{3,2,1,0:T(8,128)(2,1)}) custom-call(bf16[256,384]{1,0:T(8,128)(2,1)S(1)} %get-tuple-element.34.rkv, bf16[256,128]{1,0:T(8,128)(2,1)S(1)} %get-tuple-element.35.dlow, bf16[256,128]{1,0:T(8,128)(2,1)S(1)} %get-tuple-element.36.rlow, ...), custom_call_target="tpu_custom_call" | custom-call | flops 8589934592 | bytes 4194304 | tf_op jit(solution)/shard_map/pallas_call | solution.py:57
  104.4 6.2 %all-to-all-done.2.own = bf16[4,16,40,256]{3,2,1,0:T(8,128)(2,1)S(1)} async-done(((bf16[4,16,40,256]{3,2,1,0:T(8,128)(2,1)}), bf16[4,16,40,256]{3,2,1,0:T(8,128)(2,1)S(1)}, u32[]{:S(2)}, u32[]{:S(2)}) %all-to-all-start.2) | async-done | bytes 1310752 | tf_op jit(solution)/shard_map/all_to_all | solution.py:376
  112.5 12.0 %all-to-all-start.3 = ((bf16[16,2,64,128]{3,2,1,0:T(8,128)(2,1)}), bf16[16,2,64,128]{3,2,1,0:T(8,128)(2,1)S(1)}, u32[]{:S(2)}, u32[]{:S(2)}) async-start(bf16[16,2,64,128]{3,2,1,0:T(8,128)(2,1)} %get-tuple-element.46), calls=%async_computation.3 | async-start | bytes 1048576 | tf_op jit(solution)/shard_map/all_to_all | solution.py:376
  126.5 3.9 %collective-permute-start.8 = (bf16[256,512]{1,0:T(8,128)(2,1)S(1)}, bf16[256,512]{1,0:T(8,128)(2,1)S(1)}, u32[]{:S(2)}, u32[]{:S(2)}) collective-permute-start(bf16[256,512]{1,0:T(8,128)(2,1)S(1)} %constant_dynamic-update-slice_fusion.o0), channel_id=1, source_target_pairs={{0,24},{8,0},{16,8},{24,16},{1,25},{9,1},{17,9},{25,17},{2,26},{10... | collective-permute-start | bytes 786440 | tf_op jit(solution)/shard_map/ppermute | solution.py:381
  130.5 3.2 %collective-permute-start.9 = (bf16[256,512]{1,0:T(8,128)(2,1)S(1)}, bf16[256,512]{1,0:T(8,128)(2,1)S(1)}, u32[]{:S(2)}, u32[]{:S(2)}) collective-permute-start(bf16[256,512]{1,0:T(8,128)(2,1)S(1)} %constant_dynamic-update-slice_fusion.o0), channel_id=1, source_target_pairs={{0,16},{8,24},{16,0},{24,8},{1,17},{9,25},{17,1},{25,9},{2,18},{10... | collective-permute-start | bytes 786440 | tf_op jit(solution)/shard_map/ppermute | solution.py:381
  134.7 3.7 %shard_map.261 = (bf16[256,128]{1,0:T(8,128)(2,1)S(1)}, f32[2,256]{1,0:T(2,128)}) custom-call(s32[3]{0:T(128)S(1)} %pad_add_fusion.place, bf16[2,256,128]{2,1,0:T(8,128)(2,1)S(1)} %get-tuple-element.32.q, bf16[4,16,40,256]{3,2,1,0:T(8,128)(2,1)S(1)} %all-to-all-done.2.own, bf16[4,16,40,256]{3,2,1,0:T(8,128)(2,1)} %collective-permute-done.6.peer, ...), custom_call_target="tpu_custom_call" | custom-call | flops 8589934592 | bytes 4194304 | tf_op jit(solution)/shard_map/pallas_call | solution.py:57
  138.4 4.7 %collective-permute-done.9.o3 = bf16[256,512]{1,0:T(8,128)(2,1)S(1)} collective-permute-done((bf16[256,512]{1,0:T(8,128)(2,1)S(1)}, bf16[256,512]{1,0:T(8,128)(2,1)S(1)}, u32[]{:S(2)}, u32[]{:S(2)}) %collective-permute-start.9) | collective-permute-done | bytes 262176 | tf_op jit(solution)/shard_map/ppermute | solution.py:381
  143.2 11.3 %all-to-all-done.3.states = bf16[16,2,64,128]{3,2,1,0:T(8,128)(2,1)S(1)} async-done(((bf16[16,2,64,128]{3,2,1,0:T(8,128)(2,1)}), bf16[16,2,64,128]{3,2,1,0:T(8,128)(2,1)S(1)}, u32[]{:S(2)}, u32[]{:S(2)}) %all-to-all-start.3) | async-done | bytes 524320 | tf_op jit(solution)/shard_map/all_to_all | solution.py:376
  157.9 18.4 %all_to_all.25 = bf16[8,32,2048]{2,1,0:T(8,128)(2,1)S(1)} all-to-all(bf16[8,32,2048]{2,1,0:T(8,128)(2,1)S(1)} %bitcast.28), channel_id=1, replica_groups=mesh['sp'=16,'fs'=4,'tp'=8] {'tp'}, dimensions={0} | all-to-all | bytes 2097152 | tf_op jit(solution)/shard_map/all_to_all | solution.py:376
  (94 shorter events, 26.7 us)
Async XLA Ops:
  9.4 20.2 %all-to-all-start = ((bf16[8,32,2048]{2,1,0:T(8,128)(2,1)}), bf16[8,32,2048]{2,1,0:T(8,128)(2,1)S(1)}, u32[]{:S(2)}, u32[]{:S(2)}) async-start(bf16[8,32,2048]{2,1,0:T(8,128)(2,1)} %get-tuple-element.25), calls=%async_computation | async-start | bytes 2097152 | tf_op jit(solution)/shard_map/all_to_all | solution.py:376
  13.7 10.1 %collective-permute-start = (bf16[64,512]{1,0:T(8,128)(2,1)S(1)}, bf16[64,512]{1,0:T(8,128)(2,1)S(1)}, u32[]{:S(2)}, u32[]{:S(2)}) collective-permute-start(bf16[64,512]{1,0:T(8,128)(2,1)S(1)} %get-tuple-element.26.w0), channel_id=1, source_target_pairs={{0,8},{8,16},{16,24},{24,0},{1,9},{9,17},{17,25},{25,1},{2,10},{10... | collective-permute-start | bytes 196616 | tf_op jit(solution)/shard_map/ppermute | solution.py:381
  17.2 6.6 %collective-permute-start.1 = (bf16[64,512]{1,0:T(8,128)(2,1)S(1)}, bf16[64,512]{1,0:T(8,128)(2,1)S(1)}, u32[]{:S(2)}, u32[]{:S(2)}) collective-permute-start(bf16[64,512]{1,0:T(8,128)(2,1)S(1)} %get-tuple-element.26.w0), channel_id=1, source_target_pairs={{0,24},{8,0},{16,8},{24,16},{1,25},{9,1},{17,9},{25,17},{2,26},{10... | collective-permute-start | bytes 196616 | tf_op jit(solution)/shard_map/ppermute | solution.py:381
  19.5 7.7 %collective-permute-start.2 = (bf16[64,512]{1,0:T(8,128)(2,1)S(1)}, bf16[64,512]{1,0:T(8,128)(2,1)S(1)}, u32[]{:S(2)}, u32[]{:S(2)}) collective-permute-start(bf16[64,512]{1,0:T(8,128)(2,1)S(1)} %get-tuple-element.26.w0), channel_id=1, source_target_pairs={{0,16},{8,24},{16,0},{24,8},{1,17},{9,25},{17,1},{25,9},{2,18},{10... | collective-permute-start | bytes 196616 | tf_op jit(solution)/shard_map/ppermute | solution.py:381
  29.6 27.2 %copy-start.27 = (f32[96]{0:T(128)S(1)}, f32[96]{0:T(128)}, u32[]{:S(2)}) copy-start(f32[96]{0:T(128)} %param.34) | copy-start | bytes 1156
  29.6 27.3 %copy-start.23 = (bf16[256,128]{1,0:T(8,128)(2,1)S(1)}, bf16[256,128]{1,0:T(8,128)(2,1)}, u32[]{:S(2)}) copy-start(bf16[256,128]{1,0:T(8,128)(2,1)} %param.33) | copy-start | bytes 196612
  29.6 27.3 %copy-start.24 = (bf16[256,128]{1,0:T(8,128)(2,1)S(1)}, bf16[256,128]{1,0:T(8,128)(2,1)}, u32[]{:S(2)}) copy-start(bf16[256,128]{1,0:T(8,128)(2,1)} %param.32) | copy-start | bytes 196612
  31.4 25.8 %copy-start.26 = (f32[256]{0:T(256)S(1)}, f32[256]{0:T(256)}, u32[]{:S(2)}) copy-start(f32[256]{0:T(256)} %param.31) | copy-start | bytes 3076
  31.4 26.0 %copy-start.28 = (f32[96]{0:T(128)S(1)}, f32[96]{0:T(128)}, u32[]{:S(2)}) copy-start(f32[96]{0:T(128)} %param.35) | copy-start | bytes 1156
  31.4 26.2 %copy-start.29 = (f32[1,2,256]{2,1,0:T(2,128)S(1)}, f32[1,2,256]{2,1,0:T(2,128)}, u32[]{:S(2)}) copy-start(f32[1,2,256]{2,1,0:T(2,128)} %param.42) | copy-start | bytes 6148
  31.4 26.4 %copy-start.25 = (f32[1,2,256]{2,1,0:T(2,128)S(1)}, f32[1,2,256]{2,1,0:T(2,128)}, u32[]{:S(2)}) copy-start(f32[1,2,256]{2,1,0:T(2,128)} %param.43) | copy-start | bytes 6148
  31.4 26.6 %copy-start.30 = (f32[2,64]{1,0:T(2,128)S(1)}, f32[2,64]{1,0:T(2,128)}, u32[]{:S(2)}) copy-start(f32[2,64]{1,0:T(2,128)} %param.47) | copy-start | bytes 1540
  31.4 57.1 %all-to-all-start.1 = ((bf16[16,40,256]{2,1,0:T(8,128)(2,1)}), bf16[16,40,256]{2,1,0:T(8,128)(2,1)}, u32[]{:S(2)}, u32[]{:S(2)}) async-start(bf16[16,40,256]{2,1,0:T(8,128)(2,1)} %shard_map.258), calls=%async_computation.1 | async-start | bytes 655360 | tf_op jit(solution)/shard_map/all_to_all | solution.py:376
  46.8 19.6 %collective-permute-start.3 = (bf16[512,640]{1,0:T(8,128)(2,1)S(1)}, bf16[512,640]{1,0:T(8,128)(2,1)}, u32[]{:S(2)}, u32[]{:S(2)}) collective-permute-start(bf16[512,640]{1,0:T(8,128)(2,1)S(1)} %get-tuple-element.27.w0), channel_id=1, source_target_pairs={{0,8},{8,16},{16,24},{24,0},{1,9},{9,17},{17,25},{25,1},{2,10},{10... | collective-permute-start | bytes 1966088 | tf_op jit(solution)/shard_map/ppermute | solution.py:381
  50.2 18.9 %collective-permute-start.4 = (bf16[512,640]{1,0:T(8,128)(2,1)S(1)}, bf16[512,640]{1,0:T(8,128)(2,1)}, u32[]{:S(2)}, u32[]{:S(2)}) collective-permute-start(bf16[512,640]{1,0:T(8,128)(2,1)S(1)} %get-tuple-element.27.w0), channel_id=1, source_target_pairs={{0,24},{8,0},{16,8},{24,16},{1,25},{9,1},{17,9},{25,17},{2,26},{10... | collective-permute-start | bytes 1966088 | tf_op jit(solution)/shard_map/ppermute | solution.py:381
  52.6 29.7 %collective-permute-start.5 = (bf16[512,640]{1,0:T(8,128)(2,1)S(1)}, bf16[512,640]{1,0:T(8,128)(2,1)}, u32[]{:S(2)}, u32[]{:S(2)}) collective-permute-start(bf16[512,640]{1,0:T(8,128)(2,1)S(1)} %get-tuple-element.27.w0), channel_id=1, source_target_pairs={{0,16},{8,24},{16,0},{24,8},{1,17},{9,25},{17,1},{25,9},{2,18},{10... | collective-permute-start | bytes 1966088 | tf_op jit(solution)/shard_map/ppermute | solution.py:381
  90.7 19.9 %all-to-all-start.2 = ((bf16[4,16,40,256]{3,2,1,0:T(8,128)(2,1)}), bf16[4,16,40,256]{3,2,1,0:T(8,128)(2,1)S(1)}, u32[]{:S(2)}, u32[]{:S(2)}) async-start(bf16[4,16,40,256]{3,2,1,0:T(8,128)(2,1)} %broadcast_in_dim.16), calls=%async_computation.2 | async-start | bytes 2621440 | tf_op jit(solution)/shard_map/all_to_all | solution.py:376
  94.4 30.1 %copy-start.21 = (bf16[128,512]{1,0:T(8,128)(2,1)S(1)}, bf16[128,512]{1,0:T(8,128)(2,1)}, u32[]{:S(2)}) copy-start(bf16[128,512]{1,0:T(8,128)(2,1)} %param.49) | copy-start | bytes 393220
  110.6 23.1 %collective-permute-start.6 = (bf16[4,16,40,256]{3,2,1,0:T(8,128)(2,1)S(1)}, bf16[4,16,40,256]{3,2,1,0:T(8,128)(2,1)}, u32[]{:S(2)}, u32[]{:S(2)}) collective-permute-start(bf16[4,16,40,256]{3,2,1,0:T(8,128)(2,1)S(1)} %all-to-all-done.2.own), channel_id=1, source_target_pairs={{0,1},{1,0},{2,3},{3,2},{4,5},{5,4},{6,7},{7,6},{8,9},{9,8},{10,11... | collective-permute-start | bytes 3932168 | tf_op jit(solution)/shard_map/ppermute | solution.py:385
  112.5 42.0 %all-to-all-start.3 = ((bf16[16,2,64,128]{3,2,1,0:T(8,128)(2,1)}), bf16[16,2,64,128]{3,2,1,0:T(8,128)(2,1)S(1)}, u32[]{:S(2)}, u32[]{:S(2)}) async-start(bf16[16,2,64,128]{3,2,1,0:T(8,128)(2,1)} %get-tuple-element.46), calls=%async_computation.3 | async-start | bytes 1048576 | tf_op jit(solution)/shard_map/all_to_all | solution.py:376
  124.6 29.9 %copy-start.14 = (f32[128]{0:T(128)S(1)}, f32[128]{0:T(128)}, u32[]{:S(2)}) copy-start(f32[128]{0:T(128)} %param.48) | copy-start | bytes 1540
  124.6 13.8 %collective-permute-start.7 = (bf16[256,512]{1,0:T(8,128)(2,1)S(1)}, bf16[256,512]{1,0:T(8,128)(2,1)S(1)}, u32[]{:S(2)}, u32[]{:S(2)}) collective-permute-start(bf16[256,512]{1,0:T(8,128)(2,1)S(1)} %constant_dynamic-update-slice_fusion.o0), channel_id=1, source_target_pairs={{0,8},{8,16},{16,24},{24,0},{1,9},{9,17},{17,25},{25,1},{2,10},{10... | collective-permute-start | bytes 786440 | tf_op jit(solution)/shard_map/ppermute | solution.py:381
  126.5 11.9 %collective-permute-start.8 = (bf16[256,512]{1,0:T(8,128)(2,1)S(1)}, bf16[256,512]{1,0:T(8,128)(2,1)S(1)}, u32[]{:S(2)}, u32[]{:S(2)}) collective-permute-start(bf16[256,512]{1,0:T(8,128)(2,1)S(1)} %constant_dynamic-update-slice_fusion.o0), channel_id=1, source_target_pairs={{0,24},{8,0},{16,8},{24,16},{1,25},{9,1},{17,9},{25,17},{2,26},{10... | collective-permute-start | bytes 786440 | tf_op jit(solution)/shard_map/ppermute | solution.py:381
  130.5 12.7 %collective-permute-start.9 = (bf16[256,512]{1,0:T(8,128)(2,1)S(1)}, bf16[256,512]{1,0:T(8,128)(2,1)S(1)}, u32[]{:S(2)}, u32[]{:S(2)}) collective-permute-start(bf16[256,512]{1,0:T(8,128)(2,1)S(1)} %constant_dynamic-update-slice_fusion.o0), channel_id=1, source_target_pairs={{0,16},{8,24},{16,0},{24,8},{1,17},{9,25},{17,1},{25,9},{2,18},{10... | collective-permute-start | bytes 786440 | tf_op jit(solution)/shard_map/ppermute | solution.py:381
  (21 other events, 56.7 us)

commit v3 on v2

--- a/solution.py
+++ b/solution.py
@@ -25,6 +25,7 @@
 VMEM = pl.BlockSpec(memory_space=pltpu.VMEM)
 SMEM = pl.BlockSpec(memory_space=pltpu.SMEM)
 ANY = pl.BlockSpec(memory_space=pl.ANY)
+HBM = pl.BlockSpec(memory_space=pltpu.HBM)
 
 
 def dot(a, b, dims=NN):
@@ -60,7 +61,7 @@
         in_specs=specs or [VMEM] * len(args),
         out_specs=jax.tree.map(lambda _: VMEM, outs),
         scratch_shapes=scratch,
-        compiler_params=pltpu.CompilerParams(vmem_limit_bytes=limit << 20),
+        compiler_params=pltpu.CompilerParams(vmem_limit_bytes=int(limit * (1 << 20))),
         cost_estimate=pl.CostEstimate(flops=flops, bytes_accessed=4 << 20, transcendentals=0),
     )(*args)
 
@@ -72,16 +73,32 @@
     return a * cosine - b * sine, b * cosine + a * sine
 
 
-def prepare_body(place, x, gain, wa, wk, wv, wq, wc, wr, xs, small, big, turned_wc):
+def prepare_body(
+    place, x_in, gain_in, wa_in, wk_in, wv_in, wq_in, wc_in, wr_in, xs, small, big,
+    x, gain, wa, wk, wv, wq, wc, wr, turned_wc, arrived,
+):
+    pairs = [
+        (x_in, x), (gain_in, gain), (wc_in, wc), (wr_in, wr),
+        (wa_in, wa), (wk_in, wk), (wv_in, wv), (wq_in, wq),
+    ]
+    copies = [pltpu.make_async_copy(a, b, arrived.at[i]) for i, (a, b) in enumerate(pairs)]
+    for copy in copies:
+        copy.start()
+    copies[0].wait()
+    copies[1].wait()
     v = x[...].astype(F32)
     v = v * lax.rsqrt(jnp.mean(v * v, axis=-1, keepdims=True) + EPS) * gain[...]
     v = v.astype(BF16)
     for i in range(8):
         xs[i] = v
+    copies[2].wait()
+    copies[3].wait()
     turned_wc[...] = wc[...].astype(F32).T
     start = pl.multiple_of(place[1] * 32, 32)
     small[0:32] = turned_wc[pl.ds(start, 32), :].astype(BF16)
     small[32:64] = wr[...]
+    for copy in copies[4:]:
+        copy.wait()
     big[:, 0:128] = wa[...]
     big[:, 128:256] = wk[...]
     big[:, 256:384] = wv[...]
@@ -96,8 +113,34 @@
         jax.ShapeDtypeStruct((64, 512), BF16),
         jax.ShapeDtypeStruct((512, 640), BF16),
     ]
-    scratch = [pltpu.VMEM((256, 512), F32)]
-    return call(prepare_body, outs, args, 1 << 29, scratch, [SMEM] + [VMEM] * 8)
+    scratch = [pltpu.VMEM(a.shape, a.dtype) for a in args[1:]]
+    scratch += [pltpu.VMEM((256, 512), F32), pltpu.SemaphoreType.DMA((8,))]
+    return call(prepare_body, outs, args, 1 << 29, scratch, [SMEM] + [HBM] * 8, 63.9)
+
+
+def fan_body(value, out):
+    v = value[...]
+    for i in range(4):
+        out[i] = v
+
+
+def fan(value):
+    return call(fan_body, jax.ShapeDtypeStruct((4, *value.shape), value.dtype), (value,), 1 << 29)
+
+
+def lowrank_body(place, x, fd, fa, table, dlow, rlow, turn):
+    dlow[...] = jnp.tanh(dot(x[...], fd[...]).astype(BF16).astype(F32)).astype(BF16)
+    rlow[...] = dot(x[...], fa[...]).astype(BF16)
+    turn[...] = table[place[0]]
+
+
+def lowrank(*args):
+    outs = [
+        jax.ShapeDtypeStruct((ROWS, 128), BF16),
+        jax.ShapeDtypeStruct((ROWS, 128), BF16),
+        jax.ShapeDtypeStruct((ROPE, ROWS), F32),
+    ]
+    return call(lowrank_body, outs, args, 1 << 29, specs=[SMEM] + [VMEM] * 4)
 
 
 def columns(place, k):
@@ -125,8 +168,7 @@
 
 
 def project_body(
-    place, x, w0, w1, w2, w3, fd, fa, table, gain, up, glat, kgain, mult, extra, present,
-    rkv, q, dlow, rlow,
+    place, x, w0, w1, w2, w3, turn, gain, up, glat, kgain, mult, extra, present, rkv, q,
 ):
     y = jnp.zeros((ROWS, 384), F32)
     t = jnp.zeros((192, ROWS), F32)
@@ -136,25 +178,20 @@
         t += dot(jnp.concatenate([w[0:192, 384:640], w[192:384, 384:640]], axis=1), part, NT)
     rkv[...] = y.astype(BF16)
     t = t.astype(BF16).astype(F32)
-    turn = table[place[0]]
     for h in range(2):
         v = t[QK * h : QK * (h + 1)]
         n = v * lax.rsqrt(jnp.mean(v * v, axis=0, keepdims=True) + EPS) * gain[...]
-        a, b = turned(n, turn)
+        a, b = turned(n, turn[...])
         ready = jnp.concatenate([n[:NOPE], a, b, jnp.zeros((128 - QK, ROWS), F32)], axis=0)
         q[h] = ready.T.astype(BF16)
-    dlow[...] = jnp.tanh(dot(x[...], fd[...]).astype(BF16).astype(F32)).astype(BF16)
-    rlow[...] = dot(x[...], fa[...]).astype(BF16)
 
 
 def project(*args):
     outs = [
         jax.ShapeDtypeStruct((ROWS, 384), BF16),
         jax.ShapeDtypeStruct((2, ROWS, 128), BF16),
-        jax.ShapeDtypeStruct((ROWS, 128), BF16),
-        jax.ShapeDtypeStruct((ROWS, 128), BF16),
     ]
-    return call(project_body, outs, args, 4 << 30, specs=[SMEM] + [VMEM] * 9 + [ANY] * 6)
+    return call(project_body, outs, args, 4 << 30, specs=[SMEM] + [VMEM] * 7 + [ANY] * 6)
 
 
 def recur_body(rkv, dlow, rlow, wd, bd, wa, ba, mult, extra, present, free, along, bonus, state):
@@ -263,7 +300,7 @@
 def recur(*args):
     wide = jax.ShapeDtypeStruct((ROWS, 128), F32)
     outs = [wide, wide, wide, jax.ShapeDtypeStruct((16, 2, 64, 128), BF16)]
-    return call(recur_body, outs, args, 8 << 30)
+    return call(recur_body, outs, args, 8 << 30, limit=60)
 
 
 def attend_body(place, q, own, peer, w, glat, gain, table, att, logs, acc, top):
@@ -453,14 +490,13 @@
     table = jnp.asarray(turn_table())
     pay = latents(place, normed, *smalls)
     lat = exchanged(pay, "sp")
+    dlow, rlow, turn = lowrank(place, normed, fade1, adapt1, table)
     wo = around(jnp.concatenate([wo_att, wo_rec], axis=0))
     projected = project(
         place,
         normed,
         *bigs,
-        fade1,
-        adapt1,
-        table,
+        turn,
         q_gain.reshape(QK, 1),
         up,
         glat,
@@ -469,9 +505,9 @@
         extra,
         present,
     )
-    lat, (rkv, q, dlow, rlow) = lax.optimization_barrier((lat, tuple(projected)))
+    lat, (rkv, q) = lax.optimization_barrier((lat, tuple(projected)))
     same_core = [[0, 2, 4, 6], [1, 3, 5, 7]]
-    lat_own = exchanged(jnp.broadcast_to(lat[None], (4, *lat.shape)), "tp", same_core)
+    lat_own = exchanged(fan(lat), "tp", same_core)
     recurrent = recur(
         rkv,
         dlow,

time: 178 us -> 173 us (0.972)
  local copies, waits for them, and re-layouts: 16.9 us -> 10.1 us
  Pallas kernels: 21.1 us -> 25.7 us
  waiting for transfers between devices: 52.4 us -> 48.4 us
    pallas_call x6 -> x8, Pallas kernels: 21.1 us -> 25.7 us  [call(): pl.pallas_call(body, out_shape=outs, in_specs=specs or [VMEM] * len(args)...]
    unnamed x64 -> x70, local copies, waits for them, and re-layouts: 13.8 us -> 9.16 us
    ppermute x9, waiting for transfers between devices: 32.5 us -> 29.8 us  [around(): return [value] + [lax.ppermute(value, 'fs', move) for move in moves]]
    broadcast_in_dim x1 -> x0, local copies, waits for them, and re-layouts: 2.17 us -> none  [shards(): jnp.broadcast_to(lat[None], (4, *lat.shape))]
  transfers between devices with their start and end apart: 14 -> 14, of which waited for: 8 -> 8; matrix products, arithmetic and copies ran while one was open for 1% -> 1% of each run, Pallas kernels for 9% -> 11%
where the time goes in v3:
time: 173 us; the launch traced here: 172 us
  starting transfers between devices  66.4 us (38%)
  waiting for transfers between devices  48.4 us (28%)
  Pallas kernels  25.7 us (15%)
  blocking collectives  18.4 us (11%)
  local copies, waits for them, and re-layouts  10.1 us (6%)
    all_to_all x4, starting transfers between devices, exchanged(): lax.all_to_all(copies, axis, 0, 0, axis_index_groups=groups, tiled=True)  35.4 us
    ppermute x9, waiting for transfers between devices, around(): return [value] + [lax.ppermute(value, 'fs', move) for move in moves]  29.8 us
    ppermute x9, starting transfers between devices, around(): return [value] + [lax.ppermute(value, 'fs', move) for move in moves]  29.1 us
    pallas_call x8, Pallas kernels, call(): pl.pallas_call(body, out_shape=outs, in_specs=specs or [VMEM] * len(args)...  25.7 us
    all_to_all x4, waiting for transfers between devices, exchanged(): lax.all_to_all(copies, axis, 0, 0, axis_index_groups=groups, tiled=True)  18.6 us
    all_to_all x1, blocking collectives, exchanged(): lax.all_to_all(copies, axis, 0, 0, axis_index_groups=groups, tiled=True)  18.4 us
    unnamed x70, local copies, waits for them, and re-layouts  9.16 us
  transfers between devices with their start and end apart: 14, of which 8 were waited for; matrix products, arithmetic and copies ran while one was open for 1% of the time, Pallas kernels for 11%

profile of v3, /device:TPU:40, one launch (start us, length us, event | category | flops | bytes accessed | tf_op | source)
XLA Modules:
  0.0 171.6 jit_solution(1881791564986247636)
XLA Ops:
  1.3 3.2 %shard_map.257 = (bf16[8,32,2048]{2,1,0:T(8,128)(2,1)}, bf16[64,512]{1,0:T(8,128)(2,1)}, bf16[512,640]{1,0:T(8,128)(2,1)}) custom-call(s32[3]{0:T(128)} %pad_add_fusion.place, bf16[32,2048]{1,0:T(8,128)(2,1)} %bitcast.41, f32[1,2048]{1,0:T(1,128)} %bitcast.43, bf16[512,128]{1,0:T(8,128)(2,1)} %wa_in.1, bf16[512,128]{1,0:T(8,128)(2,1)} %wk_in.1, ...), custom_call_target="tpu_custom_call" | custom-call | flops 536870912 | bytes 4194304 | tf_op jit(solution)/shard_map/pallas_call | solution.py:58
  4.5 4.4 %all-to-all-start = ((bf16[8,32,2048]{2,1,0:T(8,128)(2,1)}), bf16[8,32,2048]{2,1,0:T(8,128)(2,1)S(1)}, u32[]{:S(2)}, u32[]{:S(2)}) async-start(bf16[8,32,2048]{2,1,0:T(8,128)(2,1)} %get-tuple-element.24), calls=%async_computation | async-start | bytes 2097152 | tf_op jit(solution)/shard_map/all_to_all | solution.py:413
  8.9 3.5 %collective-permute-start = (bf16[64,512]{1,0:T(8,128)(2,1)S(1)}, bf16[64,512]{1,0:T(8,128)(2,1)S(1)}, u32[]{:S(2)}, u32[]{:S(2)}) collective-permute-start(bf16[64,512]{1,0:T(8,128)(2,1)S(1)} %copy-done.14), channel_id=1, source_target_pairs={{0,8},{8,16},{16,24},{24,0},{1,9},{9,17},{17,25},{25,1},{2,10},{10... | collective-permute-start | bytes 196616 | tf_op jit(solution)/shard_map/ppermute | solution.py:418
  14.8 4.2 %collective-permute-start.2 = (bf16[64,512]{1,0:T(8,128)(2,1)S(1)}, bf16[64,512]{1,0:T(8,128)(2,1)S(1)}, u32[]{:S(2)}, u32[]{:S(2)}) collective-permute-start(bf16[64,512]{1,0:T(8,128)(2,1)S(1)} %copy-done.14), channel_id=1, source_target_pairs={{0,16},{8,24},{16,0},{24,8},{1,17},{9,25},{17,1},{25,9},{2,18},{10... | collective-permute-start | bytes 196616 | tf_op jit(solution)/shard_map/ppermute | solution.py:418
  19.0 3.4 %collective-permute-done.2.w3 = bf16[64,512]{1,0:T(8,128)(2,1)S(1)} collective-permute-done((bf16[64,512]{1,0:T(8,128)(2,1)S(1)}, bf16[64,512]{1,0:T(8,128)(2,1)S(1)}, u32[]{:S(2)}, u32[]{:S(2)}) %collective-permute-start.2) | collective-permute-done | bytes 65568 | tf_op jit(solution)/shard_map/ppermute | solution.py:418
  22.4 2.4 %all-to-all-done = bf16[8,32,2048]{2,1,0:T(8,128)(2,1)S(1)} async-done(((bf16[8,32,2048]{2,1,0:T(8,128)(2,1)}), bf16[8,32,2048]{2,1,0:T(8,128)(2,1)S(1)}, u32[]{:S(2)}, u32[]{:S(2)}) %all-to-all-start) | async-done | bytes 1048608 | tf_op jit(solution)/shard_map/all_to_all | solution.py:413
  26.6 15.4 %all-to-all-start.1 = ((bf16[16,40,256]{2,1,0:T(8,128)(2,1)}), bf16[16,40,256]{2,1,0:T(8,128)(2,1)S(1)}, u32[]{:S(2)}, u32[]{:S(2)}) async-start(bf16[16,40,256]{2,1,0:T(8,128)(2,1)} %shard_map.258), calls=%async_computation.1 | async-start | bytes 655360 | tf_op jit(solution)/shard_map/all_to_all | solution.py:413
  42.0 3.5 %collective-permute-start.3 = (bf16[512,640]{1,0:T(8,128)(2,1)}, bf16[512,640]{1,0:T(8,128)(2,1)}, u32[]{:S(2)}, u32[]{:S(2)}) collective-permute-start(bf16[512,640]{1,0:T(8,128)(2,1)} %get-tuple-element.26.w0), channel_id=1, source_target_pairs={{0,8},{8,16},{16,24},{24,0},{1,9},{9,17},{17,25},{25,1},{2,10},{10... | collective-permute-start | bytes 1966088 | tf_op jit(solution)/shard_map/ppermute | solution.py:418
  45.5 2.4 %collective-permute-start.4 = (bf16[512,640]{1,0:T(8,128)(2,1)}, bf16[512,640]{1,0:T(8,128)(2,1)}, u32[]{:S(2)}, u32[]{:S(2)}) collective-permute-start(bf16[512,640]{1,0:T(8,128)(2,1)} %get-tuple-element.26.w0), channel_id=1, source_target_pairs={{0,24},{8,0},{16,8},{24,16},{1,25},{9,1},{17,9},{25,17},{2,26},{10... | collective-permute-start | bytes 1966088 | tf_op jit(solution)/shard_map/ppermute | solution.py:418
  47.9 4.2 %collective-permute-start.5 = (bf16[512,640]{1,0:T(8,128)(2,1)}, bf16[512,640]{1,0:T(8,128)(2,1)}, u32[]{:S(2)}, u32[]{:S(2)}) collective-permute-start(bf16[512,640]{1,0:T(8,128)(2,1)} %get-tuple-element.26.w0), channel_id=1, source_target_pairs={{0,16},{8,24},{16,0},{24,8},{1,17},{9,25},{17,1},{25,9},{2,18},{10... | collective-permute-start | bytes 1966088 | tf_op jit(solution)/shard_map/ppermute | solution.py:418
  55.8 6.0 %collective-permute-done.3.w1 = bf16[512,640]{1,0:T(8,128)(2,1)} collective-permute-done((bf16[512,640]{1,0:T(8,128)(2,1)}, bf16[512,640]{1,0:T(8,128)(2,1)}, u32[]{:S(2)}, u32[]{:S(2)}) %collective-permute-start.3) | collective-permute-done | bytes 655392 | tf_op jit(solution)/shard_map/ppermute | solution.py:418
  61.8 2.8 %collective-permute-done.4.w2 = bf16[512,640]{1,0:T(8,128)(2,1)} collective-permute-done((bf16[512,640]{1,0:T(8,128)(2,1)}, bf16[512,640]{1,0:T(8,128)(2,1)}, u32[]{:S(2)}, u32[]{:S(2)}) %collective-permute-start.4) | collective-permute-done | bytes 655392 | tf_op jit(solution)/shard_map/ppermute | solution.py:418
  64.6 13.2 %collective-permute-done.5.w3 = bf16[512,640]{1,0:T(8,128)(2,1)} collective-permute-done((bf16[512,640]{1,0:T(8,128)(2,1)}, bf16[512,640]{1,0:T(8,128)(2,1)}, u32[]{:S(2)}, u32[]{:S(2)}) %collective-permute-start.5) | collective-permute-done | bytes 655392 | tf_op jit(solution)/shard_map/ppermute | solution.py:418
  77.8 2.6 %shard_map.260 = (bf16[256,384]{1,0:T(8,128)(2,1)S(1)}, bf16[2,256,128]{2,1,0:T(8,128)(2,1)S(1)}) custom-call(s32[3]{0:T(128)S(1)} %copy-done.4, bf16[256,2048]{1,0:T(8,128)(2,1)S(1)} %bitcast.28, bf16[512,640]{1,0:T(8,128)(2,1)S(1)} %copy-done.5, bf16[512,640]{1,0:T(8,128)(2,1)} %collective-permute-done.3.w1, bf16[512,640]{1,0:T(8,128)(2,1)} %collective-permute-done.4.w2, ...), custom_call_target="tpu_custom_call" | custom-call | flops 4294967296 | bytes 4194304 | tf_op jit(solution)/shard_map/pallas_call | solution.py:58
  81.6 3.5 %all-to-all-start.2 = ((bf16[4,16,40,256]{3,2,1,0:T(8,128)(2,1)}), bf16[4,16,40,256]{3,2,1,0:T(8,128)(2,1)S(1)}, u32[]{:S(2)}, u32[]{:S(2)}) async-start(bf16[4,16,40,256]{3,2,1,0:T(8,128)(2,1)} %shard_map.261), calls=%async_computation.2 | async-start | bytes 2621440 | tf_op jit(solution)/shard_map/all_to_all | solution.py:413
  85.2 10.5 %shard_map.262 = (f32[256,128]{1,0:T(8,128)}, f32[256,128]{1,0:T(8,128)}, f32[256,128]{1,0:T(8,128)}, bf16[16,2,64,128]{3,2,1,0:T(8,128)(2,1)}) custom-call(bf16[256,384]{1,0:T(8,128)(2,1)} %copy-done.18, bf16[256,128]{1,0:T(8,128)(2,1)} %copy-done.12, bf16[256,128]{1,0:T(8,128)(2,1)} %copy-done.13, bf16[128,128]{1,0:T(8,128)(2,1)} %wd.1, ...), custom_call_target="tpu_custom_call" | custom-call | flops 8589934592 | bytes 4194304 | tf_op jit(solution)/shard_map/pallas_call | solution.py:58
  95.7 5.6 %all-to-all-done.2.own = bf16[4,16,40,256]{3,2,1,0:T(8,128)(2,1)S(1)} async-done(((bf16[4,16,40,256]{3,2,1,0:T(8,128)(2,1)}), bf16[4,16,40,256]{3,2,1,0:T(8,128)(2,1)S(1)}, u32[]{:S(2)}, u32[]{:S(2)}) %all-to-all-start.2) | async-done | bytes 1310752 | tf_op jit(solution)/shard_map/all_to_all | solution.py:413
  103.3 12.0 %all-to-all-start.3 = ((bf16[16,2,64,128]{3,2,1,0:T(8,128)(2,1)}), bf16[16,2,64,128]{3,2,1,0:T(8,128)(2,1)S(1)}, u32[]{:S(2)}, u32[]{:S(2)}) async-start(bf16[16,2,64,128]{3,2,1,0:T(8,128)(2,1)} %get-tuple-element.44), calls=%async_computation.3 | async-start | bytes 1048576 | tf_op jit(solution)/shard_map/all_to_all | solution.py:413
  117.3 3.9 %collective-permute-start.8 = (bf16[256,512]{1,0:T(8,128)(2,1)S(1)}, bf16[256,512]{1,0:T(8,128)(2,1)S(1)}, u32[]{:S(2)}, u32[]{:S(2)}) collective-permute-start(bf16[256,512]{1,0:T(8,128)(2,1)S(1)} %constant_dynamic-update-slice_fusion.o0), channel_id=1, source_target_pairs={{0,24},{8,0},{16,8},{24,16},{1,25},{9,1},{17,9},{25,17},{2,26},{10... | collective-permute-start | bytes 786440 | tf_op jit(solution)/shard_map/ppermute | solution.py:418
  121.2 3.2 %collective-permute-start.9 = (bf16[256,512]{1,0:T(8,128)(2,1)S(1)}, bf16[256,512]{1,0:T(8,128)(2,1)S(1)}, u32[]{:S(2)}, u32[]{:S(2)}) collective-permute-start(bf16[256,512]{1,0:T(8,128)(2,1)S(1)} %constant_dynamic-update-slice_fusion.o0), channel_id=1, source_target_pairs={{0,16},{8,24},{16,0},{24,8},{1,17},{9,25},{17,1},{25,9},{2,18},{10... | collective-permute-start | bytes 786440 | tf_op jit(solution)/shard_map/ppermute | solution.py:418
  124.4 3.7 %shard_map.263 = (bf16[256,128]{1,0:T(8,128)(2,1)S(1)}, f32[2,256]{1,0:T(2,128)}) custom-call(s32[3]{0:T(128)S(1)} %copy-done.4, bf16[2,256,128]{2,1,0:T(8,128)(2,1)S(1)} %copy-done.20, bf16[4,16,40,256]{3,2,1,0:T(8,128)(2,1)S(1)} %all-to-all-done.2.own, bf16[4,16,40,256]{3,2,1,0:T(8,128)(2,1)} %collective-permute-done.6.peer, ...), custom_call_target="tpu_custom_call" | custom-call | flops 8589934592 | bytes 4194304 | tf_op jit(solution)/shard_map/pallas_call | solution.py:58
  129.6 4.4 %collective-permute-done.9.o3 = bf16[256,512]{1,0:T(8,128)(2,1)S(1)} collective-permute-done((bf16[256,512]{1,0:T(8,128)(2,1)S(1)}, bf16[256,512]{1,0:T(8,128)(2,1)S(1)}, u32[]{:S(2)}, u32[]{:S(2)}) %collective-permute-start.9) | collective-permute-done | bytes 262176 | tf_op jit(solution)/shard_map/ppermute | solution.py:418
  134.7 10.6 %all-to-all-done.3.states = bf16[16,2,64,128]{3,2,1,0:T(8,128)(2,1)S(1)} async-done(((bf16[16,2,64,128]{3,2,1,0:T(8,128)(2,1)}), bf16[16,2,64,128]{3,2,1,0:T(8,128)(2,1)S(1)}, u32[]{:S(2)}, u32[]{:S(2)}) %all-to-all-start.3) | async-done | bytes 524320 | tf_op jit(solution)/shard_map/all_to_all | solution.py:413
  152.4 18.4 %all_to_all.25 = bf16[8,32,2048]{2,1,0:T(8,128)(2,1)S(1)} all-to-all(bf16[8,32,2048]{2,1,0:T(8,128)(2,1)S(1)} %bitcast.29), channel_id=1, replica_groups=mesh['sp'=16,'fs'=4,'tp'=8] {'tp'}, dimensions={0} | all-to-all | bytes 2097152 | tf_op jit(solution)/shard_map/all_to_all | solution.py:413
  (101 shorter events, 23.5 us)
Async XLA Ops:
  4.5 20.4 %all-to-all-start = ((bf16[8,32,2048]{2,1,0:T(8,128)(2,1)}), bf16[8,32,2048]{2,1,0:T(8,128)(2,1)S(1)}, u32[]{:S(2)}, u32[]{:S(2)}) async-start(bf16[8,32,2048]{2,1,0:T(8,128)(2,1)} %get-tuple-element.24), calls=%async_computation | async-start | bytes 2097152 | tf_op jit(solution)/shard_map/all_to_all | solution.py:413
  8.9 10.1 %collective-permute-start = (bf16[64,512]{1,0:T(8,128)(2,1)S(1)}, bf16[64,512]{1,0:T(8,128)(2,1)S(1)}, u32[]{:S(2)}, u32[]{:S(2)}) collective-permute-start(bf16[64,512]{1,0:T(8,128)(2,1)S(1)} %copy-done.14), channel_id=1, source_target_pairs={{0,8},{8,16},{16,24},{24,0},{1,9},{9,17},{17,25},{25,1},{2,10},{10... | collective-permute-start | bytes 196616 | tf_op jit(solution)/shard_map/ppermute | solution.py:418
  12.4 6.6 %collective-permute-start.1 = (bf16[64,512]{1,0:T(8,128)(2,1)S(1)}, bf16[64,512]{1,0:T(8,128)(2,1)S(1)}, u32[]{:S(2)}, u32[]{:S(2)}) collective-permute-start(bf16[64,512]{1,0:T(8,128)(2,1)S(1)} %copy-done.14), channel_id=1, source_target_pairs={{0,24},{8,0},{16,8},{24,16},{1,25},{9,1},{17,9},{25,17},{2,26},{10... | collective-permute-start | bytes 196616 | tf_op jit(solution)/shard_map/ppermute | solution.py:418
  14.8 7.7 %collective-permute-start.2 = (bf16[64,512]{1,0:T(8,128)(2,1)S(1)}, bf16[64,512]{1,0:T(8,128)(2,1)S(1)}, u32[]{:S(2)}, u32[]{:S(2)}) collective-permute-start(bf16[64,512]{1,0:T(8,128)(2,1)S(1)} %copy-done.14), channel_id=1, source_target_pairs={{0,16},{8,24},{16,0},{24,8},{1,17},{9,25},{17,1},{25,9},{2,18},{10... | collective-permute-start | bytes 196616 | tf_op jit(solution)/shard_map/ppermute | solution.py:418
  24.8 27.2 %copy-start.29 = (f32[256]{0:T(256)S(1)}, f32[256]{0:T(256)}, u32[]{:S(2)}) copy-start(f32[256]{0:T(256)} %param.31) | copy-start | bytes 3076
  24.8 27.5 %copy-start.26 = (bf16[256,128]{1,0:T(8,128)(2,1)S(1)}, bf16[256,128]{1,0:T(8,128)(2,1)}, u32[]{:S(2)}) copy-start(bf16[256,128]{1,0:T(8,128)(2,1)} %param.33) | copy-start | bytes 196612
  24.8 27.5 %copy-start.27 = (bf16[256,128]{1,0:T(8,128)(2,1)S(1)}, bf16[256,128]{1,0:T(8,128)(2,1)}, u32[]{:S(2)}) copy-start(bf16[256,128]{1,0:T(8,128)(2,1)} %param.32) | copy-start | bytes 196612
  26.6 26.6 %copy-start.31 = (f32[96]{0:T(128)S(1)}, f32[96]{0:T(128)}, u32[]{:S(2)}) copy-start(f32[96]{0:T(128)} %param.34) | copy-start | bytes 1156
  26.6 26.7 %copy-start = (bf16[2048,128]{1,0:T(8,128)(2,1)S(1)}, bf16[2048,128]{1,0:T(8,128)(2,1)}, u32[]{:S(2)}) copy-start(bf16[2048,128]{1,0:T(8,128)(2,1)} %fd.1) | copy-start | bytes 1572868
  26.6 26.7 %copy-start.1 = (bf16[2048,128]{1,0:T(8,128)(2,1)S(1)}, bf16[2048,128]{1,0:T(8,128)(2,1)}, u32[]{:S(2)}) copy-start(bf16[2048,128]{1,0:T(8,128)(2,1)} %fa.1) | copy-start | bytes 1572868
  26.6 26.7 %copy-start.2 = (f32[16,32,256]{2,1,0:T(8,128)S(1)}, f32[16,32,256]{2,1,0:T(8,128)}, u32[]{:S(2)}) copy-start(f32[16,32,256]{2,1,0:T(8,128)} %constant.25.clone.table) | copy-start | bytes 1572868
  26.6 53.8 %all-to-all-start.1 = ((bf16[16,40,256]{2,1,0:T(8,128)(2,1)}), bf16[16,40,256]{2,1,0:T(8,128)(2,1)S(1)}, u32[]{:S(2)}, u32[]{:S(2)}) async-start(bf16[16,40,256]{2,1,0:T(8,128)(2,1)} %shard_map.258), calls=%async_computation.1 | async-start | bytes 655360 | tf_op jit(solution)/shard_map/all_to_all | solution.py:413
  42.0 19.8 %collective-permute-start.3 = (bf16[512,640]{1,0:T(8,128)(2,1)}, bf16[512,640]{1,0:T(8,128)(2,1)}, u32[]{:S(2)}, u32[]{:S(2)}) collective-permute-start(bf16[512,640]{1,0:T(8,128)(2,1)} %get-tuple-element.26.w0), channel_id=1, source_target_pairs={{0,8},{8,16},{16,24},{24,0},{1,9},{9,17},{17,25},{25,1},{2,10},{10... | collective-permute-start | bytes 1966088 | tf_op jit(solution)/shard_map/ppermute | solution.py:418
  45.5 19.1 %collective-permute-start.4 = (bf16[512,640]{1,0:T(8,128)(2,1)}, bf16[512,640]{1,0:T(8,128)(2,1)}, u32[]{:S(2)}, u32[]{:S(2)}) collective-permute-start(bf16[512,640]{1,0:T(8,128)(2,1)} %get-tuple-element.26.w0), channel_id=1, source_target_pairs={{0,24},{8,0},{16,8},{24,16},{1,25},{9,1},{17,9},{25,17},{2,26},{10... | collective-permute-start | bytes 1966088 | tf_op jit(solution)/shard_map/ppermute | solution.py:418
  47.9 29.9 %collective-permute-start.5 = (bf16[512,640]{1,0:T(8,128)(2,1)}, bf16[512,640]{1,0:T(8,128)(2,1)}, u32[]{:S(2)}, u32[]{:S(2)}) collective-permute-start(bf16[512,640]{1,0:T(8,128)(2,1)} %get-tuple-element.26.w0), channel_id=1, source_target_pairs={{0,16},{8,24},{16,0},{24,8},{1,17},{9,25},{17,1},{25,9},{2,18},{10... | collective-permute-start | bytes 1966088 | tf_op jit(solution)/shard_map/ppermute | solution.py:418
  81.6 19.7 %all-to-all-start.2 = ((bf16[4,16,40,256]{3,2,1,0:T(8,128)(2,1)}), bf16[4,16,40,256]{3,2,1,0:T(8,128)(2,1)S(1)}, u32[]{:S(2)}, u32[]{:S(2)}) async-start(bf16[4,16,40,256]{3,2,1,0:T(8,128)(2,1)} %shard_map.261), calls=%async_computation.2 | async-start | bytes 2621440 | tf_op jit(solution)/shard_map/all_to_all | solution.py:413
  85.2 30.1 %copy-start.24 = (bf16[128,512]{1,0:T(8,128)(2,1)S(1)}, bf16[128,512]{1,0:T(8,128)(2,1)}, u32[]{:S(2)}) copy-start(bf16[128,512]{1,0:T(8,128)(2,1)} %param.49) | copy-start | bytes 393220
  95.7 28.7 %copy-start.20 = (bf16[2,256,128]{2,1,0:T(8,128)(2,1)S(1)}, bf16[2,256,128]{2,1,0:T(8,128)(2,1)}, u32[]{:S(2)}) copy-start(bf16[2,256,128]{2,1,0:T(8,128)(2,1)} %copy-done.19) | copy-start | bytes 393220
  101.3 23.1 %collective-permute-start.6 = (bf16[4,16,40,256]{3,2,1,0:T(8,128)(2,1)S(1)}, bf16[4,16,40,256]{3,2,1,0:T(8,128)(2,1)}, u32[]{:S(2)}, u32[]{:S(2)}) collective-permute-start(bf16[4,16,40,256]{3,2,1,0:T(8,128)(2,1)S(1)} %all-to-all-done.2.own), channel_id=1, source_target_pairs={{0,1},{1,0},{2,3},{3,2},{4,5},{5,4},{6,7},{7,6},{8,9},{9,8},{10,11... | collective-permute-start | bytes 3932168 | tf_op jit(solution)/shard_map/ppermute | solution.py:422
  103.3 42.0 %all-to-all-start.3 = ((bf16[16,2,64,128]{3,2,1,0:T(8,128)(2,1)}), bf16[16,2,64,128]{3,2,1,0:T(8,128)(2,1)S(1)}, u32[]{:S(2)}, u32[]{:S(2)}) async-start(bf16[16,2,64,128]{3,2,1,0:T(8,128)(2,1)} %get-tuple-element.44), calls=%async_computation.3 | async-start | bytes 1048576 | tf_op jit(solution)/shard_map/all_to_all | solution.py:413
  115.4 29.9 %copy-start.15 = (f32[128]{0:T(128)S(1)}, f32[128]{0:T(128)}, u32[]{:S(2)}) copy-start(f32[128]{0:T(128)} %param.48) | copy-start | bytes 1540
  115.4 12.8 %collective-permute-start.7 = (bf16[256,512]{1,0:T(8,128)(2,1)S(1)}, bf16[256,512]{1,0:T(8,128)(2,1)S(1)}, u32[]{:S(2)}, u32[]{:S(2)}) collective-permute-start(bf16[256,512]{1,0:T(8,128)(2,1)S(1)} %constant_dynamic-update-slice_fusion.o0), channel_id=1, source_target_pairs={{0,8},{8,16},{16,24},{24,0},{1,9},{9,17},{17,25},{25,1},{2,10},{10... | collective-permute-start | bytes 786440 | tf_op jit(solution)/shard_map/ppermute | solution.py:418
  117.3 11.5 %collective-permute-start.8 = (bf16[256,512]{1,0:T(8,128)(2,1)S(1)}, bf16[256,512]{1,0:T(8,128)(2,1)S(1)}, u32[]{:S(2)}, u32[]{:S(2)}) collective-permute-start(bf16[256,512]{1,0:T(8,128)(2,1)S(1)} %constant_dynamic-update-slice_fusion.o0), channel_id=1, source_target_pairs={{0,24},{8,0},{16,8},{24,16},{1,25},{9,1},{17,9},{25,17},{2,26},{10... | collective-permute-start | bytes 786440 | tf_op jit(solution)/shard_map/ppermute | solution.py:418
  121.2 12.7 %collective-permute-start.9 = (bf16[256,512]{1,0:T(8,128)(2,1)S(1)}, bf16[256,512]{1,0:T(8,128)(2,1)S(1)}, u32[]{:S(2)}, u32[]{:S(2)}) collective-permute-start(bf16[256,512]{1,0:T(8,128)(2,1)S(1)} %constant_dynamic-update-slice_fusion.o0), channel_id=1, source_target_pairs={{0,16},{8,24},{16,0},{24,8},{1,17},{9,25},{17,1},{25,9},{2,18},{10... | collective-permute-start | bytes 786440 | tf_op jit(solution)/shard_map/ppermute | solution.py:418
  (24 other events, 259.6 us)

commit v4 on v3

--- a/solution.py
+++ b/solution.py
@@ -74,12 +74,12 @@
 
 
 def prepare_body(
-    place, x_in, gain_in, wa_in, wk_in, wv_in, wq_in, wc_in, wr_in, xs, small, big,
-    x, gain, wa, wk, wv, wq, wc, wr, turned_wc, arrived,
+    place, x_in, gain_in, wa_in, wk_in, wv_in, wq_in, wc_in, wr_in, oa_in, or_in,
+    xs, small, big, late, x, gain, wa, wk, wv, wq, wc, wr, oa, orr, turned_wc, arrived,
 ):
     pairs = [
-        (x_in, x), (gain_in, gain), (wc_in, wc), (wr_in, wr),
-        (wa_in, wa), (wk_in, wk), (wv_in, wv), (wq_in, wq),
+        (x_in, x), (gain_in, gain), (wc_in, wc), (wr_in, wr), (wa_in, wa), (wk_in, wk),
+        (wv_in, wv), (wq_in, wq), (oa_in, oa), (or_in, orr),
     ]
     copies = [pltpu.make_async_copy(a, b, arrived.at[i]) for i, (a, b) in enumerate(pairs)]
     for copy in copies:
@@ -102,30 +102,32 @@
     big[:, 0:128] = wa[...]
     big[:, 128:256] = wk[...]
     big[:, 256:384] = wv[...]
-    big[0:192, 384:640] = wq[:, 0:256]
-    big[192:384, 384:640] = wq[:, 256:512]
-    big[384:512, 384:640] = jnp.zeros((128, 256), BF16)
+    late[0:192] = wq[...]
+    late[192:320] = oa[...]
+    late[320:448] = orr[...]
 
 
 def prepare(*args):
     outs = [
         jax.ShapeDtypeStruct((8, 32, 2048), BF16),
         jax.ShapeDtypeStruct((64, 512), BF16),
-        jax.ShapeDtypeStruct((512, 640), BF16),
+        jax.ShapeDtypeStruct((512, 384), BF16),
+        jax.ShapeDtypeStruct((448, 512), BF16),
     ]
     scratch = [pltpu.VMEM(a.shape, a.dtype) for a in args[1:]]
-    scratch += [pltpu.VMEM((256, 512), F32), pltpu.SemaphoreType.DMA((8,))]
-    return call(prepare_body, outs, args, 1 << 29, scratch, [SMEM] + [HBM] * 8, 63.9)
-
-
-def fan_body(value, out):
-    v = value[...]
-    for i in range(4):
-        out[i] = v
-
-
-def fan(value):
-    return call(fan_body, jax.ShapeDtypeStruct((4, *value.shape), value.dtype), (value,), 1 << 29)
+    scratch += [pltpu.VMEM((256, 512), F32), pltpu.SemaphoreType.DMA((10,))]
+    return call(prepare_body, outs, args, 1 << 29, scratch, [SMEM] + [HBM] * 10, 63.9)
+
+
+def collect_body(place, own, left, right, far, out):
+    chip = place[1] // 2
+    for by, part in ((0, own), (3, left), (1, right), (2, far)):
+        out[lax.rem(chip + by, 4)] = part[...]
+
+
+def collect(place, *parts):
+    outs = jax.ShapeDtypeStruct((4, *parts[0].shape), BF16)
+    return call(collect_body, outs, (place, *parts), 1 << 29, specs=[SMEM] + [VMEM] * 4)
 
 
 def lowrank_body(place, x, fd, fa, table, dlow, rlow, turn):
@@ -168,30 +170,36 @@
 
 
 def project_body(
-    place, x, w0, w1, w2, w3, turn, gain, up, glat, kgain, mult, extra, present, rkv, q,
+    place, x, w0, w1, w2, w3, up, glat, kgain, mult, extra, present, gain, rkv
 ):
     y = jnp.zeros((ROWS, 384), F32)
+    for k, w in enumerate((w0, w1, w2, w3)):
+        y += dot(x[:, columns(place, k)], w[...])
+    rkv[...] = y.astype(BF16)
+
+
+def project(*args):
+    outs = jax.ShapeDtypeStruct((ROWS, 384), BF16)
+    return call(project_body, outs, args, 4 << 30, specs=[SMEM] + [VMEM] * 5 + [ANY] * 7)
+
+
+def queries_body(place, x, w0, w1, w2, w3, turn, gain, q):
     t = jnp.zeros((192, ROWS), F32)
     for k, w in enumerate((w0, w1, w2, w3)):
-        part = x[:, columns(place, k)]
-        y += dot(part, w[:, 0:384])
-        t += dot(jnp.concatenate([w[0:192, 384:640], w[192:384, 384:640]], axis=1), part, NT)
-    rkv[...] = y.astype(BF16)
+        t += dot(w[0:192], x[:, columns(place, k)], NT)
     t = t.astype(BF16).astype(F32)
+    factor = np.float32(QK**-0.5 * np.log2(np.e))
     for h in range(2):
         v = t[QK * h : QK * (h + 1)]
-        n = v * lax.rsqrt(jnp.mean(v * v, axis=0, keepdims=True) + EPS) * gain[...]
+        n = v * (lax.rsqrt(jnp.mean(v * v, axis=0, keepdims=True) + EPS) * factor) * gain[...]
         a, b = turned(n, turn[...])
         ready = jnp.concatenate([n[:NOPE], a, b, jnp.zeros((128 - QK, ROWS), F32)], axis=0)
         q[h] = ready.T.astype(BF16)
 
 
-def project(*args):
-    outs = [
-        jax.ShapeDtypeStruct((ROWS, 384), BF16),
-        jax.ShapeDtypeStruct((2, ROWS, 128), BF16),
-    ]
-    return call(project_body, outs, args, 4 << 30, specs=[SMEM] + [VMEM] * 7 + [ANY] * 6)
+def queries(*args):
+    outs = jax.ShapeDtypeStruct((2, ROWS, 128), BF16)
+    return call(queries_body, outs, args, 1 << 29, specs=[SMEM] + [VMEM] * 7)
 
 
 def recur_body(rkv, dlow, rlow, wd, bd, wa, ba, mult, extra, present, free, along, bonus, state):
@@ -305,7 +313,6 @@
 
 def attend_body(place, q, own, peer, w, glat, gain, table, att, logs, acc, top):
     sp = place[0]
-    factor = np.float32(QK**-0.5 * np.log2(np.e))
     ones = jnp.where(iota((NOPE, ROWS), 0) == 0, 1.0, 0.0).astype(BF16)
 
     def keys(j):
@@ -341,7 +348,7 @@
         for h in range(2):
             ready = jnp.concatenate([m[0][h] for m in made], axis=1)
             v = jnp.concatenate([m[1][h] for m in made], axis=1)
-            s = dot(q[h, :, 0:QK], ready) * factor
+            s = dot(q[h, :, 0:QK], ready)
             if first:
                 s = jnp.where(iota((ROWS, ROWS), 1) <= iota((ROWS, ROWS), 0), s, -jnp.inf)
             peak = jnp.max(s, axis=1, keepdims=True)
@@ -358,14 +365,18 @@
     block([sp], True)
 
     def loop(i, carry):
-        block([2 * i, 2 * i + 1], False)
+        block([3 * i, 3 * i + 1, 3 * i + 2], False)
         return carry
 
-    lax.fori_loop(0, sp // 2, loop, 0)
-
-    @pl.when(lax.rem(sp, 2) == 1)
+    lax.fori_loop(0, sp // 3, loop, 0)
+
+    @pl.when(lax.rem(sp, 3) == 1)
     def _():
         block([sp - 1], False)
+
+    @pl.when(lax.rem(sp, 3) == 2)
+    def _():
+        block([sp - 2, sp - 1], False)
 
     parts = []
     rows = []
@@ -384,7 +395,7 @@
     return call(attend_body, outs, args, 8 << 30, scratch, [SMEM] + [VMEM] * 7)
 
 
-def merge_body(place, att, free, along, bonus, states, branch, o0, o1, o2, o3, out):
+def merge_body(place, att, free, along, bonus, states, branch, o0, o1, o2, o3, keep, send):
     head = iota((128, 128), 0) // 64 == iota((128, 128), 1) // 64
 
     def spread(v):
@@ -399,13 +410,19 @@
     read = read - dot_wide(read, mean)
     spread_of = dot_wide(read * read, mean)
     rec = read * lax.rsqrt(spread_of + GROUP_EPS) * branch[...] + bonus[...]
-    both = jnp.concatenate([att[...], rec.astype(BF16)], axis=1)
+    both = jnp.concatenate([att[...].astype(F32), rec], axis=1).reshape(4, 2, 32, 256)
+    core = lax.rem(place[1], 2)
+    even, odd = both[:, 0].reshape(128, 256), both[:, 1].reshape(128, 256)
+    kept = jnp.where(core == 0, even, odd).astype(BF16)
+    sent = jnp.where(core == 0, odd, even).astype(BF16)
     for k, o in enumerate((o0, o1, o2, o3)):
-        out[:, columns(place, k)] = dot(both, o[...]).astype(BF16)
+        send[:, columns(place, k)] = dot(sent, o[192:448]).astype(BF16)
+    for k, o in enumerate((o0, o1, o2, o3)):
+        keep[:, columns(place, k)] = dot(kept, o[192:448])
 
 
 def merge(*args):
-    outs = jax.ShapeDtypeStruct((ROWS, 2048), BF16)
+    outs = [jax.ShapeDtypeStruct((128, 2048), F32), jax.ShapeDtypeStruct((128, 2048), BF16)]
     return call(merge_body, outs, args, 4 << 30, specs=[SMEM] + [VMEM] * 10)
 
 
@@ -461,7 +478,7 @@
     sp = lax.axis_index("sp")
     core = lax.rem(tp, 2)
     place = jnp.stack([sp, tp, lax.axis_index("fs")]).astype(jnp.int32)
-    xs, small, big = prepare(
+    xs, small, big, late = prepare(
         place,
         entering[0],
         entering_gain.reshape(1, 2048),
@@ -471,10 +488,22 @@
         wq.T,
         wc,
         wr.T,
+        wo_att,
+        wo_rec,
     )
     normed = exchanged(xs, "tp").reshape(ROWS, 2048)
     smalls = around(small)
     bigs = around(big)
+    lates = around(late)
+
+    table = jnp.asarray(turn_table())
+    pay = latents(place, normed, *smalls)
+    pay, (wk_up, wv_up, compact_gain, k_gain, q_gain, fade_mult, fade_extra, present) = (
+        lax.optimization_barrier(
+            (pay, (wk_up, wv_up, compact_gain, k_gain, q_gain, fade_mult, fade_extra, present))
+        )
+    )
+    lat = exchanged(pay, "sp")
 
     def reordered(v):
         v = v.reshape(4, 2, 32, *v.shape[1:])
@@ -484,31 +513,15 @@
     up = reordered(jnp.concatenate([wk_up, wv_up], axis=1)).T
     glat = reordered(compact_gain).reshape(256, 1)
     key_gain = k_gain.reshape(QK, 1)
+    query_gain = q_gain.reshape(QK, 1)
     mult = jnp.repeat(fade_mult[0, :, 0], 64).reshape(1, 128)
     extra = fade_extra[0].T
     present = present.reshape(1, 128)
-    table = jnp.asarray(turn_table())
-    pay = latents(place, normed, *smalls)
-    lat = exchanged(pay, "sp")
     dlow, rlow, turn = lowrank(place, normed, fade1, adapt1, table)
-    wo = around(jnp.concatenate([wo_att, wo_rec], axis=0))
-    projected = project(
-        place,
-        normed,
-        *bigs,
-        turn,
-        q_gain.reshape(QK, 1),
-        up,
-        glat,
-        key_gain,
-        mult,
-        extra,
-        present,
-    )
-    lat, (rkv, q) = lax.optimization_barrier((lat, tuple(projected)))
-    same_core = [[0, 2, 4, 6], [1, 3, 5, 7]]
-    lat_own = exchanged(fan(lat), "tp", same_core)
-    recurrent = recur(
+    rkv = project(
+        place, normed, *bigs, up, glat, key_gain, mult, extra, present, query_gain
+    )
+    free, along, bonus, state = recur(
         rkv,
         dlow,
         rlow,
@@ -520,12 +533,17 @@
         extra,
         present,
     )
-    lat_own, (free, along, bonus, state) = lax.optimization_barrier((lat_own, tuple(recurrent)))
+    lat, state = lax.optimization_barrier((lat, state))
     states = exchanged(state, "sp")
+    others = [lax.ppermute(lat, "tp", [(i, (i + by) % 8) for i in range(8)]) for by in (2, 6, 4)]
+    lat_own = collect(place, lat, *others)
     lat_peer = other_core(lat_own)
+    q = queries(place, normed, *lates, turn, query_gain)
     att, logs = attend(place, q, lat_own, lat_peer, up, glat, key_gain, table)
-    partial = merge(place, att, free, along, bonus, states, branch.reshape(1, 128), *wo)
-    parts = exchanged(partial.reshape(8, 32, 2048), "tp")
+    keep, send = merge(place, att, free, along, bonus, states, branch.reshape(1, 128), *lates)
+    pair = (keep + other_core(send).astype(F32)).astype(BF16)
+    same_core = [[0, 2, 4, 6], [1, 3, 5, 7]]
+    parts = exchanged(pair.reshape(4, 32, 2048), "tp", same_core)
     mixed = jnp.sum(parts.astype(F32), axis=0).astype(BF16)
     return mixed[None], logs[None]
 

time: 173 us -> 158 us (0.913)
  the two profiles are of different devices: /device:TPU:40 before, /device:TPU:480 now
where the time goes in v4:
time: 158 us; the launch traced here: 157 us
  starting transfers between devices  68.1 us (43%)
  Pallas kernels  34.3 us (22%)
  waiting for transfers between devices  28.5 us (18%)
  blocking collectives  13.2 us (8%)
  local copies, waits for them, and re-layouts  10 us (6%)
  other arithmetic  1.58 us (1%)
    pallas_call x9, Pallas kernels, call(): pl.pallas_call(body, out_shape=outs, in_specs=specs or [VMEM] * len(args)...  34.3 us
    ppermute x9, starting transfers between devices, around(): return [value] + [lax.ppermute(value, 'fs', move) for move in moves]  29.9 us
    all_to_all x3, starting transfers between devices, exchanged(): lax.all_to_all(copies, axis, 0, 0, axis_index_groups=groups, tiled=True)  22.5 us
    ppermute x9, waiting for transfers between devices, around(): return [value] + [lax.ppermute(value, 'fs', move) for move in moves]  16.2 us
    all_to_all x1, blocking collectives, exchanged(): lax.all_to_all(copies, axis, 0, 0, axis_index_groups=groups, tiled=True)  13.2 us
    ppermute x3, starting transfers between devices, shards(): lax.ppermute(lat, 'tp', [(i, (i + by) % 8) for i in range(8)])  11.7 us
    unnamed x76, local copies, waits for them, and re-layouts  8.98 us
    ppermute x3, waiting for transfers between devices, shards(): lax.ppermute(lat, 'tp', [(i, (i + by) % 8) for i in range(8)])  7.4 us
  transfers between devices with their start and end apart: 17, of which 7 were waited for; matrix products, arithmetic and copies ran while one was open for 1% of the time, Pallas kernels for 17%

profile of v4, /device:TPU:480, one launch (start us, length us, event | category | flops | bytes accessed | tf_op | source)
XLA Modules:
  0.0 157.0 jit_solution(13980966625546282824)
XLA Ops:
  1.3 3.4 %shard_map.257 = (bf16[8,32,2048]{2,1,0:T(8,128)(2,1)}, bf16[64,512]{1,0:T(8,128)(2,1)}, bf16[512,384]{1,0:T(8,128)(2,1)}, bf16[448,512]{1,0:T(8,128)(2,1)}) custom-call(s32[3]{0:T(128)} %pad_add_fusion.place, bf16[32,2048]{1,0:T(8,128)(2,1)} %bitcast.42, f32[1,2048]{1,0:T(1,128)} %bitcast.44, bf16[512,128]{1,0:T(8,128)(2,1)} %wa_in.1, ...), custom_call_target="tpu_custom_call" | custom-call | flops 536870912 | bytes 4194304 | tf_op jit(solution)/shard_map/pallas_call | solution.py:58
  4.7 4.4 %all-to-all-start = ((bf16[8,32,2048]{2,1,0:T(8,128)(2,1)}), bf16[8,32,2048]{2,1,0:T(8,128)(2,1)S(1)}, u32[]{:S(2)}, u32[]{:S(2)}) async-start(bf16[8,32,2048]{2,1,0:T(8,128)(2,1)} %get-tuple-element.28), calls=%async_computation | async-start | bytes 2097152 | tf_op jit(solution)/shard_map/all_to_all | solution.py:430
  9.1 5.1 %collective-permute-start.5 = (bf16[64,512]{1,0:T(8,128)(2,1)S(1)}, bf16[64,512]{1,0:T(8,128)(2,1)S(1)}, u32[]{:S(2)}, u32[]{:S(2)}) collective-permute-start(bf16[64,512]{1,0:T(8,128)(2,1)S(1)} %copy-done.18), channel_id=1, source_target_pairs={{0,16},{8,24},{16,0},{24,8},{1,17},{9,25},{17,1},{25,9},{2,18},{10... | collective-permute-start | bytes 196616 | tf_op jit(solution)/shard_map/ppermute | solution.py:435
  14.2 3.0 %collective-permute-start.4 = (bf16[64,512]{1,0:T(8,128)(2,1)S(1)}, bf16[64,512]{1,0:T(8,128)(2,1)S(1)}, u32[]{:S(2)}, u32[]{:S(2)}) collective-permute-start(bf16[64,512]{1,0:T(8,128)(2,1)S(1)} %copy-done.18), channel_id=1, source_target_pairs={{0,24},{8,0},{16,8},{24,16},{1,25},{9,1},{17,9},{25,17},{2,26},{10... | collective-permute-start | bytes 196616 | tf_op jit(solution)/shard_map/ppermute | solution.py:435
  17.2 2.9 %collective-permute-start.3 = (bf16[64,512]{1,0:T(8,128)(2,1)S(1)}, bf16[64,512]{1,0:T(8,128)(2,1)S(1)}, u32[]{:S(2)}, u32[]{:S(2)}) collective-permute-start(bf16[64,512]{1,0:T(8,128)(2,1)S(1)} %copy-done.18), channel_id=1, source_target_pairs={{0,8},{8,16},{16,24},{24,0},{1,9},{9,17},{17,25},{25,1},{2,10},{10... | collective-permute-start | bytes 196616 | tf_op jit(solution)/shard_map/ppermute | solution.py:435
  20.1 2.6 %collective-permute-start.8 = (bf16[512,384]{1,0:T(8,128)(2,1)}, bf16[512,384]{1,0:T(8,128)(2,1)}, u32[]{:S(2)}, u32[]{:S(2)}) collective-permute-start(bf16[512,384]{1,0:T(8,128)(2,1)} %get-tuple-element.34.w0), channel_id=1, source_target_pairs={{0,16},{8,24},{16,0},{24,8},{1,17},{9,25},{17,1},{25,9},{2,18},{10... | collective-permute-start | bytes 1179656 | tf_op jit(solution)/shard_map/ppermute | solution.py:435
  22.8 4.5 %collective-permute-start.7 = (bf16[512,384]{1,0:T(8,128)(2,1)}, bf16[512,384]{1,0:T(8,128)(2,1)}, u32[]{:S(2)}, u32[]{:S(2)}) collective-permute-start(bf16[512,384]{1,0:T(8,128)(2,1)} %get-tuple-element.34.w0), channel_id=1, source_target_pairs={{0,24},{8,0},{16,8},{24,16},{1,25},{9,1},{17,9},{25,17},{2,26},{10... | collective-permute-start | bytes 1179656 | tf_op jit(solution)/shard_map/ppermute | solution.py:435
  31.1 8.9 %all-to-all-start.1 = ((bf16[16,40,256]{2,1,0:T(8,128)(2,1)}), bf16[16,40,256]{2,1,0:T(8,128)(2,1)S(1)}, u32[]{:S(2)}, u32[]{:S(2)}) async-start(bf16[16,40,256]{2,1,0:T(8,128)(2,1)} %copy-done.11), calls=%async_computation.1 | async-start | bytes 655360 | tf_op jit(solution)/shard_map/all_to_all | solution.py:430
  43.3 2.1 %shard_map.261.rkv = bf16[256,384]{1,0:T(8,128)(2,1)S(1)} custom-call(s32[3]{0:T(128)S(1)} %copy-done.17, bf16[256,2048]{1,0:T(8,128)(2,1)S(1)} %bitcast.28, bf16[512,384]{1,0:T(8,128)(2,1)} %get-tuple-element.34.w0, bf16[512,384]{1,0:T(8,128)(2,1)} %collective-permute-done.6.w1, bf16[512,384]{1,0:T(8,128)(2,1)} %collective-permute-done.7.w2, ...), custom_call_target="tpu_custom_call" | custom-call | flops 4294967296 | bytes 4194304 | tf_op jit(solution)/shard_map/pallas_call | solution.py:58
  46.2 10.5 %shard_map.262 = (f32[256,128]{1,0:T(8,128)}, f32[256,128]{1,0:T(8,128)}, f32[256,128]{1,0:T(8,128)}, bf16[16,2,64,128]{3,2,1,0:T(8,128)(2,1)}) custom-call(bf16[256,384]{1,0:T(8,128)(2,1)} %copy-done.24, bf16[256,128]{1,0:T(8,128)(2,1)} %copy-done.19, bf16[256,128]{1,0:T(8,128)(2,1)} %copy-done.20, bf16[128,128]{1,0:T(8,128)(2,1)} %wd.1, ...), custom_call_target="tpu_custom_call" | custom-call | flops 8589934592 | bytes 4194304 | tf_op jit(solution)/shard_map/pallas_call | solution.py:58
  56.6 3.1 %all-to-all-done.1.own = bf16[16,40,256]{2,1,0:T(8,128)(2,1)S(1)} async-done(((bf16[16,40,256]{2,1,0:T(8,128)(2,1)}), bf16[16,40,256]{2,1,0:T(8,128)(2,1)S(1)}, u32[]{:S(2)}, u32[]{:S(2)}) %all-to-all-start.1) | async-done | bytes 327712 | tf_op jit(solution)/shard_map/all_to_all | solution.py:430
  59.7 5.9 %collective-permute-start.11 = (bf16[16,40,256]{2,1,0:T(8,128)(2,1)S(1)}, bf16[16,40,256]{2,1,0:T(8,128)(2,1)S(1)}, u32[]{:S(2)}, u32[]{:S(2)}) collective-permute-start(bf16[16,40,256]{2,1,0:T(8,128)(2,1)S(1)} %all-to-all-done.1.own), channel_id=1, source_target_pairs={{0,4},{1,5},{2,6},{3,7},{4,0},{5,1},{6,2},{7,3},{8,12},{9,13},{10,... | collective-permute-start | bytes 983048 | tf_op jit(solution)/shard_map/ppermute | solution.py:538
  65.6 3.1 %collective-permute-start.10 = (bf16[16,40,256]{2,1,0:T(8,128)(2,1)S(1)}, bf16[16,40,256]{2,1,0:T(8,128)(2,1)S(1)}, u32[]{:S(2)}, u32[]{:S(2)}) collective-permute-start(bf16[16,40,256]{2,1,0:T(8,128)(2,1)S(1)} %all-to-all-done.1.own), channel_id=1, source_target_pairs={{0,6},{1,7},{2,0},{3,1},{4,2},{5,3},{6,4},{7,5},{8,14},{9,15},{10,... | collective-permute-start | bytes 983048 | tf_op jit(solution)/shard_map/ppermute | solution.py:538
  68.7 2.8 %collective-permute-start.9 = (bf16[16,40,256]{2,1,0:T(8,128)(2,1)S(1)}, bf16[16,40,256]{2,1,0:T(8,128)(2,1)S(1)}, u32[]{:S(2)}, u32[]{:S(2)}) collective-permute-start(bf16[16,40,256]{2,1,0:T(8,128)(2,1)S(1)} %all-to-all-done.1.own), channel_id=1, source_target_pairs={{0,2},{1,3},{2,4},{3,5},{4,6},{5,7},{6,0},{7,1},{8,10},{9,11},{10,... | collective-permute-start | bytes 983048 | tf_op jit(solution)/shard_map/ppermute | solution.py:538
  73.0 2.7 %collective-permute-done.10.right = bf16[16,40,256]{2,1,0:T(8,128)(2,1)S(1)} collective-permute-done((bf16[16,40,256]{2,1,0:T(8,128)(2,1)S(1)}, bf16[16,40,256]{2,1,0:T(8,128)(2,1)S(1)}, u32[]{:S(2)}, u32[]{:S(2)}) %collective-permute-start.10) | collective-permute-done | bytes 327712 | tf_op jit(solution)/shard_map/ppermute | solution.py:538
  75.7 3.2 %collective-permute-done.9.left = bf16[16,40,256]{2,1,0:T(8,128)(2,1)S(1)} collective-permute-done((bf16[16,40,256]{2,1,0:T(8,128)(2,1)S(1)}, bf16[16,40,256]{2,1,0:T(8,128)(2,1)S(1)}, u32[]{:S(2)}, u32[]{:S(2)}) %collective-permute-start.9) | collective-permute-done | bytes 327712 | tf_op jit(solution)/shard_map/ppermute | solution.py:538
  81.5 9.2 %all-to-all-start.2 = ((bf16[16,2,64,128]{3,2,1,0:T(8,128)(2,1)}), bf16[16,2,64,128]{3,2,1,0:T(8,128)(2,1)S(1)}, u32[]{:S(2)}, u32[]{:S(2)}) async-start(bf16[16,2,64,128]{3,2,1,0:T(8,128)(2,1)} %get-tuple-element.50), calls=%async_computation.2 | async-start | bytes 1048576 | tf_op jit(solution)/shard_map/all_to_all | solution.py:430
  90.7 3.8 %collective-permute-start.2 = (bf16[448,512]{1,0:T(8,128)(2,1)}, bf16[448,512]{1,0:T(8,128)(2,1)S(1)}, u32[]{:S(2)}, u32[]{:S(2)}) collective-permute-start(bf16[448,512]{1,0:T(8,128)(2,1)} %get-tuple-element.29.w0.o0), channel_id=1, source_target_pairs={{0,16},{8,24},{16,0},{24,8},{1,17},{9,25},{17,1},{25,9},{2,18},{10... | collective-permute-start | bytes 1376264 | tf_op jit(solution)/shard_map/ppermute | solution.py:435
  94.5 4.2 %collective-permute-start.1 = (bf16[448,512]{1,0:T(8,128)(2,1)}, bf16[448,512]{1,0:T(8,128)(2,1)S(1)}, u32[]{:S(2)}, u32[]{:S(2)}) collective-permute-start(bf16[448,512]{1,0:T(8,128)(2,1)} %get-tuple-element.29.w0.o0), channel_id=1, source_target_pairs={{0,24},{8,0},{16,8},{24,16},{1,25},{9,1},{17,9},{25,17},{2,26},{10... | collective-permute-start | bytes 1376264 | tf_op jit(solution)/shard_map/ppermute | solution.py:435
  100.6 7.1 %collective-permute-done.2.w3.o3 = bf16[448,512]{1,0:T(8,128)(2,1)S(1)} collective-permute-done((bf16[448,512]{1,0:T(8,128)(2,1)}, bf16[448,512]{1,0:T(8,128)(2,1)S(1)}, u32[]{:S(2)}, u32[]{:S(2)}) %collective-permute-start.2) | collective-permute-done | bytes 458784 | tf_op jit(solution)/shard_map/ppermute | solution.py:435
  107.7 9.1 %collective-permute-done.1.w2.o2 = bf16[448,512]{1,0:T(8,128)(2,1)S(1)} collective-permute-done((bf16[448,512]{1,0:T(8,128)(2,1)}, bf16[448,512]{1,0:T(8,128)(2,1)S(1)}, u32[]{:S(2)}, u32[]{:S(2)}) %collective-permute-start.1) | collective-permute-done | bytes 458784 | tf_op jit(solution)/shard_map/ppermute | solution.py:435
  119.4 10.5 %shard_map.264 = (bf16[256,128]{1,0:T(8,128)(2,1)S(1)}, f32[2,256]{1,0:T(2,128)}) custom-call(s32[3]{0:T(128)S(1)} %copy-done.17, bf16[2,256,128]{2,1,0:T(8,128)(2,1)S(1)} %shard_map.260.q, bf16[4,16,40,256]{3,2,1,0:T(8,128)(2,1)S(1)} %shard_map.263.own, bf16[4,16,40,256]{3,2,1,0:T(8,128)(2,1)} %collective-permute-done.12.peer, ...), custom_call_target="tpu_custom_call" | custom-call | flops 8589934592 | bytes 4194304 | tf_op jit(solution)/shard_map/pallas_call | solution.py:58
  135.3 3.8 %shard_map.265 = (f32[128,2048]{1,0:T(8,128)S(1)}, bf16[128,2048]{1,0:T(8,128)(2,1)S(1)}) custom-call(s32[3]{0:T(128)S(1)} %copy-done.17, bf16[256,128]{1,0:T(8,128)(2,1)S(1)} %copy-done.29, f32[256,128]{1,0:T(8,128)S(1)} %copy-done.25, f32[256,128]{1,0:T(8,128)S(1)} %copy-done.26, f32[256,128]{1,0:T(8,128)S(1)} %copy-done.27, ...), custom_call_target="tpu_custom_call" | custom-call | flops 4294967296 | bytes 4194304 | tf_op jit(solution)/shard_map/pallas_call | solution.py:58
  143.0 13.2 %all_to_all.20 = bf16[4,32,2048]{2,1,0:T(8,128)(2,1)S(1)} all-to-all(bf16[4,32,2048]{2,1,0:T(8,128)(2,1)S(1)} %bitcast.35), channel_id=1, replica_groups={{0,2,4,6},{1,3,5,7},{8,10,12,14},{9,11,13,15},{16,18,20,22},{17,19,21,2..., dimensions={0} | all-to-all | bytes 1048576 | tf_op jit(solution)/shard_map/all_to_all | solution.py:430
  (115 shorter events, 26.7 us)
Async XLA Ops:
  4.7 24.6 %copy-start.17 = (s32[3]{0:T(128)S(1)}, s32[3]{0:T(128)}, u32[]{:S(2)}) copy-start(s32[3]{0:T(128)} %pad_add_fusion.place) | copy-start | bytes 40
  4.7 24.6 %all-to-all-start = ((bf16[8,32,2048]{2,1,0:T(8,128)(2,1)}), bf16[8,32,2048]{2,1,0:T(8,128)(2,1)S(1)}, u32[]{:S(2)}, u32[]{:S(2)}) async-start(bf16[8,32,2048]{2,1,0:T(8,128)(2,1)} %get-tuple-element.28), calls=%async_computation | async-start | bytes 2097152 | tf_op jit(solution)/shard_map/all_to_all | solution.py:430
  9.1 21.2 %copy-start.33 = (f32[256]{0:T(256)S(1)}, f32[256]{0:T(256)}, u32[]{:S(2)}) copy-start(f32[256]{0:T(256)} %param.31) | copy-start | bytes 3076
  9.1 18.2 %collective-permute-start.5 = (bf16[64,512]{1,0:T(8,128)(2,1)S(1)}, bf16[64,512]{1,0:T(8,128)(2,1)S(1)}, u32[]{:S(2)}, u32[]{:S(2)}) collective-permute-start(bf16[64,512]{1,0:T(8,128)(2,1)S(1)} %copy-done.18), channel_id=1, source_target_pairs={{0,16},{8,24},{16,0},{24,8},{1,17},{9,25},{17,1},{25,9},{2,18},{10... | collective-permute-start | bytes 196616 | tf_op jit(solution)/shard_map/ppermute | solution.py:435
  14.2 15.0 %collective-permute-start.4 = (bf16[64,512]{1,0:T(8,128)(2,1)S(1)}, bf16[64,512]{1,0:T(8,128)(2,1)S(1)}, u32[]{:S(2)}, u32[]{:S(2)}) collective-permute-start(bf16[64,512]{1,0:T(8,128)(2,1)S(1)} %copy-done.18), channel_id=1, source_target_pairs={{0,24},{8,0},{16,8},{24,16},{1,25},{9,1},{17,9},{25,17},{2,26},{10... | collective-permute-start | bytes 196616 | tf_op jit(solution)/shard_map/ppermute | solution.py:435
  17.2 12.0 %collective-permute-start.3 = (bf16[64,512]{1,0:T(8,128)(2,1)S(1)}, bf16[64,512]{1,0:T(8,128)(2,1)S(1)}, u32[]{:S(2)}, u32[]{:S(2)}) collective-permute-start(bf16[64,512]{1,0:T(8,128)(2,1)S(1)} %copy-done.18), channel_id=1, source_target_pairs={{0,8},{8,16},{16,24},{24,0},{1,9},{9,17},{17,25},{25,1},{2,10},{10... | collective-permute-start | bytes 196616 | tf_op jit(solution)/shard_map/ppermute | solution.py:435
  20.1 23.2 %collective-permute-start.8 = (bf16[512,384]{1,0:T(8,128)(2,1)}, bf16[512,384]{1,0:T(8,128)(2,1)}, u32[]{:S(2)}, u32[]{:S(2)}) collective-permute-start(bf16[512,384]{1,0:T(8,128)(2,1)} %get-tuple-element.34.w0), channel_id=1, source_target_pairs={{0,16},{8,24},{16,0},{24,8},{1,17},{9,25},{17,1},{25,9},{2,18},{10... | collective-permute-start | bytes 1179656 | tf_op jit(solution)/shard_map/ppermute | solution.py:435
  22.8 20.6 %collective-permute-start.7 = (bf16[512,384]{1,0:T(8,128)(2,1)}, bf16[512,384]{1,0:T(8,128)(2,1)}, u32[]{:S(2)}, u32[]{:S(2)}) collective-permute-start(bf16[512,384]{1,0:T(8,128)(2,1)} %get-tuple-element.34.w0), channel_id=1, source_target_pairs={{0,24},{8,0},{16,8},{24,16},{1,25},{9,1},{17,9},{25,17},{2,26},{10... | collective-permute-start | bytes 1179656 | tf_op jit(solution)/shard_map/ppermute | solution.py:435
  27.3 16.0 %collective-permute-start.6 = (bf16[512,384]{1,0:T(8,128)(2,1)}, bf16[512,384]{1,0:T(8,128)(2,1)}, u32[]{:S(2)}, u32[]{:S(2)}) collective-permute-start(bf16[512,384]{1,0:T(8,128)(2,1)} %get-tuple-element.34.w0), channel_id=1, source_target_pairs={{0,8},{8,16},{16,24},{24,0},{1,9},{9,17},{17,25},{25,1},{2,10},{10... | collective-permute-start | bytes 1179656 | tf_op jit(solution)/shard_map/ppermute | solution.py:435
  31.1 28.6 %all-to-all-start.1 = ((bf16[16,40,256]{2,1,0:T(8,128)(2,1)}), bf16[16,40,256]{2,1,0:T(8,128)(2,1)S(1)}, u32[]{:S(2)}, u32[]{:S(2)}) async-start(bf16[16,40,256]{2,1,0:T(8,128)(2,1)} %copy-done.11), calls=%async_computation.1 | async-start | bytes 655360 | tf_op jit(solution)/shard_map/all_to_all | solution.py:430
  59.7 13.3 %collective-permute-start.11 = (bf16[16,40,256]{2,1,0:T(8,128)(2,1)S(1)}, bf16[16,40,256]{2,1,0:T(8,128)(2,1)S(1)}, u32[]{:S(2)}, u32[]{:S(2)}) collective-permute-start(bf16[16,40,256]{2,1,0:T(8,128)(2,1)S(1)} %all-to-all-done.1.own), channel_id=1, source_target_pairs={{0,4},{1,5},{2,6},{3,7},{4,0},{5,1},{6,2},{7,3},{8,12},{9,13},{10,... | collective-permute-start | bytes 983048 | tf_op jit(solution)/shard_map/ppermute | solution.py:538
  65.6 10.1 %collective-permute-start.10 = (bf16[16,40,256]{2,1,0:T(8,128)(2,1)S(1)}, bf16[16,40,256]{2,1,0:T(8,128)(2,1)S(1)}, u32[]{:S(2)}, u32[]{:S(2)}) collective-permute-start(bf16[16,40,256]{2,1,0:T(8,128)(2,1)S(1)} %all-to-all-done.1.own), channel_id=1, source_target_pairs={{0,6},{1,7},{2,0},{3,1},{4,2},{5,3},{6,4},{7,5},{8,14},{9,15},{10,... | collective-permute-start | bytes 983048 | tf_op jit(solution)/shard_map/ppermute | solution.py:538
  68.7 10.2 %collective-permute-start.9 = (bf16[16,40,256]{2,1,0:T(8,128)(2,1)S(1)}, bf16[16,40,256]{2,1,0:T(8,128)(2,1)S(1)}, u32[]{:S(2)}, u32[]{:S(2)}) collective-permute-start(bf16[16,40,256]{2,1,0:T(8,128)(2,1)S(1)} %all-to-all-done.1.own), channel_id=1, source_target_pairs={{0,2},{1,3},{2,4},{3,5},{4,6},{5,7},{6,0},{7,1},{8,10},{9,11},{10,... | collective-permute-start | bytes 983048 | tf_op jit(solution)/shard_map/ppermute | solution.py:538
  79.5 39.9 %collective-permute-start.12 = (bf16[4,16,40,256]{3,2,1,0:T(8,128)(2,1)S(1)}, bf16[4,16,40,256]{3,2,1,0:T(8,128)(2,1)}, u32[]{:S(2)}, u32[]{:S(2)}) collective-permute-start(bf16[4,16,40,256]{3,2,1,0:T(8,128)(2,1)S(1)} %shard_map.263.own), channel_id=1, source_target_pairs={{0,1},{1,0},{2,3},{3,2},{4,5},{5,4},{6,7},{7,6},{8,9},{9,8},{10,11... | collective-permute-start | bytes 3932168 | tf_op jit(solution)/shard_map/ppermute | solution.py:439
  81.5 49.2 %all-to-all-start.2 = ((bf16[16,2,64,128]{3,2,1,0:T(8,128)(2,1)}), bf16[16,2,64,128]{3,2,1,0:T(8,128)(2,1)S(1)}, u32[]{:S(2)}, u32[]{:S(2)}) async-start(bf16[16,2,64,128]{3,2,1,0:T(8,128)(2,1)} %get-tuple-element.50), calls=%async_computation.2 | async-start | bytes 1048576 | tf_op jit(solution)/shard_map/all_to_all | solution.py:430
  90.7 17.0 %collective-permute-start.2 = (bf16[448,512]{1,0:T(8,128)(2,1)}, bf16[448,512]{1,0:T(8,128)(2,1)S(1)}, u32[]{:S(2)}, u32[]{:S(2)}) collective-permute-start(bf16[448,512]{1,0:T(8,128)(2,1)} %get-tuple-element.29.w0.o0), channel_id=1, source_target_pairs={{0,16},{8,24},{16,0},{24,8},{1,17},{9,25},{17,1},{25,9},{2,18},{10... | collective-permute-start | bytes 1376264 | tf_op jit(solution)/shard_map/ppermute | solution.py:435
  94.5 22.3 %collective-permute-start.1 = (bf16[448,512]{1,0:T(8,128)(2,1)}, bf16[448,512]{1,0:T(8,128)(2,1)S(1)}, u32[]{:S(2)}, u32[]{:S(2)}) collective-permute-start(bf16[448,512]{1,0:T(8,128)(2,1)} %get-tuple-element.29.w0.o0), channel_id=1, source_target_pairs={{0,24},{8,0},{16,8},{24,16},{1,25},{9,1},{17,9},{25,17},{2,26},{10... | collective-permute-start | bytes 1376264 | tf_op jit(solution)/shard_map/ppermute | solution.py:435
  98.7 18.1 %collective-permute-start = (bf16[448,512]{1,0:T(8,128)(2,1)}, bf16[448,512]{1,0:T(8,128)(2,1)S(1)}, u32[]{:S(2)}, u32[]{:S(2)}) collective-permute-start(bf16[448,512]{1,0:T(8,128)(2,1)} %get-tuple-element.29.w0.o0), channel_id=1, source_target_pairs={{0,8},{8,16},{16,24},{24,0},{1,9},{9,17},{17,25},{25,1},{2,10},{10... | collective-permute-start | bytes 1376264 | tf_op jit(solution)/shard_map/ppermute | solution.py:435
  107.7 11.6 %copy-start.5 = (bf16[448,512]{1,0:T(8,128)(2,1)}, bf16[448,512]{1,0:T(8,128)(2,1)S(1)}, u32[]{:S(2)}) copy-start(bf16[448,512]{1,0:T(8,128)(2,1)S(1)} %collective-permute-done.2.w3.o3) | copy-start | bytes 1376260
  119.4 11.2 %copy-start.4 = (bf16[448,512]{1,0:T(8,128)(2,1)S(1)}, bf16[448,512]{1,0:T(8,128)(2,1)}, u32[]{:S(2)}) copy-start(bf16[448,512]{1,0:T(8,128)(2,1)} %get-tuple-element.29.w0.o0) | copy-start | bytes 1376260
  119.4 11.2 %copy-start.21 = (f32[128]{0:T(128)S(1)}, f32[128]{0:T(128)}, u32[]{:S(2)}) copy-start(f32[128]{0:T(128)} %param.48) | copy-start | bytes 1540
  119.4 11.2 %copy-start.25 = (f32[256,128]{1,0:T(8,128)S(1)}, f32[256,128]{1,0:T(8,128)}, u32[]{:S(2)}) copy-start(f32[256,128]{1,0:T(8,128)} %get-tuple-element.47.free) | copy-start | bytes 393220
  119.4 11.2 %copy-start.6 = (bf16[448,512]{1,0:T(8,128)(2,1)S(1)}, bf16[448,512]{1,0:T(8,128)(2,1)}, u32[]{:S(2)}) copy-start(bf16[448,512]{1,0:T(8,128)(2,1)} %copy-done.5) | copy-start | bytes 1376260
  139.1 3.8 %collective-permute-start.13 = (bf16[128,2048]{1,0:T(8,128)(2,1)S(1)}, bf16[128,2048]{1,0:T(8,128)(2,1)S(1)}, u32[]{:S(2)}, u32[]{:S(2)}) collective-permute-start(bf16[128,2048]{1,0:T(8,128)(2,1)S(1)} %get-tuple-element.52), channel_id=1, source_target_pairs={{0,1},{1,0},{2,3},{3,2},{4,5},{5,4},{6,7},{7,6},{8,9},{9,8},{10,11... | collective-permute-start | bytes 1572872 | tf_op jit(solution)/shard_map/ppermute | solution.py:439
  (31 other events, 109.0 us)

commit v5 on v4

--- a/solution.py
+++ b/solution.py
@@ -15,6 +15,7 @@
 ROPE = 32
 QK = NOPE + ROPE
 CHUNK = 64
+RECUR_LIMIT = 40
 CHUNKS = ROWS // CHUNK
 EPS = 1e-6
 GROUP_EPS = 0.00064
@@ -130,19 +131,41 @@
     return call(collect_body, outs, (place, *parts), 1 << 29, specs=[SMEM] + [VMEM] * 4)
 
 
-def lowrank_body(place, x, fd, fa, table, dlow, rlow, turn):
+def lowrank_body(
+    place, x, fd, fa, table, wk_up, wv_up, compact_gain, kg, qg,
+    dlow, rlow, turn, up, glat, key_gain, query_gain,
+):
+    core = lax.rem(place[1], 2)
     dlow[...] = jnp.tanh(dot(x[...], fd[...]).astype(BF16).astype(F32)).astype(BF16)
     rlow[...] = dot(x[...], fa[...]).astype(BF16)
     turn[...] = table[place[0]]
 
+    def reordered(v):
+        v = v.reshape(4, 2, 32, v.shape[-1])
+        even, odd = v[:, 0].reshape(128, -1), v[:, 1].reshape(128, -1)
+        first, second = jnp.where(core == 0, even, odd), jnp.where(core == 0, odd, even)
+        return jnp.concatenate([first, second], axis=0)
+
+    both = jnp.concatenate([wk_up[...], wv_up[...]], axis=1).astype(F32)
+    up[...] = reordered(both).T.astype(BF16)
+    glat[...] = reordered(jnp.broadcast_to(compact_gain[...], (128, 256)).T)
+    for source, out in ((kg, key_gain), (qg, query_gain)):
+        wide = jnp.concatenate([source[...], jnp.zeros((1, 128 - QK), F32)], axis=1)
+        out[...] = jnp.broadcast_to(wide, (128, 128)).T[0:QK]
+
 
 def lowrank(*args):
+    column = jax.ShapeDtypeStruct((QK, 128), F32)
     outs = [
         jax.ShapeDtypeStruct((ROWS, 128), BF16),
         jax.ShapeDtypeStruct((ROWS, 128), BF16),
         jax.ShapeDtypeStruct((ROPE, ROWS), F32),
+        jax.ShapeDtypeStruct((256, 256), BF16),
+        jax.ShapeDtypeStruct((256, 128), F32),
+        column,
+        column,
     ]
-    return call(lowrank_body, outs, args, 1 << 29, specs=[SMEM] + [VMEM] * 4)
+    return call(lowrank_body, outs, args, 1 << 29, specs=[SMEM] + [VMEM] * 9)
 
 
 def columns(place, k):
@@ -166,21 +189,7 @@
 
 def latents(*args):
     outs = jax.ShapeDtypeStruct((16, 40, ROWS), BF16)
-    return call(latents_body, outs, args, 1 << 29, specs=[SMEM] + [VMEM] * 5)
-
-
-def project_body(
-    place, x, w0, w1, w2, w3, up, glat, kgain, mult, extra, present, gain, rkv
-):
-    y = jnp.zeros((ROWS, 384), F32)
-    for k, w in enumerate((w0, w1, w2, w3)):
-        y += dot(x[:, columns(place, k)], w[...])
-    rkv[...] = y.astype(BF16)
-
-
-def project(*args):
-    outs = jax.ShapeDtypeStruct((ROWS, 384), BF16)
-    return call(project_body, outs, args, 4 << 30, specs=[SMEM] + [VMEM] * 5 + [ANY] * 7)
+    return call(latents_body, outs, args, 1 << 29, specs=[SMEM] + [VMEM] * 5, limit=63.9)
 
 
 def queries_body(place, x, w0, w1, w2, w3, turn, gain, q):
@@ -191,7 +200,7 @@
     factor = np.float32(QK**-0.5 * np.log2(np.e))
     for h in range(2):
         v = t[QK * h : QK * (h + 1)]
-        n = v * (lax.rsqrt(jnp.mean(v * v, axis=0, keepdims=True) + EPS) * factor) * gain[...]
+        n = v * (lax.rsqrt(jnp.mean(v * v, axis=0, keepdims=True) + EPS) * factor) * gain[:, 0:1]
         a, b = turned(n, turn[...])
         ready = jnp.concatenate([n[:NOPE], a, b, jnp.zeros((128 - QK, ROWS), F32)], axis=0)
         q[h] = ready.T.astype(BF16)
@@ -202,16 +211,24 @@
     return call(queries_body, outs, args, 1 << 29, specs=[SMEM] + [VMEM] * 7)
 
 
-def recur_body(rkv, dlow, rlow, wd, bd, wa, ba, mult, extra, present, free, along, bonus, state):
-    lane = iota((ROWS, 128), 1)
-    recept, key, value = (rkv[:, 128 * i : 128 * (i + 1)].astype(F32) for i in range(3))
+def recur_body(
+    place, x, w0, w1, w2, w3, dlow, rlow, wd, bd, wa, ba, mult, extra, present, up, glat, kgain,
+    qgain, free, along, bonus, state,
+):
+    lane = iota((1, 128), 1)
+    y = jnp.zeros((ROWS, 384), F32)
+    for k, w in enumerate((w0, w1, w2, w3)):
+        y += dot(x[:, columns(place, k)], w[...])
+    y = y.astype(BF16).astype(F32)
+    recept, key, value = (y[:, 128 * i : 128 * (i + 1)] for i in range(3))
     speed = jax.nn.sigmoid(bd[...] + dot(dlow[...], wd[...])) * np.float32(np.exp(-0.5))
-    added = jnp.where(lane < 64, extra[:, 0:1], extra[:, 1:2])
-    ld = added - speed * mult[...]
+    added = jnp.where(iota((128, ROWS), 0) < 64, extra[0:1], extra[1:2]).T
+    ld = added - speed * jnp.where(lane < 64, mult[0:1, 0:1], mult[1:2, 0:1])
+    here = jnp.concatenate([present[0:1], present[1:2]], axis=1)
     learn = jax.nn.sigmoid(ba[...] + dot(rlow[...], wa[...]))
     same = (iota((128, 128), 0) // 64 == iota((128, 128), 1) // 64).astype(BF16)
     unit = key * lax.rsqrt(dot_wide(key * key, same) + EPS)
-    bonus[...] = dot_wide(recept * key * present[...], same) * value
+    bonus[...] = dot_wide(recept * key * here, same) * value
     r, c = iota((ROWS, ROWS), 0), iota((ROWS, ROWS), 1)
     block = r // CHUNK == c // CHUNK
     sums = jnp.concatenate(
@@ -308,7 +325,8 @@
 def recur(*args):
     wide = jax.ShapeDtypeStruct((ROWS, 128), F32)
     outs = [wide, wide, wide, jax.ShapeDtypeStruct((16, 2, 64, 128), BF16)]
-    return call(recur_body, outs, args, 8 << 30, limit=60)
+    specs = [SMEM] + [VMEM] * 14 + [ANY] * 4
+    return call(recur_body, outs, args, 8 << 30, specs=specs, limit=RECUR_LIMIT)
 
 
 def attend_body(place, q, own, peer, w, glat, gain, table, att, logs, acc, top):
@@ -322,12 +340,12 @@
         rope = (own[:, j, 32:40, :].astype(F32) + peer[:, j, 32:40, :].astype(F32)).reshape(
             ROPE, ROWS
         )
-        lat = lat * lax.rsqrt(jnp.mean(lat * lat, axis=0, keepdims=True) + EPS) * glat[...]
+        lat = lat * lax.rsqrt(jnp.mean(lat * lat, axis=0, keepdims=True) + EPS) * glat[:, 0:1]
         kv = dot(w[...], lat.astype(BF16)).astype(BF16)
         rope_sum = jnp.sum(rope * rope, axis=0, keepdims=True)
         turn = table[j]
         cosine, sine = turn[:16], turn[16:]
-        ra, rb = rope[:16] * gain[64:80], rope[16:] * gain[80:96]
+        ra, rb = rope[:16] * gain[64:80, 0:1], rope[16:] * gain[80:96, 0:1]
         ra, rb = ra * cosine - rb * sine, rb * cosine + ra * sine
         ready, values = [], []
         for h in range(2):
@@ -336,7 +354,7 @@
                 (jnp.sum(k * k, axis=0, keepdims=True) + rope_sum) * np.float32(1 / QK) + EPS
             )
             ready.append(
-                jnp.concatenate([k * scale * gain[0:64], ra * scale, rb * scale], axis=0).astype(
+                jnp.concatenate([k * scale * gain[0:64, 0:1], ra * scale, rb * scale], axis=0).astype(
                     BF16
                 )
             )
@@ -401,10 +419,24 @@
     def spread(v):
         return jnp.where(head, jnp.concatenate([v, v], axis=0), jnp.zeros((), v.dtype))
 
-    def step(r, entering):
-        return dot_wide(entering, spread(states[r, 0])) + spread(states[r, 1]).astype(F32)
-
-    entering = lax.fori_loop(0, place[0], step, jnp.zeros((128, 128), F32))
+    sp = place[0]
+    eye = jnp.where(iota((128, 128), 0) == iota((128, 128), 1), 1.0, 0.0).astype(BF16)
+    below = jnp.zeros((128, 128), F32)
+    entering = below
+    groups = []
+    for g in range(4):
+        pair = None
+        for r in range(4 * g, 4 * g + 4):
+            move = jnp.where(r < sp, spread(states[r, 0]), eye)
+            add = jnp.where(r < sp, spread(states[r, 1]).astype(F32), 0.0)
+            if pair is None:
+                pair = jnp.concatenate([add, move.astype(F32)], axis=0)
+            else:
+                pair = dot_wide(pair, move) + jnp.concatenate([add, below], axis=0)
+        groups.append(pair)
+    entering = groups[0][:128]
+    for pair in groups[1:]:
+        entering = fine(entering, pair[128:]) + pair[:128]
     read = free[...] + fine(along[...], entering, NT)
     mean = jnp.where(head, 1.0 / 64, 0.0).astype(BF16)
     read = read - dot_wide(read, mean)
@@ -476,7 +508,6 @@
 ):
     tp = lax.axis_index("tp")
     sp = lax.axis_index("sp")
-    core = lax.rem(tp, 2)
     place = jnp.stack([sp, tp, lax.axis_index("fs")]).astype(jnp.int32)
     xs, small, big, late = prepare(
         place,
@@ -498,40 +529,37 @@
 
     table = jnp.asarray(turn_table())
     pay = latents(place, normed, *smalls)
-    pay, (wk_up, wv_up, compact_gain, k_gain, q_gain, fade_mult, fade_extra, present) = (
-        lax.optimization_barrier(
-            (pay, (wk_up, wv_up, compact_gain, k_gain, q_gain, fade_mult, fade_extra, present))
-        )
-    )
     lat = exchanged(pay, "sp")
 
-    def reordered(v):
-        v = v.reshape(4, 2, 32, *v.shape[1:])
-        v = jnp.where(core == 0, v, v[:, ::-1])
-        return jnp.moveaxis(v, 1, 0).reshape(256, *v.shape[3:])
-
-    up = reordered(jnp.concatenate([wk_up, wv_up], axis=1)).T
-    glat = reordered(compact_gain).reshape(256, 1)
-    key_gain = k_gain.reshape(QK, 1)
-    query_gain = q_gain.reshape(QK, 1)
-    mult = jnp.repeat(fade_mult[0, :, 0], 64).reshape(1, 128)
-    extra = fade_extra[0].T
-    present = present.reshape(1, 128)
-    dlow, rlow, turn = lowrank(place, normed, fade1, adapt1, table)
-    rkv = project(
-        place, normed, *bigs, up, glat, key_gain, mult, extra, present, query_gain
+    dlow, rlow, turn, up, glat, key_gain, query_gain = lowrank(
+        place,
+        normed,
+        fade1,
+        adapt1,
+        table,
+        wk_up,
+        wv_up,
+        compact_gain.reshape(1, 256),
+        k_gain.reshape(1, QK),
+        q_gain.reshape(1, QK),
     )
     free, along, bonus, state = recur(
-        rkv,
+        place,
+        normed,
+        *bigs,
         dlow,
         rlow,
         fade2,
         fade_bias.reshape(1, 128),
         adapt2,
         adapt_bias.reshape(1, 128),
-        mult,
-        extra,
+        fade_mult[0],
+        fade_extra[0],
         present,
+        up,
+        glat,
+        key_gain,
+        query_gain,
     )
     lat, state = lax.optimization_barrier((lat, state))
     states = exchanged(state, "sp")

time: 158 us -> 171 us (1.082)
  waiting for transfers between devices: 28.5 us -> 35.5 us
  starting transfers between devices: 68.1 us -> 71.8 us
  local copies, waits for them, and re-layouts: 10 us -> 12.2 us
    ppermute x9, waiting for transfers between devices: 16.2 us -> 23.3 us  [around(): return [value] + [lax.ppermute(value, 'fs', move) for move in moves]]
    unnamed x76 -> x66, local copies, waits for them, and re-layouts: 8.98 us -> 12.2 us
    ppermute x9, starting transfers between devices: 29.9 us -> 32.9 us  [around(): return [value] + [lax.ppermute(value, 'fs', move) for move in moves]]
    all_to_all x3, starting transfers between devices: 22.5 us -> 25.3 us  [exchanged(): lax.all_to_all(copies, axis, 0, 0, axis_index_groups=groups, tiled=True)]
    all_to_all x3, waiting for transfers between devices: 3.06 us -> 0.48 us  [exchanged(): lax.all_to_all(copies, axis, 0, 0, axis_index_groups=groups, tiled=True)]
    ppermute x3, waiting for transfers between devices: 7.4 us -> 9.86 us  [shards(): lax.ppermute(lat, 'tp', [(i, (i + by) % 8) for i in range(8)])]
    ppermute x3, starting transfers between devices: 11.7 us -> 9.79 us  [shards(): lax.ppermute(lat, 'tp', [(i, (i + by) % 8) for i in range(8)])]
    pallas_call x9 -> x8, Pallas kernels: 34.3 us -> 34.9 us  [call(): pl.pallas_call(body, out_shape=outs, in_specs=specs or [VMEM] * len(args)...]
  transfers between devices with their start and end apart: 17 -> 17, of which waited for: 7 -> 10; matrix products, arithmetic and copies ran while one was open for 1% -> 0% of each run, Pallas kernels for 17% -> 15%
where the time goes in v5:
time: 171 us; the launch traced here: 169 us
  starting transfers between devices  71.8 us (42%)
  waiting for transfers between devices  35.5 us (21%)
  Pallas kernels  34.9 us (20%)
  blocking collectives  12.5 us (7%)
  local copies, waits for them, and re-layouts  12.2 us (7%)
    pallas_call x8, Pallas kernels, call(): pl.pallas_call(body, out_shape=outs, in_specs=specs or [VMEM] * len(args)...  34.9 us
    ppermute x9, starting transfers between devices, around(): return [value] + [lax.ppermute(value, 'fs', move) for move in moves]  32.9 us
    all_to_all x3, starting transfers between devices, exchanged(): lax.all_to_all(copies, axis, 0, 0, axis_index_groups=groups, tiled=True)  25.3 us
    ppermute x9, waiting for transfers between devices, around(): return [value] + [lax.ppermute(value, 'fs', move) for move in moves]  23.3 us
    all_to_all x1, blocking collectives, exchanged(): lax.all_to_all(copies, axis, 0, 0, axis_index_groups=groups, tiled=True)  12.5 us
    unnamed x66, local copies, waits for them, and re-layouts  12.2 us
    ppermute x3, waiting for transfers between devices, shards(): lax.ppermute(lat, 'tp', [(i, (i + by) % 8) for i in range(8)])  9.86 us
    ppermute x3, starting transfers between devices, shards(): lax.ppermute(lat, 'tp', [(i, (i + by) % 8) for i in range(8)])  9.79 us
  transfers between devices with their start and end apart: 17, of which 10 were waited for; matrix products, arithmetic and copies ran while one was open for 0% of the time, Pallas kernels for 15%

profile of v5, /device:TPU:480, one launch (start us, length us, event | category | flops | bytes accessed | tf_op | source)
XLA Modules:
  0.0 169.4 jit_solution(757845331094968873)
XLA Ops:
  1.3 3.3 %shard_map.257 = (bf16[8,32,2048]{2,1,0:T(8,128)(2,1)}, bf16[64,512]{1,0:T(8,128)(2,1)}, bf16[512,384]{1,0:T(8,128)(2,1)}, bf16[448,512]{1,0:T(8,128)(2,1)}) custom-call(s32[3]{0:T(128)} %pad_add_fusion.place, bf16[32,2048]{1,0:T(8,128)(2,1)} %bitcast.30, f32[1,2048]{1,0:T(1,128)} %bitcast.32, bf16[512,128]{1,0:T(8,128)(2,1)} %wa_in.1, ...), custom_call_target="tpu_custom_call" | custom-call | flops 536870912 | bytes 4194304 | tf_op jit(solution)/shard_map/pallas_call | solution.py:59
  4.6 4.4 %all-to-all-start = ((bf16[8,32,2048]{2,1,0:T(8,128)(2,1)}), bf16[8,32,2048]{2,1,0:T(8,128)(2,1)}, u32[]{:S(2)}, u32[]{:S(2)}) async-start(bf16[8,32,2048]{2,1,0:T(8,128)(2,1)} %get-tuple-element.23), calls=%async_computation | async-start | bytes 2097152 | tf_op jit(solution)/shard_map/all_to_all | solution.py:462
  9.1 5.1 %collective-permute-start.5 = (bf16[64,512]{1,0:T(8,128)(2,1)S(1)}, bf16[64,512]{1,0:T(8,128)(2,1)S(1)}, u32[]{:S(2)}, u32[]{:S(2)}) collective-permute-start(bf16[64,512]{1,0:T(8,128)(2,1)S(1)} %copy-done.30), channel_id=1, source_target_pairs={{0,16},{8,24},{16,0},{24,8},{1,17},{9,25},{17,1},{25,9},{2,18},{10... | collective-permute-start | bytes 196616 | tf_op jit(solution)/shard_map/ppermute | solution.py:467
  14.2 3.0 %collective-permute-start.4 = (bf16[64,512]{1,0:T(8,128)(2,1)S(1)}, bf16[64,512]{1,0:T(8,128)(2,1)S(1)}, u32[]{:S(2)}, u32[]{:S(2)}) collective-permute-start(bf16[64,512]{1,0:T(8,128)(2,1)S(1)} %copy-done.30), channel_id=1, source_target_pairs={{0,24},{8,0},{16,8},{24,16},{1,25},{9,1},{17,9},{25,17},{2,26},{10... | collective-permute-start | bytes 196616 | tf_op jit(solution)/shard_map/ppermute | solution.py:467
  17.2 2.9 %collective-permute-start.3 = (bf16[64,512]{1,0:T(8,128)(2,1)S(1)}, bf16[64,512]{1,0:T(8,128)(2,1)}, u32[]{:S(2)}, u32[]{:S(2)}) collective-permute-start(bf16[64,512]{1,0:T(8,128)(2,1)S(1)} %copy-done.30), channel_id=1, source_target_pairs={{0,8},{8,16},{16,24},{24,0},{1,9},{9,17},{17,25},{25,1},{2,10},{10... | collective-permute-start | bytes 196616 | tf_op jit(solution)/shard_map/ppermute | solution.py:467
  21.3 3.3 %collective-permute-done.3.w1 = bf16[64,512]{1,0:T(8,128)(2,1)} collective-permute-done((bf16[64,512]{1,0:T(8,128)(2,1)S(1)}, bf16[64,512]{1,0:T(8,128)(2,1)}, u32[]{:S(2)}, u32[]{:S(2)}) %collective-permute-start.3) | collective-permute-done | bytes 65568 | tf_op jit(solution)/shard_map/ppermute | solution.py:467
  27.7 8.8 %all-to-all-start.1 = ((bf16[16,40,256]{2,1,0:T(8,128)(2,1)}), bf16[16,40,256]{2,1,0:T(8,128)(2,1)S(1)}, u32[]{:S(2)}, u32[]{:S(2)}) async-start(bf16[16,40,256]{2,1,0:T(8,128)(2,1)} %shard_map.260), calls=%async_computation.1 | async-start | bytes 655360 | tf_op jit(solution)/shard_map/all_to_all | solution.py:462
  36.5 5.1 %collective-permute-start.8 = (bf16[512,384]{1,0:T(8,128)(2,1)}, bf16[512,384]{1,0:T(8,128)(2,1)S(1)}, u32[]{:S(2)}, u32[]{:S(2)}) collective-permute-start(bf16[512,384]{1,0:T(8,128)(2,1)} %get-tuple-element.28.w0), channel_id=1, source_target_pairs={{0,16},{8,24},{16,0},{24,8},{1,17},{9,25},{17,1},{25,9},{2,18},{10... | collective-permute-start | bytes 1179656 | tf_op jit(solution)/shard_map/ppermute | solution.py:467
  41.6 3.0 %collective-permute-start.7 = (bf16[512,384]{1,0:T(8,128)(2,1)}, bf16[512,384]{1,0:T(8,128)(2,1)S(1)}, u32[]{:S(2)}, u32[]{:S(2)}) collective-permute-start(bf16[512,384]{1,0:T(8,128)(2,1)} %get-tuple-element.28.w0), channel_id=1, source_target_pairs={{0,24},{8,0},{16,8},{24,16},{1,25},{9,1},{17,9},{25,17},{2,26},{10... | collective-permute-start | bytes 1179656 | tf_op jit(solution)/shard_map/ppermute | solution.py:467
  44.6 2.9 %collective-permute-start.6 = (bf16[512,384]{1,0:T(8,128)(2,1)}, bf16[512,384]{1,0:T(8,128)(2,1)S(1)}, u32[]{:S(2)}, u32[]{:S(2)}) collective-permute-start(bf16[512,384]{1,0:T(8,128)(2,1)} %get-tuple-element.28.w0), channel_id=1, source_target_pairs={{0,8},{8,16},{16,24},{24,0},{1,9},{9,17},{17,25},{25,1},{2,10},{10... | collective-permute-start | bytes 1179656 | tf_op jit(solution)/shard_map/ppermute | solution.py:467
  54.4 4.5 %collective-permute-done.7.w2 = bf16[512,384]{1,0:T(8,128)(2,1)S(1)} collective-permute-done((bf16[512,384]{1,0:T(8,128)(2,1)}, bf16[512,384]{1,0:T(8,128)(2,1)S(1)}, u32[]{:S(2)}, u32[]{:S(2)}) %collective-permute-start.7) | collective-permute-done | bytes 393248 | tf_op jit(solution)/shard_map/ppermute | solution.py:467
  59.0 11.1 %shard_map.261 = (f32[256,128]{1,0:T(8,128)S(1)}, f32[256,128]{1,0:T(8,128)S(1)}, f32[256,128]{1,0:T(8,128)S(1)}, bf16[16,2,64,128]{3,2,1,0:T(8,128)(2,1)}) custom-call(s32[3]{0:T(128)S(1)} %copy-done.9, bf16[256,2048]{1,0:T(8,128)(2,1)} %bitcast.7.x, bf16[512,384]{1,0:T(8,128)(2,1)S(1)} %copy-done.13, bf16[512,384]{1,0:T(8,128)(2,1)S(1)} %collective-permute-done.6.w1, ...), custom_call_target="tpu_custom_call" | custom-call | flops 8589934592 | bytes 4194304 | tf_op jit(solution)/shard_map/pallas_call | solution.py:59
  72.7 3.9 %collective-permute-start.11 = (bf16[16,40,256]{2,1,0:T(8,128)(2,1)S(1)}, bf16[16,40,256]{2,1,0:T(8,128)(2,1)S(1)}, u32[]{:S(2)}, u32[]{:S(2)}) collective-permute-start(bf16[16,40,256]{2,1,0:T(8,128)(2,1)S(1)} %all-to-all-done.1.own), channel_id=1, source_target_pairs={{0,4},{1,5},{2,6},{3,7},{4,0},{5,1},{6,2},{7,3},{8,12},{9,13},{10,... | collective-permute-start | bytes 983048 | tf_op jit(solution)/shard_map/ppermute | solution.py:566
  76.6 3.5 %collective-permute-start.10 = (bf16[16,40,256]{2,1,0:T(8,128)(2,1)S(1)}, bf16[16,40,256]{2,1,0:T(8,128)(2,1)S(1)}, u32[]{:S(2)}, u32[]{:S(2)}) collective-permute-start(bf16[16,40,256]{2,1,0:T(8,128)(2,1)S(1)} %all-to-all-done.1.own), channel_id=1, source_target_pairs={{0,6},{1,7},{2,0},{3,1},{4,2},{5,3},{6,4},{7,5},{8,14},{9,15},{10,... | collective-permute-start | bytes 983048 | tf_op jit(solution)/shard_map/ppermute | solution.py:566
  82.5 4.1 %collective-permute-done.11.far = bf16[16,40,256]{2,1,0:T(8,128)(2,1)S(1)} collective-permute-done((bf16[16,40,256]{2,1,0:T(8,128)(2,1)S(1)}, bf16[16,40,256]{2,1,0:T(8,128)(2,1)S(1)}, u32[]{:S(2)}, u32[]{:S(2)}) %collective-permute-start.11) | collective-permute-done | bytes 327712 | tf_op jit(solution)/shard_map/ppermute | solution.py:566
  86.6 4.4 %collective-permute-done.10.right = bf16[16,40,256]{2,1,0:T(8,128)(2,1)S(1)} collective-permute-done((bf16[16,40,256]{2,1,0:T(8,128)(2,1)S(1)}, bf16[16,40,256]{2,1,0:T(8,128)(2,1)S(1)}, u32[]{:S(2)}, u32[]{:S(2)}) %collective-permute-start.10) | collective-permute-done | bytes 327712 | tf_op jit(solution)/shard_map/ppermute | solution.py:566
  94.9 12.0 %all-to-all-start.2 = ((bf16[16,2,64,128]{3,2,1,0:T(8,128)(2,1)}), bf16[16,2,64,128]{3,2,1,0:T(8,128)(2,1)S(1)}, u32[]{:S(2)}, u32[]{:S(2)}) async-start(bf16[16,2,64,128]{3,2,1,0:T(8,128)(2,1)} %get-tuple-element.40), calls=%async_computation.2 | async-start | bytes 1048576 | tf_op jit(solution)/shard_map/all_to_all | solution.py:462
  107.0 5.2 %collective-permute-start.2 = (bf16[448,512]{1,0:T(8,128)(2,1)S(1)}, bf16[448,512]{1,0:T(8,128)(2,1)S(1)}, u32[]{:S(2)}, u32[]{:S(2)}) collective-permute-start(bf16[448,512]{1,0:T(8,128)(2,1)S(1)} %copy-done.4), channel_id=1, source_target_pairs={{0,16},{8,24},{16,0},{24,8},{1,17},{9,25},{17,1},{25,9},{2,18},{10... | collective-permute-start | bytes 1376264 | tf_op jit(solution)/shard_map/ppermute | solution.py:467
  112.1 3.2 %collective-permute-start.1 = (bf16[448,512]{1,0:T(8,128)(2,1)S(1)}, bf16[448,512]{1,0:T(8,128)(2,1)S(1)}, u32[]{:S(2)}, u32[]{:S(2)}) collective-permute-start(bf16[448,512]{1,0:T(8,128)(2,1)S(1)} %copy-done.4), channel_id=1, source_target_pairs={{0,24},{8,0},{16,8},{24,16},{1,25},{9,1},{17,9},{25,17},{2,26},{10... | collective-permute-start | bytes 1376264 | tf_op jit(solution)/shard_map/ppermute | solution.py:467
  118.0 5.8 %collective-permute-done.2.w3.o3 = bf16[448,512]{1,0:T(8,128)(2,1)S(1)} collective-permute-done((bf16[448,512]{1,0:T(8,128)(2,1)S(1)}, bf16[448,512]{1,0:T(8,128)(2,1)S(1)}, u32[]{:S(2)}, u32[]{:S(2)}) %collective-permute-start.2) | collective-permute-done | bytes 458784 | tf_op jit(solution)/shard_map/ppermute | solution.py:467
  123.8 9.4 %collective-permute-done.1.w2.o2 = bf16[448,512]{1,0:T(8,128)(2,1)S(1)} collective-permute-done((bf16[448,512]{1,0:T(8,128)(2,1)S(1)}, bf16[448,512]{1,0:T(8,128)(2,1)S(1)}, u32[]{:S(2)}, u32[]{:S(2)}) %collective-permute-start.1) | collective-permute-done | bytes 458784 | tf_op jit(solution)/shard_map/ppermute | solution.py:467
  135.3 10.5 %shard_map.263 = (bf16[256,128]{1,0:T(8,128)(2,1)S(1)}, f32[2,256]{1,0:T(2,128)}) custom-call(s32[3]{0:T(128)S(1)} %copy-done.9, bf16[2,256,128]{2,1,0:T(8,128)(2,1)S(1)} %shard_map.259.q, bf16[4,16,40,256]{3,2,1,0:T(8,128)(2,1)S(1)} %shard_map.262.own, bf16[4,16,40,256]{3,2,1,0:T(8,128)(2,1)} %collective-permute-done.12.peer, ...), custom_call_target="tpu_custom_call" | custom-call | flops 8589934592 | bytes 4194304 | tf_op jit(solution)/shard_map/pallas_call | solution.py:59
  149.5 2.8 %shard_map.264 = (f32[128,2048]{1,0:T(8,128)S(1)}, bf16[128,2048]{1,0:T(8,128)(2,1)S(1)}) custom-call(s32[3]{0:T(128)S(1)} %copy-done.9, bf16[256,128]{1,0:T(8,128)(2,1)S(1)} %get-tuple-element.36.att, f32[256,128]{1,0:T(8,128)S(1)} %copy-done.25, f32[256,128]{1,0:T(8,128)S(1)} %copy-done.27, f32[256,128]{1,0:T(8,128)S(1)} %copy-done.29, ...), custom_call_target="tpu_custom_call" | custom-call | flops 4294967296 | bytes 4194304 | tf_op jit(solution)/shard_map/pallas_call | solution.py:59
  156.2 12.5 %all_to_all.20 = bf16[4,32,2048]{2,1,0:T(8,128)(2,1)S(1)} all-to-all(bf16[4,32,2048]{2,1,0:T(8,128)(2,1)S(1)} %bitcast.27), channel_id=1, replica_groups={{0,2,4,6},{1,3,5,7},{8,10,12,14},{9,11,13,15},{16,18,20,22},{17,19,21,2..., dimensions={0} | all-to-all | bytes 1048576 | tf_op jit(solution)/shard_map/all_to_all | solution.py:462
  (88 shorter events, 33.8 us)
Async XLA Ops:
  4.6 20.5 %all-to-all-start = ((bf16[8,32,2048]{2,1,0:T(8,128)(2,1)}), bf16[8,32,2048]{2,1,0:T(8,128)(2,1)}, u32[]{:S(2)}, u32[]{:S(2)}) async-start(bf16[8,32,2048]{2,1,0:T(8,128)(2,1)} %get-tuple-element.23), calls=%async_computation | async-start | bytes 2097152 | tf_op jit(solution)/shard_map/all_to_all | solution.py:462
  9.1 11.0 %collective-permute-start.5 = (bf16[64,512]{1,0:T(8,128)(2,1)S(1)}, bf16[64,512]{1,0:T(8,128)(2,1)S(1)}, u32[]{:S(2)}, u32[]{:S(2)}) collective-permute-start(bf16[64,512]{1,0:T(8,128)(2,1)S(1)} %copy-done.30), channel_id=1, source_target_pairs={{0,16},{8,24},{16,0},{24,8},{1,17},{9,25},{17,1},{25,9},{2,18},{10... | collective-permute-start | bytes 196616 | tf_op jit(solution)/shard_map/ppermute | solution.py:467
  14.2 6.2 %collective-permute-start.4 = (bf16[64,512]{1,0:T(8,128)(2,1)S(1)}, bf16[64,512]{1,0:T(8,128)(2,1)S(1)}, u32[]{:S(2)}, u32[]{:S(2)}) collective-permute-start(bf16[64,512]{1,0:T(8,128)(2,1)S(1)} %copy-done.30), channel_id=1, source_target_pairs={{0,24},{8,0},{16,8},{24,16},{1,25},{9,1},{17,9},{25,17},{2,26},{10... | collective-permute-start | bytes 196616 | tf_op jit(solution)/shard_map/ppermute | solution.py:467
  17.2 7.5 %collective-permute-start.3 = (bf16[64,512]{1,0:T(8,128)(2,1)S(1)}, bf16[64,512]{1,0:T(8,128)(2,1)}, u32[]{:S(2)}, u32[]{:S(2)}) collective-permute-start(bf16[64,512]{1,0:T(8,128)(2,1)S(1)} %copy-done.30), channel_id=1, source_target_pairs={{0,8},{8,16},{16,24},{24,0},{1,9},{9,17},{17,25},{25,1},{2,10},{10... | collective-permute-start | bytes 196616 | tf_op jit(solution)/shard_map/ppermute | solution.py:467
  25.1 22.4 %copy-start.9 = (s32[3]{0:T(128)S(1)}, s32[3]{0:T(128)}, u32[]{:S(2)}) copy-start(s32[3]{0:T(128)} %pad_add_fusion.place) | copy-start | bytes 40
  25.1 22.4 %copy-start.10 = (f32[256]{0:T(256)S(1)}, f32[256]{0:T(256)}, u32[]{:S(2)}) copy-start(f32[256]{0:T(256)} %param.31) | copy-start | bytes 3076
  25.1 22.4 %copy-start.11 = (f32[96]{0:T(128)S(1)}, f32[96]{0:T(128)}, u32[]{:S(2)}) copy-start(f32[96]{0:T(128)} %param.35) | copy-start | bytes 1156
  25.1 22.4 %copy-start.12 = (f32[96]{0:T(128)S(1)}, f32[96]{0:T(128)}, u32[]{:S(2)}) copy-start(f32[96]{0:T(128)} %param.34) | copy-start | bytes 1156
  27.7 45.0 %all-to-all-start.1 = ((bf16[16,40,256]{2,1,0:T(8,128)(2,1)}), bf16[16,40,256]{2,1,0:T(8,128)(2,1)S(1)}, u32[]{:S(2)}, u32[]{:S(2)}) async-start(bf16[16,40,256]{2,1,0:T(8,128)(2,1)} %shard_map.260), calls=%async_computation.1 | async-start | bytes 655360 | tf_op jit(solution)/shard_map/all_to_all | solution.py:462
  36.5 17.9 %collective-permute-start.8 = (bf16[512,384]{1,0:T(8,128)(2,1)}, bf16[512,384]{1,0:T(8,128)(2,1)S(1)}, u32[]{:S(2)}, u32[]{:S(2)}) collective-permute-start(bf16[512,384]{1,0:T(8,128)(2,1)} %get-tuple-element.28.w0), channel_id=1, source_target_pairs={{0,16},{8,24},{16,0},{24,8},{1,17},{9,25},{17,1},{25,9},{2,18},{10... | collective-permute-start | bytes 1179656 | tf_op jit(solution)/shard_map/ppermute | solution.py:467
  41.6 17.3 %collective-permute-start.7 = (bf16[512,384]{1,0:T(8,128)(2,1)}, bf16[512,384]{1,0:T(8,128)(2,1)S(1)}, u32[]{:S(2)}, u32[]{:S(2)}) collective-permute-start(bf16[512,384]{1,0:T(8,128)(2,1)} %get-tuple-element.28.w0), channel_id=1, source_target_pairs={{0,24},{8,0},{16,8},{24,16},{1,25},{9,1},{17,9},{25,17},{2,26},{10... | collective-permute-start | bytes 1179656 | tf_op jit(solution)/shard_map/ppermute | solution.py:467
  44.6 14.3 %collective-permute-start.6 = (bf16[512,384]{1,0:T(8,128)(2,1)}, bf16[512,384]{1,0:T(8,128)(2,1)S(1)}, u32[]{:S(2)}, u32[]{:S(2)}) collective-permute-start(bf16[512,384]{1,0:T(8,128)(2,1)} %get-tuple-element.28.w0), channel_id=1, source_target_pairs={{0,8},{8,16},{16,24},{24,0},{1,9},{9,17},{17,25},{25,1},{2,10},{10... | collective-permute-start | bytes 1179656 | tf_op jit(solution)/shard_map/ppermute | solution.py:467
  52.3 6.6 %copy-start.19 = (f32[1,2,256]{2,1,0:T(2,128)S(1)}, f32[1,2,256]{2,1,0:T(2,128)}, u32[]{:S(2)}) copy-start(f32[1,2,256]{2,1,0:T(2,128)} %param.43) | copy-start | bytes 6148
  72.7 34.3 %copy-start.4 = (bf16[448,512]{1,0:T(8,128)(2,1)S(1)}, bf16[448,512]{1,0:T(8,128)(2,1)}, u32[]{:S(2)}) copy-start(bf16[448,512]{1,0:T(8,128)(2,1)} %get-tuple-element.24.w0.o0) | copy-start | bytes 1376260
  72.7 13.9 %collective-permute-start.11 = (bf16[16,40,256]{2,1,0:T(8,128)(2,1)S(1)}, bf16[16,40,256]{2,1,0:T(8,128)(2,1)S(1)}, u32[]{:S(2)}, u32[]{:S(2)}) collective-permute-start(bf16[16,40,256]{2,1,0:T(8,128)(2,1)S(1)} %all-to-all-done.1.own), channel_id=1, source_target_pairs={{0,4},{1,5},{2,6},{3,7},{4,0},{5,1},{6,2},{7,3},{8,12},{9,13},{10,... | collective-permute-start | bytes 983048 | tf_op jit(solution)/shard_map/ppermute | solution.py:566
  76.6 14.4 %collective-permute-start.10 = (bf16[16,40,256]{2,1,0:T(8,128)(2,1)S(1)}, bf16[16,40,256]{2,1,0:T(8,128)(2,1)S(1)}, u32[]{:S(2)}, u32[]{:S(2)}) collective-permute-start(bf16[16,40,256]{2,1,0:T(8,128)(2,1)S(1)} %all-to-all-done.1.own), channel_id=1, source_target_pairs={{0,6},{1,7},{2,0},{3,1},{4,2},{5,3},{6,4},{7,5},{8,14},{9,15},{10,... | collective-permute-start | bytes 983048 | tf_op jit(solution)/shard_map/ppermute | solution.py:566
  80.1 12.3 %collective-permute-start.9 = (bf16[16,40,256]{2,1,0:T(8,128)(2,1)S(1)}, bf16[16,40,256]{2,1,0:T(8,128)(2,1)S(1)}, u32[]{:S(2)}, u32[]{:S(2)}) collective-permute-start(bf16[16,40,256]{2,1,0:T(8,128)(2,1)S(1)} %all-to-all-done.1.own), channel_id=1, source_target_pairs={{0,2},{1,3},{2,4},{3,5},{4,6},{5,7},{6,0},{7,1},{8,10},{9,11},{10,... | collective-permute-start | bytes 983048 | tf_op jit(solution)/shard_map/ppermute | solution.py:566
  93.0 42.2 %collective-permute-start.12 = (bf16[4,16,40,256]{3,2,1,0:T(8,128)(2,1)S(1)}, bf16[4,16,40,256]{3,2,1,0:T(8,128)(2,1)}, u32[]{:S(2)}, u32[]{:S(2)}) collective-permute-start(bf16[4,16,40,256]{3,2,1,0:T(8,128)(2,1)S(1)} %shard_map.262.own), channel_id=1, source_target_pairs={{0,1},{1,0},{2,3},{3,2},{4,5},{5,4},{6,7},{7,6},{8,9},{9,8},{10,11... | collective-permute-start | bytes 3932168 | tf_op jit(solution)/shard_map/ppermute | solution.py:471
  94.9 50.8 %all-to-all-start.2 = ((bf16[16,2,64,128]{3,2,1,0:T(8,128)(2,1)}), bf16[16,2,64,128]{3,2,1,0:T(8,128)(2,1)S(1)}, u32[]{:S(2)}, u32[]{:S(2)}) async-start(bf16[16,2,64,128]{3,2,1,0:T(8,128)(2,1)} %get-tuple-element.40), calls=%async_computation.2 | async-start | bytes 1048576 | tf_op jit(solution)/shard_map/all_to_all | solution.py:462
  107.0 16.8 %collective-permute-start.2 = (bf16[448,512]{1,0:T(8,128)(2,1)S(1)}, bf16[448,512]{1,0:T(8,128)(2,1)S(1)}, u32[]{:S(2)}, u32[]{:S(2)}) collective-permute-start(bf16[448,512]{1,0:T(8,128)(2,1)S(1)} %copy-done.4), channel_id=1, source_target_pairs={{0,16},{8,24},{16,0},{24,8},{1,17},{9,25},{17,1},{25,9},{2,18},{10... | collective-permute-start | bytes 1376264 | tf_op jit(solution)/shard_map/ppermute | solution.py:467
  112.1 21.0 %collective-permute-start.1 = (bf16[448,512]{1,0:T(8,128)(2,1)S(1)}, bf16[448,512]{1,0:T(8,128)(2,1)S(1)}, u32[]{:S(2)}, u32[]{:S(2)}) collective-permute-start(bf16[448,512]{1,0:T(8,128)(2,1)S(1)} %copy-done.4), channel_id=1, source_target_pairs={{0,24},{8,0},{16,8},{24,16},{1,25},{9,1},{17,9},{25,17},{2,26},{10... | collective-permute-start | bytes 1376264 | tf_op jit(solution)/shard_map/ppermute | solution.py:467
  115.3 17.8 %collective-permute-start = (bf16[448,512]{1,0:T(8,128)(2,1)S(1)}, bf16[448,512]{1,0:T(8,128)(2,1)S(1)}, u32[]{:S(2)}, u32[]{:S(2)}) collective-permute-start(bf16[448,512]{1,0:T(8,128)(2,1)S(1)} %copy-done.4), channel_id=1, source_target_pairs={{0,8},{8,16},{16,24},{24,0},{1,9},{9,17},{17,25},{25,1},{2,10},{10... | collective-permute-start | bytes 1376264 | tf_op jit(solution)/shard_map/ppermute | solution.py:467
  135.2 10.5 %copy-start.23 = (f32[128]{0:T(128)S(1)}, f32[128]{0:T(128)}, u32[]{:S(2)}) copy-start(f32[128]{0:T(128)} %param.48) | copy-start | bytes 1540
  152.3 3.8 %collective-permute-start.13 = (bf16[128,2048]{1,0:T(8,128)(2,1)S(1)}, bf16[128,2048]{1,0:T(8,128)(2,1)S(1)}, u32[]{:S(2)}, u32[]{:S(2)}) collective-permute-start(bf16[128,2048]{1,0:T(8,128)(2,1)S(1)} %get-tuple-element.42), channel_id=1, source_target_pairs={{0,1},{1,0},{2,3},{3,2},{4,5},{5,4},{6,7},{7,6},{8,9},{9,8},{10,11... | collective-permute-start | bytes 1572872 | tf_op jit(solution)/shard_map/ppermute | solution.py:471
  (26 other events, 69.4 us)

commit v6 on v5

--- a/solution.py
+++ b/solution.py
@@ -15,7 +15,7 @@
 ROPE = 32
 QK = NOPE + ROPE
 CHUNK = 64
-RECUR_LIMIT = 40
+RECUR_LIMIT = 63.9
 CHUNKS = ROWS // CHUNK
 EPS = 1e-6
 GROUP_EPS = 0.00064
@@ -24,8 +24,6 @@
 TN = (((0,), (0,)), ((), ()))
 
 VMEM = pl.BlockSpec(memory_space=pltpu.VMEM)
-SMEM = pl.BlockSpec(memory_space=pltpu.SMEM)
-ANY = pl.BlockSpec(memory_space=pl.ANY)
 HBM = pl.BlockSpec(memory_space=pltpu.HBM)
 
 
@@ -75,7 +73,7 @@
 
 
 def prepare_body(
-    place, x_in, gain_in, wa_in, wk_in, wv_in, wq_in, wc_in, wr_in, oa_in, or_in,
+    x_in, gain_in, wa_in, wk_in, wv_in, wq_in, wc_in, wr_in, oa_in, or_in,
     xs, small, big, late, x, gain, wa, wk, wv, wq, wc, wr, oa, orr, turned_wc, arrived,
 ):
     pairs = [
@@ -95,7 +93,7 @@
     copies[2].wait()
     copies[3].wait()
     turned_wc[...] = wc[...].astype(F32).T
-    start = pl.multiple_of(place[1] * 32, 32)
+    start = pl.multiple_of(lax.axis_index("tp") * 32, 32)
     small[0:32] = turned_wc[pl.ds(start, 32), :].astype(BF16)
     small[32:64] = wr[...]
     for copy in copies[4:]:
@@ -115,30 +113,30 @@
         jax.ShapeDtypeStruct((512, 384), BF16),
         jax.ShapeDtypeStruct((448, 512), BF16),
     ]
-    scratch = [pltpu.VMEM(a.shape, a.dtype) for a in args[1:]]
+    scratch = [pltpu.VMEM(a.shape, a.dtype) for a in args]
     scratch += [pltpu.VMEM((256, 512), F32), pltpu.SemaphoreType.DMA((10,))]
-    return call(prepare_body, outs, args, 1 << 29, scratch, [SMEM] + [HBM] * 10, 63.9)
-
-
-def collect_body(place, own, left, right, far, out):
-    chip = place[1] // 2
+    return call(prepare_body, outs, args, 1 << 29, scratch, [HBM] * 10, 63.9)
+
+
+def collect_body(own, left, right, far, out):
+    chip = lax.axis_index("tp") // 2
     for by, part in ((0, own), (3, left), (1, right), (2, far)):
         out[lax.rem(chip + by, 4)] = part[...]
 
 
-def collect(place, *parts):
+def collect(*parts):
     outs = jax.ShapeDtypeStruct((4, *parts[0].shape), BF16)
-    return call(collect_body, outs, (place, *parts), 1 << 29, specs=[SMEM] + [VMEM] * 4)
+    return call(collect_body, outs, parts, 1 << 29)
 
 
 def lowrank_body(
-    place, x, fd, fa, table, wk_up, wv_up, compact_gain, kg, qg,
+    x, fd, fa, table, wk_up, wv_up, compact_gain, kg, qg,
     dlow, rlow, turn, up, glat, key_gain, query_gain,
 ):
-    core = lax.rem(place[1], 2)
+    core = lax.rem(lax.axis_index("tp"), 2)
     dlow[...] = jnp.tanh(dot(x[...], fd[...]).astype(BF16).astype(F32)).astype(BF16)
     rlow[...] = dot(x[...], fa[...]).astype(BF16)
-    turn[...] = table[place[0]]
+    turn[...] = table[lax.axis_index("sp")]
 
     def reordered(v):
         v = v.reshape(4, 2, 32, v.shape[-1])
@@ -165,19 +163,19 @@
         column,
         column,
     ]
-    return call(lowrank_body, outs, args, 1 << 29, specs=[SMEM] + [VMEM] * 9)
-
-
-def columns(place, k):
-    shard = lax.rem(place[2] + (0, 3, 1, 2)[k], 4)
+    return call(lowrank_body, outs, args, 1 << 29, specs=[VMEM] * 9, limit=63.9)
+
+
+def columns(k):
+    shard = lax.rem(lax.axis_index("fs") + (0, 3, 1, 2)[k], 4)
     return pl.ds(pl.multiple_of(shard * 512, 512), 512)
 
 
-def latents_body(place, x, w0, w1, w2, w3, pay):
+def latents_body(x, w0, w1, w2, w3, pay):
     t = jnp.zeros((64, ROWS), F32)
     for k, w in enumerate((w0, w1, w2, w3)):
-        t += dot(w[...], x[:, columns(place, k)], NT)
-    tp = place[1]
+        t += dot(w[...], x[:, columns(k)], NT)
+    tp = lax.axis_index("tp")
     group = jnp.zeros((8, ROWS), F32)
     for g in range(4):
         group += jnp.where(tp // 2 == g, t[32 + 8 * g : 40 + 8 * g], 0.0)
@@ -189,13 +187,13 @@
 
 def latents(*args):
     outs = jax.ShapeDtypeStruct((16, 40, ROWS), BF16)
-    return call(latents_body, outs, args, 1 << 29, specs=[SMEM] + [VMEM] * 5, limit=63.9)
-
-
-def queries_body(place, x, w0, w1, w2, w3, turn, gain, q):
+    return call(latents_body, outs, args, 1 << 29, specs=[VMEM] * 5, limit=63.9)
+
+
+def queries_body(x, w0, w1, w2, w3, turn, gain, q):
     t = jnp.zeros((192, ROWS), F32)
     for k, w in enumerate((w0, w1, w2, w3)):
-        t += dot(w[0:192], x[:, columns(place, k)], NT)
+        t += dot(w[0:192], x[:, columns(k)], NT)
     t = t.astype(BF16).astype(F32)
     factor = np.float32(QK**-0.5 * np.log2(np.e))
     for h in range(2):
@@ -208,17 +206,17 @@
 
 def queries(*args):
     outs = jax.ShapeDtypeStruct((2, ROWS, 128), BF16)
-    return call(queries_body, outs, args, 1 << 29, specs=[SMEM] + [VMEM] * 7)
+    return call(queries_body, outs, args, 1 << 29, specs=[VMEM] * 7)
 
 
 def recur_body(
-    place, x, w0, w1, w2, w3, dlow, rlow, wd, bd, wa, ba, mult, extra, present, up, glat, kgain,
-    qgain, free, along, bonus, state,
+    x, w0, w1, w2, w3, dlow, rlow, wd, bd, wa, ba, mult, extra, present,
+    free, along, bonus, state,
 ):
     lane = iota((1, 128), 1)
     y = jnp.zeros((ROWS, 384), F32)
     for k, w in enumerate((w0, w1, w2, w3)):
-        y += dot(x[:, columns(place, k)], w[...])
+        y += dot(x[:, columns(k)], w[...])
     y = y.astype(BF16).astype(F32)
     recept, key, value = (y[:, 128 * i : 128 * (i + 1)] for i in range(3))
     speed = jax.nn.sigmoid(bd[...] + dot(dlow[...], wd[...])) * np.float32(np.exp(-0.5))
@@ -325,12 +323,12 @@
 def recur(*args):
     wide = jax.ShapeDtypeStruct((ROWS, 128), F32)
     outs = [wide, wide, wide, jax.ShapeDtypeStruct((16, 2, 64, 128), BF16)]
-    specs = [SMEM] + [VMEM] * 14 + [ANY] * 4
+    specs = [VMEM] * 14
     return call(recur_body, outs, args, 8 << 30, specs=specs, limit=RECUR_LIMIT)
 
 
-def attend_body(place, q, own, peer, w, glat, gain, table, att, logs, acc, top):
-    sp = place[0]
+def attend_body(q, own, peer, w, glat, gain, table, att, logs, acc, top):
+    sp = lax.axis_index("sp")
     ones = jnp.where(iota((NOPE, ROWS), 0) == 0, 1.0, 0.0).astype(BF16)
 
     def keys(j):
@@ -410,16 +408,16 @@
 def attend(*args):
     outs = [jax.ShapeDtypeStruct((ROWS, 128), BF16), jax.ShapeDtypeStruct((2, ROWS), F32)]
     scratch = [pltpu.VMEM((2, ROWS, 128), F32), pltpu.VMEM((2, ROWS, 128), F32)]
-    return call(attend_body, outs, args, 8 << 30, scratch, [SMEM] + [VMEM] * 7)
-
-
-def merge_body(place, att, free, along, bonus, states, branch, o0, o1, o2, o3, keep, send):
+    return call(attend_body, outs, args, 8 << 30, scratch, [VMEM] * 7)
+
+
+def merge_body(att, free, along, bonus, states, branch, o0, o1, o2, o3, keep, send):
     head = iota((128, 128), 0) // 64 == iota((128, 128), 1) // 64
 
     def spread(v):
         return jnp.where(head, jnp.concatenate([v, v], axis=0), jnp.zeros((), v.dtype))
 
-    sp = place[0]
+    sp = lax.axis_index("sp")
     eye = jnp.where(iota((128, 128), 0) == iota((128, 128), 1), 1.0, 0.0).astype(BF16)
     below = jnp.zeros((128, 128), F32)
     entering = below
@@ -443,19 +441,19 @@
     spread_of = dot_wide(read * read, mean)
     rec = read * lax.rsqrt(spread_of + GROUP_EPS) * branch[...] + bonus[...]
     both = jnp.concatenate([att[...].astype(F32), rec], axis=1).reshape(4, 2, 32, 256)
-    core = lax.rem(place[1], 2)
+    core = lax.rem(lax.axis_index("tp"), 2)
     even, odd = both[:, 0].reshape(128, 256), both[:, 1].reshape(128, 256)
     kept = jnp.where(core == 0, even, odd).astype(BF16)
     sent = jnp.where(core == 0, odd, even).astype(BF16)
     for k, o in enumerate((o0, o1, o2, o3)):
-        send[:, columns(place, k)] = dot(sent, o[192:448]).astype(BF16)
+        send[:, columns(k)] = dot(sent, o[192:448]).astype(BF16)
     for k, o in enumerate((o0, o1, o2, o3)):
-        keep[:, columns(place, k)] = dot(kept, o[192:448])
+        keep[:, columns(k)] = dot(kept, o[192:448])
 
 
 def merge(*args):
     outs = [jax.ShapeDtypeStruct((128, 2048), F32), jax.ShapeDtypeStruct((128, 2048), BF16)]
-    return call(merge_body, outs, args, 4 << 30, specs=[SMEM] + [VMEM] * 10)
+    return call(merge_body, outs, args, 4 << 30, specs=[VMEM] * 10)
 
 
 def exchanged(copies, axis, groups=None):
@@ -506,11 +504,7 @@
     wo_att,
     wo_rec,
 ):
-    tp = lax.axis_index("tp")
-    sp = lax.axis_index("sp")
-    place = jnp.stack([sp, tp, lax.axis_index("fs")]).astype(jnp.int32)
     xs, small, big, late = prepare(
-        place,
         entering[0],
         entering_gain.reshape(1, 2048),
         w_accept,
@@ -528,11 +522,10 @@
     lates = around(late)
 
     table = jnp.asarray(turn_table())
-    pay = latents(place, normed, *smalls)
+    pay = latents(normed, *smalls)
     lat = exchanged(pay, "sp")
 
     dlow, rlow, turn, up, glat, key_gain, query_gain = lowrank(
-        place,
         normed,
         fade1,
         adapt1,
@@ -544,7 +537,6 @@
         q_gain.reshape(1, QK),
     )
     free, along, bonus, state = recur(
-        place,
         normed,
         *bigs,
         dlow,
@@ -556,19 +548,15 @@
         fade_mult[0],
         fade_extra[0],
         present,
-        up,
-        glat,
-        key_gain,
-        query_gain,
     )
     lat, state = lax.optimization_barrier((lat, state))
     states = exchanged(state, "sp")
     others = [lax.ppermute(lat, "tp", [(i, (i + by) % 8) for i in range(8)]) for by in (2, 6, 4)]
-    lat_own = collect(place, lat, *others)
+    lat_own = collect(lat, *others)
     lat_peer = other_core(lat_own)
-    q = queries(place, normed, *lates, turn, query_gain)
-    att, logs = attend(place, q, lat_own, lat_peer, up, glat, key_gain, table)
-    keep, send = merge(place, att, free, along, bonus, states, branch.reshape(1, 128), *lates)
+    q = queries(normed, *lates, turn, query_gain)
+    att, logs = attend(q, lat_own, lat_peer, up, glat, key_gain, table)
+    keep, send = merge(att, free, along, bonus, states, branch.reshape(1, 128), *lates)
     pair = (keep + other_core(send).astype(F32)).astype(BF16)
     same_core = [[0, 2, 4, 6], [1, 3, 5, 7]]
     parts = exchanged(pair.reshape(4, 32, 2048), "tp", same_core)

time: 171 us -> 166 us (0.971)
  local copies, waits for them, and re-layouts: 12.2 us -> 2.94 us
  waiting for transfers between devices: 35.5 us -> 39.6 us
    unnamed x66 -> x32, local copies, waits for them, and re-layouts: 12.2 us -> 2.94 us
    ppermute x9, waiting for transfers between devices: 23.3 us -> 27.2 us  [around(): return [value] + [lax.ppermute(value, 'fs', move) for move in moves]]
  transfers between devices with their start and end apart: 17 -> 17, of which waited for: 10 -> 11; matrix products, arithmetic and copies ran while one was open for 0% -> 0% of each run, Pallas kernels for 15% -> 17%
where the time goes in v6:
time: 166 us; the launch traced here: 165 us
  starting transfers between devices  71.9 us (43%)
  waiting for transfers between devices  39.6 us (24%)
  Pallas kernels  35.8 us (22%)
  blocking collectives  12.5 us (8%)
  local copies, waits for them, and re-layouts  2.94 us (2%)
    pallas_call x8, Pallas kernels, call(): pl.pallas_call(body, out_shape=outs, in_specs=specs or [VMEM] * len(args)...  35.8 us
    ppermute x9, starting transfers between devices, around(): return [value] + [lax.ppermute(value, 'fs', move) for move in moves]  32.9 us
    ppermute x9, waiting for transfers between devices, around(): return [value] + [lax.ppermute(value, 'fs', move) for move in moves]  27.2 us
    all_to_all x3, starting transfers between devices, exchanged(): lax.all_to_all(copies, axis, 0, 0, axis_index_groups=groups, tiled=True)  25.3 us
    all_to_all x1, blocking collectives, exchanged(): lax.all_to_all(copies, axis, 0, 0, axis_index_groups=groups, tiled=True)  12.5 us
    ppermute x3, waiting for transfers between devices, shards(): lax.ppermute(lat, 'tp', [(i, (i + by) % 8) for i in range(8)])  10 us
    ppermute x3, starting transfers between devices, shards(): lax.ppermute(lat, 'tp', [(i, (i + by) % 8) for i in range(8)])  9.8 us
    ppermute x2, starting transfers between devices, other_core(): return lax.ppermute(value, 'tp', [(i, i ^ 1) for i in range(8)])  3.84 us
  transfers between devices with their start and end apart: 17, of which 11 were waited for; matrix products, arithmetic and copies ran while one was open for 0% of the time, Pallas kernels for 17%

profile of v6, /device:TPU:480, one launch (start us, length us, event | category | flops | bytes accessed | tf_op | source)
XLA Modules:
  0.0 164.5 jit_solution(3625429279026947213)
XLA Ops:
  3.3 4.4 %all-to-all-start = ((bf16[8,32,2048]{2,1,0:T(8,128)(2,1)}), bf16[8,32,2048]{2,1,0:T(8,128)(2,1)}, u32[]{:S(2)}, u32[]{:S(2)}) async-start(bf16[8,32,2048]{2,1,0:T(8,128)(2,1)} %get-tuple-element.23), calls=%async_computation | async-start | bytes 2097152 | tf_op jit(solution)/shard_map/all_to_all | solution.py:460
  7.8 5.1 %collective-permute-start.5 = (bf16[64,512]{1,0:T(8,128)(2,1)S(1)}, bf16[64,512]{1,0:T(8,128)(2,1)S(1)}, u32[]{:S(2)}, u32[]{:S(2)}) collective-permute-start(bf16[64,512]{1,0:T(8,128)(2,1)S(1)} %copy-done.13), channel_id=1, source_target_pairs={{0,16},{8,24},{16,0},{24,8},{1,17},{9,25},{17,1},{25,9},{2,18},{10... | collective-permute-start | bytes 196616 | tf_op jit(solution)/shard_map/ppermute | solution.py:465
  12.9 3.0 %collective-permute-start.4 = (bf16[64,512]{1,0:T(8,128)(2,1)S(1)}, bf16[64,512]{1,0:T(8,128)(2,1)S(1)}, u32[]{:S(2)}, u32[]{:S(2)}) collective-permute-start(bf16[64,512]{1,0:T(8,128)(2,1)S(1)} %copy-done.13), channel_id=1, source_target_pairs={{0,24},{8,0},{16,8},{24,16},{1,25},{9,1},{17,9},{25,17},{2,26},{10... | collective-permute-start | bytes 196616 | tf_op jit(solution)/shard_map/ppermute | solution.py:465
  15.9 2.9 %collective-permute-start.3 = (bf16[64,512]{1,0:T(8,128)(2,1)S(1)}, bf16[64,512]{1,0:T(8,128)(2,1)}, u32[]{:S(2)}, u32[]{:S(2)}) collective-permute-start(bf16[64,512]{1,0:T(8,128)(2,1)S(1)} %copy-done.13), channel_id=1, source_target_pairs={{0,8},{8,16},{16,24},{24,0},{1,9},{9,17},{17,25},{25,1},{2,10},{10... | collective-permute-start | bytes 196616 | tf_op jit(solution)/shard_map/ppermute | solution.py:465
  20.0 3.3 %collective-permute-done.3.w1 = bf16[64,512]{1,0:T(8,128)(2,1)} collective-permute-done((bf16[64,512]{1,0:T(8,128)(2,1)S(1)}, bf16[64,512]{1,0:T(8,128)(2,1)}, u32[]{:S(2)}, u32[]{:S(2)}) %collective-permute-start.3) | collective-permute-done | bytes 65568 | tf_op jit(solution)/shard_map/ppermute | solution.py:465
  26.3 8.8 %all-to-all-start.1 = ((bf16[16,40,256]{2,1,0:T(8,128)(2,1)}), bf16[16,40,256]{2,1,0:T(8,128)(2,1)}, u32[]{:S(2)}, u32[]{:S(2)}) async-start(bf16[16,40,256]{2,1,0:T(8,128)(2,1)} %shard_map.260), calls=%async_computation.1 | async-start | bytes 655360 | tf_op jit(solution)/shard_map/all_to_all | solution.py:460
  35.2 5.1 %collective-permute-start.8 = (bf16[512,384]{1,0:T(8,128)(2,1)}, bf16[512,384]{1,0:T(8,128)(2,1)}, u32[]{:S(2)}, u32[]{:S(2)}) collective-permute-start(bf16[512,384]{1,0:T(8,128)(2,1)} %get-tuple-element.28.w0), channel_id=1, source_target_pairs={{0,16},{8,24},{16,0},{24,8},{1,17},{9,25},{17,1},{25,9},{2,18},{10... | collective-permute-start | bytes 1179656 | tf_op jit(solution)/shard_map/ppermute | solution.py:465
  40.3 3.0 %collective-permute-start.7 = (bf16[512,384]{1,0:T(8,128)(2,1)}, bf16[512,384]{1,0:T(8,128)(2,1)}, u32[]{:S(2)}, u32[]{:S(2)}) collective-permute-start(bf16[512,384]{1,0:T(8,128)(2,1)} %get-tuple-element.28.w0), channel_id=1, source_target_pairs={{0,24},{8,0},{16,8},{24,16},{1,25},{9,1},{17,9},{25,17},{2,26},{10... | collective-permute-start | bytes 1179656 | tf_op jit(solution)/shard_map/ppermute | solution.py:465
  43.2 2.9 %collective-permute-start.6 = (bf16[512,384]{1,0:T(8,128)(2,1)}, bf16[512,384]{1,0:T(8,128)(2,1)}, u32[]{:S(2)}, u32[]{:S(2)}) collective-permute-start(bf16[512,384]{1,0:T(8,128)(2,1)} %get-tuple-element.28.w0), channel_id=1, source_target_pairs={{0,8},{8,16},{16,24},{24,0},{1,9},{9,17},{17,25},{25,1},{2,10},{10... | collective-permute-start | bytes 1179656 | tf_op jit(solution)/shard_map/ppermute | solution.py:465
  46.1 3.1 %shard_map.258 = (bf16[256,128]{1,0:T(8,128)(2,1)}, bf16[256,128]{1,0:T(8,128)(2,1)}, f32[32,256]{1,0:T(8,128)}, bf16[256,256]{1,0:T(8,128)(2,1)}, f32[256,128]{...) custom-call(bf16[256,2048]{1,0:T(8,128)(2,1)} %bitcast.4.x, bf16[2048,128]{1,0:T(8,128)(2,1)} %fd.1, ...), custom_call_target="tpu_custom_call" | custom-call | flops 536870912 | bytes 4194304 | tf_op jit(solution)/shard_map/pallas_call | solution.py:57
  50.8 6.8 %collective-permute-done.7.w2 = bf16[512,384]{1,0:T(8,128)(2,1)} collective-permute-done((bf16[512,384]{1,0:T(8,128)(2,1)}, bf16[512,384]{1,0:T(8,128)(2,1)}, u32[]{:S(2)}, u32[]{:S(2)}) %collective-permute-start.7) | collective-permute-done | bytes 393248 | tf_op jit(solution)/shard_map/ppermute | solution.py:465
  57.7 11.7 %shard_map.261 = (f32[256,128]{1,0:T(8,128)}, f32[256,128]{1,0:T(8,128)}, f32[256,128]{1,0:T(8,128)}, bf16[16,2,64,128]{3,2,1,0:T(8,128)(2,1)}) custom-call(bf16[256,2048]{1,0:T(8,128)(2,1)} %bitcast.4.x, bf16[512,384]{1,0:T(8,128)(2,1)} %get-tuple-element.28.w0, bf16[512,384]{1,0:T(8,128)(2,1)} %collective-permute-done.6.w1, ...), custom_call_target="tpu_custom_call" | custom-call | flops 8589934592 | bytes 4194304 | tf_op jit(solution)/shard_map/pallas_call | solution.py:57
  69.4 4.0 %collective-permute-start.11 = (bf16[16,40,256]{2,1,0:T(8,128)(2,1)}, bf16[16,40,256]{2,1,0:T(8,128)(2,1)S(1)}, u32[]{:S(2)}, u32[]{:S(2)}) collective-permute-start(bf16[16,40,256]{2,1,0:T(8,128)(2,1)} %all-to-all-done.1.own), channel_id=1, source_target_pairs={{0,4},{1,5},{2,6},{3,7},{4,0},{5,1},{6,2},{7,3},{8,12},{9,13},{10,... | collective-permute-start | bytes 983048 | tf_op jit(solution)/shard_map/ppermute | solution.py:554
  73.3 3.5 %collective-permute-start.10 = (bf16[16,40,256]{2,1,0:T(8,128)(2,1)}, bf16[16,40,256]{2,1,0:T(8,128)(2,1)S(1)}, u32[]{:S(2)}, u32[]{:S(2)}) collective-permute-start(bf16[16,40,256]{2,1,0:T(8,128)(2,1)} %all-to-all-done.1.own), channel_id=1, source_target_pairs={{0,6},{1,7},{2,0},{3,1},{4,2},{5,3},{6,4},{7,5},{8,14},{9,15},{10,... | collective-permute-start | bytes 983048 | tf_op jit(solution)/shard_map/ppermute | solution.py:554
  79.2 4.2 %collective-permute-done.11.far = bf16[16,40,256]{2,1,0:T(8,128)(2,1)S(1)} collective-permute-done((bf16[16,40,256]{2,1,0:T(8,128)(2,1)}, bf16[16,40,256]{2,1,0:T(8,128)(2,1)S(1)}, u32[]{:S(2)}, u32[]{:S(2)}) %collective-permute-start.11) | collective-permute-done | bytes 327712 | tf_op jit(solution)/shard_map/ppermute | solution.py:554
  83.4 4.5 %collective-permute-done.10.right = bf16[16,40,256]{2,1,0:T(8,128)(2,1)S(1)} collective-permute-done((bf16[16,40,256]{2,1,0:T(8,128)(2,1)}, bf16[16,40,256]{2,1,0:T(8,128)(2,1)S(1)}, u32[]{:S(2)}, u32[]{:S(2)}) %collective-permute-start.10) | collective-permute-done | bytes 327712 | tf_op jit(solution)/shard_map/ppermute | solution.py:554
  92.2 12.0 %all-to-all-start.2 = ((bf16[16,2,64,128]{3,2,1,0:T(8,128)(2,1)}), bf16[16,2,64,128]{3,2,1,0:T(8,128)(2,1)S(1)}, u32[]{:S(2)}, u32[]{:S(2)}) async-start(bf16[16,2,64,128]{3,2,1,0:T(8,128)(2,1)} %get-tuple-element.40), calls=%async_computation.2 | async-start | bytes 1048576 | tf_op jit(solution)/shard_map/all_to_all | solution.py:460
  104.3 5.2 %collective-permute-start.2 = (bf16[448,512]{1,0:T(8,128)(2,1)S(1)}, bf16[448,512]{1,0:T(8,128)(2,1)S(1)}, u32[]{:S(2)}, u32[]{:S(2)}) collective-permute-start(bf16[448,512]{1,0:T(8,128)(2,1)S(1)} %copy-done.1), channel_id=1, source_target_pairs={{0,16},{8,24},{16,0},{24,8},{1,17},{9,25},{17,1},{25,9},{2,18},{10... | collective-permute-start | bytes 1376264 | tf_op jit(solution)/shard_map/ppermute | solution.py:465
  109.5 3.2 %collective-permute-start.1 = (bf16[448,512]{1,0:T(8,128)(2,1)S(1)}, bf16[448,512]{1,0:T(8,128)(2,1)S(1)}, u32[]{:S(2)}, u32[]{:S(2)}) collective-permute-start(bf16[448,512]{1,0:T(8,128)(2,1)S(1)} %copy-done.1), channel_id=1, source_target_pairs={{0,24},{8,0},{16,8},{24,16},{1,25},{9,1},{17,9},{25,17},{2,26},{10... | collective-permute-start | bytes 1376264 | tf_op jit(solution)/shard_map/ppermute | solution.py:465
  112.7 2.7 %collective-permute-start = (bf16[448,512]{1,0:T(8,128)(2,1)S(1)}, bf16[448,512]{1,0:T(8,128)(2,1)S(1)}, u32[]{:S(2)}, u32[]{:S(2)}) collective-permute-start(bf16[448,512]{1,0:T(8,128)(2,1)S(1)} %copy-done.1), channel_id=1, source_target_pairs={{0,8},{8,16},{16,24},{24,0},{1,9},{9,17},{17,25},{25,1},{2,10},{10... | collective-permute-start | bytes 1376264 | tf_op jit(solution)/shard_map/ppermute | solution.py:465
  115.4 5.7 %collective-permute-done.2.w3.o3 = bf16[448,512]{1,0:T(8,128)(2,1)S(1)} collective-permute-done((bf16[448,512]{1,0:T(8,128)(2,1)S(1)}, bf16[448,512]{1,0:T(8,128)(2,1)S(1)}, u32[]{:S(2)}, u32[]{:S(2)}) %collective-permute-start.2) | collective-permute-done | bytes 458784 | tf_op jit(solution)/shard_map/ppermute | solution.py:465
  121.1 9.4 %collective-permute-done.1.w2.o2 = bf16[448,512]{1,0:T(8,128)(2,1)S(1)} collective-permute-done((bf16[448,512]{1,0:T(8,128)(2,1)S(1)}, bf16[448,512]{1,0:T(8,128)(2,1)S(1)}, u32[]{:S(2)}, u32[]{:S(2)}) %collective-permute-start.1) | collective-permute-done | bytes 458784 | tf_op jit(solution)/shard_map/ppermute | solution.py:465
  132.7 10.5 %shard_map.263 = (bf16[256,128]{1,0:T(8,128)(2,1)S(1)}, f32[2,256]{1,0:T(2,128)}) custom-call(bf16[2,256,128]{2,1,0:T(8,128)(2,1)S(1)} %shard_map.259.q, bf16[4,16,40,256]{3,2,1,0:T(8,128)(2,1)S(1)} %shard_map.262.own, bf16[4,16,40,256]{3,2,1,0:T(8,128)(2,1)} %collective-permute-done.12.peer, bf16[256,256]{1,0:T(8,128)(2,1)S(1)} %copy-done.6, ...), custom_call_target="tpu_custom_call" | custom-call | flops 8589934592 | bytes 4194304 | tf_op jit(solution)/shard_map/pallas_call | solution.py:57
  151.3 12.5 %all_to_all.20 = bf16[4,32,2048]{2,1,0:T(8,128)(2,1)S(1)} all-to-all(bf16[4,32,2048]{2,1,0:T(8,128)(2,1)S(1)} %bitcast.17), channel_id=1, replica_groups={{0,2,4,6},{1,3,5,7},{8,10,12,14},{9,11,13,15},{16,18,20,22},{17,19,21,2..., dimensions={0} | all-to-all | bytes 1048576 | tf_op jit(solution)/shard_map/all_to_all | solution.py:460
  (53 shorter events, 26.2 us)
Async XLA Ops:
  3.3 4.5 %copy-start.13 = (bf16[64,512]{1,0:T(8,128)(2,1)S(1)}, bf16[64,512]{1,0:T(8,128)(2,1)}, u32[]{:S(2)}) copy-start(bf16[64,512]{1,0:T(8,128)(2,1)} %get-tuple-element.27.w0) | copy-start | bytes 196612
  3.3 20.5 %all-to-all-start = ((bf16[8,32,2048]{2,1,0:T(8,128)(2,1)}), bf16[8,32,2048]{2,1,0:T(8,128)(2,1)}, u32[]{:S(2)}, u32[]{:S(2)}) async-start(bf16[8,32,2048]{2,1,0:T(8,128)(2,1)} %get-tuple-element.23), calls=%async_computation | async-start | bytes 2097152 | tf_op jit(solution)/shard_map/all_to_all | solution.py:460
  7.8 11.0 %collective-permute-start.5 = (bf16[64,512]{1,0:T(8,128)(2,1)S(1)}, bf16[64,512]{1,0:T(8,128)(2,1)S(1)}, u32[]{:S(2)}, u32[]{:S(2)}) collective-permute-start(bf16[64,512]{1,0:T(8,128)(2,1)S(1)} %copy-done.13), channel_id=1, source_target_pairs={{0,16},{8,24},{16,0},{24,8},{1,17},{9,25},{17,1},{25,9},{2,18},{10... | collective-permute-start | bytes 196616 | tf_op jit(solution)/shard_map/ppermute | solution.py:465
  12.9 6.2 %collective-permute-start.4 = (bf16[64,512]{1,0:T(8,128)(2,1)S(1)}, bf16[64,512]{1,0:T(8,128)(2,1)S(1)}, u32[]{:S(2)}, u32[]{:S(2)}) collective-permute-start(bf16[64,512]{1,0:T(8,128)(2,1)S(1)} %copy-done.13), channel_id=1, source_target_pairs={{0,24},{8,0},{16,8},{24,16},{1,25},{9,1},{17,9},{25,17},{2,26},{10... | collective-permute-start | bytes 196616 | tf_op jit(solution)/shard_map/ppermute | solution.py:465
  15.9 7.5 %collective-permute-start.3 = (bf16[64,512]{1,0:T(8,128)(2,1)S(1)}, bf16[64,512]{1,0:T(8,128)(2,1)}, u32[]{:S(2)}, u32[]{:S(2)}) collective-permute-start(bf16[64,512]{1,0:T(8,128)(2,1)S(1)} %copy-done.13), channel_id=1, source_target_pairs={{0,8},{8,16},{16,24},{24,0},{1,9},{9,17},{17,25},{25,1},{2,10},{10... | collective-permute-start | bytes 196616 | tf_op jit(solution)/shard_map/ppermute | solution.py:465
  26.3 43.0 %all-to-all-start.1 = ((bf16[16,40,256]{2,1,0:T(8,128)(2,1)}), bf16[16,40,256]{2,1,0:T(8,128)(2,1)}, u32[]{:S(2)}, u32[]{:S(2)}) async-start(bf16[16,40,256]{2,1,0:T(8,128)(2,1)} %shard_map.260), calls=%async_computation.1 | async-start | bytes 655360 | tf_op jit(solution)/shard_map/all_to_all | solution.py:460
  35.2 15.7 %collective-permute-start.8 = (bf16[512,384]{1,0:T(8,128)(2,1)}, bf16[512,384]{1,0:T(8,128)(2,1)}, u32[]{:S(2)}, u32[]{:S(2)}) collective-permute-start(bf16[512,384]{1,0:T(8,128)(2,1)} %get-tuple-element.28.w0), channel_id=1, source_target_pairs={{0,16},{8,24},{16,0},{24,8},{1,17},{9,25},{17,1},{25,9},{2,18},{10... | collective-permute-start | bytes 1179656 | tf_op jit(solution)/shard_map/ppermute | solution.py:465
  40.3 17.4 %collective-permute-start.7 = (bf16[512,384]{1,0:T(8,128)(2,1)}, bf16[512,384]{1,0:T(8,128)(2,1)}, u32[]{:S(2)}, u32[]{:S(2)}) collective-permute-start(bf16[512,384]{1,0:T(8,128)(2,1)} %get-tuple-element.28.w0), channel_id=1, source_target_pairs={{0,24},{8,0},{16,8},{24,16},{1,25},{9,1},{17,9},{25,17},{2,26},{10... | collective-permute-start | bytes 1179656 | tf_op jit(solution)/shard_map/ppermute | solution.py:465
  43.2 14.5 %collective-permute-start.6 = (bf16[512,384]{1,0:T(8,128)(2,1)}, bf16[512,384]{1,0:T(8,128)(2,1)}, u32[]{:S(2)}, u32[]{:S(2)}) collective-permute-start(bf16[512,384]{1,0:T(8,128)(2,1)} %get-tuple-element.28.w0), channel_id=1, source_target_pairs={{0,8},{8,16},{16,24},{24,0},{1,9},{9,17},{17,25},{25,1},{2,10},{10... | collective-permute-start | bytes 1179656 | tf_op jit(solution)/shard_map/ppermute | solution.py:465
  69.4 34.9 %copy-start.1 = (bf16[448,512]{1,0:T(8,128)(2,1)S(1)}, bf16[448,512]{1,0:T(8,128)(2,1)}, u32[]{:S(2)}) copy-start(bf16[448,512]{1,0:T(8,128)(2,1)} %get-tuple-element.24.w0.o0) | copy-start | bytes 1376260
  69.4 61.1 %copy-start.4 = (f32[96,128]{1,0:T(8,128)S(1)}, f32[96,128]{1,0:T(8,128)}, u32[]{:S(2)}) copy-start(f32[96,128]{1,0:T(8,128)} %get-tuple-element.26.gain) | copy-start | bytes 147460
  69.4 61.1 %copy-start.5 = (f32[32,256]{1,0:T(8,128)S(1)}, f32[32,256]{1,0:T(8,128)}, u32[]{:S(2)}) copy-start(f32[32,256]{1,0:T(8,128)} %get-tuple-element.25.turn) | copy-start | bytes 98308
  69.4 14.0 %collective-permute-start.11 = (bf16[16,40,256]{2,1,0:T(8,128)(2,1)}, bf16[16,40,256]{2,1,0:T(8,128)(2,1)S(1)}, u32[]{:S(2)}, u32[]{:S(2)}) collective-permute-start(bf16[16,40,256]{2,1,0:T(8,128)(2,1)} %all-to-all-done.1.own), channel_id=1, source_target_pairs={{0,4},{1,5},{2,6},{3,7},{4,0},{5,1},{6,2},{7,3},{8,12},{9,13},{10,... | collective-permute-start | bytes 983048 | tf_op jit(solution)/shard_map/ppermute | solution.py:554
  73.3 14.6 %collective-permute-start.10 = (bf16[16,40,256]{2,1,0:T(8,128)(2,1)}, bf16[16,40,256]{2,1,0:T(8,128)(2,1)S(1)}, u32[]{:S(2)}, u32[]{:S(2)}) collective-permute-start(bf16[16,40,256]{2,1,0:T(8,128)(2,1)} %all-to-all-done.1.own), channel_id=1, source_target_pairs={{0,6},{1,7},{2,0},{3,1},{4,2},{5,3},{6,4},{7,5},{8,14},{9,15},{10,... | collective-permute-start | bytes 983048 | tf_op jit(solution)/shard_map/ppermute | solution.py:554
  76.8 12.4 %collective-permute-start.9 = (bf16[16,40,256]{2,1,0:T(8,128)(2,1)}, bf16[16,40,256]{2,1,0:T(8,128)(2,1)S(1)}, u32[]{:S(2)}, u32[]{:S(2)}) collective-permute-start(bf16[16,40,256]{2,1,0:T(8,128)(2,1)} %all-to-all-done.1.own), channel_id=1, source_target_pairs={{0,2},{1,3},{2,4},{3,5},{4,6},{5,7},{6,0},{7,1},{8,10},{9,11},{10,... | collective-permute-start | bytes 983048 | tf_op jit(solution)/shard_map/ppermute | solution.py:554
  90.3 42.3 %collective-permute-start.12 = (bf16[4,16,40,256]{3,2,1,0:T(8,128)(2,1)S(1)}, bf16[4,16,40,256]{3,2,1,0:T(8,128)(2,1)}, u32[]{:S(2)}, u32[]{:S(2)}) collective-permute-start(bf16[4,16,40,256]{3,2,1,0:T(8,128)(2,1)S(1)} %shard_map.262.own), channel_id=1, source_target_pairs={{0,1},{1,0},{2,3},{3,2},{4,5},{5,4},{6,7},{7,6},{8,9},{9,8},{10,11... | collective-permute-start | bytes 3932168 | tf_op jit(solution)/shard_map/ppermute | solution.py:469
  92.2 50.9 %all-to-all-start.2 = ((bf16[16,2,64,128]{3,2,1,0:T(8,128)(2,1)}), bf16[16,2,64,128]{3,2,1,0:T(8,128)(2,1)S(1)}, u32[]{:S(2)}, u32[]{:S(2)}) async-start(bf16[16,2,64,128]{3,2,1,0:T(8,128)(2,1)} %get-tuple-element.40), calls=%async_computation.2 | async-start | bytes 1048576 | tf_op jit(solution)/shard_map/all_to_all | solution.py:460
  104.3 16.8 %collective-permute-start.2 = (bf16[448,512]{1,0:T(8,128)(2,1)S(1)}, bf16[448,512]{1,0:T(8,128)(2,1)S(1)}, u32[]{:S(2)}, u32[]{:S(2)}) collective-permute-start(bf16[448,512]{1,0:T(8,128)(2,1)S(1)} %copy-done.1), channel_id=1, source_target_pairs={{0,16},{8,24},{16,0},{24,8},{1,17},{9,25},{17,1},{25,9},{2,18},{10... | collective-permute-start | bytes 1376264 | tf_op jit(solution)/shard_map/ppermute | solution.py:465
  109.5 21.0 %collective-permute-start.1 = (bf16[448,512]{1,0:T(8,128)(2,1)S(1)}, bf16[448,512]{1,0:T(8,128)(2,1)S(1)}, u32[]{:S(2)}, u32[]{:S(2)}) collective-permute-start(bf16[448,512]{1,0:T(8,128)(2,1)S(1)} %copy-done.1), channel_id=1, source_target_pairs={{0,24},{8,0},{16,8},{24,16},{1,25},{9,1},{17,9},{25,17},{2,26},{10... | collective-permute-start | bytes 1376264 | tf_op jit(solution)/shard_map/ppermute | solution.py:465
  112.7 17.8 %collective-permute-start = (bf16[448,512]{1,0:T(8,128)(2,1)S(1)}, bf16[448,512]{1,0:T(8,128)(2,1)S(1)}, u32[]{:S(2)}, u32[]{:S(2)}) collective-permute-start(bf16[448,512]{1,0:T(8,128)(2,1)S(1)} %copy-done.1), channel_id=1, source_target_pairs={{0,8},{8,16},{16,24},{24,0},{1,9},{9,17},{17,25},{25,1},{2,10},{10... | collective-permute-start | bytes 1376264 | tf_op jit(solution)/shard_map/ppermute | solution.py:465
  132.7 10.5 %copy-start.9 = (f32[128]{0:T(128)S(1)}, f32[128]{0:T(128)}, u32[]{:S(2)}) copy-start(f32[128]{0:T(128)} %param.48) | copy-start | bytes 1540
  132.7 10.5 %copy-start.10 = (f32[256,128]{1,0:T(8,128)S(1)}, f32[256,128]{1,0:T(8,128)}, u32[]{:S(2)}) copy-start(f32[256,128]{1,0:T(8,128)} %get-tuple-element.37.free) | copy-start | bytes 393220
  132.7 10.5 %copy-start.11 = (f32[256,128]{1,0:T(8,128)S(1)}, f32[256,128]{1,0:T(8,128)}, u32[]{:S(2)}) copy-start(f32[256,128]{1,0:T(8,128)} %get-tuple-element.38.along) | copy-start | bytes 393220
  147.4 3.8 %collective-permute-start.13 = (bf16[128,2048]{1,0:T(8,128)(2,1)S(1)}, bf16[128,2048]{1,0:T(8,128)(2,1)S(1)}, u32[]{:S(2)}, u32[]{:S(2)}) collective-permute-start(bf16[128,2048]{1,0:T(8,128)(2,1)S(1)} %get-tuple-element.42), channel_id=1, source_target_pairs={{0,1},{1,0},{2,3},{3,2},{4,5},{5,4},{6,7},{7,6},{8,9},{9,8},{10,11... | collective-permute-start | bytes 1572872 | tf_op jit(solution)/shard_map/ppermute | solution.py:469
  (9 other events, 13.7 us)

commit v7 on v6

--- a/solution.py
+++ b/solution.py
@@ -263,7 +263,7 @@
     rr, cc = iota((128, 128), 0), iota((128, 128), 1)
     head = rr // 64 == cc // 64
     eye = jnp.where(rr == cc, 1.0, 0.0)
-    in16, in32 = rr // 16 == cc // 16, rr // 32 == cc // 32
+    in8, in16, in32 = (rr // n == cc // n for n in (8, 16, 32))
     strict, upto = head & (rr > cc), head & (rr >= cc)
 
     def square(top, mask):
@@ -284,14 +284,16 @@
     inverse = []
     for k in range(CHUNKS):
         a = stage[k][0]
-        small = jnp.where(in16, a, 0.0)
+        small = jnp.where(in8, a, 0.0)
         power = small
         t = eye + small
-        for _ in range(3):
+        for _ in range(2):
             power = fine(power, power)
             t = t + fine(t, power)
-        t = t + fine(fine(t, jnp.where(in32 & ~in16, a, 0.0)), t)
-        t = t + fine(fine(t, jnp.where(in32, 0.0, a)), t)
+        for wider, narrower in ((in16, in8), (in32, in16), (None, in32)):
+            rest = jnp.where(narrower, 0.0, a)
+            rest = rest if wider is None else jnp.where(wider, rest, 0.0)
+            t = t + fine(fine(t, rest), t)
         inverse.append(t)
     pair = jnp.concatenate([jnp.zeros((128, 128), F32), eye], axis=0)
     for k in range(CHUNKS):

time: 166 us -> 166 us (level)
  no operation moved by 1% of the time
where the time goes in v7:
time: 166 us; the launch traced here: 165 us
  starting transfers between devices  71.9 us (43%)
  waiting for transfers between devices  39.6 us (24%)
  Pallas kernels  36.2 us (22%)
  blocking collectives  12.5 us (8%)
  local copies, waits for them, and re-layouts  2.94 us (2%)
    pallas_call x8, Pallas kernels, call(): pl.pallas_call(body, out_shape=outs, in_specs=specs or [VMEM] * len(args)...  36.2 us
    ppermute x9, starting transfers between devices, around(): return [value] + [lax.ppermute(value, 'fs', move) for move in moves]  32.9 us
    ppermute x9, waiting for transfers between devices, around(): return [value] + [lax.ppermute(value, 'fs', move) for move in moves]  27.2 us
    all_to_all x3, starting transfers between devices, exchanged(): lax.all_to_all(copies, axis, 0, 0, axis_index_groups=groups, tiled=True)  25.3 us
    all_to_all x1, blocking collectives, exchanged(): lax.all_to_all(copies, axis, 0, 0, axis_index_groups=groups, tiled=True)  12.5 us
    ppermute x3, waiting for transfers between devices, shards(): lax.ppermute(lat, 'tp', [(i, (i + by) % 8) for i in range(8)])  10 us
    ppermute x3, starting transfers between devices, shards(): lax.ppermute(lat, 'tp', [(i, (i + by) % 8) for i in range(8)])  9.79 us
    ppermute x2, starting transfers between devices, other_core(): return lax.ppermute(value, 'tp', [(i, i ^ 1) for i in range(8)])  3.84 us
  transfers between devices with their start and end apart: 17, of which 11 were waited for; matrix products, arithmetic and copies ran while one was open for 0% of the time, Pallas kernels for 17%

profile of v7, /device:TPU:480, one launch (start us, length us, event | category | flops | bytes accessed | tf_op | source)
XLA Modules:
  0.0 165.0 jit_solution(1478475518405883065)
XLA Ops:
  0.6 2.7 %shard_map.257 = (bf16[8,32,2048]{2,1,0:T(8,128)(2,1)}, bf16[64,512]{1,0:T(8,128)(2,1)}, bf16[512,384]{1,0:T(8,128)(2,1)}, bf16[448,512]{1,0:T(8,128)(2,1)}) custom-call(bf16[32,2048]{1,0:T(8,128)(2,1)} %bitcast.23, f32[1,2048]{1,0:T(1,128)} %bitcast.25, bf16[512,128]{1,0:T(8,128)(2,1)} %wa_in.1, bf16[512,128]{1,0:T(8,128)(2,1)} %wk_in.1, ...), custom_call_target="tpu_custom_call" | custom-call | flops 536870912 | bytes 4194304 | tf_op jit(solution)/shard_map/pallas_call | solution.py:57
  3.3 4.4 %all-to-all-start = ((bf16[8,32,2048]{2,1,0:T(8,128)(2,1)}), bf16[8,32,2048]{2,1,0:T(8,128)(2,1)}, u32[]{:S(2)}, u32[]{:S(2)}) async-start(bf16[8,32,2048]{2,1,0:T(8,128)(2,1)} %get-tuple-element.23), calls=%async_computation | async-start | bytes 2097152 | tf_op jit(solution)/shard_map/all_to_all | solution.py:462
  7.8 5.1 %collective-permute-start.5 = (bf16[64,512]{1,0:T(8,128)(2,1)S(1)}, bf16[64,512]{1,0:T(8,128)(2,1)S(1)}, u32[]{:S(2)}, u32[]{:S(2)}) collective-permute-start(bf16[64,512]{1,0:T(8,128)(2,1)S(1)} %copy-done.13), channel_id=1, source_target_pairs={{0,16},{8,24},{16,0},{24,8},{1,17},{9,25},{17,1},{25,9},{2,18},{10... | collective-permute-start | bytes 196616 | tf_op jit(solution)/shard_map/ppermute | solution.py:467
  12.9 3.0 %collective-permute-start.4 = (bf16[64,512]{1,0:T(8,128)(2,1)S(1)}, bf16[64,512]{1,0:T(8,128)(2,1)S(1)}, u32[]{:S(2)}, u32[]{:S(2)}) collective-permute-start(bf16[64,512]{1,0:T(8,128)(2,1)S(1)} %copy-done.13), channel_id=1, source_target_pairs={{0,24},{8,0},{16,8},{24,16},{1,25},{9,1},{17,9},{25,17},{2,26},{10... | collective-permute-start | bytes 196616 | tf_op jit(solution)/shard_map/ppermute | solution.py:467
  15.9 2.9 %collective-permute-start.3 = (bf16[64,512]{1,0:T(8,128)(2,1)S(1)}, bf16[64,512]{1,0:T(8,128)(2,1)}, u32[]{:S(2)}, u32[]{:S(2)}) collective-permute-start(bf16[64,512]{1,0:T(8,128)(2,1)S(1)} %copy-done.13), channel_id=1, source_target_pairs={{0,8},{8,16},{16,24},{24,0},{1,9},{9,17},{17,25},{25,1},{2,10},{10... | collective-permute-start | bytes 196616 | tf_op jit(solution)/shard_map/ppermute | solution.py:467
  20.0 3.3 %collective-permute-done.3.w1 = bf16[64,512]{1,0:T(8,128)(2,1)} collective-permute-done((bf16[64,512]{1,0:T(8,128)(2,1)S(1)}, bf16[64,512]{1,0:T(8,128)(2,1)}, u32[]{:S(2)}, u32[]{:S(2)}) %collective-permute-start.3) | collective-permute-done | bytes 65568 | tf_op jit(solution)/shard_map/ppermute | solution.py:467
  26.3 8.8 %all-to-all-start.1 = ((bf16[16,40,256]{2,1,0:T(8,128)(2,1)}), bf16[16,40,256]{2,1,0:T(8,128)(2,1)}, u32[]{:S(2)}, u32[]{:S(2)}) async-start(bf16[16,40,256]{2,1,0:T(8,128)(2,1)} %shard_map.260), calls=%async_computation.1 | async-start | bytes 655360 | tf_op jit(solution)/shard_map/all_to_all | solution.py:462
  35.2 5.1 %collective-permute-start.8 = (bf16[512,384]{1,0:T(8,128)(2,1)}, bf16[512,384]{1,0:T(8,128)(2,1)}, u32[]{:S(2)}, u32[]{:S(2)}) collective-permute-start(bf16[512,384]{1,0:T(8,128)(2,1)} %get-tuple-element.28.w0), channel_id=1, source_target_pairs={{0,16},{8,24},{16,0},{24,8},{1,17},{9,25},{17,1},{25,9},{2,18},{10... | collective-permute-start | bytes 1179656 | tf_op jit(solution)/shard_map/ppermute | solution.py:467
  40.3 3.0 %collective-permute-start.7 = (bf16[512,384]{1,0:T(8,128)(2,1)}, bf16[512,384]{1,0:T(8,128)(2,1)}, u32[]{:S(2)}, u32[]{:S(2)}) collective-permute-start(bf16[512,384]{1,0:T(8,128)(2,1)} %get-tuple-element.28.w0), channel_id=1, source_target_pairs={{0,24},{8,0},{16,8},{24,16},{1,25},{9,1},{17,9},{25,17},{2,26},{10... | collective-permute-start | bytes 1179656 | tf_op jit(solution)/shard_map/ppermute | solution.py:467
  43.2 2.9 %collective-permute-start.6 = (bf16[512,384]{1,0:T(8,128)(2,1)}, bf16[512,384]{1,0:T(8,128)(2,1)}, u32[]{:S(2)}, u32[]{:S(2)}) collective-permute-start(bf16[512,384]{1,0:T(8,128)(2,1)} %get-tuple-element.28.w0), channel_id=1, source_target_pairs={{0,8},{8,16},{16,24},{24,0},{1,9},{9,17},{17,25},{25,1},{2,10},{10... | collective-permute-start | bytes 1179656 | tf_op jit(solution)/shard_map/ppermute | solution.py:467
  46.1 3.1 %shard_map.258 = (bf16[256,128]{1,0:T(8,128)(2,1)}, bf16[256,128]{1,0:T(8,128)(2,1)}, f32[32,256]{1,0:T(8,128)}, bf16[256,256]{1,0:T(8,128)(2,1)}, f32[256,128]{...) custom-call(bf16[256,2048]{1,0:T(8,128)(2,1)} %bitcast.4.x, bf16[2048,128]{1,0:T(8,128)(2,1)} %fd.1, ...), custom_call_target="tpu_custom_call" | custom-call | flops 536870912 | bytes 4194304 | tf_op jit(solution)/shard_map/pallas_call | solution.py:57
  50.8 6.8 %collective-permute-done.7.w2 = bf16[512,384]{1,0:T(8,128)(2,1)} collective-permute-done((bf16[512,384]{1,0:T(8,128)(2,1)}, bf16[512,384]{1,0:T(8,128)(2,1)}, u32[]{:S(2)}, u32[]{:S(2)}) %collective-permute-start.7) | collective-permute-done | bytes 393248 | tf_op jit(solution)/shard_map/ppermute | solution.py:467
  57.7 12.1 %shard_map.261 = (f32[256,128]{1,0:T(8,128)}, f32[256,128]{1,0:T(8,128)}, f32[256,128]{1,0:T(8,128)}, bf16[16,2,64,128]{3,2,1,0:T(8,128)(2,1)}) custom-call(bf16[256,2048]{1,0:T(8,128)(2,1)} %bitcast.4.x, bf16[512,384]{1,0:T(8,128)(2,1)} %get-tuple-element.28.w0, bf16[512,384]{1,0:T(8,128)(2,1)} %collective-permute-done.6.w1, ...), custom_call_target="tpu_custom_call" | custom-call | flops 8589934592 | bytes 4194304 | tf_op jit(solution)/shard_map/pallas_call | solution.py:57
  69.8 4.0 %collective-permute-start.11 = (bf16[16,40,256]{2,1,0:T(8,128)(2,1)}, bf16[16,40,256]{2,1,0:T(8,128)(2,1)S(1)}, u32[]{:S(2)}, u32[]{:S(2)}) collective-permute-start(bf16[16,40,256]{2,1,0:T(8,128)(2,1)} %all-to-all-done.1.own), channel_id=1, source_target_pairs={{0,4},{1,5},{2,6},{3,7},{4,0},{5,1},{6,2},{7,3},{8,12},{9,13},{10,... | collective-permute-start | bytes 983048 | tf_op jit(solution)/shard_map/ppermute | solution.py:556
  73.8 3.5 %collective-permute-start.10 = (bf16[16,40,256]{2,1,0:T(8,128)(2,1)}, bf16[16,40,256]{2,1,0:T(8,128)(2,1)S(1)}, u32[]{:S(2)}, u32[]{:S(2)}) collective-permute-start(bf16[16,40,256]{2,1,0:T(8,128)(2,1)} %all-to-all-done.1.own), channel_id=1, source_target_pairs={{0,6},{1,7},{2,0},{3,1},{4,2},{5,3},{6,4},{7,5},{8,14},{9,15},{10,... | collective-permute-start | bytes 983048 | tf_op jit(solution)/shard_map/ppermute | solution.py:556
  79.6 4.2 %collective-permute-done.11.far = bf16[16,40,256]{2,1,0:T(8,128)(2,1)S(1)} collective-permute-done((bf16[16,40,256]{2,1,0:T(8,128)(2,1)}, bf16[16,40,256]{2,1,0:T(8,128)(2,1)S(1)}, u32[]{:S(2)}, u32[]{:S(2)}) %collective-permute-start.11) | collective-permute-done | bytes 327712 | tf_op jit(solution)/shard_map/ppermute | solution.py:556
  83.8 4.5 %collective-permute-done.10.right = bf16[16,40,256]{2,1,0:T(8,128)(2,1)S(1)} collective-permute-done((bf16[16,40,256]{2,1,0:T(8,128)(2,1)}, bf16[16,40,256]{2,1,0:T(8,128)(2,1)S(1)}, u32[]{:S(2)}, u32[]{:S(2)}) %collective-permute-start.10) | collective-permute-done | bytes 327712 | tf_op jit(solution)/shard_map/ppermute | solution.py:556
  92.7 12.0 %all-to-all-start.2 = ((bf16[16,2,64,128]{3,2,1,0:T(8,128)(2,1)}), bf16[16,2,64,128]{3,2,1,0:T(8,128)(2,1)S(1)}, u32[]{:S(2)}, u32[]{:S(2)}) async-start(bf16[16,2,64,128]{3,2,1,0:T(8,128)(2,1)} %get-tuple-element.40), calls=%async_computation.2 | async-start | bytes 1048576 | tf_op jit(solution)/shard_map/all_to_all | solution.py:462
  104.7 5.2 %collective-permute-start.2 = (bf16[448,512]{1,0:T(8,128)(2,1)S(1)}, bf16[448,512]{1,0:T(8,128)(2,1)S(1)}, u32[]{:S(2)}, u32[]{:S(2)}) collective-permute-start(bf16[448,512]{1,0:T(8,128)(2,1)S(1)} %copy-done.1), channel_id=1, source_target_pairs={{0,16},{8,24},{16,0},{24,8},{1,17},{9,25},{17,1},{25,9},{2,18},{10... | collective-permute-start | bytes 1376264 | tf_op jit(solution)/shard_map/ppermute | solution.py:467
  109.9 3.2 %collective-permute-start.1 = (bf16[448,512]{1,0:T(8,128)(2,1)S(1)}, bf16[448,512]{1,0:T(8,128)(2,1)S(1)}, u32[]{:S(2)}, u32[]{:S(2)}) collective-permute-start(bf16[448,512]{1,0:T(8,128)(2,1)S(1)} %copy-done.1), channel_id=1, source_target_pairs={{0,24},{8,0},{16,8},{24,16},{1,25},{9,1},{17,9},{25,17},{2,26},{10... | collective-permute-start | bytes 1376264 | tf_op jit(solution)/shard_map/ppermute | solution.py:467
  115.8 5.7 %collective-permute-done.2.w3.o3 = bf16[448,512]{1,0:T(8,128)(2,1)S(1)} collective-permute-done((bf16[448,512]{1,0:T(8,128)(2,1)S(1)}, bf16[448,512]{1,0:T(8,128)(2,1)S(1)}, u32[]{:S(2)}, u32[]{:S(2)}) %collective-permute-start.2) | collective-permute-done | bytes 458784 | tf_op jit(solution)/shard_map/ppermute | solution.py:467
  121.5 9.4 %collective-permute-done.1.w2.o2 = bf16[448,512]{1,0:T(8,128)(2,1)S(1)} collective-permute-done((bf16[448,512]{1,0:T(8,128)(2,1)S(1)}, bf16[448,512]{1,0:T(8,128)(2,1)S(1)}, u32[]{:S(2)}, u32[]{:S(2)}) %collective-permute-start.1) | collective-permute-done | bytes 458784 | tf_op jit(solution)/shard_map/ppermute | solution.py:467
  133.1 10.5 %shard_map.263 = (bf16[256,128]{1,0:T(8,128)(2,1)S(1)}, f32[2,256]{1,0:T(2,128)}) custom-call(bf16[2,256,128]{2,1,0:T(8,128)(2,1)S(1)} %shard_map.259.q, bf16[4,16,40,256]{3,2,1,0:T(8,128)(2,1)S(1)} %shard_map.262.own, bf16[4,16,40,256]{3,2,1,0:T(8,128)(2,1)} %collective-permute-done.12.peer, bf16[256,256]{1,0:T(8,128)(2,1)S(1)} %copy-done.6, ...), custom_call_target="tpu_custom_call" | custom-call | flops 8589934592 | bytes 4194304 | tf_op jit(solution)/shard_map/pallas_call | solution.py:57
  151.8 12.5 %all_to_all.20 = bf16[4,32,2048]{2,1,0:T(8,128)(2,1)S(1)} all-to-all(bf16[4,32,2048]{2,1,0:T(8,128)(2,1)S(1)} %bitcast.17), channel_id=1, replica_groups={{0,2,4,6},{1,3,5,7},{8,10,12,14},{9,11,13,15},{16,18,20,22},{17,19,21,2..., dimensions={0} | all-to-all | bytes 1048576 | tf_op jit(solution)/shard_map/all_to_all | solution.py:462
  (53 shorter events, 26.2 us)
Async XLA Ops:
  3.3 4.5 %copy-start.13 = (bf16[64,512]{1,0:T(8,128)(2,1)S(1)}, bf16[64,512]{1,0:T(8,128)(2,1)}, u32[]{:S(2)}) copy-start(bf16[64,512]{1,0:T(8,128)(2,1)} %get-tuple-element.27.w0) | copy-start | bytes 196612
  3.3 20.5 %all-to-all-start = ((bf16[8,32,2048]{2,1,0:T(8,128)(2,1)}), bf16[8,32,2048]{2,1,0:T(8,128)(2,1)}, u32[]{:S(2)}, u32[]{:S(2)}) async-start(bf16[8,32,2048]{2,1,0:T(8,128)(2,1)} %get-tuple-element.23), calls=%async_computation | async-start | bytes 2097152 | tf_op jit(solution)/shard_map/all_to_all | solution.py:462
  7.8 11.0 %collective-permute-start.5 = (bf16[64,512]{1,0:T(8,128)(2,1)S(1)}, bf16[64,512]{1,0:T(8,128)(2,1)S(1)}, u32[]{:S(2)}, u32[]{:S(2)}) collective-permute-start(bf16[64,512]{1,0:T(8,128)(2,1)S(1)} %copy-done.13), channel_id=1, source_target_pairs={{0,16},{8,24},{16,0},{24,8},{1,17},{9,25},{17,1},{25,9},{2,18},{10... | collective-permute-start | bytes 196616 | tf_op jit(solution)/shard_map/ppermute | solution.py:467
  12.9 6.2 %collective-permute-start.4 = (bf16[64,512]{1,0:T(8,128)(2,1)S(1)}, bf16[64,512]{1,0:T(8,128)(2,1)S(1)}, u32[]{:S(2)}, u32[]{:S(2)}) collective-permute-start(bf16[64,512]{1,0:T(8,128)(2,1)S(1)} %copy-done.13), channel_id=1, source_target_pairs={{0,24},{8,0},{16,8},{24,16},{1,25},{9,1},{17,9},{25,17},{2,26},{10... | collective-permute-start | bytes 196616 | tf_op jit(solution)/shard_map/ppermute | solution.py:467
  15.9 7.5 %collective-permute-start.3 = (bf16[64,512]{1,0:T(8,128)(2,1)S(1)}, bf16[64,512]{1,0:T(8,128)(2,1)}, u32[]{:S(2)}, u32[]{:S(2)}) collective-permute-start(bf16[64,512]{1,0:T(8,128)(2,1)S(1)} %copy-done.13), channel_id=1, source_target_pairs={{0,8},{8,16},{16,24},{24,0},{1,9},{9,17},{17,25},{25,1},{2,10},{10... | collective-permute-start | bytes 196616 | tf_op jit(solution)/shard_map/ppermute | solution.py:467
  26.3 43.5 %all-to-all-start.1 = ((bf16[16,40,256]{2,1,0:T(8,128)(2,1)}), bf16[16,40,256]{2,1,0:T(8,128)(2,1)}, u32[]{:S(2)}, u32[]{:S(2)}) async-start(bf16[16,40,256]{2,1,0:T(8,128)(2,1)} %shard_map.260), calls=%async_computation.1 | async-start | bytes 655360 | tf_op jit(solution)/shard_map/all_to_all | solution.py:462
  35.2 15.7 %collective-permute-start.8 = (bf16[512,384]{1,0:T(8,128)(2,1)}, bf16[512,384]{1,0:T(8,128)(2,1)}, u32[]{:S(2)}, u32[]{:S(2)}) collective-permute-start(bf16[512,384]{1,0:T(8,128)(2,1)} %get-tuple-element.28.w0), channel_id=1, source_target_pairs={{0,16},{8,24},{16,0},{24,8},{1,17},{9,25},{17,1},{25,9},{2,18},{10... | collective-permute-start | bytes 1179656 | tf_op jit(solution)/shard_map/ppermute | solution.py:467
  40.3 17.4 %collective-permute-start.7 = (bf16[512,384]{1,0:T(8,128)(2,1)}, bf16[512,384]{1,0:T(8,128)(2,1)}, u32[]{:S(2)}, u32[]{:S(2)}) collective-permute-start(bf16[512,384]{1,0:T(8,128)(2,1)} %get-tuple-element.28.w0), channel_id=1, source_target_pairs={{0,24},{8,0},{16,8},{24,16},{1,25},{9,1},{17,9},{25,17},{2,26},{10... | collective-permute-start | bytes 1179656 | tf_op jit(solution)/shard_map/ppermute | solution.py:467
  43.2 14.5 %collective-permute-start.6 = (bf16[512,384]{1,0:T(8,128)(2,1)}, bf16[512,384]{1,0:T(8,128)(2,1)}, u32[]{:S(2)}, u32[]{:S(2)}) collective-permute-start(bf16[512,384]{1,0:T(8,128)(2,1)} %get-tuple-element.28.w0), channel_id=1, source_target_pairs={{0,8},{8,16},{16,24},{24,0},{1,9},{9,17},{17,25},{25,1},{2,10},{10... | collective-permute-start | bytes 1179656 | tf_op jit(solution)/shard_map/ppermute | solution.py:467
  69.8 34.9 %copy-start.1 = (bf16[448,512]{1,0:T(8,128)(2,1)S(1)}, bf16[448,512]{1,0:T(8,128)(2,1)}, u32[]{:S(2)}) copy-start(bf16[448,512]{1,0:T(8,128)(2,1)} %get-tuple-element.24.w0.o0) | copy-start | bytes 1376260
  69.8 61.1 %copy-start.4 = (f32[96,128]{1,0:T(8,128)S(1)}, f32[96,128]{1,0:T(8,128)}, u32[]{:S(2)}) copy-start(f32[96,128]{1,0:T(8,128)} %get-tuple-element.26.gain) | copy-start | bytes 147460
  69.8 61.1 %copy-start.5 = (f32[32,256]{1,0:T(8,128)S(1)}, f32[32,256]{1,0:T(8,128)}, u32[]{:S(2)}) copy-start(f32[32,256]{1,0:T(8,128)} %get-tuple-element.25.turn) | copy-start | bytes 98308
  69.8 14.0 %collective-permute-start.11 = (bf16[16,40,256]{2,1,0:T(8,128)(2,1)}, bf16[16,40,256]{2,1,0:T(8,128)(2,1)S(1)}, u32[]{:S(2)}, u32[]{:S(2)}) collective-permute-start(bf16[16,40,256]{2,1,0:T(8,128)(2,1)} %all-to-all-done.1.own), channel_id=1, source_target_pairs={{0,4},{1,5},{2,6},{3,7},{4,0},{5,1},{6,2},{7,3},{8,12},{9,13},{10,... | collective-permute-start | bytes 983048 | tf_op jit(solution)/shard_map/ppermute | solution.py:556
  73.8 14.6 %collective-permute-start.10 = (bf16[16,40,256]{2,1,0:T(8,128)(2,1)}, bf16[16,40,256]{2,1,0:T(8,128)(2,1)S(1)}, u32[]{:S(2)}, u32[]{:S(2)}) collective-permute-start(bf16[16,40,256]{2,1,0:T(8,128)(2,1)} %all-to-all-done.1.own), channel_id=1, source_target_pairs={{0,6},{1,7},{2,0},{3,1},{4,2},{5,3},{6,4},{7,5},{8,14},{9,15},{10,... | collective-permute-start | bytes 983048 | tf_op jit(solution)/shard_map/ppermute | solution.py:556
  77.2 12.4 %collective-permute-start.9 = (bf16[16,40,256]{2,1,0:T(8,128)(2,1)}, bf16[16,40,256]{2,1,0:T(8,128)(2,1)S(1)}, u32[]{:S(2)}, u32[]{:S(2)}) collective-permute-start(bf16[16,40,256]{2,1,0:T(8,128)(2,1)} %all-to-all-done.1.own), channel_id=1, source_target_pairs={{0,2},{1,3},{2,4},{3,5},{4,6},{5,7},{6,0},{7,1},{8,10},{9,11},{10,... | collective-permute-start | bytes 983048 | tf_op jit(solution)/shard_map/ppermute | solution.py:556
  90.7 42.3 %collective-permute-start.12 = (bf16[4,16,40,256]{3,2,1,0:T(8,128)(2,1)S(1)}, bf16[4,16,40,256]{3,2,1,0:T(8,128)(2,1)}, u32[]{:S(2)}, u32[]{:S(2)}) collective-permute-start(bf16[4,16,40,256]{3,2,1,0:T(8,128)(2,1)S(1)} %shard_map.262.own), channel_id=1, source_target_pairs={{0,1},{1,0},{2,3},{3,2},{4,5},{5,4},{6,7},{7,6},{8,9},{9,8},{10,11... | collective-permute-start | bytes 3932168 | tf_op jit(solution)/shard_map/ppermute | solution.py:471
  92.7 51.0 %all-to-all-start.2 = ((bf16[16,2,64,128]{3,2,1,0:T(8,128)(2,1)}), bf16[16,2,64,128]{3,2,1,0:T(8,128)(2,1)S(1)}, u32[]{:S(2)}, u32[]{:S(2)}) async-start(bf16[16,2,64,128]{3,2,1,0:T(8,128)(2,1)} %get-tuple-element.40), calls=%async_computation.2 | async-start | bytes 1048576 | tf_op jit(solution)/shard_map/all_to_all | solution.py:462
  104.7 16.8 %collective-permute-start.2 = (bf16[448,512]{1,0:T(8,128)(2,1)S(1)}, bf16[448,512]{1,0:T(8,128)(2,1)S(1)}, u32[]{:S(2)}, u32[]{:S(2)}) collective-permute-start(bf16[448,512]{1,0:T(8,128)(2,1)S(1)} %copy-done.1), channel_id=1, source_target_pairs={{0,16},{8,24},{16,0},{24,8},{1,17},{9,25},{17,1},{25,9},{2,18},{10... | collective-permute-start | bytes 1376264 | tf_op jit(solution)/shard_map/ppermute | solution.py:467
  109.9 21.0 %collective-permute-start.1 = (bf16[448,512]{1,0:T(8,128)(2,1)S(1)}, bf16[448,512]{1,0:T(8,128)(2,1)S(1)}, u32[]{:S(2)}, u32[]{:S(2)}) collective-permute-start(bf16[448,512]{1,0:T(8,128)(2,1)S(1)} %copy-done.1), channel_id=1, source_target_pairs={{0,24},{8,0},{16,8},{24,16},{1,25},{9,1},{17,9},{25,17},{2,26},{10... | collective-permute-start | bytes 1376264 | tf_op jit(solution)/shard_map/ppermute | solution.py:467
  113.1 17.8 %collective-permute-start = (bf16[448,512]{1,0:T(8,128)(2,1)S(1)}, bf16[448,512]{1,0:T(8,128)(2,1)S(1)}, u32[]{:S(2)}, u32[]{:S(2)}) collective-permute-start(bf16[448,512]{1,0:T(8,128)(2,1)S(1)} %copy-done.1), channel_id=1, source_target_pairs={{0,8},{8,16},{16,24},{24,0},{1,9},{9,17},{17,25},{25,1},{2,10},{10... | collective-permute-start | bytes 1376264 | tf_op jit(solution)/shard_map/ppermute | solution.py:467
  133.1 10.5 %copy-start.9 = (f32[128]{0:T(128)S(1)}, f32[128]{0:T(128)}, u32[]{:S(2)}) copy-start(f32[128]{0:T(128)} %param.48) | copy-start | bytes 1540
  133.1 10.5 %copy-start.10 = (f32[256,128]{1,0:T(8,128)S(1)}, f32[256,128]{1,0:T(8,128)}, u32[]{:S(2)}) copy-start(f32[256,128]{1,0:T(8,128)} %get-tuple-element.37.free) | copy-start | bytes 393220
  133.1 10.5 %copy-start.11 = (f32[256,128]{1,0:T(8,128)S(1)}, f32[256,128]{1,0:T(8,128)}, u32[]{:S(2)}) copy-start(f32[256,128]{1,0:T(8,128)} %get-tuple-element.38.along) | copy-start | bytes 393220
  147.8 3.8 %collective-permute-start.13 = (bf16[128,2048]{1,0:T(8,128)(2,1)S(1)}, bf16[128,2048]{1,0:T(8,128)(2,1)S(1)}, u32[]{:S(2)}, u32[]{:S(2)}) collective-permute-start(bf16[128,2048]{1,0:T(8,128)(2,1)S(1)} %get-tuple-element.42), channel_id=1, source_target_pairs={{0,1},{1,0},{2,3},{3,2},{4,5},{5,4},{6,7},{7,6},{8,9},{9,8},{10,11... | collective-permute-start | bytes 1572872 | tf_op jit(solution)/shard_map/ppermute | solution.py:471
  (9 other events, 13.7 us)

commit v8 on v7

--- a/solution.py
+++ b/solution.py
@@ -129,43 +129,6 @@
     return call(collect_body, outs, parts, 1 << 29)
 
 
-def lowrank_body(
-    x, fd, fa, table, wk_up, wv_up, compact_gain, kg, qg,
-    dlow, rlow, turn, up, glat, key_gain, query_gain,
-):
-    core = lax.rem(lax.axis_index("tp"), 2)
-    dlow[...] = jnp.tanh(dot(x[...], fd[...]).astype(BF16).astype(F32)).astype(BF16)
-    rlow[...] = dot(x[...], fa[...]).astype(BF16)
-    turn[...] = table[lax.axis_index("sp")]
-
-    def reordered(v):
-        v = v.reshape(4, 2, 32, v.shape[-1])
-        even, odd = v[:, 0].reshape(128, -1), v[:, 1].reshape(128, -1)
-        first, second = jnp.where(core == 0, even, odd), jnp.where(core == 0, odd, even)
-        return jnp.concatenate([first, second], axis=0)
-
-    both = jnp.concatenate([wk_up[...], wv_up[...]], axis=1).astype(F32)
-    up[...] = reordered(both).T.astype(BF16)
-    glat[...] = reordered(jnp.broadcast_to(compact_gain[...], (128, 256)).T)
-    for source, out in ((kg, key_gain), (qg, query_gain)):
-        wide = jnp.concatenate([source[...], jnp.zeros((1, 128 - QK), F32)], axis=1)
-        out[...] = jnp.broadcast_to(wide, (128, 128)).T[0:QK]
-
-
-def lowrank(*args):
-    column = jax.ShapeDtypeStruct((QK, 128), F32)
-    outs = [
-        jax.ShapeDtypeStruct((ROWS, 128), BF16),
-        jax.ShapeDtypeStruct((ROWS, 128), BF16),
-        jax.ShapeDtypeStruct((ROPE, ROWS), F32),
-        jax.ShapeDtypeStruct((256, 256), BF16),
-        jax.ShapeDtypeStruct((256, 128), F32),
-        column,
-        column,
-    ]
-    return call(lowrank_body, outs, args, 1 << 29, specs=[VMEM] * 9, limit=63.9)
-
-
 def columns(k):
     shard = lax.rem(lax.axis_index("fs") + (0, 3, 1, 2)[k], 4)
     return pl.ds(pl.multiple_of(shard * 512, 512), 512)
@@ -187,30 +150,55 @@
 
 def latents(*args):
     outs = jax.ShapeDtypeStruct((16, 40, ROWS), BF16)
-    return call(latents_body, outs, args, 1 << 29, specs=[VMEM] * 5, limit=63.9)
-
-
-def queries_body(x, w0, w1, w2, w3, turn, gain, q):
+    return call(latents_body, outs, args, 1 << 29, limit=40)
+
+
+def queries_body(
+    x, w0, w1, w2, w3, table, wk_up, wv_up, compact_gain, kg, qg, q, up, glat, key_gain
+):
+    core = lax.rem(lax.axis_index("tp"), 2)
+
+    def reordered(v):
+        v = v.reshape(4, 2, 32, v.shape[-1])
+        even, odd = v[:, 0].reshape(128, -1), v[:, 1].reshape(128, -1)
+        first, second = jnp.where(core == 0, even, odd), jnp.where(core == 0, odd, even)
+        return jnp.concatenate([first, second], axis=0)
+
+    def column(source):
+        wide = jnp.concatenate([source[...], jnp.zeros((1, 128 - QK), F32)], axis=1)
+        return jnp.broadcast_to(wide, (128, 128)).T[0:QK]
+
     t = jnp.zeros((192, ROWS), F32)
     for k, w in enumerate((w0, w1, w2, w3)):
         t += dot(w[0:192], x[:, columns(k)], NT)
     t = t.astype(BF16).astype(F32)
     factor = np.float32(QK**-0.5 * np.log2(np.e))
+    turn = table[lax.axis_index("sp")]
+    gain = column(qg)[:, 0:1]
     for h in range(2):
         v = t[QK * h : QK * (h + 1)]
-        n = v * (lax.rsqrt(jnp.mean(v * v, axis=0, keepdims=True) + EPS) * factor) * gain[:, 0:1]
-        a, b = turned(n, turn[...])
+        n = v * (lax.rsqrt(jnp.mean(v * v, axis=0, keepdims=True) + EPS) * factor) * gain
+        a, b = turned(n, turn)
         ready = jnp.concatenate([n[:NOPE], a, b, jnp.zeros((128 - QK, ROWS), F32)], axis=0)
         q[h] = ready.T.astype(BF16)
+    both = jnp.concatenate([wk_up[...], wv_up[...]], axis=1).astype(F32)
+    up[...] = reordered(both).T.astype(BF16)
+    glat[...] = reordered(jnp.broadcast_to(compact_gain[...], (128, 256)).T)
+    key_gain[...] = column(kg)
 
 
 def queries(*args):
-    outs = jax.ShapeDtypeStruct((2, ROWS, 128), BF16)
-    return call(queries_body, outs, args, 1 << 29, specs=[VMEM] * 7)
+    outs = [
+        jax.ShapeDtypeStruct((2, ROWS, 128), BF16),
+        jax.ShapeDtypeStruct((256, 256), BF16),
+        jax.ShapeDtypeStruct((256, 128), F32),
+        jax.ShapeDtypeStruct((QK, 128), F32),
+    ]
+    return call(queries_body, outs, args, 1 << 29)
 
 
 def recur_body(
-    x, w0, w1, w2, w3, dlow, rlow, wd, bd, wa, ba, mult, extra, present,
+    x, w0, w1, w2, w3, fd, fa, wd, bd, wa, ba, mult, extra, present,
     free, along, bonus, state,
 ):
     lane = iota((1, 128), 1)
@@ -218,12 +206,14 @@
     for k, w in enumerate((w0, w1, w2, w3)):
         y += dot(x[:, columns(k)], w[...])
     y = y.astype(BF16).astype(F32)
+    dlow = jnp.tanh(dot(x[...], fd[...]).astype(BF16).astype(F32)).astype(BF16)
+    rlow = dot(x[...], fa[...]).astype(BF16)
     recept, key, value = (y[:, 128 * i : 128 * (i + 1)] for i in range(3))
-    speed = jax.nn.sigmoid(bd[...] + dot(dlow[...], wd[...])) * np.float32(np.exp(-0.5))
+    speed = jax.nn.sigmoid(bd[...] + dot(dlow, wd[...])) * np.float32(np.exp(-0.5))
     added = jnp.where(iota((128, ROWS), 0) < 64, extra[0:1], extra[1:2]).T
     ld = added - speed * jnp.where(lane < 64, mult[0:1, 0:1], mult[1:2, 0:1])
     here = jnp.concatenate([present[0:1], present[1:2]], axis=1)
-    learn = jax.nn.sigmoid(ba[...] + dot(rlow[...], wa[...]))
+    learn = jax.nn.sigmoid(ba[...] + dot(rlow, wa[...]))
     same = (iota((128, 128), 0) // 64 == iota((128, 128), 1) // 64).astype(BF16)
     unit = key * lax.rsqrt(dot_wide(key * key, same) + EPS)
     bonus[...] = dot_wide(recept * key * here, same) * value
@@ -413,7 +403,13 @@
     return call(attend_body, outs, args, 8 << 30, scratch, [VMEM] * 7)
 
 
-def merge_body(att, free, along, bonus, states, branch, o0, o1, o2, o3, keep, send):
+def merge_body(att, free, along, bonus, states, branch, o0, o1, o2, o3, keep, send, held, arrived):
+    copies = [
+        pltpu.make_async_copy(o.at[pl.ds(192, 256)], held.at[k], arrived.at[k])
+        for k, o in enumerate((o0, o1, o2, o3))
+    ]
+    for copy in copies:
+        copy.start()
     head = iota((128, 128), 0) // 64 == iota((128, 128), 1) // 64
 
     def spread(v):
@@ -447,15 +443,18 @@
     even, odd = both[:, 0].reshape(128, 256), both[:, 1].reshape(128, 256)
     kept = jnp.where(core == 0, even, odd).astype(BF16)
     sent = jnp.where(core == 0, odd, even).astype(BF16)
-    for k, o in enumerate((o0, o1, o2, o3)):
-        send[:, columns(k)] = dot(sent, o[192:448]).astype(BF16)
-    for k, o in enumerate((o0, o1, o2, o3)):
-        keep[:, columns(k)] = dot(kept, o[192:448])
+    for copy in copies:
+        copy.wait()
+    for k in range(4):
+        send[:, columns(k)] = dot(sent, held[k]).astype(BF16)
+    for k in range(4):
+        keep[:, columns(k)] = dot(kept, held[k])
 
 
 def merge(*args):
     outs = [jax.ShapeDtypeStruct((128, 2048), F32), jax.ShapeDtypeStruct((128, 2048), BF16)]
-    return call(merge_body, outs, args, 4 << 30, specs=[VMEM] * 10)
+    scratch = [pltpu.VMEM((4, 256, 512), BF16), pltpu.SemaphoreType.DMA((4,))]
+    return call(merge_body, outs, args, 4 << 30, scratch, [VMEM] * 6 + [HBM] * 4)
 
 
 def exchanged(copies, axis, groups=None):
@@ -527,22 +526,11 @@
     pay = latents(normed, *smalls)
     lat = exchanged(pay, "sp")
 
-    dlow, rlow, turn, up, glat, key_gain, query_gain = lowrank(
-        normed,
-        fade1,
-        adapt1,
-        table,
-        wk_up,
-        wv_up,
-        compact_gain.reshape(1, 256),
-        k_gain.reshape(1, QK),
-        q_gain.reshape(1, QK),
-    )
     free, along, bonus, state = recur(
         normed,
         *bigs,
-        dlow,
-        rlow,
+        fade1,
+        adapt1,
         fade2,
         fade_bias.reshape(1, 128),
         adapt2,
@@ -556,7 +544,16 @@
     others = [lax.ppermute(lat, "tp", [(i, (i + by) % 8) for i in range(8)]) for by in (2, 6, 4)]
     lat_own = collect(lat, *others)
     lat_peer = other_core(lat_own)
-    q = queries(normed, *lates, turn, query_gain)
+    q, up, glat, key_gain = queries(
+        normed,
+        *lates,
+        table,
+        wk_up,
+        wv_up,
+        compact_gain.reshape(1, 256),
+        k_gain.reshape(1, QK),
+        q_gain.reshape(1, QK),
+    )
     att, logs = attend(q, lat_own, lat_peer, up, glat, key_gain, table)
     keep, send = merge(att, free, along, bonus, states, branch.reshape(1, 128), *lates)
     pair = (keep + other_core(send).astype(F32)).astype(BF16)

time: 166 us -> 169 us (1.018)
  Pallas kernels: 36.2 us -> 31.4 us
  waiting for transfers between devices: 39.6 us -> 43.7 us
  local copies, waits for them, and re-layouts: 2.94 us -> 6.64 us
    pallas_call x8 -> x7, Pallas kernels: 36.2 us -> 31.4 us  [call(): pl.pallas_call(body, out_shape=outs, in_specs=specs or [VMEM] * len(args)...]
    ppermute x9, waiting for transfers between devices: 27.2 us -> 31.2 us  [around(): return [value] + [lax.ppermute(value, 'fs', move) for move in moves]]
    unnamed x32 -> x54, local copies, waits for them, and re-layouts: 2.94 us -> 6.64 us
  transfers between devices with their start and end apart: 17 -> 17, of which waited for: 11 -> 11; matrix products, arithmetic and copies ran while one was open for 0% -> 0% of each run, Pallas kernels for 17% -> 14%
where the time goes in v8:
time: 169 us; the launch traced here: 168 us
  starting transfers between devices  71.7 us (42%)
  waiting for transfers between devices  43.7 us (26%)
  Pallas kernels  31.4 us (19%)
  blocking collectives  12.5 us (7%)
  local copies, waits for them, and re-layouts  6.64 us (4%)
    ppermute x9, starting transfers between devices, around(): return [value] + [lax.ppermute(value, 'fs', move) for move in moves]  32.8 us
    pallas_call x7, Pallas kernels, call(): pl.pallas_call(body, out_shape=outs, in_specs=specs or [VMEM] * len(args)...  31.4 us
    ppermute x9, waiting for transfers between devices, around(): return [value] + [lax.ppermute(value, 'fs', move) for move in moves]  31.2 us
    all_to_all x3, starting transfers between devices, exchanged(): lax.all_to_all(copies, axis, 0, 0, axis_index_groups=groups, tiled=True)  25.3 us
    all_to_all x1, blocking collectives, exchanged(): lax.all_to_all(copies, axis, 0, 0, axis_index_groups=groups, tiled=True)  12.5 us
    ppermute x3, waiting for transfers between devices, shards(): lax.ppermute(lat, 'tp', [(i, (i + by) % 8) for i in range(8)])  10.1 us
    ppermute x3, starting transfers between devices, shards(): lax.ppermute(lat, 'tp', [(i, (i + by) % 8) for i in range(8)])  9.66 us
    unnamed x54, local copies, waits for them, and re-layouts  6.64 us
  transfers between devices with their start and end apart: 17, of which 11 were waited for; matrix products, arithmetic and copies ran while one was open for 0% of the time, Pallas kernels for 14%

profile of v8, /device:TPU:480, one launch (start us, length us, event | category | flops | bytes accessed | tf_op | source)
XLA Modules:
  0.0 167.7 jit_solution(13651883752572631300)
XLA Ops:
  0.6 2.7 %shard_map.257 = (bf16[8,32,2048]{2,1,0:T(8,128)(2,1)}, bf16[64,512]{1,0:T(8,128)(2,1)}, bf16[512,384]{1,0:T(8,128)(2,1)}, bf16[448,512]{1,0:T(8,128)(2,1)}) custom-call(bf16[32,2048]{1,0:T(8,128)(2,1)} %bitcast.26, f32[1,2048]{1,0:T(1,128)} %bitcast.28, bf16[512,128]{1,0:T(8,128)(2,1)} %wa_in.1, bf16[512,128]{1,0:T(8,128)(2,1)} %wk_in.1, ...), custom_call_target="tpu_custom_call" | custom-call | flops 536870912 | bytes 4194304 | tf_op jit(solution)/shard_map/pallas_call | solution.py:57
  3.3 4.4 %all-to-all-start = ((bf16[8,32,2048]{2,1,0:T(8,128)(2,1)}), bf16[8,32,2048]{2,1,0:T(8,128)(2,1)S(1)}, u32[]{:S(2)}, u32[]{:S(2)}) async-start(bf16[8,32,2048]{2,1,0:T(8,128)(2,1)} %get-tuple-element.20), calls=%async_computation | async-start | bytes 2097152 | tf_op jit(solution)/shard_map/all_to_all | solution.py:461
  7.8 5.1 %collective-permute-start.5 = (bf16[64,512]{1,0:T(8,128)(2,1)S(1)}, bf16[64,512]{1,0:T(8,128)(2,1)S(1)}, u32[]{:S(2)}, u32[]{:S(2)}) collective-permute-start(bf16[64,512]{1,0:T(8,128)(2,1)S(1)} %copy-done.16), channel_id=1, source_target_pairs={{0,16},{8,24},{16,0},{24,8},{1,17},{9,25},{17,1},{25,9},{2,18},{10... | collective-permute-start | bytes 196616 | tf_op jit(solution)/shard_map/ppermute | solution.py:466
  12.9 3.0 %collective-permute-start.4 = (bf16[64,512]{1,0:T(8,128)(2,1)S(1)}, bf16[64,512]{1,0:T(8,128)(2,1)S(1)}, u32[]{:S(2)}, u32[]{:S(2)}) collective-permute-start(bf16[64,512]{1,0:T(8,128)(2,1)S(1)} %copy-done.16), channel_id=1, source_target_pairs={{0,24},{8,0},{16,8},{24,16},{1,25},{9,1},{17,9},{25,17},{2,26},{10... | collective-permute-start | bytes 196616 | tf_op jit(solution)/shard_map/ppermute | solution.py:466
  15.9 2.9 %collective-permute-start.3 = (bf16[64,512]{1,0:T(8,128)(2,1)S(1)}, bf16[64,512]{1,0:T(8,128)(2,1)S(1)}, u32[]{:S(2)}, u32[]{:S(2)}) collective-permute-start(bf16[64,512]{1,0:T(8,128)(2,1)S(1)} %copy-done.16), channel_id=1, source_target_pairs={{0,8},{8,16},{16,24},{24,0},{1,9},{9,17},{17,25},{25,1},{2,10},{10... | collective-permute-start | bytes 196616 | tf_op jit(solution)/shard_map/ppermute | solution.py:466
  19.1 4.2 %collective-permute-done.3.w1 = bf16[64,512]{1,0:T(8,128)(2,1)S(1)} collective-permute-done((bf16[64,512]{1,0:T(8,128)(2,1)S(1)}, bf16[64,512]{1,0:T(8,128)(2,1)S(1)}, u32[]{:S(2)}, u32[]{:S(2)}) %collective-permute-start.3) | collective-permute-done | bytes 65568 | tf_op jit(solution)/shard_map/ppermute | solution.py:466
  24.9 8.9 %all-to-all-start.1 = ((bf16[16,40,256]{2,1,0:T(8,128)(2,1)}), bf16[16,40,256]{2,1,0:T(8,128)(2,1)}, u32[]{:S(2)}, u32[]{:S(2)}) async-start(bf16[16,40,256]{2,1,0:T(8,128)(2,1)} %shard_map.259), calls=%async_computation.1 | async-start | bytes 655360 | tf_op jit(solution)/shard_map/all_to_all | solution.py:461
  33.8 5.1 %collective-permute-start.8 = (bf16[512,384]{1,0:T(8,128)(2,1)S(1)}, bf16[512,384]{1,0:T(8,128)(2,1)S(1)}, u32[]{:S(2)}, u32[]{:S(2)}) collective-permute-start(bf16[512,384]{1,0:T(8,128)(2,1)S(1)} %copy-done.23), channel_id=1, source_target_pairs={{0,16},{8,24},{16,0},{24,8},{1,17},{9,25},{17,1},{25,9},{2,18},{10... | collective-permute-start | bytes 1179656 | tf_op jit(solution)/shard_map/ppermute | solution.py:466
  38.9 3.0 %collective-permute-start.7 = (bf16[512,384]{1,0:T(8,128)(2,1)S(1)}, bf16[512,384]{1,0:T(8,128)(2,1)S(1)}, u32[]{:S(2)}, u32[]{:S(2)}) collective-permute-start(bf16[512,384]{1,0:T(8,128)(2,1)S(1)} %copy-done.23), channel_id=1, source_target_pairs={{0,24},{8,0},{16,8},{24,16},{1,25},{9,1},{17,9},{25,17},{2,26},{10... | collective-permute-start | bytes 1179656 | tf_op jit(solution)/shard_map/ppermute | solution.py:466
  41.9 2.9 %collective-permute-start.6 = (bf16[512,384]{1,0:T(8,128)(2,1)S(1)}, bf16[512,384]{1,0:T(8,128)(2,1)S(1)}, u32[]{:S(2)}, u32[]{:S(2)}) collective-permute-start(bf16[512,384]{1,0:T(8,128)(2,1)S(1)} %copy-done.23), channel_id=1, source_target_pairs={{0,8},{8,16},{16,24},{24,0},{1,9},{9,17},{17,25},{25,1},{2,10},{10... | collective-permute-start | bytes 1179656 | tf_op jit(solution)/shard_map/ppermute | solution.py:466
  44.8 4.4 %collective-permute-done.8.w3 = bf16[512,384]{1,0:T(8,128)(2,1)S(1)} collective-permute-done((bf16[512,384]{1,0:T(8,128)(2,1)S(1)}, bf16[512,384]{1,0:T(8,128)(2,1)S(1)}, u32[]{:S(2)}, u32[]{:S(2)}) %collective-permute-start.8) | collective-permute-done | bytes 393248 | tf_op jit(solution)/shard_map/ppermute | solution.py:466
  49.2 6.8 %collective-permute-done.7.w2 = bf16[512,384]{1,0:T(8,128)(2,1)S(1)} collective-permute-done((bf16[512,384]{1,0:T(8,128)(2,1)S(1)}, bf16[512,384]{1,0:T(8,128)(2,1)S(1)}, u32[]{:S(2)}, u32[]{:S(2)}) %collective-permute-start.7) | collective-permute-done | bytes 393248 | tf_op jit(solution)/shard_map/ppermute | solution.py:466
  56.9 12.8 %shard_map.260 = (f32[256,128]{1,0:T(8,128)}, f32[256,128]{1,0:T(8,128)}, f32[256,128]{1,0:T(8,128)}, bf16[16,2,64,128]{3,2,1,0:T(8,128)(2,1)}) custom-call(bf16[256,2048]{1,0:T(8,128)(2,1)} %bitcast.17, bf16[512,384]{1,0:T(8,128)(2,1)} %get-tuple-element.24.w0, bf16[512,384]{1,0:T(8,128)(2,1)} %copy-done.26, bf16[512,384]{1,0:T(8,128)(2,1)} %copy-done.25, ...), custom_call_target="tpu_custom_call" | custom-call | flops 8589934592 | bytes 4194304 | tf_op jit(solution)/shard_map/pallas_call | solution.py:57
  69.8 3.8 %collective-permute-start.11 = (bf16[16,40,256]{2,1,0:T(8,128)(2,1)}, bf16[16,40,256]{2,1,0:T(8,128)(2,1)S(1)}, u32[]{:S(2)}, u32[]{:S(2)}) collective-permute-start(bf16[16,40,256]{2,1,0:T(8,128)(2,1)} %all-to-all-done.1.own), channel_id=1, source_target_pairs={{0,4},{1,5},{2,6},{3,7},{4,0},{5,1},{6,2},{7,3},{8,12},{9,13},{10,... | collective-permute-start | bytes 983048 | tf_op jit(solution)/shard_map/ppermute | solution.py:544
  73.6 3.5 %collective-permute-start.10 = (bf16[16,40,256]{2,1,0:T(8,128)(2,1)}, bf16[16,40,256]{2,1,0:T(8,128)(2,1)S(1)}, u32[]{:S(2)}, u32[]{:S(2)}) collective-permute-start(bf16[16,40,256]{2,1,0:T(8,128)(2,1)} %all-to-all-done.1.own), channel_id=1, source_target_pairs={{0,6},{1,7},{2,0},{3,1},{4,2},{5,3},{6,4},{7,5},{8,14},{9,15},{10,... | collective-permute-start | bytes 983048 | tf_op jit(solution)/shard_map/ppermute | solution.py:544
  79.5 4.4 %collective-permute-done.11.far = bf16[16,40,256]{2,1,0:T(8,128)(2,1)S(1)} collective-permute-done((bf16[16,40,256]{2,1,0:T(8,128)(2,1)}, bf16[16,40,256]{2,1,0:T(8,128)(2,1)S(1)}, u32[]{:S(2)}, u32[]{:S(2)}) %collective-permute-start.11) | collective-permute-done | bytes 327712 | tf_op jit(solution)/shard_map/ppermute | solution.py:544
  83.8 4.4 %collective-permute-done.10.right = bf16[16,40,256]{2,1,0:T(8,128)(2,1)S(1)} collective-permute-done((bf16[16,40,256]{2,1,0:T(8,128)(2,1)}, bf16[16,40,256]{2,1,0:T(8,128)(2,1)S(1)}, u32[]{:S(2)}, u32[]{:S(2)}) %collective-permute-start.10) | collective-permute-done | bytes 327712 | tf_op jit(solution)/shard_map/ppermute | solution.py:544
  92.6 12.0 %all-to-all-start.2 = ((bf16[16,2,64,128]{3,2,1,0:T(8,128)(2,1)}), bf16[16,2,64,128]{3,2,1,0:T(8,128)(2,1)S(1)}, u32[]{:S(2)}, u32[]{:S(2)}) async-start(bf16[16,2,64,128]{3,2,1,0:T(8,128)(2,1)} %get-tuple-element.34), calls=%async_computation.2 | async-start | bytes 1048576 | tf_op jit(solution)/shard_map/all_to_all | solution.py:461
  104.6 5.1 %collective-permute-start.2 = (bf16[448,512]{1,0:T(8,128)(2,1)}, bf16[448,512]{1,0:T(8,128)(2,1)S(1)}, u32[]{:S(2)}, u32[]{:S(2)}) collective-permute-start(bf16[448,512]{1,0:T(8,128)(2,1)} %get-tuple-element.21.w0.o0), channel_id=1, source_target_pairs={{0,16},{8,24},{16,0},{24,8},{1,17},{9,25},{17,1},{25,9},{2,18},{10... | collective-permute-start | bytes 1376264 | tf_op jit(solution)/shard_map/ppermute | solution.py:466
  109.7 3.2 %collective-permute-start.1 = (bf16[448,512]{1,0:T(8,128)(2,1)}, bf16[448,512]{1,0:T(8,128)(2,1)S(1)}, u32[]{:S(2)}, u32[]{:S(2)}) collective-permute-start(bf16[448,512]{1,0:T(8,128)(2,1)} %get-tuple-element.21.w0.o0), channel_id=1, source_target_pairs={{0,24},{8,0},{16,8},{24,16},{1,25},{9,1},{17,9},{25,17},{2,26},{10... | collective-permute-start | bytes 1376264 | tf_op jit(solution)/shard_map/ppermute | solution.py:466
  115.6 6.0 %collective-permute-done.2.w3.o3 = bf16[448,512]{1,0:T(8,128)(2,1)S(1)} collective-permute-done((bf16[448,512]{1,0:T(8,128)(2,1)}, bf16[448,512]{1,0:T(8,128)(2,1)S(1)}, u32[]{:S(2)}, u32[]{:S(2)}) %collective-permute-start.2) | collective-permute-done | bytes 458784 | tf_op jit(solution)/shard_map/ppermute | solution.py:466
  121.6 9.5 %collective-permute-done.1.w2.o2 = bf16[448,512]{1,0:T(8,128)(2,1)S(1)} collective-permute-done((bf16[448,512]{1,0:T(8,128)(2,1)}, bf16[448,512]{1,0:T(8,128)(2,1)S(1)}, u32[]{:S(2)}, u32[]{:S(2)}) %collective-permute-start.1) | collective-permute-done | bytes 458784 | tf_op jit(solution)/shard_map/ppermute | solution.py:466
  133.2 10.5 %shard_map.262 = (bf16[256,128]{1,0:T(8,128)(2,1)S(1)}, f32[2,256]{1,0:T(2,128)}) custom-call(bf16[2,256,128]{2,1,0:T(8,128)(2,1)S(1)} %get-tuple-element.22.q, bf16[4,16,40,256]{3,2,1,0:T(8,128)(2,1)S(1)} %shard_map.261.own, bf16[4,16,40,256]{3,2,1,0:T(8,128)(2,1)} %collective-permute-done.12.peer, bf16[256,256]{1,0:T(8,128)(2,1)S(1)} %get-tuple-element.27.w, ...), custom_call_target="tpu_custom_call" | custom-call | flops 8589934592 | bytes 4194304 | tf_op jit(solution)/shard_map/pallas_call | solution.py:57
  154.5 12.5 %all_to_all.20 = bf16[4,32,2048]{2,1,0:T(8,128)(2,1)S(1)} all-to-all(bf16[4,32,2048]{2,1,0:T(8,128)(2,1)S(1)} %bitcast.23), channel_id=1, replica_groups={{0,2,4,6},{1,3,5,7},{8,10,12,14},{9,11,13,15},{16,18,20,22},{17,19,21,2..., dimensions={0} | all-to-all | bytes 1048576 | tf_op jit(solution)/shard_map/all_to_all | solution.py:461
  (74 shorter events, 25.7 us)
Async XLA Ops:
  3.3 20.4 %all-to-all-start = ((bf16[8,32,2048]{2,1,0:T(8,128)(2,1)}), bf16[8,32,2048]{2,1,0:T(8,128)(2,1)S(1)}, u32[]{:S(2)}, u32[]{:S(2)}) async-start(bf16[8,32,2048]{2,1,0:T(8,128)(2,1)} %get-tuple-element.20), calls=%async_computation | async-start | bytes 2097152 | tf_op jit(solution)/shard_map/all_to_all | solution.py:461
  7.8 11.0 %collective-permute-start.5 = (bf16[64,512]{1,0:T(8,128)(2,1)S(1)}, bf16[64,512]{1,0:T(8,128)(2,1)S(1)}, u32[]{:S(2)}, u32[]{:S(2)}) collective-permute-start(bf16[64,512]{1,0:T(8,128)(2,1)S(1)} %copy-done.16), channel_id=1, source_target_pairs={{0,16},{8,24},{16,0},{24,8},{1,17},{9,25},{17,1},{25,9},{2,18},{10... | collective-permute-start | bytes 196616 | tf_op jit(solution)/shard_map/ppermute | solution.py:466
  12.9 6.2 %collective-permute-start.4 = (bf16[64,512]{1,0:T(8,128)(2,1)S(1)}, bf16[64,512]{1,0:T(8,128)(2,1)S(1)}, u32[]{:S(2)}, u32[]{:S(2)}) collective-permute-start(bf16[64,512]{1,0:T(8,128)(2,1)S(1)} %copy-done.16), channel_id=1, source_target_pairs={{0,24},{8,0},{16,8},{24,16},{1,25},{9,1},{17,9},{25,17},{2,26},{10... | collective-permute-start | bytes 196616 | tf_op jit(solution)/shard_map/ppermute | solution.py:466
  15.9 7.4 %collective-permute-start.3 = (bf16[64,512]{1,0:T(8,128)(2,1)S(1)}, bf16[64,512]{1,0:T(8,128)(2,1)S(1)}, u32[]{:S(2)}, u32[]{:S(2)}) collective-permute-start(bf16[64,512]{1,0:T(8,128)(2,1)S(1)} %copy-done.16), channel_id=1, source_target_pairs={{0,8},{8,16},{16,24},{24,0},{1,9},{9,17},{17,25},{25,1},{2,10},{10... | collective-permute-start | bytes 196616 | tf_op jit(solution)/shard_map/ppermute | solution.py:466
  24.9 44.8 %all-to-all-start.1 = ((bf16[16,40,256]{2,1,0:T(8,128)(2,1)}), bf16[16,40,256]{2,1,0:T(8,128)(2,1)}, u32[]{:S(2)}, u32[]{:S(2)}) async-start(bf16[16,40,256]{2,1,0:T(8,128)(2,1)} %shard_map.259), calls=%async_computation.1 | async-start | bytes 655360 | tf_op jit(solution)/shard_map/all_to_all | solution.py:461
  33.8 15.4 %collective-permute-start.8 = (bf16[512,384]{1,0:T(8,128)(2,1)S(1)}, bf16[512,384]{1,0:T(8,128)(2,1)S(1)}, u32[]{:S(2)}, u32[]{:S(2)}) collective-permute-start(bf16[512,384]{1,0:T(8,128)(2,1)S(1)} %copy-done.23), channel_id=1, source_target_pairs={{0,16},{8,24},{16,0},{24,8},{1,17},{9,25},{17,1},{25,9},{2,18},{10... | collective-permute-start | bytes 1179656 | tf_op jit(solution)/shard_map/ppermute | solution.py:466
  38.9 17.1 %collective-permute-start.7 = (bf16[512,384]{1,0:T(8,128)(2,1)S(1)}, bf16[512,384]{1,0:T(8,128)(2,1)S(1)}, u32[]{:S(2)}, u32[]{:S(2)}) collective-permute-start(bf16[512,384]{1,0:T(8,128)(2,1)S(1)} %copy-done.23), channel_id=1, source_target_pairs={{0,24},{8,0},{16,8},{24,16},{1,25},{9,1},{17,9},{25,17},{2,26},{10... | collective-permute-start | bytes 1179656 | tf_op jit(solution)/shard_map/ppermute | solution.py:466
  41.9 14.1 %collective-permute-start.6 = (bf16[512,384]{1,0:T(8,128)(2,1)S(1)}, bf16[512,384]{1,0:T(8,128)(2,1)S(1)}, u32[]{:S(2)}, u32[]{:S(2)}) collective-permute-start(bf16[512,384]{1,0:T(8,128)(2,1)S(1)} %copy-done.23), channel_id=1, source_target_pairs={{0,8},{8,16},{16,24},{24,0},{1,9},{9,17},{17,25},{25,1},{2,10},{10... | collective-permute-start | bytes 1179656 | tf_op jit(solution)/shard_map/ppermute | solution.py:466
  69.7 61.4 %copy-start.1 = (bf16[8,32,2048]{2,1,0:T(8,128)(2,1)S(1)}, bf16[8,32,2048]{2,1,0:T(8,128)(2,1)}, u32[]{:S(2)}) copy-start(bf16[8,32,2048]{2,1,0:T(8,128)(2,1)} %copy-done) | copy-start | bytes 3145732
  69.7 61.4 %copy-start.2 = (f32[16,32,256]{2,1,0:T(8,128)S(1)}, f32[16,32,256]{2,1,0:T(8,128)}, u32[]{:S(2)}) copy-start(f32[16,32,256]{2,1,0:T(8,128)} %constant.5.clone.table) | copy-start | bytes 1572868
  69.7 61.4 %copy-start.11 = (bf16[256,128]{1,0:T(8,128)(2,1)S(1)}, bf16[256,128]{1,0:T(8,128)(2,1)}, u32[]{:S(2)}) copy-start(bf16[256,128]{1,0:T(8,128)(2,1)} %wk_up.1) | copy-start | bytes 196612
  69.7 61.4 %copy-start.12 = (bf16[256,128]{1,0:T(8,128)(2,1)S(1)}, bf16[256,128]{1,0:T(8,128)(2,1)}, u32[]{:S(2)}) copy-start(bf16[256,128]{1,0:T(8,128)(2,1)} %wv_up.1) | copy-start | bytes 196612
  69.7 61.4 %copy-start.13 = (f32[256]{0:T(256)S(1)}, f32[256]{0:T(256)}, u32[]{:S(2)}) copy-start(f32[256]{0:T(256)} %param.31) | copy-start | bytes 3076
  69.8 61.4 %copy-start.14 = (f32[96]{0:T(128)S(1)}, f32[96]{0:T(128)}, u32[]{:S(2)}) copy-start(f32[96]{0:T(128)} %param.35) | copy-start | bytes 1156
  69.8 61.4 %copy-start.15 = (f32[96]{0:T(128)S(1)}, f32[96]{0:T(128)}, u32[]{:S(2)}) copy-start(f32[96]{0:T(128)} %param.34) | copy-start | bytes 1156
  69.8 14.0 %collective-permute-start.11 = (bf16[16,40,256]{2,1,0:T(8,128)(2,1)}, bf16[16,40,256]{2,1,0:T(8,128)(2,1)S(1)}, u32[]{:S(2)}, u32[]{:S(2)}) collective-permute-start(bf16[16,40,256]{2,1,0:T(8,128)(2,1)} %all-to-all-done.1.own), channel_id=1, source_target_pairs={{0,4},{1,5},{2,6},{3,7},{4,0},{5,1},{6,2},{7,3},{8,12},{9,13},{10,... | collective-permute-start | bytes 983048 | tf_op jit(solution)/shard_map/ppermute | solution.py:544
  73.6 14.6 %collective-permute-start.10 = (bf16[16,40,256]{2,1,0:T(8,128)(2,1)}, bf16[16,40,256]{2,1,0:T(8,128)(2,1)S(1)}, u32[]{:S(2)}, u32[]{:S(2)}) collective-permute-start(bf16[16,40,256]{2,1,0:T(8,128)(2,1)} %all-to-all-done.1.own), channel_id=1, source_target_pairs={{0,6},{1,7},{2,0},{3,1},{4,2},{5,3},{6,4},{7,5},{8,14},{9,15},{10,... | collective-permute-start | bytes 983048 | tf_op jit(solution)/shard_map/ppermute | solution.py:544
  77.1 12.5 %collective-permute-start.9 = (bf16[16,40,256]{2,1,0:T(8,128)(2,1)}, bf16[16,40,256]{2,1,0:T(8,128)(2,1)S(1)}, u32[]{:S(2)}, u32[]{:S(2)}) collective-permute-start(bf16[16,40,256]{2,1,0:T(8,128)(2,1)} %all-to-all-done.1.own), channel_id=1, source_target_pairs={{0,2},{1,3},{2,4},{3,5},{4,6},{5,7},{6,0},{7,1},{8,10},{9,11},{10,... | collective-permute-start | bytes 983048 | tf_op jit(solution)/shard_map/ppermute | solution.py:544
  90.7 42.5 %collective-permute-start.12 = (bf16[4,16,40,256]{3,2,1,0:T(8,128)(2,1)S(1)}, bf16[4,16,40,256]{3,2,1,0:T(8,128)(2,1)}, u32[]{:S(2)}, u32[]{:S(2)}) collective-permute-start(bf16[4,16,40,256]{3,2,1,0:T(8,128)(2,1)S(1)} %shard_map.261.own), channel_id=1, source_target_pairs={{0,1},{1,0},{2,3},{3,2},{4,5},{5,4},{6,7},{7,6},{8,9},{9,8},{10,11... | collective-permute-start | bytes 3932168 | tf_op jit(solution)/shard_map/ppermute | solution.py:470
  92.6 51.8 %all-to-all-start.2 = ((bf16[16,2,64,128]{3,2,1,0:T(8,128)(2,1)}), bf16[16,2,64,128]{3,2,1,0:T(8,128)(2,1)S(1)}, u32[]{:S(2)}, u32[]{:S(2)}) async-start(bf16[16,2,64,128]{3,2,1,0:T(8,128)(2,1)} %get-tuple-element.34), calls=%async_computation.2 | async-start | bytes 1048576 | tf_op jit(solution)/shard_map/all_to_all | solution.py:461
  104.6 17.0 %collective-permute-start.2 = (bf16[448,512]{1,0:T(8,128)(2,1)}, bf16[448,512]{1,0:T(8,128)(2,1)S(1)}, u32[]{:S(2)}, u32[]{:S(2)}) collective-permute-start(bf16[448,512]{1,0:T(8,128)(2,1)} %get-tuple-element.21.w0.o0), channel_id=1, source_target_pairs={{0,16},{8,24},{16,0},{24,8},{1,17},{9,25},{17,1},{25,9},{2,18},{10... | collective-permute-start | bytes 1376264 | tf_op jit(solution)/shard_map/ppermute | solution.py:466
  109.7 21.3 %collective-permute-start.1 = (bf16[448,512]{1,0:T(8,128)(2,1)}, bf16[448,512]{1,0:T(8,128)(2,1)S(1)}, u32[]{:S(2)}, u32[]{:S(2)}) collective-permute-start(bf16[448,512]{1,0:T(8,128)(2,1)} %get-tuple-element.21.w0.o0), channel_id=1, source_target_pairs={{0,24},{8,0},{16,8},{24,16},{1,25},{9,1},{17,9},{25,17},{2,26},{10... | collective-permute-start | bytes 1376264 | tf_op jit(solution)/shard_map/ppermute | solution.py:466
  113.0 18.1 %collective-permute-start = (bf16[448,512]{1,0:T(8,128)(2,1)}, bf16[448,512]{1,0:T(8,128)(2,1)S(1)}, u32[]{:S(2)}, u32[]{:S(2)}) collective-permute-start(bf16[448,512]{1,0:T(8,128)(2,1)} %get-tuple-element.21.w0.o0), channel_id=1, source_target_pairs={{0,8},{8,16},{16,24},{24,0},{1,9},{9,17},{17,25},{25,1},{2,10},{10... | collective-permute-start | bytes 1376264 | tf_op jit(solution)/shard_map/ppermute | solution.py:466
  150.6 3.8 %collective-permute-start.13 = (bf16[128,2048]{1,0:T(8,128)(2,1)S(1)}, bf16[128,2048]{1,0:T(8,128)(2,1)S(1)}, u32[]{:S(2)}, u32[]{:S(2)}) collective-permute-start(bf16[128,2048]{1,0:T(8,128)(2,1)S(1)} %get-tuple-element.36), channel_id=1, source_target_pairs={{0,1},{1,0},{2,3},{3,2},{4,5},{5,4},{6,7},{7,6},{8,9},{9,8},{10,11... | collective-permute-start | bytes 1572872 | tf_op jit(solution)/shard_map/ppermute | solution.py:470
  (20 other events, 101.5 us)

commit v9 on v8

--- a/solution.py
+++ b/solution.py
@@ -323,6 +323,9 @@
     sp = lax.axis_index("sp")
     ones = jnp.where(iota((NOPE, ROWS), 0) == 0, 1.0, 0.0).astype(BF16)
 
+    def twice(v):
+        return jnp.concatenate([v, v], axis=1)
+
     def keys(j):
         lat = jnp.concatenate(
             [own[:, j, 0:32, :].reshape(128, ROWS), peer[:, j, 0:32, :].reshape(128, ROWS)], axis=0
@@ -330,12 +333,12 @@
         rope = (own[:, j, 32:40, :].astype(F32) + peer[:, j, 32:40, :].astype(F32)).reshape(
             ROPE, ROWS
         )
-        lat = lat * lax.rsqrt(jnp.mean(lat * lat, axis=0, keepdims=True) + EPS) * glat[:, 0:1]
+        lat = lat * lax.rsqrt(jnp.mean(lat * lat, axis=0, keepdims=True) + EPS) * twice(glat[...])
         kv = dot(w[...], lat.astype(BF16)).astype(BF16)
         rope_sum = jnp.sum(rope * rope, axis=0, keepdims=True)
         turn = table[j]
         cosine, sine = turn[:16], turn[16:]
-        ra, rb = rope[:16] * gain[64:80, 0:1], rope[16:] * gain[80:96, 0:1]
+        ra, rb = rope[:16] * twice(gain[64:80]), rope[16:] * twice(gain[80:96])
         ra, rb = ra * cosine - rb * sine, rb * cosine + ra * sine
         ready, values = [], []
         for h in range(2):
@@ -344,7 +347,7 @@
                 (jnp.sum(k * k, axis=0, keepdims=True) + rope_sum) * np.float32(1 / QK) + EPS
             )
             ready.append(
-                jnp.concatenate([k * scale * gain[0:64, 0:1], ra * scale, rb * scale], axis=0).astype(
+                jnp.concatenate([k * scale * twice(gain[0:64]), ra * scale, rb * scale], axis=0).astype(
                     BF16
                 )
             )
@@ -367,24 +370,22 @@
                 old = top[h]
                 new = jnp.maximum(old, peak)
                 top[h] = new
-                p = jnp.exp2(s - new[:, 0:1]).astype(BF16)
+                p = jnp.exp2(s - jnp.concatenate([new] * (2 * len(places)), axis=1)).astype(BF16)
                 acc[h] = acc[h] * jnp.exp2(old - new) + dot(p, v, NT)
 
     block([sp], True)
 
     def loop(i, carry):
-        block([3 * i, 3 * i + 1, 3 * i + 2], False)
+        block([5 * i + n for n in range(5)], False)
         return carry
 
-    lax.fori_loop(0, sp // 3, loop, 0)
-
-    @pl.when(lax.rem(sp, 3) == 1)
-    def _():
-        block([sp - 1], False)
-
-    @pl.when(lax.rem(sp, 3) == 2)
-    def _():
-        block([sp - 2, sp - 1], False)
+    lax.fori_loop(0, sp // 5, loop, 0)
+    left = lax.rem(sp, 5)
+    for count in range(1, 5):
+
+        @pl.when(left == count)
+        def _():
+            block([sp - count + n for n in range(count)], False)
 
     parts = []
     rows = []

time: 169 us -> 168 us (level)
  Pallas kernels: 31.4 us -> 28.8 us
    pallas_call x7, Pallas kernels: 31.4 us -> 28.8 us  [call(): pl.pallas_call(body, out_shape=outs, in_specs=specs or [VMEM] * len(args)...]
  transfers between devices with their start and end apart: 17 -> 17, of which waited for: 11 -> 11; matrix products, arithmetic and copies ran while one was open for 0% -> 0% of each run, Pallas kernels for 14% -> 13%
where the time goes in v9:
time: 168 us; the launch traced here: 165 us
  starting transfers between devices  71.7 us (43%)
  waiting for transfers between devices  43.7 us (26%)
  Pallas kernels  28.8 us (17%)
  blocking collectives  12.5 us (7%)
  local copies, waits for them, and re-layouts  6.64 us (4%)
    ppermute x9, starting transfers between devices, around(): return [value] + [lax.ppermute(value, 'fs', move) for move in moves]  32.8 us
    ppermute x9, waiting for transfers between devices, around(): return [value] + [lax.ppermute(value, 'fs', move) for move in moves]  31.2 us
    pallas_call x7, Pallas kernels, call(): pl.pallas_call(body, out_shape=outs, in_specs=specs or [VMEM] * len(args)...  28.8 us
    all_to_all x3, starting transfers between devices, exchanged(): lax.all_to_all(copies, axis, 0, 0, axis_index_groups=groups, tiled=True)  25.3 us
    all_to_all x1, blocking collectives, exchanged(): lax.all_to_all(copies, axis, 0, 0, axis_index_groups=groups, tiled=True)  12.5 us
    ppermute x3, waiting for transfers between devices, shards(): lax.ppermute(lat, 'tp', [(i, (i + by) % 8) for i in range(8)])  10.1 us
    ppermute x3, starting transfers between devices, shards(): lax.ppermute(lat, 'tp', [(i, (i + by) % 8) for i in range(8)])  9.66 us
    unnamed x54, local copies, waits for them, and re-layouts  6.64 us
  transfers between devices with their start and end apart: 17, of which 11 were waited for; matrix products, arithmetic and copies ran while one was open for 0% of the time, Pallas kernels for 13%

profile of v9, /device:TPU:480, one launch (start us, length us, event | category | flops | bytes accessed | tf_op | source)
XLA Modules:
  0.0 165.1 jit_solution(737093484958738859)
XLA Ops:
  0.6 2.7 %shard_map.257 = (bf16[8,32,2048]{2,1,0:T(8,128)(2,1)}, bf16[64,512]{1,0:T(8,128)(2,1)}, bf16[512,384]{1,0:T(8,128)(2,1)}, bf16[448,512]{1,0:T(8,128)(2,1)}) custom-call(bf16[32,2048]{1,0:T(8,128)(2,1)} %bitcast.26, f32[1,2048]{1,0:T(1,128)} %bitcast.28, bf16[512,128]{1,0:T(8,128)(2,1)} %wa_in.1, bf16[512,128]{1,0:T(8,128)(2,1)} %wk_in.1, ...), custom_call_target="tpu_custom_call" | custom-call | flops 536870912 | bytes 4194304 | tf_op jit(solution)/shard_map/pallas_call | solution.py:57
  3.3 4.4 %all-to-all-start = ((bf16[8,32,2048]{2,1,0:T(8,128)(2,1)}), bf16[8,32,2048]{2,1,0:T(8,128)(2,1)S(1)}, u32[]{:S(2)}, u32[]{:S(2)}) async-start(bf16[8,32,2048]{2,1,0:T(8,128)(2,1)} %get-tuple-element.20), calls=%async_computation | async-start | bytes 2097152 | tf_op jit(solution)/shard_map/all_to_all | solution.py:462
  7.8 5.1 %collective-permute-start.5 = (bf16[64,512]{1,0:T(8,128)(2,1)S(1)}, bf16[64,512]{1,0:T(8,128)(2,1)S(1)}, u32[]{:S(2)}, u32[]{:S(2)}) collective-permute-start(bf16[64,512]{1,0:T(8,128)(2,1)S(1)} %copy-done.16), channel_id=1, source_target_pairs={{0,16},{8,24},{16,0},{24,8},{1,17},{9,25},{17,1},{25,9},{2,18},{10... | collective-permute-start | bytes 196616 | tf_op jit(solution)/shard_map/ppermute | solution.py:467
  12.9 3.0 %collective-permute-start.4 = (bf16[64,512]{1,0:T(8,128)(2,1)S(1)}, bf16[64,512]{1,0:T(8,128)(2,1)S(1)}, u32[]{:S(2)}, u32[]{:S(2)}) collective-permute-start(bf16[64,512]{1,0:T(8,128)(2,1)S(1)} %copy-done.16), channel_id=1, source_target_pairs={{0,24},{8,0},{16,8},{24,16},{1,25},{9,1},{17,9},{25,17},{2,26},{10... | collective-permute-start | bytes 196616 | tf_op jit(solution)/shard_map/ppermute | solution.py:467
  15.9 2.9 %collective-permute-start.3 = (bf16[64,512]{1,0:T(8,128)(2,1)S(1)}, bf16[64,512]{1,0:T(8,128)(2,1)S(1)}, u32[]{:S(2)}, u32[]{:S(2)}) collective-permute-start(bf16[64,512]{1,0:T(8,128)(2,1)S(1)} %copy-done.16), channel_id=1, source_target_pairs={{0,8},{8,16},{16,24},{24,0},{1,9},{9,17},{17,25},{25,1},{2,10},{10... | collective-permute-start | bytes 196616 | tf_op jit(solution)/shard_map/ppermute | solution.py:467
  19.1 4.2 %collective-permute-done.3.w1 = bf16[64,512]{1,0:T(8,128)(2,1)S(1)} collective-permute-done((bf16[64,512]{1,0:T(8,128)(2,1)S(1)}, bf16[64,512]{1,0:T(8,128)(2,1)S(1)}, u32[]{:S(2)}, u32[]{:S(2)}) %collective-permute-start.3) | collective-permute-done | bytes 65568 | tf_op jit(solution)/shard_map/ppermute | solution.py:467
  24.9 8.9 %all-to-all-start.1 = ((bf16[16,40,256]{2,1,0:T(8,128)(2,1)}), bf16[16,40,256]{2,1,0:T(8,128)(2,1)}, u32[]{:S(2)}, u32[]{:S(2)}) async-start(bf16[16,40,256]{2,1,0:T(8,128)(2,1)} %shard_map.259), calls=%async_computation.1 | async-start | bytes 655360 | tf_op jit(solution)/shard_map/all_to_all | solution.py:462
  33.8 5.1 %collective-permute-start.8 = (bf16[512,384]{1,0:T(8,128)(2,1)S(1)}, bf16[512,384]{1,0:T(8,128)(2,1)S(1)}, u32[]{:S(2)}, u32[]{:S(2)}) collective-permute-start(bf16[512,384]{1,0:T(8,128)(2,1)S(1)} %copy-done.23), channel_id=1, source_target_pairs={{0,16},{8,24},{16,0},{24,8},{1,17},{9,25},{17,1},{25,9},{2,18},{10... | collective-permute-start | bytes 1179656 | tf_op jit(solution)/shard_map/ppermute | solution.py:467
  38.9 3.0 %collective-permute-start.7 = (bf16[512,384]{1,0:T(8,128)(2,1)S(1)}, bf16[512,384]{1,0:T(8,128)(2,1)S(1)}, u32[]{:S(2)}, u32[]{:S(2)}) collective-permute-start(bf16[512,384]{1,0:T(8,128)(2,1)S(1)} %copy-done.23), channel_id=1, source_target_pairs={{0,24},{8,0},{16,8},{24,16},{1,25},{9,1},{17,9},{25,17},{2,26},{10... | collective-permute-start | bytes 1179656 | tf_op jit(solution)/shard_map/ppermute | solution.py:467
  41.9 2.9 %collective-permute-start.6 = (bf16[512,384]{1,0:T(8,128)(2,1)S(1)}, bf16[512,384]{1,0:T(8,128)(2,1)S(1)}, u32[]{:S(2)}, u32[]{:S(2)}) collective-permute-start(bf16[512,384]{1,0:T(8,128)(2,1)S(1)} %copy-done.23), channel_id=1, source_target_pairs={{0,8},{8,16},{16,24},{24,0},{1,9},{9,17},{17,25},{25,1},{2,10},{10... | collective-permute-start | bytes 1179656 | tf_op jit(solution)/shard_map/ppermute | solution.py:467
  44.8 4.4 %collective-permute-done.8.w3 = bf16[512,384]{1,0:T(8,128)(2,1)S(1)} collective-permute-done((bf16[512,384]{1,0:T(8,128)(2,1)S(1)}, bf16[512,384]{1,0:T(8,128)(2,1)S(1)}, u32[]{:S(2)}, u32[]{:S(2)}) %collective-permute-start.8) | collective-permute-done | bytes 393248 | tf_op jit(solution)/shard_map/ppermute | solution.py:467
  49.2 6.8 %collective-permute-done.7.w2 = bf16[512,384]{1,0:T(8,128)(2,1)S(1)} collective-permute-done((bf16[512,384]{1,0:T(8,128)(2,1)S(1)}, bf16[512,384]{1,0:T(8,128)(2,1)S(1)}, u32[]{:S(2)}, u32[]{:S(2)}) %collective-permute-start.7) | collective-permute-done | bytes 393248 | tf_op jit(solution)/shard_map/ppermute | solution.py:467
  56.9 12.8 %shard_map.260 = (f32[256,128]{1,0:T(8,128)}, f32[256,128]{1,0:T(8,128)}, f32[256,128]{1,0:T(8,128)}, bf16[16,2,64,128]{3,2,1,0:T(8,128)(2,1)}) custom-call(bf16[256,2048]{1,0:T(8,128)(2,1)} %bitcast.17, bf16[512,384]{1,0:T(8,128)(2,1)} %get-tuple-element.24.w0, bf16[512,384]{1,0:T(8,128)(2,1)} %copy-done.26, bf16[512,384]{1,0:T(8,128)(2,1)} %copy-done.25, ...), custom_call_target="tpu_custom_call" | custom-call | flops 8589934592 | bytes 4194304 | tf_op jit(solution)/shard_map/pallas_call | solution.py:57
  69.8 3.8 %collective-permute-start.11 = (bf16[16,40,256]{2,1,0:T(8,128)(2,1)}, bf16[16,40,256]{2,1,0:T(8,128)(2,1)S(1)}, u32[]{:S(2)}, u32[]{:S(2)}) collective-permute-start(bf16[16,40,256]{2,1,0:T(8,128)(2,1)} %all-to-all-done.1.own), channel_id=1, source_target_pairs={{0,4},{1,5},{2,6},{3,7},{4,0},{5,1},{6,2},{7,3},{8,12},{9,13},{10,... | collective-permute-start | bytes 983048 | tf_op jit(solution)/shard_map/ppermute | solution.py:545
  73.6 3.5 %collective-permute-start.10 = (bf16[16,40,256]{2,1,0:T(8,128)(2,1)}, bf16[16,40,256]{2,1,0:T(8,128)(2,1)S(1)}, u32[]{:S(2)}, u32[]{:S(2)}) collective-permute-start(bf16[16,40,256]{2,1,0:T(8,128)(2,1)} %all-to-all-done.1.own), channel_id=1, source_target_pairs={{0,6},{1,7},{2,0},{3,1},{4,2},{5,3},{6,4},{7,5},{8,14},{9,15},{10,... | collective-permute-start | bytes 983048 | tf_op jit(solution)/shard_map/ppermute | solution.py:545
  79.5 4.4 %collective-permute-done.11.far = bf16[16,40,256]{2,1,0:T(8,128)(2,1)S(1)} collective-permute-done((bf16[16,40,256]{2,1,0:T(8,128)(2,1)}, bf16[16,40,256]{2,1,0:T(8,128)(2,1)S(1)}, u32[]{:S(2)}, u32[]{:S(2)}) %collective-permute-start.11) | collective-permute-done | bytes 327712 | tf_op jit(solution)/shard_map/ppermute | solution.py:545
  83.8 4.4 %collective-permute-done.10.right = bf16[16,40,256]{2,1,0:T(8,128)(2,1)S(1)} collective-permute-done((bf16[16,40,256]{2,1,0:T(8,128)(2,1)}, bf16[16,40,256]{2,1,0:T(8,128)(2,1)S(1)}, u32[]{:S(2)}, u32[]{:S(2)}) %collective-permute-start.10) | collective-permute-done | bytes 327712 | tf_op jit(solution)/shard_map/ppermute | solution.py:545
  92.6 12.0 %all-to-all-start.2 = ((bf16[16,2,64,128]{3,2,1,0:T(8,128)(2,1)}), bf16[16,2,64,128]{3,2,1,0:T(8,128)(2,1)S(1)}, u32[]{:S(2)}, u32[]{:S(2)}) async-start(bf16[16,2,64,128]{3,2,1,0:T(8,128)(2,1)} %get-tuple-element.34), calls=%async_computation.2 | async-start | bytes 1048576 | tf_op jit(solution)/shard_map/all_to_all | solution.py:462
  104.6 5.1 %collective-permute-start.2 = (bf16[448,512]{1,0:T(8,128)(2,1)}, bf16[448,512]{1,0:T(8,128)(2,1)S(1)}, u32[]{:S(2)}, u32[]{:S(2)}) collective-permute-start(bf16[448,512]{1,0:T(8,128)(2,1)} %get-tuple-element.21.w0.o0), channel_id=1, source_target_pairs={{0,16},{8,24},{16,0},{24,8},{1,17},{9,25},{17,1},{25,9},{2,18},{10... | collective-permute-start | bytes 1376264 | tf_op jit(solution)/shard_map/ppermute | solution.py:467
  109.7 3.2 %collective-permute-start.1 = (bf16[448,512]{1,0:T(8,128)(2,1)}, bf16[448,512]{1,0:T(8,128)(2,1)S(1)}, u32[]{:S(2)}, u32[]{:S(2)}) collective-permute-start(bf16[448,512]{1,0:T(8,128)(2,1)} %get-tuple-element.21.w0.o0), channel_id=1, source_target_pairs={{0,24},{8,0},{16,8},{24,16},{1,25},{9,1},{17,9},{25,17},{2,26},{10... | collective-permute-start | bytes 1376264 | tf_op jit(solution)/shard_map/ppermute | solution.py:467
  115.6 6.0 %collective-permute-done.2.w3.o3 = bf16[448,512]{1,0:T(8,128)(2,1)S(1)} collective-permute-done((bf16[448,512]{1,0:T(8,128)(2,1)}, bf16[448,512]{1,0:T(8,128)(2,1)S(1)}, u32[]{:S(2)}, u32[]{:S(2)}) %collective-permute-start.2) | collective-permute-done | bytes 458784 | tf_op jit(solution)/shard_map/ppermute | solution.py:467
  121.6 9.5 %collective-permute-done.1.w2.o2 = bf16[448,512]{1,0:T(8,128)(2,1)S(1)} collective-permute-done((bf16[448,512]{1,0:T(8,128)(2,1)}, bf16[448,512]{1,0:T(8,128)(2,1)S(1)}, u32[]{:S(2)}, u32[]{:S(2)}) %collective-permute-start.1) | collective-permute-done | bytes 458784 | tf_op jit(solution)/shard_map/ppermute | solution.py:467
  133.2 8.0 %shard_map.262 = (bf16[256,128]{1,0:T(8,128)(2,1)S(1)}, f32[2,256]{1,0:T(2,128)}) custom-call(bf16[2,256,128]{2,1,0:T(8,128)(2,1)S(1)} %get-tuple-element.22.q, bf16[4,16,40,256]{3,2,1,0:T(8,128)(2,1)S(1)} %shard_map.261.own, bf16[4,16,40,256]{3,2,1,0:T(8,128)(2,1)} %collective-permute-done.12.peer, bf16[256,256]{1,0:T(8,128)(2,1)S(1)} %get-tuple-element.27.w, ...), custom_call_target="tpu_custom_call" | custom-call | flops 8589934592 | bytes 4194304 | tf_op jit(solution)/shard_map/pallas_call | solution.py:57
  151.9 12.5 %all_to_all.20 = bf16[4,32,2048]{2,1,0:T(8,128)(2,1)S(1)} all-to-all(bf16[4,32,2048]{2,1,0:T(8,128)(2,1)S(1)} %bitcast.23), channel_id=1, replica_groups={{0,2,4,6},{1,3,5,7},{8,10,12,14},{9,11,13,15},{16,18,20,22},{17,19,21,2..., dimensions={0} | all-to-all | bytes 1048576 | tf_op jit(solution)/shard_map/all_to_all | solution.py:462
  (74 shorter events, 25.7 us)
Async XLA Ops:
  3.3 20.4 %all-to-all-start = ((bf16[8,32,2048]{2,1,0:T(8,128)(2,1)}), bf16[8,32,2048]{2,1,0:T(8,128)(2,1)S(1)}, u32[]{:S(2)}, u32[]{:S(2)}) async-start(bf16[8,32,2048]{2,1,0:T(8,128)(2,1)} %get-tuple-element.20), calls=%async_computation | async-start | bytes 2097152 | tf_op jit(solution)/shard_map/all_to_all | solution.py:462
  7.8 11.0 %collective-permute-start.5 = (bf16[64,512]{1,0:T(8,128)(2,1)S(1)}, bf16[64,512]{1,0:T(8,128)(2,1)S(1)}, u32[]{:S(2)}, u32[]{:S(2)}) collective-permute-start(bf16[64,512]{1,0:T(8,128)(2,1)S(1)} %copy-done.16), channel_id=1, source_target_pairs={{0,16},{8,24},{16,0},{24,8},{1,17},{9,25},{17,1},{25,9},{2,18},{10... | collective-permute-start | bytes 196616 | tf_op jit(solution)/shard_map/ppermute | solution.py:467
  12.9 6.2 %collective-permute-start.4 = (bf16[64,512]{1,0:T(8,128)(2,1)S(1)}, bf16[64,512]{1,0:T(8,128)(2,1)S(1)}, u32[]{:S(2)}, u32[]{:S(2)}) collective-permute-start(bf16[64,512]{1,0:T(8,128)(2,1)S(1)} %copy-done.16), channel_id=1, source_target_pairs={{0,24},{8,0},{16,8},{24,16},{1,25},{9,1},{17,9},{25,17},{2,26},{10... | collective-permute-start | bytes 196616 | tf_op jit(solution)/shard_map/ppermute | solution.py:467
  15.9 7.4 %collective-permute-start.3 = (bf16[64,512]{1,0:T(8,128)(2,1)S(1)}, bf16[64,512]{1,0:T(8,128)(2,1)S(1)}, u32[]{:S(2)}, u32[]{:S(2)}) collective-permute-start(bf16[64,512]{1,0:T(8,128)(2,1)S(1)} %copy-done.16), channel_id=1, source_target_pairs={{0,8},{8,16},{16,24},{24,0},{1,9},{9,17},{17,25},{25,1},{2,10},{10... | collective-permute-start | bytes 196616 | tf_op jit(solution)/shard_map/ppermute | solution.py:467
  24.9 44.8 %all-to-all-start.1 = ((bf16[16,40,256]{2,1,0:T(8,128)(2,1)}), bf16[16,40,256]{2,1,0:T(8,128)(2,1)}, u32[]{:S(2)}, u32[]{:S(2)}) async-start(bf16[16,40,256]{2,1,0:T(8,128)(2,1)} %shard_map.259), calls=%async_computation.1 | async-start | bytes 655360 | tf_op jit(solution)/shard_map/all_to_all | solution.py:462
  33.8 15.4 %collective-permute-start.8 = (bf16[512,384]{1,0:T(8,128)(2,1)S(1)}, bf16[512,384]{1,0:T(8,128)(2,1)S(1)}, u32[]{:S(2)}, u32[]{:S(2)}) collective-permute-start(bf16[512,384]{1,0:T(8,128)(2,1)S(1)} %copy-done.23), channel_id=1, source_target_pairs={{0,16},{8,24},{16,0},{24,8},{1,17},{9,25},{17,1},{25,9},{2,18},{10... | collective-permute-start | bytes 1179656 | tf_op jit(solution)/shard_map/ppermute | solution.py:467
  38.9 17.1 %collective-permute-start.7 = (bf16[512,384]{1,0:T(8,128)(2,1)S(1)}, bf16[512,384]{1,0:T(8,128)(2,1)S(1)}, u32[]{:S(2)}, u32[]{:S(2)}) collective-permute-start(bf16[512,384]{1,0:T(8,128)(2,1)S(1)} %copy-done.23), channel_id=1, source_target_pairs={{0,24},{8,0},{16,8},{24,16},{1,25},{9,1},{17,9},{25,17},{2,26},{10... | collective-permute-start | bytes 1179656 | tf_op jit(solution)/shard_map/ppermute | solution.py:467
  41.9 14.1 %collective-permute-start.6 = (bf16[512,384]{1,0:T(8,128)(2,1)S(1)}, bf16[512,384]{1,0:T(8,128)(2,1)S(1)}, u32[]{:S(2)}, u32[]{:S(2)}) collective-permute-start(bf16[512,384]{1,0:T(8,128)(2,1)S(1)} %copy-done.23), channel_id=1, source_target_pairs={{0,8},{8,16},{16,24},{24,0},{1,9},{9,17},{17,25},{25,1},{2,10},{10... | collective-permute-start | bytes 1179656 | tf_op jit(solution)/shard_map/ppermute | solution.py:467
  69.7 61.4 %copy-start.1 = (bf16[8,32,2048]{2,1,0:T(8,128)(2,1)S(1)}, bf16[8,32,2048]{2,1,0:T(8,128)(2,1)}, u32[]{:S(2)}) copy-start(bf16[8,32,2048]{2,1,0:T(8,128)(2,1)} %copy-done) | copy-start | bytes 3145732
  69.7 61.4 %copy-start.2 = (f32[16,32,256]{2,1,0:T(8,128)S(1)}, f32[16,32,256]{2,1,0:T(8,128)}, u32[]{:S(2)}) copy-start(f32[16,32,256]{2,1,0:T(8,128)} %constant.5.clone.table) | copy-start | bytes 1572868
  69.7 61.4 %copy-start.11 = (bf16[256,128]{1,0:T(8,128)(2,1)S(1)}, bf16[256,128]{1,0:T(8,128)(2,1)}, u32[]{:S(2)}) copy-start(bf16[256,128]{1,0:T(8,128)(2,1)} %wk_up.1) | copy-start | bytes 196612
  69.7 61.4 %copy-start.12 = (bf16[256,128]{1,0:T(8,128)(2,1)S(1)}, bf16[256,128]{1,0:T(8,128)(2,1)}, u32[]{:S(2)}) copy-start(bf16[256,128]{1,0:T(8,128)(2,1)} %wv_up.1) | copy-start | bytes 196612
  69.7 61.4 %copy-start.13 = (f32[256]{0:T(256)S(1)}, f32[256]{0:T(256)}, u32[]{:S(2)}) copy-start(f32[256]{0:T(256)} %param.31) | copy-start | bytes 3076
  69.8 61.4 %copy-start.14 = (f32[96]{0:T(128)S(1)}, f32[96]{0:T(128)}, u32[]{:S(2)}) copy-start(f32[96]{0:T(128)} %param.35) | copy-start | bytes 1156
  69.8 61.4 %copy-start.15 = (f32[96]{0:T(128)S(1)}, f32[96]{0:T(128)}, u32[]{:S(2)}) copy-start(f32[96]{0:T(128)} %param.34) | copy-start | bytes 1156
  69.8 14.0 %collective-permute-start.11 = (bf16[16,40,256]{2,1,0:T(8,128)(2,1)}, bf16[16,40,256]{2,1,0:T(8,128)(2,1)S(1)}, u32[]{:S(2)}, u32[]{:S(2)}) collective-permute-start(bf16[16,40,256]{2,1,0:T(8,128)(2,1)} %all-to-all-done.1.own), channel_id=1, source_target_pairs={{0,4},{1,5},{2,6},{3,7},{4,0},{5,1},{6,2},{7,3},{8,12},{9,13},{10,... | collective-permute-start | bytes 983048 | tf_op jit(solution)/shard_map/ppermute | solution.py:545
  73.6 14.6 %collective-permute-start.10 = (bf16[16,40,256]{2,1,0:T(8,128)(2,1)}, bf16[16,40,256]{2,1,0:T(8,128)(2,1)S(1)}, u32[]{:S(2)}, u32[]{:S(2)}) collective-permute-start(bf16[16,40,256]{2,1,0:T(8,128)(2,1)} %all-to-all-done.1.own), channel_id=1, source_target_pairs={{0,6},{1,7},{2,0},{3,1},{4,2},{5,3},{6,4},{7,5},{8,14},{9,15},{10,... | collective-permute-start | bytes 983048 | tf_op jit(solution)/shard_map/ppermute | solution.py:545
  77.1 12.5 %collective-permute-start.9 = (bf16[16,40,256]{2,1,0:T(8,128)(2,1)}, bf16[16,40,256]{2,1,0:T(8,128)(2,1)S(1)}, u32[]{:S(2)}, u32[]{:S(2)}) collective-permute-start(bf16[16,40,256]{2,1,0:T(8,128)(2,1)} %all-to-all-done.1.own), channel_id=1, source_target_pairs={{0,2},{1,3},{2,4},{3,5},{4,6},{5,7},{6,0},{7,1},{8,10},{9,11},{10,... | collective-permute-start | bytes 983048 | tf_op jit(solution)/shard_map/ppermute | solution.py:545
  90.7 42.5 %collective-permute-start.12 = (bf16[4,16,40,256]{3,2,1,0:T(8,128)(2,1)S(1)}, bf16[4,16,40,256]{3,2,1,0:T(8,128)(2,1)}, u32[]{:S(2)}, u32[]{:S(2)}) collective-permute-start(bf16[4,16,40,256]{3,2,1,0:T(8,128)(2,1)S(1)} %shard_map.261.own), channel_id=1, source_target_pairs={{0,1},{1,0},{2,3},{3,2},{4,5},{5,4},{6,7},{7,6},{8,9},{9,8},{10,11... | collective-permute-start | bytes 3932168 | tf_op jit(solution)/shard_map/ppermute | solution.py:471
  92.6 49.2 %all-to-all-start.2 = ((bf16[16,2,64,128]{3,2,1,0:T(8,128)(2,1)}), bf16[16,2,64,128]{3,2,1,0:T(8,128)(2,1)S(1)}, u32[]{:S(2)}, u32[]{:S(2)}) async-start(bf16[16,2,64,128]{3,2,1,0:T(8,128)(2,1)} %get-tuple-element.34), calls=%async_computation.2 | async-start | bytes 1048576 | tf_op jit(solution)/shard_map/all_to_all | solution.py:462
  104.6 17.0 %collective-permute-start.2 = (bf16[448,512]{1,0:T(8,128)(2,1)}, bf16[448,512]{1,0:T(8,128)(2,1)S(1)}, u32[]{:S(2)}, u32[]{:S(2)}) collective-permute-start(bf16[448,512]{1,0:T(8,128)(2,1)} %get-tuple-element.21.w0.o0), channel_id=1, source_target_pairs={{0,16},{8,24},{16,0},{24,8},{1,17},{9,25},{17,1},{25,9},{2,18},{10... | collective-permute-start | bytes 1376264 | tf_op jit(solution)/shard_map/ppermute | solution.py:467
  109.7 21.3 %collective-permute-start.1 = (bf16[448,512]{1,0:T(8,128)(2,1)}, bf16[448,512]{1,0:T(8,128)(2,1)S(1)}, u32[]{:S(2)}, u32[]{:S(2)}) collective-permute-start(bf16[448,512]{1,0:T(8,128)(2,1)} %get-tuple-element.21.w0.o0), channel_id=1, source_target_pairs={{0,24},{8,0},{16,8},{24,16},{1,25},{9,1},{17,9},{25,17},{2,26},{10... | collective-permute-start | bytes 1376264 | tf_op jit(solution)/shard_map/ppermute | solution.py:467
  113.0 18.1 %collective-permute-start = (bf16[448,512]{1,0:T(8,128)(2,1)}, bf16[448,512]{1,0:T(8,128)(2,1)S(1)}, u32[]{:S(2)}, u32[]{:S(2)}) collective-permute-start(bf16[448,512]{1,0:T(8,128)(2,1)} %get-tuple-element.21.w0.o0), channel_id=1, source_target_pairs={{0,8},{8,16},{16,24},{24,0},{1,9},{9,17},{17,25},{25,1},{2,10},{10... | collective-permute-start | bytes 1376264 | tf_op jit(solution)/shard_map/ppermute | solution.py:467
  148.0 3.8 %collective-permute-start.13 = (bf16[128,2048]{1,0:T(8,128)(2,1)S(1)}, bf16[128,2048]{1,0:T(8,128)(2,1)S(1)}, u32[]{:S(2)}, u32[]{:S(2)}) collective-permute-start(bf16[128,2048]{1,0:T(8,128)(2,1)S(1)} %get-tuple-element.36), channel_id=1, source_target_pairs={{0,1},{1,0},{2,3},{3,2},{4,5},{5,4},{6,7},{7,6},{8,9},{9,8},{10,11... | collective-permute-start | bytes 1572872 | tf_op jit(solution)/shard_map/ppermute | solution.py:471
  (20 other events, 88.5 us)

commit v10 on v9

--- a/solution.py
+++ b/solution.py
@@ -74,7 +74,7 @@
 
 def prepare_body(
     x_in, gain_in, wa_in, wk_in, wv_in, wq_in, wc_in, wr_in, oa_in, or_in,
-    xs, small, big, late, x, gain, wa, wk, wv, wq, wc, wr, oa, orr, turned_wc, arrived,
+    xs, big, late, x, gain, wa, wk, wv, wq, wc, wr, oa, orr, turned_wc, arrived,
 ):
     pairs = [
         (x_in, x), (gain_in, gain), (wc_in, wc), (wr_in, wr), (wa_in, wa), (wk_in, wk),
@@ -94,13 +94,17 @@
     copies[3].wait()
     turned_wc[...] = wc[...].astype(F32).T
     start = pl.multiple_of(lax.axis_index("tp") * 32, 32)
-    small[0:32] = turned_wc[pl.ds(start, 32), :].astype(BF16)
-    small[32:64] = wr[...]
+    small = jnp.concatenate([turned_wc[pl.ds(start, 32), :], wr[...].astype(F32)], axis=0)
+    big[512:576] = small[:, 0:384].astype(BF16)
+    last = jnp.concatenate([small[:, 384:512], jnp.zeros((8, 128), F32)], axis=0)
+    big[576:600] = jnp.concatenate([last[24 * i : 24 * i + 24] for i in range(3)], axis=1).astype(
+        BF16
+    )
     for copy in copies[4:]:
         copy.wait()
-    big[:, 0:128] = wa[...]
-    big[:, 128:256] = wk[...]
-    big[:, 256:384] = wv[...]
+    big[0:512, 0:128] = wa[...]
+    big[0:512, 128:256] = wk[...]
+    big[0:512, 256:384] = wv[...]
     late[0:192] = wq[...]
     late[192:320] = oa[...]
     late[320:448] = orr[...]
@@ -109,8 +113,7 @@
 def prepare(*args):
     outs = [
         jax.ShapeDtypeStruct((8, 32, 2048), BF16),
-        jax.ShapeDtypeStruct((64, 512), BF16),
-        jax.ShapeDtypeStruct((512, 384), BF16),
+        jax.ShapeDtypeStruct((600, 384), BF16),
         jax.ShapeDtypeStruct((448, 512), BF16),
     ]
     scratch = [pltpu.VMEM(a.shape, a.dtype) for a in args]
@@ -134,10 +137,21 @@
     return pl.ds(pl.multiple_of(shard * 512, 512), 512)
 
 
-def latents_body(x, w0, w1, w2, w3, pay):
+def latents_body(x, w0, w1, w2, w3, pay, held, arrived):
+    copies = [
+        pltpu.make_async_copy(w.at[pl.ds(512, 88)], held.at[k], arrived.at[k])
+        for k, w in enumerate((w0, w1, w2, w3))
+    ]
+    for copy in copies:
+        copy.start()
+    for copy in copies:
+        copy.wait()
     t = jnp.zeros((64, ROWS), F32)
-    for k, w in enumerate((w0, w1, w2, w3)):
-        t += dot(w[...], x[:, columns(k)], NT)
+    for k in range(4):
+        w = held[k].astype(F32)
+        last = jnp.concatenate([w[64:88, 128 * i : 128 * i + 128] for i in range(3)], axis=0)
+        w = jnp.concatenate([w[0:64], last[0:64]], axis=1).astype(BF16)
+        t += dot(w, x[:, columns(k)], NT)
     tp = lax.axis_index("tp")
     group = jnp.zeros((8, ROWS), F32)
     for g in range(4):
@@ -150,7 +164,8 @@
 
 def latents(*args):
     outs = jax.ShapeDtypeStruct((16, 40, ROWS), BF16)
-    return call(latents_body, outs, args, 1 << 29, limit=40)
+    scratch = [pltpu.VMEM((4, 88, 384), BF16), pltpu.SemaphoreType.DMA((4,))]
+    return call(latents_body, outs, args, 1 << 29, scratch, [VMEM] + [HBM] * 4, 40)
 
 
 def queries_body(
@@ -204,7 +219,7 @@
     lane = iota((1, 128), 1)
     y = jnp.zeros((ROWS, 384), F32)
     for k, w in enumerate((w0, w1, w2, w3)):
-        y += dot(x[:, columns(k)], w[...])
+        y += dot(x[:, columns(k)], w[0:512])
     y = y.astype(BF16).astype(F32)
     dlow = jnp.tanh(dot(x[...], fd[...]).astype(BF16).astype(F32)).astype(BF16)
     rlow = dot(x[...], fa[...]).astype(BF16)
@@ -506,7 +521,7 @@
     wo_att,
     wo_rec,
 ):
-    xs, small, big, late = prepare(
+    xs, big, late = prepare(
         entering[0],
         entering_gain.reshape(1, 2048),
         w_accept,
@@ -519,12 +534,11 @@
         wo_rec,
     )
     normed = exchanged(xs, "tp").reshape(ROWS, 2048)
-    smalls = around(small)
     bigs = around(big)
     lates = around(late)
 
     table = jnp.asarray(turn_table())
-    pay = latents(normed, *smalls)
+    pay = latents(normed, *bigs)
     lat = exchanged(pay, "sp")
 
     free, along, bonus, state = recur(

time: 168 us -> 159 us (0.946)
  starting transfers between devices: 71.7 us -> 57.2 us
  waiting for transfers between devices: 43.7 us -> 49.5 us
    ppermute x9 -> x6, starting transfers between devices: 32.8 us -> 21.9 us  [around(): return [value] + [lax.ppermute(value, 'fs', move) for move in moves]]
    all_to_all x3, waiting for transfers between devices: 0.48 us -> 9.08 us  [exchanged(): lax.all_to_all(copies, axis, 0, 0, axis_index_groups=groups, tiled=True)]
    all_to_all x3, starting transfers between devices: 25.3 us -> 20.5 us  [exchanged(): lax.all_to_all(copies, axis, 0, 0, axis_index_groups=groups, tiled=True)]
    ppermute x3, waiting for transfers between devices: 10.1 us -> 7.61 us  [shards(): lax.ppermute(lat, 'tp', [(i, (i + by) % 8) for i in range(8)])]
    unnamed x54 -> x48, local copies, waits for them, and re-layouts: 6.64 us -> 5.21 us
    ppermute x9 -> x6, waiting for transfers between devices: 31.2 us -> 30.9 us  [around(): return [value] + [lax.ppermute(value, 'fs', move) for move in moves]]
  transfers between devices with their start and end apart: 17 -> 14, of which waited for: 11 -> 9; matrix products, arithmetic and copies ran while one was open for 0% -> 0% of each run, Pallas kernels for 13% -> 14%
where the time goes in v10:
time: 159 us; the launch traced here: 156 us
  starting transfers between devices  57.2 us (36%)
  waiting for transfers between devices  49.5 us (31%)
  Pallas kernels  29.3 us (18%)
  blocking collectives  13.3 us (8%)
  local copies, waits for them, and re-layouts  5.21 us (3%)
    ppermute x6, waiting for transfers between devices, around(): return [value] + [lax.ppermute(value, 'fs', move) for move in moves]  30.9 us
    pallas_call x7, Pallas kernels, call(): pl.pallas_call(body, out_shape=outs, in_specs=specs or [VMEM] * len(args)...  29.3 us
    ppermute x6, starting transfers between devices, around(): return [value] + [lax.ppermute(value, 'fs', move) for move in moves]  21.9 us
    all_to_all x3, starting transfers between devices, exchanged(): lax.all_to_all(copies, axis, 0, 0, axis_index_groups=groups, tiled=True)  20.5 us
    all_to_all x1, blocking collectives, exchanged(): lax.all_to_all(copies, axis, 0, 0, axis_index_groups=groups, tiled=True)  13.3 us
    ppermute x3, starting transfers between devices, shards(): lax.ppermute(lat, 'tp', [(i, (i + by) % 8) for i in range(8)])  10.9 us
    all_to_all x3, waiting for transfers between devices, exchanged(): lax.all_to_all(copies, axis, 0, 0, axis_index_groups=groups, tiled=True)  9.08 us
    ppermute x3, waiting for transfers between devices, shards(): lax.ppermute(lat, 'tp', [(i, (i + by) % 8) for i in range(8)])  7.61 us
  transfers between devices with their start and end apart: 14, of which 9 were waited for; matrix products, arithmetic and copies ran while one was open for 0% of the time, Pallas kernels for 14%

profile of v10, /device:TPU:480, one launch (start us, length us, event | category | flops | bytes accessed | tf_op | source)
XLA Modules:
  0.0 156.3 jit_solution(5540269846285161902)
XLA Ops:
  0.6 2.7 %shard_map.257 = (bf16[8,32,2048]{2,1,0:T(8,128)(2,1)}, bf16[600,384]{1,0:T(8,128)(2,1)}, bf16[448,512]{1,0:T(8,128)(2,1)}) custom-call(bf16[32,2048]{1,0:T(8,128)(2,1)} %bitcast.26, f32[1,2048]{1,0:T(1,128)} %bitcast.28, bf16[512,128]{1,0:T(8,128)(2,1)} %wa_in.1, bf16[512,128]{1,0:T(8,128)(2,1)} %wk_in.1, bf16[512,128]{1,0:T(8,128)(2,1)} %wv_in.1, ...), custom_call_target="tpu_custom_call" | custom-call | flops 536870912 | bytes 4194304 | tf_op jit(solution)/shard_map/pallas_call | solution.py:57
  3.3 4.4 %all-to-all-start = ((bf16[8,32,2048]{2,1,0:T(8,128)(2,1)}), bf16[8,32,2048]{2,1,0:T(8,128)(2,1)S(1)}, u32[]{:S(2)}, u32[]{:S(2)}) async-start(bf16[8,32,2048]{2,1,0:T(8,128)(2,1)} %get-tuple-element.19), calls=%async_computation | async-start | bytes 2097152 | tf_op jit(solution)/shard_map/all_to_all | solution.py:477
  7.8 5.1 %collective-permute-start.5 = (bf16[600,384]{1,0:T(8,128)(2,1)S(1)}, bf16[600,384]{1,0:T(8,128)(2,1)S(1)}, u32[]{:S(2)}, u32[]{:S(2)}) collective-permute-start(bf16[600,384]{1,0:T(8,128)(2,1)S(1)} %copy-done.3), channel_id=1, source_target_pairs={{0,16},{8,24},{16,0},{24,8},{1,17},{9,25},{17,1},{25,9},{2,18},{10... | collective-permute-start | bytes 1382408 | tf_op jit(solution)/shard_map/ppermute | solution.py:482
  12.9 3.0 %collective-permute-start.4 = (bf16[600,384]{1,0:T(8,128)(2,1)S(1)}, bf16[600,384]{1,0:T(8,128)(2,1)S(1)}, u32[]{:S(2)}, u32[]{:S(2)}) collective-permute-start(bf16[600,384]{1,0:T(8,128)(2,1)S(1)} %copy-done.3), channel_id=1, source_target_pairs={{0,24},{8,0},{16,8},{24,16},{1,25},{9,1},{17,9},{25,17},{2,26},{10... | collective-permute-start | bytes 1382408 | tf_op jit(solution)/shard_map/ppermute | solution.py:482
  15.9 2.9 %collective-permute-start.3 = (bf16[600,384]{1,0:T(8,128)(2,1)S(1)}, bf16[600,384]{1,0:T(8,128)(2,1)S(1)}, u32[]{:S(2)}, u32[]{:S(2)}) collective-permute-start(bf16[600,384]{1,0:T(8,128)(2,1)S(1)} %copy-done.3), channel_id=1, source_target_pairs={{0,8},{8,16},{16,24},{24,0},{1,9},{9,17},{17,25},{25,1},{2,10},{10... | collective-permute-start | bytes 1382408 | tf_op jit(solution)/shard_map/ppermute | solution.py:482
  18.8 5.9 %collective-permute-done.5.w3 = bf16[600,384]{1,0:T(8,128)(2,1)S(1)} collective-permute-done((bf16[600,384]{1,0:T(8,128)(2,1)S(1)}, bf16[600,384]{1,0:T(8,128)(2,1)S(1)}, u32[]{:S(2)}, u32[]{:S(2)}) %collective-permute-start.5) | collective-permute-done | bytes 460832 | tf_op jit(solution)/shard_map/ppermute | solution.py:482
  24.7 9.7 %collective-permute-done.4.w2 = bf16[600,384]{1,0:T(8,128)(2,1)S(1)} collective-permute-done((bf16[600,384]{1,0:T(8,128)(2,1)S(1)}, bf16[600,384]{1,0:T(8,128)(2,1)S(1)}, u32[]{:S(2)}, u32[]{:S(2)}) %collective-permute-start.4) | collective-permute-done | bytes 460832 | tf_op jit(solution)/shard_map/ppermute | solution.py:482
  36.1 8.9 %all-to-all-start.1 = ((bf16[16,40,256]{2,1,0:T(8,128)(2,1)}), bf16[16,40,256]{2,1,0:T(8,128)(2,1)}, u32[]{:S(2)}, u32[]{:S(2)}) async-start(bf16[16,40,256]{2,1,0:T(8,128)(2,1)} %shard_map.259), calls=%async_computation.1 | async-start | bytes 655360 | tf_op jit(solution)/shard_map/all_to_all | solution.py:477
  44.9 12.9 %shard_map.260 = (f32[256,128]{1,0:T(8,128)}, f32[256,128]{1,0:T(8,128)}, f32[256,128]{1,0:T(8,128)}, bf16[16,2,64,128]{3,2,1,0:T(8,128)(2,1)}) custom-call(bf16[256,2048]{1,0:T(8,128)(2,1)} %bitcast.17, bf16[600,384]{1,0:T(8,128)(2,1)} %get-tuple-element.22.w0, bf16[600,384]{1,0:T(8,128)(2,1)} %copy-done.6, bf16[600,384]{1,0:T(8,128)(2,1)} %copy-done.5, ...), custom_call_target="tpu_custom_call" | custom-call | flops 8589934592 | bytes 4194304 | tf_op jit(solution)/shard_map/pallas_call | solution.py:57
  57.8 9.1 %all-to-all-done.1.own = bf16[16,40,256]{2,1,0:T(8,128)(2,1)} async-done(((bf16[16,40,256]{2,1,0:T(8,128)(2,1)}), bf16[16,40,256]{2,1,0:T(8,128)(2,1)}, u32[]{:S(2)}, u32[]{:S(2)}) %all-to-all-start.1) | async-done | bytes 327712 | tf_op jit(solution)/shard_map/all_to_all | solution.py:477
  66.9 5.1 %collective-permute-start.8 = (bf16[16,40,256]{2,1,0:T(8,128)(2,1)}, bf16[16,40,256]{2,1,0:T(8,128)(2,1)S(1)}, u32[]{:S(2)}, u32[]{:S(2)}) collective-permute-start(bf16[16,40,256]{2,1,0:T(8,128)(2,1)} %all-to-all-done.1.own), channel_id=1, source_target_pairs={{0,4},{1,5},{2,6},{3,7},{4,0},{5,1},{6,2},{7,3},{8,12},{9,13},{10,... | collective-permute-start | bytes 983048 | tf_op jit(solution)/shard_map/ppermute | solution.py:559
  72.0 3.1 %collective-permute-start.7 = (bf16[16,40,256]{2,1,0:T(8,128)(2,1)}, bf16[16,40,256]{2,1,0:T(8,128)(2,1)S(1)}, u32[]{:S(2)}, u32[]{:S(2)}) collective-permute-start(bf16[16,40,256]{2,1,0:T(8,128)(2,1)} %all-to-all-done.1.own), channel_id=1, source_target_pairs={{0,6},{1,7},{2,0},{3,1},{4,2},{5,3},{6,4},{7,5},{8,14},{9,15},{10,... | collective-permute-start | bytes 983048 | tf_op jit(solution)/shard_map/ppermute | solution.py:559
  75.1 2.8 %collective-permute-start.6 = (bf16[16,40,256]{2,1,0:T(8,128)(2,1)}, bf16[16,40,256]{2,1,0:T(8,128)(2,1)S(1)}, u32[]{:S(2)}, u32[]{:S(2)}) collective-permute-start(bf16[16,40,256]{2,1,0:T(8,128)(2,1)} %all-to-all-done.1.own), channel_id=1, source_target_pairs={{0,2},{1,3},{2,4},{3,5},{4,6},{5,7},{6,0},{7,1},{8,10},{9,11},{10,... | collective-permute-start | bytes 983048 | tf_op jit(solution)/shard_map/ppermute | solution.py:559
  77.9 2.1 %collective-permute-done.8.far = bf16[16,40,256]{2,1,0:T(8,128)(2,1)S(1)} collective-permute-done((bf16[16,40,256]{2,1,0:T(8,128)(2,1)}, bf16[16,40,256]{2,1,0:T(8,128)(2,1)S(1)}, u32[]{:S(2)}, u32[]{:S(2)}) %collective-permute-start.8) | collective-permute-done | bytes 327712 | tf_op jit(solution)/shard_map/ppermute | solution.py:559
  80.0 3.9 %collective-permute-done.7.right = bf16[16,40,256]{2,1,0:T(8,128)(2,1)S(1)} collective-permute-done((bf16[16,40,256]{2,1,0:T(8,128)(2,1)}, bf16[16,40,256]{2,1,0:T(8,128)(2,1)S(1)}, u32[]{:S(2)}, u32[]{:S(2)}) %collective-permute-start.7) | collective-permute-done | bytes 327712 | tf_op jit(solution)/shard_map/ppermute | solution.py:559
  88.5 7.2 %all-to-all-start.2 = ((bf16[16,2,64,128]{3,2,1,0:T(8,128)(2,1)}), bf16[16,2,64,128]{3,2,1,0:T(8,128)(2,1)S(1)}, u32[]{:S(2)}, u32[]{:S(2)}) async-start(bf16[16,2,64,128]{3,2,1,0:T(8,128)(2,1)} %get-tuple-element.32), calls=%async_computation.2 | async-start | bytes 1048576 | tf_op jit(solution)/shard_map/all_to_all | solution.py:477
  95.7 5.1 %collective-permute-start.2 = (bf16[448,512]{1,0:T(8,128)(2,1)}, bf16[448,512]{1,0:T(8,128)(2,1)S(1)}, u32[]{:S(2)}, u32[]{:S(2)}) collective-permute-start(bf16[448,512]{1,0:T(8,128)(2,1)} %get-tuple-element.20.w0.o0), channel_id=1, source_target_pairs={{0,16},{8,24},{16,0},{24,8},{1,17},{9,25},{17,1},{25,9},{2,18},{10... | collective-permute-start | bytes 1376264 | tf_op jit(solution)/shard_map/ppermute | solution.py:482
  100.8 2.9 %collective-permute-start.1 = (bf16[448,512]{1,0:T(8,128)(2,1)}, bf16[448,512]{1,0:T(8,128)(2,1)S(1)}, u32[]{:S(2)}, u32[]{:S(2)}) collective-permute-start(bf16[448,512]{1,0:T(8,128)(2,1)} %get-tuple-element.20.w0.o0), channel_id=1, source_target_pairs={{0,24},{8,0},{16,8},{24,16},{1,25},{9,1},{17,9},{25,17},{2,26},{10... | collective-permute-start | bytes 1376264 | tf_op jit(solution)/shard_map/ppermute | solution.py:482
  103.7 2.9 %collective-permute-start = (bf16[448,512]{1,0:T(8,128)(2,1)}, bf16[448,512]{1,0:T(8,128)(2,1)S(1)}, u32[]{:S(2)}, u32[]{:S(2)}) collective-permute-start(bf16[448,512]{1,0:T(8,128)(2,1)} %get-tuple-element.20.w0.o0), channel_id=1, source_target_pairs={{0,8},{8,16},{16,24},{24,0},{1,9},{9,17},{17,25},{25,1},{2,10},{10... | collective-permute-start | bytes 1376264 | tf_op jit(solution)/shard_map/ppermute | solution.py:482
  106.7 6.0 %collective-permute-done.2.w3.o3 = bf16[448,512]{1,0:T(8,128)(2,1)S(1)} collective-permute-done((bf16[448,512]{1,0:T(8,128)(2,1)}, bf16[448,512]{1,0:T(8,128)(2,1)S(1)}, u32[]{:S(2)}, u32[]{:S(2)}) %collective-permute-start.2) | collective-permute-done | bytes 458784 | tf_op jit(solution)/shard_map/ppermute | solution.py:482
  112.7 9.3 %collective-permute-done.1.w2.o2 = bf16[448,512]{1,0:T(8,128)(2,1)S(1)} collective-permute-done((bf16[448,512]{1,0:T(8,128)(2,1)}, bf16[448,512]{1,0:T(8,128)(2,1)S(1)}, u32[]{:S(2)}, u32[]{:S(2)}) %collective-permute-start.1) | collective-permute-done | bytes 458784 | tf_op jit(solution)/shard_map/ppermute | solution.py:482
  124.1 8.0 %shard_map.262 = (bf16[256,128]{1,0:T(8,128)(2,1)S(1)}, f32[2,256]{1,0:T(2,128)}) custom-call(bf16[2,256,128]{2,1,0:T(8,128)(2,1)S(1)} %get-tuple-element.21.q, bf16[4,16,40,256]{3,2,1,0:T(8,128)(2,1)S(1)} %shard_map.261.own, bf16[4,16,40,256]{3,2,1,0:T(8,128)(2,1)} %collective-permute-done.9.peer, bf16[256,256]{1,0:T(8,128)(2,1)S(1)} %get-tuple-element.25.w, ...), custom_call_target="tpu_custom_call" | custom-call | flops 8589934592 | bytes 4194304 | tf_op jit(solution)/shard_map/pallas_call | solution.py:57
  135.9 2.4 %shard_map.263 = (f32[128,2048]{1,0:T(8,128)S(1)}, bf16[128,2048]{1,0:T(8,128)(2,1)S(1)}) custom-call(bf16[256,128]{1,0:T(8,128)(2,1)S(1)} %get-tuple-element.28.att, f32[256,128]{1,0:T(8,128)S(1)} %copy-done.21, f32[256,128]{1,0:T(8,128)S(1)} %copy-done.22, f32[256,128]{1,0:T(8,128)S(1)} %copy-done.23, bf16[16,2,64,128]{3,2,1,0:T(8,128)(2,1)S(1)} %all-to-all-done.2.states, ...), custom_call_target="tpu_custom_call" | custom-call | flops 4294967296 | bytes 4194304 | tf_op jit(solution)/shard_map/pallas_call | solution.py:57
  142.3 13.3 %all_to_all.20 = bf16[4,32,2048]{2,1,0:T(8,128)(2,1)S(1)} all-to-all(bf16[4,32,2048]{2,1,0:T(8,128)(2,1)S(1)} %bitcast.23), channel_id=1, replica_groups={{0,2,4,6},{1,3,5,7},{8,10,12,14},{9,11,13,15},{16,18,20,22},{17,19,21,2..., dimensions={0} | all-to-all | bytes 1048576 | tf_op jit(solution)/shard_map/all_to_all | solution.py:477
  (62 shorter events, 16.7 us)
Async XLA Ops:
  3.3 31.1 %all-to-all-start = ((bf16[8,32,2048]{2,1,0:T(8,128)(2,1)}), bf16[8,32,2048]{2,1,0:T(8,128)(2,1)S(1)}, u32[]{:S(2)}, u32[]{:S(2)}) async-start(bf16[8,32,2048]{2,1,0:T(8,128)(2,1)} %get-tuple-element.19), calls=%async_computation | async-start | bytes 2097152 | tf_op jit(solution)/shard_map/all_to_all | solution.py:477
  7.8 16.9 %collective-permute-start.5 = (bf16[600,384]{1,0:T(8,128)(2,1)S(1)}, bf16[600,384]{1,0:T(8,128)(2,1)S(1)}, u32[]{:S(2)}, u32[]{:S(2)}) collective-permute-start(bf16[600,384]{1,0:T(8,128)(2,1)S(1)} %copy-done.3), channel_id=1, source_target_pairs={{0,16},{8,24},{16,0},{24,8},{1,17},{9,25},{17,1},{25,9},{2,18},{10... | collective-permute-start | bytes 1382408 | tf_op jit(solution)/shard_map/ppermute | solution.py:482
  12.9 21.5 %collective-permute-start.4 = (bf16[600,384]{1,0:T(8,128)(2,1)S(1)}, bf16[600,384]{1,0:T(8,128)(2,1)S(1)}, u32[]{:S(2)}, u32[]{:S(2)}) collective-permute-start(bf16[600,384]{1,0:T(8,128)(2,1)S(1)} %copy-done.3), channel_id=1, source_target_pairs={{0,24},{8,0},{16,8},{24,16},{1,25},{9,1},{17,9},{25,17},{2,26},{10... | collective-permute-start | bytes 1382408 | tf_op jit(solution)/shard_map/ppermute | solution.py:482
  15.9 18.5 %collective-permute-start.3 = (bf16[600,384]{1,0:T(8,128)(2,1)S(1)}, bf16[600,384]{1,0:T(8,128)(2,1)S(1)}, u32[]{:S(2)}, u32[]{:S(2)}) collective-permute-start(bf16[600,384]{1,0:T(8,128)(2,1)S(1)} %copy-done.3), channel_id=1, source_target_pairs={{0,8},{8,16},{16,24},{24,0},{1,9},{9,17},{17,25},{25,1},{2,10},{10... | collective-permute-start | bytes 1382408 | tf_op jit(solution)/shard_map/ppermute | solution.py:482
  24.7 11.3 %copy-start.4 = (bf16[600,384]{1,0:T(8,128)(2,1)}, bf16[600,384]{1,0:T(8,128)(2,1)S(1)}, u32[]{:S(2)}) copy-start(bf16[600,384]{1,0:T(8,128)(2,1)S(1)} %collective-permute-done.5.w3) | copy-start | bytes 1382404
  36.1 30.8 %all-to-all-start.1 = ((bf16[16,40,256]{2,1,0:T(8,128)(2,1)}), bf16[16,40,256]{2,1,0:T(8,128)(2,1)}, u32[]{:S(2)}, u32[]{:S(2)}) async-start(bf16[16,40,256]{2,1,0:T(8,128)(2,1)} %shard_map.259), calls=%async_computation.1 | async-start | bytes 655360 | tf_op jit(solution)/shard_map/all_to_all | solution.py:477
  66.9 55.1 %copy-start.1 = (bf16[8,32,2048]{2,1,0:T(8,128)(2,1)S(1)}, bf16[8,32,2048]{2,1,0:T(8,128)(2,1)}, u32[]{:S(2)}) copy-start(bf16[8,32,2048]{2,1,0:T(8,128)(2,1)} %copy-done) | copy-start | bytes 3145732
  66.9 55.1 %copy-start.2 = (f32[16,32,256]{2,1,0:T(8,128)S(1)}, f32[16,32,256]{2,1,0:T(8,128)}, u32[]{:S(2)}) copy-start(f32[16,32,256]{2,1,0:T(8,128)} %constant.5.clone.table) | copy-start | bytes 1572868
  66.9 55.1 %copy-start.15 = (bf16[256,128]{1,0:T(8,128)(2,1)S(1)}, bf16[256,128]{1,0:T(8,128)(2,1)}, u32[]{:S(2)}) copy-start(bf16[256,128]{1,0:T(8,128)(2,1)} %wk_up.1) | copy-start | bytes 196612
  66.9 55.1 %copy-start.16 = (bf16[256,128]{1,0:T(8,128)(2,1)S(1)}, bf16[256,128]{1,0:T(8,128)(2,1)}, u32[]{:S(2)}) copy-start(bf16[256,128]{1,0:T(8,128)(2,1)} %wv_up.1) | copy-start | bytes 196612
  66.9 55.1 %copy-start.17 = (f32[256]{0:T(256)S(1)}, f32[256]{0:T(256)}, u32[]{:S(2)}) copy-start(f32[256]{0:T(256)} %param.31) | copy-start | bytes 3076
  66.9 55.1 %copy-start.18 = (f32[96]{0:T(128)S(1)}, f32[96]{0:T(128)}, u32[]{:S(2)}) copy-start(f32[96]{0:T(128)} %param.35) | copy-start | bytes 1156
  66.9 55.1 %copy-start.19 = (f32[96]{0:T(128)S(1)}, f32[96]{0:T(128)}, u32[]{:S(2)}) copy-start(f32[96]{0:T(128)} %param.34) | copy-start | bytes 1156
  66.9 13.0 %collective-permute-start.8 = (bf16[16,40,256]{2,1,0:T(8,128)(2,1)}, bf16[16,40,256]{2,1,0:T(8,128)(2,1)S(1)}, u32[]{:S(2)}, u32[]{:S(2)}) collective-permute-start(bf16[16,40,256]{2,1,0:T(8,128)(2,1)} %all-to-all-done.1.own), channel_id=1, source_target_pairs={{0,4},{1,5},{2,6},{3,7},{4,0},{5,1},{6,2},{7,3},{8,12},{9,13},{10,... | collective-permute-start | bytes 983048 | tf_op jit(solution)/shard_map/ppermute | solution.py:559
  72.0 11.9 %collective-permute-start.7 = (bf16[16,40,256]{2,1,0:T(8,128)(2,1)}, bf16[16,40,256]{2,1,0:T(8,128)(2,1)S(1)}, u32[]{:S(2)}, u32[]{:S(2)}) collective-permute-start(bf16[16,40,256]{2,1,0:T(8,128)(2,1)} %all-to-all-done.1.own), channel_id=1, source_target_pairs={{0,6},{1,7},{2,0},{3,1},{4,2},{5,3},{6,4},{7,5},{8,14},{9,15},{10,... | collective-permute-start | bytes 983048 | tf_op jit(solution)/shard_map/ppermute | solution.py:559
  75.1 10.4 %collective-permute-start.6 = (bf16[16,40,256]{2,1,0:T(8,128)(2,1)}, bf16[16,40,256]{2,1,0:T(8,128)(2,1)S(1)}, u32[]{:S(2)}, u32[]{:S(2)}) collective-permute-start(bf16[16,40,256]{2,1,0:T(8,128)(2,1)} %all-to-all-done.1.own), channel_id=1, source_target_pairs={{0,2},{1,3},{2,4},{3,5},{4,6},{5,7},{6,0},{7,1},{8,10},{9,11},{10,... | collective-permute-start | bytes 983048 | tf_op jit(solution)/shard_map/ppermute | solution.py:559
  86.6 37.4 %collective-permute-start.9 = (bf16[4,16,40,256]{3,2,1,0:T(8,128)(2,1)S(1)}, bf16[4,16,40,256]{3,2,1,0:T(8,128)(2,1)}, u32[]{:S(2)}, u32[]{:S(2)}) collective-permute-start(bf16[4,16,40,256]{3,2,1,0:T(8,128)(2,1)S(1)} %shard_map.261.own), channel_id=1, source_target_pairs={{0,1},{1,0},{2,3},{3,2},{4,5},{5,4},{6,7},{7,6},{8,9},{9,8},{10,11... | collective-permute-start | bytes 3932168 | tf_op jit(solution)/shard_map/ppermute | solution.py:486
  88.5 43.5 %all-to-all-start.2 = ((bf16[16,2,64,128]{3,2,1,0:T(8,128)(2,1)}), bf16[16,2,64,128]{3,2,1,0:T(8,128)(2,1)S(1)}, u32[]{:S(2)}, u32[]{:S(2)}) async-start(bf16[16,2,64,128]{3,2,1,0:T(8,128)(2,1)} %get-tuple-element.32), calls=%async_computation.2 | async-start | bytes 1048576 | tf_op jit(solution)/shard_map/all_to_all | solution.py:477
  95.7 17.0 %collective-permute-start.2 = (bf16[448,512]{1,0:T(8,128)(2,1)}, bf16[448,512]{1,0:T(8,128)(2,1)S(1)}, u32[]{:S(2)}, u32[]{:S(2)}) collective-permute-start(bf16[448,512]{1,0:T(8,128)(2,1)} %get-tuple-element.20.w0.o0), channel_id=1, source_target_pairs={{0,16},{8,24},{16,0},{24,8},{1,17},{9,25},{17,1},{25,9},{2,18},{10... | collective-permute-start | bytes 1376264 | tf_op jit(solution)/shard_map/ppermute | solution.py:482
  100.8 21.1 %collective-permute-start.1 = (bf16[448,512]{1,0:T(8,128)(2,1)}, bf16[448,512]{1,0:T(8,128)(2,1)S(1)}, u32[]{:S(2)}, u32[]{:S(2)}) collective-permute-start(bf16[448,512]{1,0:T(8,128)(2,1)} %get-tuple-element.20.w0.o0), channel_id=1, source_target_pairs={{0,24},{8,0},{16,8},{24,16},{1,25},{9,1},{17,9},{25,17},{2,26},{10... | collective-permute-start | bytes 1376264 | tf_op jit(solution)/shard_map/ppermute | solution.py:482
  103.7 18.2 %collective-permute-start = (bf16[448,512]{1,0:T(8,128)(2,1)}, bf16[448,512]{1,0:T(8,128)(2,1)S(1)}, u32[]{:S(2)}, u32[]{:S(2)}) collective-permute-start(bf16[448,512]{1,0:T(8,128)(2,1)} %get-tuple-element.20.w0.o0), channel_id=1, source_target_pairs={{0,8},{8,16},{16,24},{24,0},{1,9},{9,17},{17,25},{25,1},{2,10},{10... | collective-permute-start | bytes 1376264 | tf_op jit(solution)/shard_map/ppermute | solution.py:482
  112.7 11.3 %copy-start.9 = (bf16[448,512]{1,0:T(8,128)(2,1)}, bf16[448,512]{1,0:T(8,128)(2,1)S(1)}, u32[]{:S(2)}) copy-start(bf16[448,512]{1,0:T(8,128)(2,1)S(1)} %collective-permute-done.2.w3.o3) | copy-start | bytes 1376260
  124.0 8.0 %copy-start.8 = (bf16[448,512]{1,0:T(8,128)(2,1)S(1)}, bf16[448,512]{1,0:T(8,128)(2,1)}, u32[]{:S(2)}) copy-start(bf16[448,512]{1,0:T(8,128)(2,1)} %get-tuple-element.20.w0.o0) | copy-start | bytes 1376260
  138.3 3.8 %collective-permute-start.10 = (bf16[128,2048]{1,0:T(8,128)(2,1)S(1)}, bf16[128,2048]{1,0:T(8,128)(2,1)S(1)}, u32[]{:S(2)}, u32[]{:S(2)}) collective-permute-start(bf16[128,2048]{1,0:T(8,128)(2,1)S(1)} %get-tuple-element.34), channel_id=1, source_target_pairs={{0,1},{1,0},{2,3},{3,2},{4,5},{5,4},{6,7},{7,6},{8,9},{9,8},{10,11... | collective-permute-start | bytes 1572872 | tf_op jit(solution)/shard_map/ppermute | solution.py:486
  (14 other events, 42.5 us)
